TPU v7x, 512 devices: a whole 4x8x8 slice. The times are simulated.
512 devices in a mesh: ra: 32 (over z, x), cb: 16 (over y, core).
Axes of the slice: x: 4, y: 8, z: 8, core: 2. Of those that a mesh axis runs over, the one named last changes fastest.
Arguments:
- tokens: bfloat16 [384, 4096], P(None, 'ra'), may hold values from -260 to 260
- up_weight: float32 [2, 4096, 16384], P(None, 'ra', 'cb'), may hold values from -0.1875 to 0.1875
- up_scale: float32 [2, 16384], P(None, 'cb'), may hold values from 0.5 to 2
- down_weight: float32 [2, 16384, 4096], P(None, 'cb', 'ra'), may hold values from -0.046875 to 0.046875
- down_scale: float32 [2, 4096], P(None, 'ra'), may hold values from 0.7 to 14
- pre_gain: float32 [2, 4096], P(None, 'ra'), may hold values from 0.1 to 1.9
- post_gain: float32 [2, 4096], P(None, 'ra'), may hold values from 0.1 to 1.9
Outputs:
- stream_out: bfloat16 [384, 4096], P(None, 'ra')
All inputs are finite; a program needn't handle non-finite values.
Results may differ from a plain program's by a relative error of at most 0.023.
Values may be sent and summed in bfloat16 or wider, within the bound.
No kernel may reach another device: no remote copies, remote signals or barrier semaphores. Data moves between devices by JAX's collectives and lax.ppermute only.
A program may use at most 64 MiB of HBM per device.

v0:
```python
import jax
import jax.numpy as jnp
from jax import lax
from jax.sharding import PartitionSpec as P

norm_eps = 1e-06
residual_keep = 0.5


def split_up(shard, dim, size):
    before, after = (shard.shape[:dim], shard.shape[dim + 1 :])
    return jnp.moveaxis(shard.reshape(*before, size, -1, *after), dim, 0)


def summed_on_arrival(shard, axis, dim):
    pieces = split_up(shard, dim, lax.axis_size(axis))
    arrived = lax.all_to_all(pieces, axis, split_axis=0, concat_axis=0, tiled=True)
    return arrived.astype(jnp.float32).sum(axis=0)


def laid_out(pieces, dim):
    pieces = jnp.moveaxis(pieces, 0, dim)
    lengths = pieces.shape
    return pieces.reshape(*lengths[:dim], lengths[dim] * lengths[dim + 1], *lengths[dim + 2 :])


def copy_for_each(shard, axis):
    size = lax.axis_size(axis)
    return lax.all_to_all(
        jnp.broadcast_to(shard[None], (size, *shard.shape)), axis, 0, 0, tiled=True
    )


def gather_directly(shard, axis, dim):
    return laid_out(copy_for_each(shard, axis), dim)


def of_everyone(shard, axis):
    return copy_for_each(shard, axis).astype(jnp.float32).sum(axis=0)


def of_everyone_2(shard, axis):
    everything = copy_for_each(shard, axis)
    return jnp.sum(everything, axis=0)


def local(tokens, up_weight, up_scale, down_weight, down_scale, pre_gain, post_gain):
    values = tokens.astype(jnp.float32)
    model_width = tokens.shape[1] * lax.axis_size("ra")
    stream = tokens
    for sublayer in range(up_weight.shape[0]):
        scaled = (values * pre_gain[sublayer][None, :]).astype(jnp.bfloat16)
        up_matrix = up_weight[sublayer].astype(jnp.bfloat16)
        down_matrix = down_weight[sublayer].astype(jnp.bfloat16)
        partial_up = jnp.dot(scaled, up_matrix, preferred_element_type=jnp.float32)
        share_up = summed_on_arrival(partial_up.astype(jnp.bfloat16), "ra", 1)
        share_cols = share_up.shape[1]
        col_scale = lax.dynamic_slice_in_dim(
            up_scale[sublayer], lax.axis_index("ra") * share_cols, share_cols, 0
        )
        hidden_share = jnp.square(jax.nn.relu(share_up * col_scale[None, :])).astype(jnp.bfloat16)
        partial_down = jnp.dot(
            gather_directly(hidden_share, "ra", 1), down_matrix, preferred_element_type=jnp.float32
        )
        summed = of_everyone(partial_down.astype(jnp.bfloat16), "cb").astype(jnp.float32)
        branch_in = summed * down_scale[sublayer][None, :]
        post_squares = of_everyone_2(jnp.sum(branch_in * branch_in, axis=1), "ra")
        inv_post = lax.rsqrt(post_squares / model_width + norm_eps)[:, None]
        branch = branch_in * inv_post * post_gain[sublayer][None, :]
        stream = (residual_keep * values + branch).astype(jnp.bfloat16)
        values = stream.astype(jnp.float32)
    return stream


def solution(mesh):
    return jax.shard_map(
        local,
        mesh=mesh,
        in_specs=(
            P(None, "ra"),
            P(None, "ra", "cb"),
            P(None, "cb"),
            P(None, "cb", "ra"),
            P(None, "ra"),
            P(None, "ra"),
            P(None, "ra"),
        ),
        out_specs=P(None, "ra"),
        check_vma=False,
    )
```

profile of v0, /device:TPU:1, one launch (start us, length us, event | category | flops | bytes accessed | tf_op | source)
XLA Modules:
  0.0 246.5 jit_solution(1323146805992287475)
XLA Ops:
  0.0 0.8 slice_bitcast_fusion.10
  0.8 1.3 convert.8
  2.1 0.0 copy-done.3
  2.1 0.4 convolution_convert_fusion.1
  2.4 0.0 copy-start.4
  2.4 1.2 copy.12
  3.6 13.7 %all-to-all-start = ((bf16[32,384,32]{1,2,0:T(8,128)(2,1)}), bf16[32,384,32]{1,2,0:T(8,128)(2,1)S(1)}, u32[]{:S(2)}, u32[]{:S(2)}) async-start(bf16[32,384,32]{1,2,0:T(8,128)(2,1)} %bitcast.3), calls=%async_computation | async-start | bytes 1572864 | tf_op jit(solution)/shard_map/all_to_all | solution.py:17
  17.3 0.0 copy-done.4
  17.3 0.1 dynamic-slice_bitcast_fusion.1
  17.4 21.0 %all-to-all-done = bf16[32,384,32]{1,2,0:T(8,128)(2,1)S(1)} async-done(((bf16[32,384,32]{1,2,0:T(8,128)(2,1)}), bf16[32,384,32]{1,2,0:T(8,128)(2,1)S(1)}, u32[]{:S(2)}, u32[]{:S(2)}) %all-to-all-start) | async-done | bytes 786464 | tf_op jit(solution)/shard_map/all_to_all | solution.py:17
  38.4 0.1 convert_reduce_fusion.3
  38.5 0.1 multiply_convert_fusion.1
  38.6 0.9 broadcast_in_dim.12
  39.5 5.8 %all-to-all-start.1 = ((bf16[32,384,32]{1,2,0:T(8,128)(2,1)}), bf16[32,384,32]{1,2,0:T(8,128)(2,1)S(1)}, u32[]{:S(2)}, u32[]{:S(2)}) async-start(bf16[32,384,32]{1,2,0:T(8,128)(2,1)} %broadcast_in_dim.12), calls=%async_computation.1 | async-start | bytes 1572864 | tf_op jit(solution)/shard_map/all_to_all | solution.py:29
  45.3 0.0 copy-done
  45.3 0.1 convert.9
  45.4 0.0 copy-start.1
  45.4 19.7 %all-to-all-done.1 = bf16[32,384,32]{1,2,0:T(8,128)(2,1)S(1)} async-done(((bf16[32,384,32]{1,2,0:T(8,128)(2,1)}), bf16[32,384,32]{1,2,0:T(8,128)(2,1)S(1)}, u32[]{:S(2)}, u32[]{:S(2)}) %all-to-all-start.1) | async-done | bytes 786464 | tf_op jit(solution)/shard_map/all_to_all | solution.py:29
  65.1 0.4 convolution_convert_fusion.3
  65.5 1.5 broadcast_in_dim.13
  67.0 11.4 %all-to-all-start.2 = ((bf16[16,384,128]{2,1,0:T(8,128)(2,1)}), bf16[16,384,128]{2,1,0:T(8,128)(2,1)S(1)}, u32[]{:S(2)}, u32[]{:S(2)}) async-start(bf16[16,384,128]{2,1,0:T(8,128)(2,1)} %broadcast_in_dim.13), calls=%async_computation.2 | async-start | bytes 3145728 | tf_op jit(solution)/shard_map/all_to_all | solution.py:29
  78.4 0.0 copy-start.6
  78.4 38.5 %all-to-all-done.2 = bf16[16,384,128]{2,1,0:T(8,128)(2,1)S(1)} async-done(((bf16[16,384,128]{2,1,0:T(8,128)(2,1)}), bf16[16,384,128]{2,1,0:T(8,128)(2,1)S(1)}, u32[]{:S(2)}, u32[]{:S(2)}) %all-to-all-start.2) | async-done | bytes 1572896 | tf_op jit(solution)/shard_map/all_to_all | solution.py:29
  116.9 0.2 convert_reduce_fusion.1
  117.1 0.1 multiply_reduce_fusion.1
  117.3 0.7 broadcast_in_dim.14
  117.9 4.7 %all-to-all-start.3 = ((f32[32,1,384]{2,1,0:T(1,128)}), f32[32,1,384]{2,1,0:T(1,128)S(1)}, u32[]{:S(2)}, u32[]{:S(2)}) async-start(f32[32,1,384]{2,1,0:T(1,128)} %broadcast_in_dim.14), calls=%async_computation.3 | async-start | bytes 98304 | tf_op jit(solution)/shard_map/all_to_all | solution.py:29
  122.7 0.0 copy-done.6
  122.7 9.2 %all-to-all-done.3 = f32[32,1,384]{2,1,0:T(1,128)S(1)} async-done(((f32[32,1,384]{2,1,0:T(1,128)}), f32[32,1,384]{2,1,0:T(1,128)S(1)}, u32[]{:S(2)}, u32[]{:S(2)}) %all-to-all-start.3) | async-done | bytes 49184 | tf_op jit(solution)/shard_map/all_to_all | solution.py:29
  131.9 0.1 reduce_sum.75
  132.0 0.1 fusion.1
  132.1 0.4 convolution_convert_fusion
  132.4 1.2 copy.14
  133.6 3.9 %all-to-all-start.4 = ((bf16[32,384,32]{1,2,0:T(8,128)(2,1)}), bf16[32,384,32]{1,2,0:T(8,128)(2,1)S(1)}, u32[]{:S(2)}, u32[]{:S(2)}) async-start(bf16[32,384,32]{1,2,0:T(8,128)(2,1)} %bitcast.13), calls=%async_computation.4 | async-start | bytes 1572864 | tf_op jit(solution)/shard_map/all_to_all | solution.py:17
  137.5 0.1 dynamic-slice_bitcast_fusion
  137.6 21.1 %all-to-all-done.4 = bf16[32,384,32]{1,2,0:T(8,128)(2,1)S(1)} async-done(((bf16[32,384,32]{1,2,0:T(8,128)(2,1)}), bf16[32,384,32]{1,2,0:T(8,128)(2,1)S(1)}, u32[]{:S(2)}, u32[]{:S(2)}) %all-to-all-start.4) | async-done | bytes 786464 | tf_op jit(solution)/shard_map/all_to_all | solution.py:17
  158.7 0.1 convert_reduce_fusion.2
  158.8 0.1 multiply_convert_fusion
  158.9 0.1 broadcast_in_dim.15
  159.0 25.6 %all_to_all.42 = bf16[32,384,32]{1,2,0:T(8,128)(2,1)S(1)} all-to-all(bf16[32,384,32]{1,2,0:T(8,128)(2,1)S(1)} %broadcast_in_dim.15), channel_id=1, replica_groups=mesh['ra'=32,'cb'=16] {'ra'}, dimensions={0} | all-to-all | bytes 1572864 | tf_op jit(solution)/shard_map/all_to_all | solution.py:29
  184.6 0.4 convolution_convert_fusion.2
  185.0 0.3 broadcast_in_dim.16
  185.3 46.5 %all_to_all.43 = bf16[16,384,128]{2,1,0:T(8,128)(2,1)S(1)} all-to-all(bf16[16,384,128]{2,1,0:T(8,128)(2,1)S(1)} %broadcast_in_dim.16), channel_id=1, replica_groups=mesh['ra'=32,'cb'=16] {'cb'}, dimensions={0} | all-to-all | bytes 3145728 | tf_op jit(solution)/shard_map/all_to_all | solution.py:29
  231.8 0.2 convert_reduce_fusion
  232.0 0.1 multiply_reduce_fusion
  232.2 13.4 %all_to_all.44 = f32[32,1,384]{2,1,0:T(1,128)S(1)} all-to-all(f32[32,1,384]{2,1,0:T(1,128)S(1)} %broadcast_in_dim.17), channel_id=1, replica_groups=mesh['ra'=32,'cb'=16] {'ra'}, dimensions={0} | all-to-all | bytes 98304 | tf_op jit(solution)/shard_map/all_to_all | solution.py:29
  245.6 0.1 reduce_sum.79
  245.7 0.8 fusion.4
  (13 shorter events, 0.1 us)
Async XLA Ops:
  0.0 2.1 copy-start.3
  2.4 14.9 %copy-start.4 = (f32[2,1024]{1,0:T(2,128)S(1)}, f32[2,1024]{1,0:T(2,128)}, u32[]{:S(2)}) copy-start(f32[2,1024]{1,0:T(2,128)} %param.9) | copy-start | bytes 24580
  3.6 34.8 %all-to-all-start = ((bf16[32,384,32]{1,2,0:T(8,128)(2,1)}), bf16[32,384,32]{1,2,0:T(8,128)(2,1)S(1)}, u32[]{:S(2)}, u32[]{:S(2)}) async-start(bf16[32,384,32]{1,2,0:T(8,128)(2,1)} %bitcast.3), calls=%async_computation | async-start | bytes 1572864 | tf_op jit(solution)/shard_map/all_to_all | solution.py:17
  17.4 27.9 %copy-start = (f32[2,1024,128]{2,1,0:T(8,128)S(1)}, f32[2,1024,128]{2,1,0:T(8,128)}, u32[]{:S(2)}) copy-start(f32[2,1024,128]{2,1,0:T(8,128)} %param.10) | copy-start | bytes 3145732
  39.5 25.6 %all-to-all-start.1 = ((bf16[32,384,32]{1,2,0:T(8,128)(2,1)}), bf16[32,384,32]{1,2,0:T(8,128)(2,1)S(1)}, u32[]{:S(2)}, u32[]{:S(2)}) async-start(bf16[32,384,32]{1,2,0:T(8,128)(2,1)} %broadcast_in_dim.12), calls=%async_computation.1 | async-start | bytes 1572864 | tf_op jit(solution)/shard_map/all_to_all | solution.py:29
  45.4 21.6 %copy-start.1 = (bf16[2,1024,128]{2,1,0:T(8,128)(2,1)}, bf16[2,1024,128]{2,1,0:T(8,128)(2,1)S(1)}, u32[]{:S(2)}) copy-start(bf16[2,1024,128]{2,1,0:T(8,128)(2,1)S(1)} %convert.9) | copy-start | bytes 1572868
  67.0 11.4 %copy-start.5 = (f32[2,128]{1,0:T(2,128)S(1)}, f32[2,128]{1,0:T(2,128)}, u32[]{:S(2)}) copy-start(f32[2,128]{1,0:T(2,128)} %param.11) | copy-start | bytes 3076
  67.0 49.9 %all-to-all-start.2 = ((bf16[16,384,128]{2,1,0:T(8,128)(2,1)}), bf16[16,384,128]{2,1,0:T(8,128)(2,1)S(1)}, u32[]{:S(2)}, u32[]{:S(2)}) async-start(bf16[16,384,128]{2,1,0:T(8,128)(2,1)} %broadcast_in_dim.13), calls=%async_computation.2 | async-start | bytes 3145728 | tf_op jit(solution)/shard_map/all_to_all | solution.py:29
  78.4 44.3 %copy-start.6 = (f32[2,128]{1,0:T(2,128)S(1)}, f32[2,128]{1,0:T(2,128)}, u32[]{:S(2)}) copy-start(f32[2,128]{1,0:T(2,128)} %param.13) | copy-start | bytes 3076
  117.9 13.9 %all-to-all-start.3 = ((f32[32,1,384]{2,1,0:T(1,128)}), f32[32,1,384]{2,1,0:T(1,128)S(1)}, u32[]{:S(2)}, u32[]{:S(2)}) async-start(f32[32,1,384]{2,1,0:T(1,128)} %broadcast_in_dim.14), calls=%async_computation.3 | async-start | bytes 98304 | tf_op jit(solution)/shard_map/all_to_all | solution.py:29
  133.6 25.1 %all-to-all-start.4 = ((bf16[32,384,32]{1,2,0:T(8,128)(2,1)}), bf16[32,384,32]{1,2,0:T(8,128)(2,1)S(1)}, u32[]{:S(2)}, u32[]{:S(2)}) async-start(bf16[32,384,32]{1,2,0:T(8,128)(2,1)} %bitcast.13), calls=%async_computation.4 | async-start | bytes 1572864 | tf_op jit(solution)/shard_map/all_to_all | solution.py:17
  137.6 47.0 %copy-start.2 = (bf16[2,1024,128]{2,1,0:T(8,128)(2,1)S(1)}, bf16[2,1024,128]{2,1,0:T(8,128)(2,1)}, u32[]{:S(2)}) copy-start(bf16[2,1024,128]{2,1,0:T(8,128)(2,1)} %copy-done.1) | copy-start | bytes 1572868
where the time goes:
time: 247 us; the launch traced here: 246 us
  waiting for transfers between devices  109 us (44%)
  blocking collectives  85.5 us (35%)
  starting transfers between devices  39.6 us (16%)
  local copies, waits for them, and re-layouts  6.72 us (3%)
  other arithmetic  3.53 us (1%)
    all_to_all x3, blocking collectives, copy_for_each(): lax.all_to_all(jnp.broadcast_to(shard[None], (size, *shard.shape)), axis,...  85.5 us
    all_to_all x3, waiting for transfers between devices, copy_for_each(): lax.all_to_all(jnp.broadcast_to(shard[None], (size, *shard.shape)), axis,...  67.3 us
    all_to_all x2, waiting for transfers between devices, summed_on_arrival(): lax.all_to_all(pieces, axis, split_axis=0, concat_axis=0, tiled=True)  42.1 us
    all_to_all x3, starting transfers between devices, copy_for_each(): lax.all_to_all(jnp.broadcast_to(shard[None], (size, *shard.shape)), axis,...  21.9 us
    all_to_all x2, starting transfers between devices, summed_on_arrival(): lax.all_to_all(pieces, axis, split_axis=0, concat_axis=0, tiled=True)  17.6 us
  transfers between devices with their start and end apart: 5, of which 5 were waited for; matrix products, arithmetic and copies ran while one was open for 0% of the time, Pallas kernels for 0%

commit v1 on v0

v1 whole, which is shorter than its diff:
```python
import jax
import jax.numpy as jnp
from jax import lax
from jax.sharding import Mesh, PartitionSpec as P


norm_eps = 1e-06
residual_keep = 0.5
Z, X, Y, C = 8, 4, 8, 2
bf16 = jnp.bfloat16
f32 = jnp.float32


def exchange(pieces, axis):
    return lax.all_to_all(pieces, axis, split_axis=0, concat_axis=0, tiled=True)


def to_all(shard, axis):
    size = lax.axis_size(axis)
    return exchange(jnp.broadcast_to(shard[None], (size, *shard.shape)), axis)


def high_low(v):
    high = lax.reduce_precision(v, 8, 7)
    return high.astype(bf16), (v - high).astype(bf16)


def other_core(v):
    return lax.ppermute(v, "core", [(0, 1), (1, 0)])


def half(v, which, axis, size):
    return lax.dynamic_slice_in_dim(v, which * size, size, axis)


def hidden_of(part):
    tokens, width = part.shape
    share = width // Z
    pieces = part.astype(bf16).reshape(tokens, Z, share).transpose(1, 0, 2)
    summed = exchange(pieces, "z").astype(f32).sum(axis=0)
    chunk = jnp.square(jnp.maximum(summed, 0.0)).astype(bf16)
    whole = to_all(chunk, "z")
    return whole.transpose(1, 0, 2).reshape(tokens, width)


def down_sum(hidden, weight):
    core = lax.axis_index("core")
    part = jnp.stack(
        [jnp.dot(hidden, weight[i], preferred_element_type=f32) for i in range(X)]
    )
    t = hidden.shape[0] // C
    got = other_core(half(part.astype(bf16), 1 - core, 1, t))
    mine = half(part, core, 1, t) + got.astype(f32)
    return to_all(mine.astype(bf16), "y").astype(f32).sum(axis=0)


def inv_norm(branch_in, width):
    squares = jnp.sum(branch_in * branch_in, axis=(0, 2))
    squares = to_all(squares[None], "z").sum(axis=0)[0]
    return lax.rsqrt(squares / width + norm_eps)[None, :, None]


def inner(tokens, up_weight, up_scale, down_weight, down_scale, pre_gain, post_gain):
    n_tok, feats = tokens.shape
    hid = up_weight.shape[2]
    width = feats * X * Z
    t_x = n_tok // X
    t_c = t_x // C
    core = lax.axis_index("core")

    scaled = (tokens.astype(f32) * pre_gain[0][None, :]).astype(bf16)
    part = jnp.dot(scaled, up_weight[0].astype(bf16), preferred_element_type=f32)
    part = (part * up_scale[0][None, :]).astype(bf16)
    body = jnp.concatenate([part, tokens], axis=1).reshape(X, t_x, hid + feats)
    vectors = [down_scale[0], post_gain[0], pre_gain[1], down_scale[1], post_gain[1]]
    highs, lows = zip(*[high_low(v) for v in vectors])
    spare = jnp.zeros((hid + feats - feats * len(vectors),), bf16)
    rows = jnp.stack([jnp.concatenate([*highs, spare]), jnp.concatenate([*lows, spare])])
    rows = jnp.concatenate([rows, jnp.zeros((6, hid + feats), bf16)])
    sent = jnp.concatenate([body, jnp.broadcast_to(rows[None], (X, *rows.shape))], axis=1)
    came = exchange(sent, "x")
    part = came[:, :t_x, :hid].astype(f32).sum(axis=0)

    def from_here(v):
        return lax.dynamic_slice_in_dim(jnp.concatenate([v, v]), lax.axis_index("x"), X, 0)

    def from_zero(v):
        back = (X - lax.axis_index("x")) % X
        return lax.dynamic_slice_in_dim(jnp.concatenate([v, v]), back, X, 0)

    own_tokens = from_here(half(came[:, :t_x, hid:], core, 1, t_c)).astype(f32)
    vec = came[:, t_x].astype(f32) + came[:, t_x + 1].astype(f32)
    vec = from_here(vec[:, : feats * len(vectors)].reshape(X, len(vectors), feats))
    down_0, post_0, pre_1, down_1, post_1 = [vec[:, k][:, None, :] for k in range(len(vectors))]

    def gathered(w, after):
        w, _ = lax.optimization_barrier((w.astype(bf16), after))
        blocks = [w]
        for s in (1, 2, 3):
            blocks.append(lax.ppermute(w, "x", [(i, (i - s) % X) for i in range(X)]))
        return blocks

    down_w0 = gathered(down_weight[0], came)
    hidden = hidden_of(part)
    up_w1 = gathered(up_weight[1], came)
    summed = down_sum(hidden, down_w0)
    branch_in = summed * down_0
    branch = branch_in * inv_norm(branch_in, width) * post_0
    stream = (residual_keep * own_tokens + branch).astype(bf16)

    values = stream.astype(f32)
    scaled = (values * pre_1).astype(bf16)
    got = other_core(scaled)
    first = jnp.where(core == 0, scaled, got)
    second = jnp.where(core == 0, got, scaled)
    scaled = jnp.concatenate([first, second], axis=1).transpose(1, 0, 2).reshape(t_x, X * feats)
    part = jnp.dot(scaled, jnp.concatenate(up_w1), preferred_element_type=f32)
    part = part * up_scale[1][None, :]
    down_w1 = gathered(down_weight[1], came)
    hidden = hidden_of(part)
    summed = down_sum(hidden, down_w1)
    branch_in = summed * down_1
    branch = branch_in * inv_norm(branch_in, width) * post_1
    out = (residual_keep * values + branch).astype(bf16)
    out = from_zero(out)
    out = jnp.broadcast_to(out[:, None], (X, C, t_c, feats)).reshape(X * C, t_c, feats)
    return exchange(out, ("x", "core")).reshape(n_tok, feats)


def solution(mesh):
    split = Mesh(mesh.devices.reshape(Z, X, Y, C), ("z", "x", "y", "core"))
    ra, cb = ("z", "x"), ("y", "core")
    return jax.shard_map(
        inner,
        mesh=split,
        in_specs=(
            P(None, ra),
            P(None, ra, cb),
            P(None, cb),
            P(None, cb, ra),
            P(None, ra),
            P(None, ra),
            P(None, ra),
        ),
        out_specs=P(None, ra),
        check_vma=False,
    )
```

time: 247 us -> 215 us (0.87)
  waiting for transfers between devices: 109 us -> 68.2 us
  starting transfers between devices: 39.6 us -> 76.7 us
  blocking collectives: 85.5 us -> 52.8 us
    all_to_all x5 -> x6, waiting for transfers between devices: 109 us -> 38.4 us  [exchange(): return lax.all_to_all(pieces, axis, split_axis=0, concat_axis=0, tiled=True)]
    ppermute x0 -> x12, starting transfers between devices: none -> 36.1 us  [the longest x9 22.8 us: gathered(): blocks.append(lax.ppermute(w, 'x', [(i, (i - s) % X) for i in range(X)]))]
    all_to_all x3 -> x4, blocking collectives: 85.5 us -> 52.8 us  [exchange(): return lax.all_to_all(pieces, axis, split_axis=0, concat_axis=0, tiled=True)]
    ppermute x0 -> x12, waiting for transfers between devices: none -> 29.8 us  [the longest x9 28.1 us: gathered(): blocks.append(lax.ppermute(w, 'x', [(i, (i - s) % X) for i in range(X)]))]
    unnamed x14 -> x19, local copies, waits for them, and re-layouts: 0.03 us -> 2.75 us
    all_to_all x5 -> x6, starting transfers between devices: 39.6 us -> 40.6 us  [exchange(): return lax.all_to_all(pieces, axis, split_axis=0, concat_axis=0, tiled=True)]
  transfers between devices with their start and end apart: 5 -> 18, of which waited for: 5 -> 15; matrix products, arithmetic and copies ran while one was open for 0% -> 1% of each run, Pallas kernels for 0% -> 0%
where the time goes in v1:
time: 215 us; the launch traced here: 214 us
  starting transfers between devices  76.7 us (36%)
  waiting for transfers between devices  68.2 us (32%)
  blocking collectives  52.8 us (25%)
  local copies, waits for them, and re-layouts  8.3 us (4%)
  other arithmetic  4.77 us (2%)
  matrix products  2.27 us (1%)
    all_to_all x4, blocking collectives, exchange(): return lax.all_to_all(pieces, axis, split_axis=0, concat_axis=0, tiled=True)  52.8 us
    all_to_all x6, starting transfers between devices, exchange(): return lax.all_to_all(pieces, axis, split_axis=0, concat_axis=0, tiled=True)  40.6 us
    all_to_all x6, waiting for transfers between devices, exchange(): return lax.all_to_all(pieces, axis, split_axis=0, concat_axis=0, tiled=True)  38.4 us
    ppermute x9, waiting for transfers between devices, gathered(): blocks.append(lax.ppermute(w, 'x', [(i, (i - s) % X) for i in range(X)]))  28.1 us
    ppermute x9, starting transfers between devices, gathered(): blocks.append(lax.ppermute(w, 'x', [(i, (i - s) % X) for i in range(X)]))  22.8 us
    ppermute x3, starting transfers between devices, other_core(): return lax.ppermute(v, 'core', [(0, 1), (1, 0)])  13.4 us
  transfers between devices with their start and end apart: 18, of which 15 were waited for; matrix products, arithmetic and copies ran while one was open for 1% of the time, Pallas kernels for 0%

profile of v1, /device:TPU:1, one launch (start us, length us, event | category | flops | bytes accessed | tf_op | source)
XLA Modules:
  0.0 213.6 jit_solution(12092899582102814363)
XLA Ops:
  0.0 0.7 reduce-precision_convert_fusion.2
  0.7 0.7 slice_bitcast_fusion.5
  1.4 0.8 reduce-precision_convert_fusion.1
  2.2 0.8 reduce-precision_convert_fusion
  5.5 1.3 convert.9
  7.5 14.0 %all_to_all.50 = bf16[4,104,1152]{2,1,0:T(8,128)(2,1)S(1)} all-to-all(bf16[4,104,1152]{2,1,0:T(8,128)(2,1)S(1)} %pad_maximum_fusion), channel_id=1, replica_groups=mesh['z'=8,'x'=4,'y'=8,'core'=2] {'x'}, dimensions={0} | all-to-all | bytes 1916928 | tf_op jit(solution)/shard_map/all_to_all | solution.py:15
  21.6 0.7 copy.24
  22.3 13.7 %all-to-all-start.1 = ((bf16[8,96,128]{2,1,0:T(8,128)(2,1)}), bf16[8,96,128]{2,1,0:T(8,128)(2,1)S(1)}, u32[]{:S(2)}, u32[]{:S(2)}) async-start(bf16[8,96,128]{2,1,0:T(8,128)(2,1)} %copy.24), calls=%async_computation.1 | async-start | bytes 393216 | tf_op jit(solution)/shard_map/all_to_all | solution.py:15
  36.1 8.7 %all-to-all-done.1 = bf16[8,96,128]{2,1,0:T(8,128)(2,1)S(1)} async-done(((bf16[8,96,128]{2,1,0:T(8,128)(2,1)}), bf16[8,96,128]{2,1,0:T(8,128)(2,1)S(1)}, u32[]{:S(2)}, u32[]{:S(2)}) %all-to-all-start.1) | async-done | bytes 196640 | tf_op jit(solution)/shard_map/all_to_all | solution.py:15
  44.8 0.7 broadcast_in_dim.23
  45.5 3.4 %all-to-all-start.2 = ((bf16[8,96,128]{2,1,0:T(8,128)(2,1)}), bf16[8,96,128]{2,1,0:T(8,128)(2,1)S(1)}, u32[]{:S(2)}, u32[]{:S(2)}) async-start(bf16[8,96,128]{2,1,0:T(8,128)(2,1)} %broadcast_in_dim.23), calls=%async_computation.2 | async-start | bytes 393216 | tf_op jit(solution)/shard_map/all_to_all | solution.py:15
  48.9 2.8 %collective-permute-start = (bf16[1024,128]{1,0:T(8,128)(2,1)S(1)}, bf16[1024,128]{1,0:T(8,128)(2,1)S(1)}, u32[]{:S(2)}, u32[]{:S(2)}) collective-permute-start(bf16[1024,128]{1,0:T(8,128)(2,1)S(1)} %get-tuple-element.8), channel_id=1, source_target_pairs={{0,48},{16,0},{32,16},{48,32},{1,49},{17,1},{33,17},{49,33},{2,50}... | collective-permute-start | bytes 786440 | tf_op jit(solution)/shard_map/ppermute | solution.py:100
  51.7 3.1 %collective-permute-start.1 = (bf16[1024,128]{1,0:T(8,128)(2,1)S(1)}, bf16[1024,128]{1,0:T(8,128)(2,1)S(1)}, u32[]{:S(2)}, u32[]{:S(2)}) collective-permute-start(bf16[1024,128]{1,0:T(8,128)(2,1)S(1)} %get-tuple-element.8), channel_id=1, source_target_pairs={{0,32},{16,48},{32,0},{48,16},{1,33},{17,49},{33,1},{49,17},{2,34}... | collective-permute-start | bytes 786440 | tf_op jit(solution)/shard_map/ppermute | solution.py:100
  54.8 1.9 collective-permute-start.2
  56.7 0.7 all-to-all-done.2
  57.8 2.5 %collective-permute-done.1 = bf16[1024,128]{1,0:T(8,128)(2,1)S(1)} collective-permute-done((bf16[1024,128]{1,0:T(8,128)(2,1)S(1)}, bf16[1024,128]{1,0:T(8,128)(2,1)S(1)}, u32[]{:S(2)}, u32[]{:S(2)}) %collective-permute-start.1) | collective-permute-done | bytes 262176 | tf_op jit(solution)/shard_map/ppermute | solution.py:100
  60.5 4.3 %collective-permute-done.2 = bf16[1024,128]{1,0:T(8,128)(2,1)S(1)} collective-permute-done((bf16[1024,128]{1,0:T(8,128)(2,1)S(1)}, bf16[1024,128]{1,0:T(8,128)(2,1)S(1)}, u32[]{:S(2)}, u32[]{:S(2)}) %collective-permute-start.2) | collective-permute-done | bytes 262176 | tf_op jit(solution)/shard_map/ppermute | solution.py:100
  65.1 6.6 %collective-permute-start.3 = (bf16[4,48,128]{2,1,0:T(8,128)(2,1)S(1)}, bf16[4,48,128]{2,1,0:T(8,128)(2,1)S(1)}, u32[]{:S(2)}, u32[]{:S(2)}) collective-permute-start(bf16[4,48,128]{2,1,0:T(8,128)(2,1)S(1)} %dynamic-slice_convert_fusion.1), channel_id=1, source_target_pairs={{0,1},{1,0},{2,3},{3,2},{4,5},{5,4},{6,7},{7,6},{8,9},{9,8},{10,11... | collective-permute-start | bytes 147464 | tf_op jit(solution)/shard_map/ppermute | solution.py:29
  71.7 0.8 collective-permute-done.3
  72.6 0.8 broadcast_in_dim.24
  73.4 6.8 %all-to-all-start.3 = ((bf16[8,4,48,128]{3,2,1,0:T(8,128)(2,1)}), bf16[8,4,48,128]{3,2,1,0:T(8,128)(2,1)S(1)}, u32[]{:S(2)}, u32[]{:S(2)}) async-start(bf16[8,4,48,128]{3,2,1,0:T(8,128)(2,1)} %broadcast_in_dim.24), calls=%async_computation.3 | async-start | bytes 786432 | tf_op jit(solution)/shard_map/all_to_all | solution.py:15
  80.4 15.0 %all-to-all-done.3 = bf16[8,4,48,128]{3,2,1,0:T(8,128)(2,1)S(1)} async-done(((bf16[8,4,48,128]{3,2,1,0:T(8,128)(2,1)}), bf16[8,4,48,128]{3,2,1,0:T(8,128)(2,1)S(1)}, u32[]{:S(2)}, u32[]{:S(2)}) %all-to-all-start.3) | async-done | bytes 393248 | tf_op jit(solution)/shard_map/all_to_all | solution.py:15
  95.5 0.6 broadcast_in_dim.25
  96.1 6.8 %all-to-all-start.4 = ((f32[8,1,48]{2,1,0:T(1,128)}), f32[8,1,48]{2,1,0:T(1,128)S(1)}, u32[]{:S(2)}, u32[]{:S(2)}) async-start(f32[8,1,48]{2,1,0:T(1,128)} %broadcast_in_dim.25), calls=%async_computation.4 | async-start | bytes 8192 | tf_op jit(solution)/shard_map/all_to_all | solution.py:15
  102.9 6.5 %all-to-all-done.4 = f32[8,1,48]{2,1,0:T(1,128)S(1)} async-done(((f32[8,1,48]{2,1,0:T(1,128)}), f32[8,1,48]{2,1,0:T(1,128)S(1)}, u32[]{:S(2)}, u32[]{:S(2)}) %all-to-all-start.4) | async-done | bytes 1568 | tf_op jit(solution)/shard_map/all_to_all | solution.py:15
  109.5 3.8 %collective-permute-start.4 = (bf16[4,48,128]{2,1,0:T(8,128)(2,1)S(1)}, bf16[4,48,128]{2,1,0:T(8,128)(2,1)S(1)}, u32[]{:S(2)}, u32[]{:S(2)}) collective-permute-start(bf16[4,48,128]{2,1,0:T(8,128)(2,1)S(1)} %get-tuple-element.11), channel_id=1, source_target_pairs={{0,1},{1,0},{2,3},{3,2},{4,5},{5,4},{6,7},{7,6},{8,9},{9,8},{10,11... | collective-permute-start | bytes 147464 | tf_op jit(solution)/shard_map/ppermute | solution.py:29
  113.4 2.2 %collective-permute-start.5 = (bf16[128,1024]{1,0:T(8,128)(2,1)S(1)}, bf16[128,1024]{1,0:T(8,128)(2,1)S(1)}, u32[]{:S(2)}, u32[]{:S(2)}) collective-permute-start(bf16[128,1024]{1,0:T(8,128)(2,1)S(1)} %slice_bitcast_fusion.1), channel_id=1, source_target_pairs={{0,48},{16,0},{32,16},{48,32},{1,49},{17,1},{33,17},{49,33},{2,50}... | collective-permute-start | bytes 786440 | tf_op jit(solution)/shard_map/ppermute | solution.py:100
  115.6 2.8 %collective-permute-start.6 = (bf16[128,1024]{1,0:T(8,128)(2,1)S(1)}, bf16[128,1024]{1,0:T(8,128)(2,1)S(1)}, u32[]{:S(2)}, u32[]{:S(2)}) collective-permute-start(bf16[128,1024]{1,0:T(8,128)(2,1)S(1)} %slice_bitcast_fusion.1), channel_id=1, source_target_pairs={{0,32},{16,48},{32,0},{48,16},{1,33},{17,49},{33,1},{49,17},{2,34}... | collective-permute-start | bytes 786440 | tf_op jit(solution)/shard_map/ppermute | solution.py:100
  118.4 2.5 %collective-permute-start.7 = (bf16[128,1024]{1,0:T(8,128)(2,1)S(1)}, bf16[128,1024]{1,0:T(8,128)(2,1)S(1)}, u32[]{:S(2)}, u32[]{:S(2)}) collective-permute-start(bf16[128,1024]{1,0:T(8,128)(2,1)S(1)} %slice_bitcast_fusion.1), channel_id=1, source_target_pairs={{0,16},{16,32},{32,48},{48,0},{1,17},{17,33},{33,49},{49,1},{2,18}... | collective-permute-start | bytes 786440 | tf_op jit(solution)/shard_map/ppermute | solution.py:100
  120.9 2.2 %collective-permute-done.5 = bf16[128,1024]{1,0:T(8,128)(2,1)S(1)} collective-permute-done((bf16[128,1024]{1,0:T(8,128)(2,1)S(1)}, bf16[128,1024]{1,0:T(8,128)(2,1)S(1)}, u32[]{:S(2)}, u32[]{:S(2)}) %collective-permute-start.5) | collective-permute-done | bytes 262176 | tf_op jit(solution)/shard_map/ppermute | solution.py:100
  123.1 3.5 %collective-permute-done.6 = bf16[128,1024]{1,0:T(8,128)(2,1)S(1)} collective-permute-done((bf16[128,1024]{1,0:T(8,128)(2,1)S(1)}, bf16[128,1024]{1,0:T(8,128)(2,1)S(1)}, u32[]{:S(2)}, u32[]{:S(2)}) %collective-permute-start.6) | collective-permute-done | bytes 262176 | tf_op jit(solution)/shard_map/ppermute | solution.py:100
  126.6 6.2 %collective-permute-done.7 = bf16[128,1024]{1,0:T(8,128)(2,1)S(1)} collective-permute-done((bf16[128,1024]{1,0:T(8,128)(2,1)S(1)}, bf16[128,1024]{1,0:T(8,128)(2,1)S(1)}, u32[]{:S(2)}, u32[]{:S(2)}) %collective-permute-start.7) | collective-permute-done | bytes 262176 | tf_op jit(solution)/shard_map/ppermute | solution.py:100
  133.2 12.1 %all_to_all.51 = bf16[8,96,128]{2,1,0:T(8,128)(2,1)S(1)} all-to-all(bf16[8,96,128]{2,1,0:T(8,128)(2,1)S(1)} %bitcast.133), channel_id=1, replica_groups=mesh['z'=8,'x'=4,'y'=8,'core'=2] {'z'}, dimensions={0} | all-to-all | bytes 393216 | tf_op jit(solution)/shard_map/all_to_all | solution.py:15
  145.3 0.7 broadcast_in_dim.26
  146.0 3.4 %all-to-all-start.6 = ((bf16[8,96,128]{2,1,0:T(8,128)(2,1)}), bf16[8,96,128]{2,1,0:T(8,128)(2,1)S(1)}, u32[]{:S(2)}, u32[]{:S(2)}) async-start(bf16[8,96,128]{2,1,0:T(8,128)(2,1)} %broadcast_in_dim.26), calls=%async_computation.6 | async-start | bytes 393216 | tf_op jit(solution)/shard_map/all_to_all | solution.py:15
  149.4 1.9 collective-permute-start.8
  151.3 2.8 %collective-permute-start.9 = (bf16[1024,128]{1,0:T(8,128)(2,1)S(1)}, bf16[1024,128]{1,0:T(8,128)(2,1)S(1)}, u32[]{:S(2)}, u32[]{:S(2)}) collective-permute-start(bf16[1024,128]{1,0:T(8,128)(2,1)S(1)} %get-tuple-element.10), channel_id=1, source_target_pairs={{0,32},{16,48},{32,0},{48,16},{1,33},{17,49},{33,1},{49,17},{2,34}... | collective-permute-start | bytes 786440 | tf_op jit(solution)/shard_map/ppermute | solution.py:100
  154.1 2.8 %collective-permute-start.10 = (bf16[1024,128]{1,0:T(8,128)(2,1)S(1)}, bf16[1024,128]{1,0:T(8,128)(2,1)S(1)}, u32[]{:S(2)}, u32[]{:S(2)}) collective-permute-start(bf16[1024,128]{1,0:T(8,128)(2,1)S(1)} %get-tuple-element.10), channel_id=1, source_target_pairs={{0,16},{16,32},{32,48},{48,0},{1,17},{17,33},{33,49},{49,1},{2,18}... | collective-permute-start | bytes 786440 | tf_op jit(solution)/shard_map/ppermute | solution.py:100
  156.9 1.1 all-to-all-done.6
  158.4 2.4 %collective-permute-done.9 = bf16[1024,128]{1,0:T(8,128)(2,1)S(1)} collective-permute-done((bf16[1024,128]{1,0:T(8,128)(2,1)S(1)}, bf16[1024,128]{1,0:T(8,128)(2,1)S(1)}, u32[]{:S(2)}, u32[]{:S(2)}) %collective-permute-start.9) | collective-permute-done | bytes 262176 | tf_op jit(solution)/shard_map/ppermute | solution.py:100
  161.0 7.0 %collective-permute-done.10 = bf16[1024,128]{1,0:T(8,128)(2,1)S(1)} collective-permute-done((bf16[1024,128]{1,0:T(8,128)(2,1)S(1)}, bf16[1024,128]{1,0:T(8,128)(2,1)S(1)}, u32[]{:S(2)}, u32[]{:S(2)}) %collective-permute-start.10) | collective-permute-done | bytes 262176 | tf_op jit(solution)/shard_map/ppermute | solution.py:100
  168.2 3.0 %collective-permute-start.11 = (bf16[4,48,128]{2,1,0:T(8,128)(2,1)S(1)}, bf16[4,48,128]{2,1,0:T(8,128)(2,1)S(1)}, u32[]{:S(2)}, u32[]{:S(2)}) collective-permute-start(bf16[4,48,128]{2,1,0:T(8,128)(2,1)S(1)} %dynamic-slice_convert_fusion), channel_id=1, source_target_pairs={{0,1},{1,0},{2,3},{3,2},{4,5},{5,4},{6,7},{7,6},{8,9},{9,8},{10,11... | collective-permute-start | bytes 147464 | tf_op jit(solution)/shard_map/ppermute | solution.py:29
  171.2 0.9 collective-permute-done.11
  172.2 17.5 %all_to_all.52 = bf16[8,4,48,128]{3,2,1,0:T(8,128)(2,1)S(1)} all-to-all(bf16[8,4,48,128]{3,2,1,0:T(8,128)(2,1)S(1)} %broadcast_in_dim.27), channel_id=1, replica_groups=mesh['z'=8,'x'=4,'y'=8,'core'=2] {'y'}, dimensions={0} | all-to-all | bytes 786432 | tf_op jit(solution)/shard_map/all_to_all | solution.py:15
  190.5 6.6 %all-to-all-start.8 = ((f32[8,1,48]{2,1,0:T(1,128)}), f32[8,1,48]{2,1,0:T(1,128)S(1)}, u32[]{:S(2)}, u32[]{:S(2)}) async-start(f32[8,1,48]{2,1,0:T(1,128)} %broadcast_in_dim.28), calls=%async_computation.8 | async-start | bytes 8192 | tf_op jit(solution)/shard_map/all_to_all | solution.py:15
  197.0 6.5 %all-to-all-done.8 = f32[8,1,48]{2,1,0:T(1,128)S(1)} async-done(((f32[8,1,48]{2,1,0:T(1,128)}), f32[8,1,48]{2,1,0:T(1,128)S(1)}, u32[]{:S(2)}, u32[]{:S(2)}) %all-to-all-start.8) | async-done | bytes 1568 | tf_op jit(solution)/shard_map/all_to_all | solution.py:15
  203.7 9.3 %all_to_all.53 = bf16[8,48,128]{2,1,0:T(8,128)(2,1)S(1)} all-to-all(bf16[8,48,128]{2,1,0:T(8,128)(2,1)S(1)} %bitcast.135), channel_id=1, replica_groups=mesh['z'=8,'x'=4,'y'=8,'core'=2] {'x','core'}, dimensions={0} | all-to-all | bytes 196608 | tf_op jit(solution)/shard_map/all_to_all | solution.py:15
  213.0 0.6 copy.90
  (82 shorter events, 7.0 us)
Async XLA Ops:
  0.0 6.8 %copy-start.2 = (f32[2,1024]{1,0:T(2,128)S(1)}, f32[2,1024]{1,0:T(2,128)}, u32[]{:S(2)}) copy-start(f32[2,1024]{1,0:T(2,128)} %param.9) | copy-start | bytes 24580
  0.0 6.8 %copy-start.1 = (bf16[384,128]{1,0:T(8,128)(2,1)S(1)}, bf16[384,128]{1,0:T(8,128)(2,1)}, u32[]{:S(2)}) copy-start(bf16[384,128]{1,0:T(8,128)(2,1)} %param.7) | copy-start | bytes 294916
  21.5 14.5 %copy-start = (f32[2,1024,128]{2,1,0:T(8,128)S(1)}, f32[2,1024,128]{2,1,0:T(8,128)}, u32[]{:S(2)}) copy-start(f32[2,1024,128]{2,1,0:T(8,128)} %param.10) | copy-start | bytes 3145732
  22.3 22.4 %all-to-all-start.1 = ((bf16[8,96,128]{2,1,0:T(8,128)(2,1)}), bf16[8,96,128]{2,1,0:T(8,128)(2,1)S(1)}, u32[]{:S(2)}, u32[]{:S(2)}) async-start(bf16[8,96,128]{2,1,0:T(8,128)(2,1)} %copy.24), calls=%async_computation.1 | async-start | bytes 393216 | tf_op jit(solution)/shard_map/all_to_all | solution.py:15
  45.5 11.9 %all-to-all-start.2 = ((bf16[8,96,128]{2,1,0:T(8,128)(2,1)}), bf16[8,96,128]{2,1,0:T(8,128)(2,1)S(1)}, u32[]{:S(2)}, u32[]{:S(2)}) async-start(bf16[8,96,128]{2,1,0:T(8,128)(2,1)} %broadcast_in_dim.23), calls=%async_computation.2 | async-start | bytes 393216 | tf_op jit(solution)/shard_map/all_to_all | solution.py:15
  48.9 8.7 %collective-permute-start = (bf16[1024,128]{1,0:T(8,128)(2,1)S(1)}, bf16[1024,128]{1,0:T(8,128)(2,1)S(1)}, u32[]{:S(2)}, u32[]{:S(2)}) collective-permute-start(bf16[1024,128]{1,0:T(8,128)(2,1)S(1)} %get-tuple-element.8), channel_id=1, source_target_pairs={{0,48},{16,0},{32,16},{48,32},{1,49},{17,1},{33,17},{49,33},{2,50}... | collective-permute-start | bytes 786440 | tf_op jit(solution)/shard_map/ppermute | solution.py:100
  51.7 8.6 %collective-permute-start.1 = (bf16[1024,128]{1,0:T(8,128)(2,1)S(1)}, bf16[1024,128]{1,0:T(8,128)(2,1)S(1)}, u32[]{:S(2)}, u32[]{:S(2)}) collective-permute-start(bf16[1024,128]{1,0:T(8,128)(2,1)S(1)} %get-tuple-element.8), channel_id=1, source_target_pairs={{0,32},{16,48},{32,0},{48,16},{1,33},{17,49},{33,1},{49,17},{2,34}... | collective-permute-start | bytes 786440 | tf_op jit(solution)/shard_map/ppermute | solution.py:100
  54.8 10.1 %collective-permute-start.2 = (bf16[1024,128]{1,0:T(8,128)(2,1)S(1)}, bf16[1024,128]{1,0:T(8,128)(2,1)S(1)}, u32[]{:S(2)}, u32[]{:S(2)}) collective-permute-start(bf16[1024,128]{1,0:T(8,128)(2,1)S(1)} %get-tuple-element.8), channel_id=1, source_target_pairs={{0,16},{16,32},{32,48},{48,0},{1,17},{17,33},{33,49},{49,1},{2,18}... | collective-permute-start | bytes 786440 | tf_op jit(solution)/shard_map/ppermute | solution.py:100
  65.1 7.4 %collective-permute-start.3 = (bf16[4,48,128]{2,1,0:T(8,128)(2,1)S(1)}, bf16[4,48,128]{2,1,0:T(8,128)(2,1)S(1)}, u32[]{:S(2)}, u32[]{:S(2)}) collective-permute-start(bf16[4,48,128]{2,1,0:T(8,128)(2,1)S(1)} %dynamic-slice_convert_fusion.1), channel_id=1, source_target_pairs={{0,1},{1,0},{2,3},{3,2},{4,5},{5,4},{6,7},{7,6},{8,9},{9,8},{10,11... | collective-permute-start | bytes 147464 | tf_op jit(solution)/shard_map/ppermute | solution.py:29
  73.4 22.0 %all-to-all-start.3 = ((bf16[8,4,48,128]{3,2,1,0:T(8,128)(2,1)}), bf16[8,4,48,128]{3,2,1,0:T(8,128)(2,1)S(1)}, u32[]{:S(2)}, u32[]{:S(2)}) async-start(bf16[8,4,48,128]{3,2,1,0:T(8,128)(2,1)} %broadcast_in_dim.24), calls=%async_computation.3 | async-start | bytes 786432 | tf_op jit(solution)/shard_map/all_to_all | solution.py:15
  96.1 13.3 %all-to-all-start.4 = ((f32[8,1,48]{2,1,0:T(1,128)}), f32[8,1,48]{2,1,0:T(1,128)S(1)}, u32[]{:S(2)}, u32[]{:S(2)}) async-start(f32[8,1,48]{2,1,0:T(1,128)} %broadcast_in_dim.25), calls=%async_computation.4 | async-start | bytes 8192 | tf_op jit(solution)/shard_map/all_to_all | solution.py:15
  109.5 11.4 %collective-permute-start.4 = (bf16[4,48,128]{2,1,0:T(8,128)(2,1)S(1)}, bf16[4,48,128]{2,1,0:T(8,128)(2,1)S(1)}, u32[]{:S(2)}, u32[]{:S(2)}) collective-permute-start(bf16[4,48,128]{2,1,0:T(8,128)(2,1)S(1)} %get-tuple-element.11), channel_id=1, source_target_pairs={{0,1},{1,0},{2,3},{3,2},{4,5},{5,4},{6,7},{7,6},{8,9},{9,8},{10,11... | collective-permute-start | bytes 147464 | tf_op jit(solution)/shard_map/ppermute | solution.py:29
  113.4 9.7 %collective-permute-start.5 = (bf16[128,1024]{1,0:T(8,128)(2,1)S(1)}, bf16[128,1024]{1,0:T(8,128)(2,1)S(1)}, u32[]{:S(2)}, u32[]{:S(2)}) collective-permute-start(bf16[128,1024]{1,0:T(8,128)(2,1)S(1)} %slice_bitcast_fusion.1), channel_id=1, source_target_pairs={{0,48},{16,0},{32,16},{48,32},{1,49},{17,1},{33,17},{49,33},{2,50}... | collective-permute-start | bytes 786440 | tf_op jit(solution)/shard_map/ppermute | solution.py:100
  115.6 11.0 %collective-permute-start.6 = (bf16[128,1024]{1,0:T(8,128)(2,1)S(1)}, bf16[128,1024]{1,0:T(8,128)(2,1)S(1)}, u32[]{:S(2)}, u32[]{:S(2)}) collective-permute-start(bf16[128,1024]{1,0:T(8,128)(2,1)S(1)} %slice_bitcast_fusion.1), channel_id=1, source_target_pairs={{0,32},{16,48},{32,0},{48,16},{1,33},{17,49},{33,1},{49,17},{2,34}... | collective-permute-start | bytes 786440 | tf_op jit(solution)/shard_map/ppermute | solution.py:100
  118.4 14.4 %collective-permute-start.7 = (bf16[128,1024]{1,0:T(8,128)(2,1)S(1)}, bf16[128,1024]{1,0:T(8,128)(2,1)S(1)}, u32[]{:S(2)}, u32[]{:S(2)}) collective-permute-start(bf16[128,1024]{1,0:T(8,128)(2,1)S(1)} %slice_bitcast_fusion.1), channel_id=1, source_target_pairs={{0,16},{16,32},{32,48},{48,0},{1,17},{17,33},{33,49},{49,1},{2,18}... | collective-permute-start | bytes 786440 | tf_op jit(solution)/shard_map/ppermute | solution.py:100
  146.0 12.0 %all-to-all-start.6 = ((bf16[8,96,128]{2,1,0:T(8,128)(2,1)}), bf16[8,96,128]{2,1,0:T(8,128)(2,1)S(1)}, u32[]{:S(2)}, u32[]{:S(2)}) async-start(bf16[8,96,128]{2,1,0:T(8,128)(2,1)} %broadcast_in_dim.26), calls=%async_computation.6 | async-start | bytes 393216 | tf_op jit(solution)/shard_map/all_to_all | solution.py:15
  149.4 8.8 %collective-permute-start.8 = (bf16[1024,128]{1,0:T(8,128)(2,1)S(1)}, bf16[1024,128]{1,0:T(8,128)(2,1)S(1)}, u32[]{:S(2)}, u32[]{:S(2)}) collective-permute-start(bf16[1024,128]{1,0:T(8,128)(2,1)S(1)} %get-tuple-element.10), channel_id=1, source_target_pairs={{0,48},{16,0},{32,16},{48,32},{1,49},{17,1},{33,17},{49,33},{2,50}... | collective-permute-start | bytes 786440 | tf_op jit(solution)/shard_map/ppermute | solution.py:100
  151.3 9.5 %collective-permute-start.9 = (bf16[1024,128]{1,0:T(8,128)(2,1)S(1)}, bf16[1024,128]{1,0:T(8,128)(2,1)S(1)}, u32[]{:S(2)}, u32[]{:S(2)}) collective-permute-start(bf16[1024,128]{1,0:T(8,128)(2,1)S(1)} %get-tuple-element.10), channel_id=1, source_target_pairs={{0,32},{16,48},{32,0},{48,16},{1,33},{17,49},{33,1},{49,17},{2,34}... | collective-permute-start | bytes 786440 | tf_op jit(solution)/shard_map/ppermute | solution.py:100
  154.1 13.9 %collective-permute-start.10 = (bf16[1024,128]{1,0:T(8,128)(2,1)S(1)}, bf16[1024,128]{1,0:T(8,128)(2,1)S(1)}, u32[]{:S(2)}, u32[]{:S(2)}) collective-permute-start(bf16[1024,128]{1,0:T(8,128)(2,1)S(1)} %get-tuple-element.10), channel_id=1, source_target_pairs={{0,16},{16,32},{32,48},{48,0},{1,17},{17,33},{33,49},{49,1},{2,18}... | collective-permute-start | bytes 786440 | tf_op jit(solution)/shard_map/ppermute | solution.py:100
  168.2 3.8 %collective-permute-start.11 = (bf16[4,48,128]{2,1,0:T(8,128)(2,1)S(1)}, bf16[4,48,128]{2,1,0:T(8,128)(2,1)S(1)}, u32[]{:S(2)}, u32[]{:S(2)}) collective-permute-start(bf16[4,48,128]{2,1,0:T(8,128)(2,1)S(1)} %dynamic-slice_convert_fusion), channel_id=1, source_target_pairs={{0,1},{1,0},{2,3},{3,2},{4,5},{5,4},{6,7},{7,6},{8,9},{9,8},{10,11... | collective-permute-start | bytes 147464 | tf_op jit(solution)/shard_map/ppermute | solution.py:29
  190.5 13.0 %all-to-all-start.8 = ((f32[8,1,48]{2,1,0:T(1,128)}), f32[8,1,48]{2,1,0:T(1,128)S(1)}, u32[]{:S(2)}, u32[]{:S(2)}) async-start(f32[8,1,48]{2,1,0:T(1,128)} %broadcast_in_dim.28), calls=%async_computation.8 | async-start | bytes 8192 | tf_op jit(solution)/shard_map/all_to_all | solution.py:15

commit v2 on v1

v2 whole, which is shorter than its diff:
```python
import jax
import jax.numpy as jnp
from jax import lax
from jax.sharding import Mesh, PartitionSpec as P


norm_eps = 1e-06
residual_keep = 0.5
Z, X, Y, C = 8, 4, 8, 2
bf16 = jnp.bfloat16
f32 = jnp.float32


def exchange(pieces, axis):
    return lax.all_to_all(pieces, axis, split_axis=0, concat_axis=0, tiled=True)


def to_all(shard, axis):
    size = lax.axis_size(axis)
    return exchange(jnp.broadcast_to(shard[None], (size, *shard.shape)), axis)


def high_low(v):
    high = lax.reduce_precision(v, 8, 7)
    return high.astype(bf16), (v - high).astype(bf16)


def other_core(v):
    return lax.ppermute(v, "core", [(0, 1), (1, 0)])


def half(v, which, axis, size):
    return lax.dynamic_slice_in_dim(v, which * size, size, axis)


def hidden_of(part):
    summed = exchange(part.astype(bf16), "z").astype(f32).sum(axis=0)
    chunk = jnp.square(jnp.maximum(summed, 0.0)).astype(bf16)
    whole = to_all(chunk, "z")
    return whole.transpose(1, 0, 2).reshape(whole.shape[1], -1)


def down_sum(hidden, weight):
    core = lax.axis_index("core")
    part = jnp.stack(
        [jnp.dot(hidden, weight[i], preferred_element_type=f32) for i in range(X)]
    )
    t = hidden.shape[0] // C
    got = other_core(half(part.astype(bf16), 1 - core, 1, t))
    mine = half(part, core, 1, t) + got.astype(f32)
    return to_all(mine.astype(bf16), "y").astype(f32).sum(axis=0)


def inv_norm(branch_in, width):
    squares = jnp.sum(branch_in * branch_in, axis=(0, 2))
    squares = to_all(squares[None], "z").sum(axis=0)[0]
    return lax.rsqrt(squares / width + norm_eps)[None, :, None]


def inner(tokens, up_weight, up_scale, down_weight, down_scale, pre_gain, post_gain):
    n_tok, feats = tokens.shape
    hid = up_weight.shape[2]
    width = feats * X * Z
    t_x = n_tok // X
    t_c = t_x // C
    x, core = lax.axis_index("x"), lax.axis_index("core")

    scaled = (tokens.astype(f32) * pre_gain[0][None, :]).astype(bf16)
    part = jnp.dot(scaled, up_weight[0].astype(bf16), preferred_element_type=f32)
    part = (part * up_scale[0][None, :]).astype(bf16).reshape(X, t_x, hid)
    part = exchange(part, "x").astype(f32).sum(axis=0)

    def from_x(send):
        blocks = []
        for s in (1, 2, 3):
            pairs = [(i, (i - s) % X) for i in range(X)]
            blocks.append(lax.ppermute(send(s), "x", pairs))
        return blocks

    vectors = [down_scale[0], post_gain[0], pre_gain[1], down_scale[1], post_gain[1]]
    highs, lows = high_low(jnp.stack(vectors))
    nothing = jnp.zeros((3, feats), bf16)
    columns = jnp.concatenate([highs, nothing, lows, nothing])
    down_w0 = down_weight[0].astype(bf16)

    def tokens_of(s):
        return lax.dynamic_slice_in_dim(tokens, (x - s) % X * t_x, t_x, 0)

    came = from_x(lambda s: jnp.concatenate([down_w0, columns, tokens_of(s)]))
    down_w0 = [down_w0, *(b[:hid] for b in came)]
    columns = jnp.stack([columns, *(b[hid : hid + 16] for b in came)]).astype(f32)
    columns = columns[:, :8] + columns[:, 8:]
    down_0, post_0, pre_1, down_1, post_1 = [columns[:, k : k + 1] for k in range(5)]
    own_tokens = jnp.stack([tokens_of(0), *(b[hid + 16 :] for b in came)])
    own_tokens = half(own_tokens, core, 1, t_c).astype(f32)

    up_w1 = up_weight[1].astype(bf16).reshape(feats, Z, hid // Z).transpose(1, 0, 2)
    down_w1 = down_weight[1].astype(bf16)
    both = jnp.concatenate([up_w1.reshape(hid, feats), down_w1])
    came = from_x(lambda s: both)
    up_w1 = jnp.concatenate([up_w1, *(b[:hid].reshape(up_w1.shape) for b in came)], axis=1)
    down_w1 = [down_w1, *(b[hid:] for b in came)]

    hidden = hidden_of(part.reshape(t_x, Z, hid // Z).transpose(1, 0, 2))
    summed = down_sum(hidden, down_w0)
    branch_in = summed * down_0
    branch = branch_in * inv_norm(branch_in, width) * post_0
    stream = (residual_keep * own_tokens + branch).astype(bf16)

    values = stream.astype(f32)
    scaled = (values * pre_1).astype(bf16)
    got = other_core(scaled)
    first = jnp.where(core == 0, scaled, got)
    second = jnp.where(core == 0, got, scaled)
    scaled = jnp.concatenate([first, second], axis=1).transpose(1, 0, 2).reshape(t_x, X * feats)
    part = jnp.stack(
        [jnp.dot(scaled, up_w1[c], preferred_element_type=f32) for c in range(Z)]
    )
    hidden = hidden_of(part * up_scale[1].reshape(Z, 1, hid // Z))
    summed = down_sum(hidden, down_w1)
    branch_in = summed * down_1
    branch = branch_in * inv_norm(branch_in, width) * post_1
    out = (residual_keep * values + branch).astype(bf16)
    out = lax.dynamic_slice_in_dim(jnp.concatenate([out, out]), (X - x) % X, X, 0)
    out = jnp.broadcast_to(out[:, None], (X, C, t_c, feats)).reshape(X * C, t_c, feats)
    return exchange(out, ("x", "core")).reshape(n_tok, feats)


def solution(mesh):
    split = Mesh(mesh.devices.reshape(Z, X, Y, C), ("z", "x", "y", "core"))
    ra, cb = ("z", "x"), ("y", "core")
    return jax.shard_map(
        inner,
        mesh=split,
        in_specs=(
            P(None, ra),
            P(None, ra, cb),
            P(None, cb),
            P(None, cb, ra),
            P(None, ra),
            P(None, ra),
            P(None, ra),
        ),
        out_specs=P(None, ra),
        check_vma=False,
    )
```

time: 215 us -> 196 us (0.912)
  waiting for transfers between devices: 68.2 us -> 49.3 us
  matrix products: 2.27 us -> 7.96 us
  starting transfers between devices: 76.7 us -> 72.5 us
  local copies, waits for them, and re-layouts: 8.3 us -> 11.1 us
  other arithmetic: 4.77 us -> 2.39 us
    ppermute x9 -> x6, waiting for transfers between devices: 28.1 us -> 17.5 us  [from_x(): blocks.append(lax.ppermute(send(s), 'x', pairs))]
    all_to_all x6, waiting for transfers between devices: 38.4 us -> 29.3 us  [exchange(): return lax.all_to_all(pieces, axis, split_axis=0, concat_axis=0, tiled=True)]
    another operation x2 -> x8, local copies, waits for them, and re-layouts: 0.02 us -> 4.29 us  [the longest x4 2.24 us: inner(): own_tokens = jnp.stack([tokens_of(0), *(b[hid + 16:] for b in came)])]
    ppermute x9 -> x6, starting transfers between devices: 22.8 us -> 18.8 us  [from_x(): blocks.append(lax.ppermute(send(s), 'x', pairs))]
    dot_general x8, matrix products: 1.59 us -> 5.4 us  [down_sum(): jnp.dot(hidden, weight[i], preferred_element_type=f32)]
    convert_element_type x3 -> x1, other arithmetic: 2.24 us -> 0.01 us  [high_low(): return (high.astype(bf16), (v - high).astype(bf16))]
  transfers between devices with their start and end apart: 18 -> 15, of which waited for: 15 -> 9; matrix products, arithmetic and copies ran while one was open for 1% -> 7% of each run, Pallas kernels for 0% -> 0%
where the time goes in v2:
time: 196 us; the launch traced here: 195 us
  starting transfers between devices  72.5 us (37%)
  blocking collectives  51.2 us (26%)
  waiting for transfers between devices  49.3 us (25%)
  local copies, waits for them, and re-layouts  11.1 us (6%)
  matrix products  7.96 us (4%)
  other arithmetic  2.39 us (1%)
    all_to_all x4, blocking collectives, exchange(): return lax.all_to_all(pieces, axis, split_axis=0, concat_axis=0, tiled=True)  51.2 us
    all_to_all x6, starting transfers between devices, exchange(): return lax.all_to_all(pieces, axis, split_axis=0, concat_axis=0, tiled=True)  41.5 us
    all_to_all x6, waiting for transfers between devices, exchange(): return lax.all_to_all(pieces, axis, split_axis=0, concat_axis=0, tiled=True)  29.3 us
    ppermute x6, starting transfers between devices, from_x(): blocks.append(lax.ppermute(send(s), 'x', pairs))  18.8 us
    ppermute x6, waiting for transfers between devices, from_x(): blocks.append(lax.ppermute(send(s), 'x', pairs))  17.5 us
    ppermute x3, starting transfers between devices, other_core(): return lax.ppermute(v, 'core', [(0, 1), (1, 0)])  12.3 us
    dot_general x8, matrix products, down_sum(): jnp.dot(hidden, weight[i], preferred_element_type=f32)  5.4 us
  transfers between devices with their start and end apart: 15, of which 9 were waited for; matrix products, arithmetic and copies ran while one was open for 7% of the time, Pallas kernels for 0%

profile of v2, /device:TPU:1, one launch (start us, length us, event | category | flops | bytes accessed | tf_op | source)
XLA Modules:
  0.0 195.0 jit_solution(9413713575307817575)
XLA Ops:
  0.0 0.8 fusion.58
  0.8 1.3 convert.5
  2.1 1.2 multiply_convert_fusion
  3.4 5.0 %all-to-all-start = ((bf16[4,96,1024]{2,1,0:T(8,128)(2,1)}), bf16[4,96,1024]{2,1,0:T(8,128)(2,1)S(1)}, u32[]{:S(2)}, u32[]{:S(2)}) async-start(bf16[4,96,1024]{2,1,0:T(8,128)(2,1)} %bitcast.8), calls=%async_computation | async-start | bytes 1572864 | tf_op jit(solution)/shard_map/all_to_all | solution.py:15
  8.7 3.4 %collective-permute-start.2 = (bf16[1136,128]{1,0:T(8,128)(2,1)S(1)}, bf16[1136,128]{1,0:T(8,128)(2,1)}, u32[]{:S(2)}, u32[]{:S(2)}) collective-permute-start(bf16[1136,128]{1,0:T(8,128)(2,1)S(1)} %concatenate.29), channel_id=1, source_target_pairs={{0,16},{16,32},{32,48},{48,0},{1,17},{17,33},{33,49},{49,1},{2,18}... | collective-permute-start | bytes 872456 | tf_op jit(solution)/shard_map/ppermute | solution.py:77
  12.2 4.6 %all-to-all-done = bf16[4,96,1024]{2,1,0:T(8,128)(2,1)S(1)} async-done(((bf16[4,96,1024]{2,1,0:T(8,128)(2,1)}), bf16[4,96,1024]{2,1,0:T(8,128)(2,1)S(1)}, u32[]{:S(2)}, u32[]{:S(2)}) %all-to-all-start) | async-done | bytes 786464 | tf_op jit(solution)/shard_map/all_to_all | solution.py:15
  17.0 0.7 copy.25
  17.7 13.1 %all-to-all-start.1 = ((bf16[8,96,128]{2,1,0:T(8,128)(2,1)}), bf16[8,96,128]{2,1,0:T(8,128)(2,1)S(1)}, u32[]{:S(2)}, u32[]{:S(2)}) async-start(bf16[8,96,128]{2,1,0:T(8,128)(2,1)} %copy.25), calls=%async_computation.1 | async-start | bytes 393216 | tf_op jit(solution)/shard_map/all_to_all | solution.py:15
  30.8 2.1 %collective-permute-start.7 = (bf16[2048,128]{1,0:T(8,128)(2,1)S(1)}, bf16[2048,128]{1,0:T(8,128)(2,1)S(1)}, u32[]{:S(2)}, u32[]{:S(2)}) collective-permute-start(bf16[2048,128]{1,0:T(8,128)(2,1)S(1)} %pad_maximum_fusion.1), channel_id=1, source_target_pairs={{0,16},{16,32},{32,48},{48,0},{1,17},{17,33},{33,49},{49,1},{2,18}... | collective-permute-start | bytes 1572872 | tf_op jit(solution)/shard_map/ppermute | solution.py:77
  32.9 3.7 %collective-permute-start.6 = (bf16[2048,128]{1,0:T(8,128)(2,1)S(1)}, bf16[2048,128]{1,0:T(8,128)(2,1)S(1)}, u32[]{:S(2)}, u32[]{:S(2)}) collective-permute-start(bf16[2048,128]{1,0:T(8,128)(2,1)S(1)} %pad_maximum_fusion.1), channel_id=1, source_target_pairs={{0,32},{16,48},{32,0},{48,16},{1,33},{17,49},{33,1},{49,17},{2,34}... | collective-permute-start | bytes 1572872 | tf_op jit(solution)/shard_map/ppermute | solution.py:77
  36.6 2.6 %collective-permute-start.5 = (bf16[2048,128]{1,0:T(8,128)(2,1)S(1)}, bf16[2048,128]{1,0:T(8,128)(2,1)}, u32[]{:S(2)}, u32[]{:S(2)}) collective-permute-start(bf16[2048,128]{1,0:T(8,128)(2,1)S(1)} %pad_maximum_fusion.1), channel_id=1, source_target_pairs={{0,48},{16,0},{32,16},{48,32},{1,49},{17,1},{33,17},{49,33},{2,50}... | collective-permute-start | bytes 1572872 | tf_op jit(solution)/shard_map/ppermute | solution.py:77
  39.4 4.3 %collective-permute-start.1 = (bf16[1136,128]{1,0:T(8,128)(2,1)S(1)}, bf16[1136,128]{1,0:T(8,128)(2,1)}, u32[]{:S(2)}, u32[]{:S(2)}) collective-permute-start(bf16[1136,128]{1,0:T(8,128)(2,1)S(1)} %concatenate.28), channel_id=1, source_target_pairs={{0,32},{16,48},{32,0},{48,16},{1,33},{17,49},{33,1},{49,17},{2,34}... | collective-permute-start | bytes 872456 | tf_op jit(solution)/shard_map/ppermute | solution.py:77
  43.9 2.8 %collective-permute-start = (bf16[1136,128]{1,0:T(8,128)(2,1)S(1)}, bf16[1136,128]{1,0:T(8,128)(2,1)}, u32[]{:S(2)}, u32[]{:S(2)}) collective-permute-start(bf16[1136,128]{1,0:T(8,128)(2,1)S(1)} %concatenate.27), channel_id=1, source_target_pairs={{0,48},{16,0},{32,16},{48,32},{1,49},{17,1},{33,17},{49,33},{2,50}... | collective-permute-start | bytes 872456 | tf_op jit(solution)/shard_map/ppermute | solution.py:77
  46.6 0.7 slice_bitcast_fusion.22
  47.4 0.7 broadcast_in_dim.17
  48.1 6.6 %all-to-all-start.2 = ((bf16[8,96,128]{2,1,0:T(8,128)(2,1)}), bf16[8,96,128]{2,1,0:T(8,128)(2,1)S(1)}, u32[]{:S(2)}, u32[]{:S(2)}) async-start(bf16[8,96,128]{2,1,0:T(8,128)(2,1)} %broadcast_in_dim.17), calls=%async_computation.2 | async-start | bytes 393216 | tf_op jit(solution)/shard_map/all_to_all | solution.py:15
  54.7 7.5 %collective-permute-done.1 = bf16[1136,128]{1,0:T(8,128)(2,1)} collective-permute-done((bf16[1136,128]{1,0:T(8,128)(2,1)S(1)}, bf16[1136,128]{1,0:T(8,128)(2,1)}, u32[]{:S(2)}, u32[]{:S(2)}) %collective-permute-start.1) | collective-permute-done | bytes 290848 | tf_op jit(solution)/shard_map/ppermute | solution.py:77
  62.3 0.7 slice_bitcast_fusion.23
  62.9 10.0 %collective-permute-done = bf16[1136,128]{1,0:T(8,128)(2,1)} collective-permute-done((bf16[1136,128]{1,0:T(8,128)(2,1)S(1)}, bf16[1136,128]{1,0:T(8,128)(2,1)}, u32[]{:S(2)}, u32[]{:S(2)}) %collective-permute-start) | collective-permute-done | bytes 290848 | tf_op jit(solution)/shard_map/ppermute | solution.py:77
  72.9 0.7 slice_bitcast_fusion.24
  73.6 1.1 convolution_bitcast_fusion.12
  74.8 1.1 convolution_bitcast_fusion.13
  75.9 1.1 convolution_bitcast_fusion.14
  77.3 3.6 %collective-permute-start.3 = (bf16[4,48,128]{2,1,0:T(8,128)(2,1)S(1)}, bf16[4,48,128]{2,1,0:T(8,128)(2,1)S(1)}, u32[]{:S(2)}, u32[]{:S(2)}) collective-permute-start(bf16[4,48,128]{2,1,0:T(8,128)(2,1)S(1)} %dynamic-slice_convert_fusion.1), channel_id=1, source_target_pairs={{0,1},{1,0},{2,3},{3,2},{4,5},{5,4},{6,7},{7,6},{8,9},{9,8},{10,11... | collective-permute-start | bytes 147464 | tf_op jit(solution)/shard_map/ppermute | solution.py:29
  80.9 0.8 collective-permute-done.3
  81.8 0.8 broadcast_in_dim.18
  82.6 6.8 %all-to-all-start.3 = ((bf16[8,4,48,128]{3,2,1,0:T(8,128)(2,1)}), bf16[8,4,48,128]{3,2,1,0:T(8,128)(2,1)S(1)}, u32[]{:S(2)}, u32[]{:S(2)}) async-start(bf16[8,4,48,128]{3,2,1,0:T(8,128)(2,1)} %broadcast_in_dim.18), calls=%async_computation.3 | async-start | bytes 786432 | tf_op jit(solution)/shard_map/all_to_all | solution.py:15
  89.4 0.7 slice_bitcast_fusion.19
  90.2 0.7 slice_bitcast_fusion.20
  90.9 13.6 %all-to-all-done.3 = bf16[8,4,48,128]{3,2,1,0:T(8,128)(2,1)S(1)} async-done(((bf16[8,4,48,128]{3,2,1,0:T(8,128)(2,1)}), bf16[8,4,48,128]{3,2,1,0:T(8,128)(2,1)S(1)}, u32[]{:S(2)}, u32[]{:S(2)}) %all-to-all-start.3) | async-done | bytes 393248 | tf_op jit(solution)/shard_map/all_to_all | solution.py:15
  104.7 0.6 broadcast_in_dim.19
  105.4 6.6 %all-to-all-start.4 = ((f32[8,1,48]{2,1,0:T(1,128)}), f32[8,1,48]{2,1,0:T(1,128)S(1)}, u32[]{:S(2)}, u32[]{:S(2)}) async-start(f32[8,1,48]{2,1,0:T(1,128)} %broadcast_in_dim.19), calls=%async_computation.4 | async-start | bytes 8192 | tf_op jit(solution)/shard_map/all_to_all | solution.py:15
  112.0 0.7 slice_bitcast_fusion.21
  112.8 1.0 slice.186
  113.8 4.7 %all-to-all-done.4 = f32[8,1,48]{2,1,0:T(1,128)S(1)} async-done(((f32[8,1,48]{2,1,0:T(1,128)}), f32[8,1,48]{2,1,0:T(1,128)S(1)}, u32[]{:S(2)}, u32[]{:S(2)}) %all-to-all-start.4) | async-done | bytes 1568 | tf_op jit(solution)/shard_map/all_to_all | solution.py:15
  118.6 3.8 %collective-permute-start.4 = (bf16[4,48,128]{2,1,0:T(8,128)(2,1)S(1)}, bf16[4,48,128]{2,1,0:T(8,128)(2,1)S(1)}, u32[]{:S(2)}, u32[]{:S(2)}) collective-permute-start(bf16[4,48,128]{2,1,0:T(8,128)(2,1)S(1)} %get-tuple-element.5), channel_id=1, source_target_pairs={{0,1},{1,0},{2,3},{3,2},{4,5},{5,4},{6,7},{7,6},{8,9},{9,8},{10,11... | collective-permute-start | bytes 147464 | tf_op jit(solution)/shard_map/ppermute | solution.py:29
  122.5 0.8 collective-permute-done.4
  124.8 12.5 %all_to_all.50 = bf16[8,96,128]{2,1,0:T(8,128)(2,1)S(1)} all-to-all(bf16[8,96,128]{2,1,0:T(8,128)(2,1)S(1)} %multiply_convert_fusion.1), channel_id=1, replica_groups=mesh['z'=8,'x'=4,'y'=8,'core'=2] {'z'}, dimensions={0} | all-to-all | bytes 393216 | tf_op jit(solution)/shard_map/all_to_all | solution.py:15
  137.3 10.9 %all_to_all.51 = bf16[8,96,128]{2,1,0:T(8,128)(2,1)S(1)} all-to-all(bf16[8,96,128]{2,1,0:T(8,128)(2,1)S(1)} %broadcast_in_dim.20), channel_id=1, replica_groups=mesh['z'=8,'x'=4,'y'=8,'core'=2] {'z'}, dimensions={0} | all-to-all | bytes 393216 | tf_op jit(solution)/shard_map/all_to_all | solution.py:15
  148.7 1.2 convolution_bitcast_fusion.10
  150.1 4.8 %collective-permute-start.8 = (bf16[4,48,128]{2,1,0:T(8,128)(2,1)S(1)}, bf16[4,48,128]{2,1,0:T(8,128)(2,1)S(1)}, u32[]{:S(2)}, u32[]{:S(2)}) collective-permute-start(bf16[4,48,128]{2,1,0:T(8,128)(2,1)S(1)} %dynamic-slice_convert_fusion), channel_id=1, source_target_pairs={{0,1},{1,0},{2,3},{3,2},{4,5},{5,4},{6,7},{7,6},{8,9},{9,8},{10,11... | collective-permute-start | bytes 147464 | tf_op jit(solution)/shard_map/ppermute | solution.py:29
  154.9 0.9 collective-permute-done.8
  155.9 17.5 %all_to_all.52 = bf16[8,4,48,128]{3,2,1,0:T(8,128)(2,1)S(1)} all-to-all(bf16[8,4,48,128]{3,2,1,0:T(8,128)(2,1)S(1)} %broadcast_in_dim.21), channel_id=1, replica_groups=mesh['z'=8,'x'=4,'y'=8,'core'=2] {'y'}, dimensions={0} | all-to-all | bytes 786432 | tf_op jit(solution)/shard_map/all_to_all | solution.py:15
  173.6 0.6 broadcast_in_dim.22
  174.2 3.3 %all-to-all-start.8 = ((f32[8,1,48]{2,1,0:T(1,128)}), f32[8,1,48]{2,1,0:T(1,128)S(1)}, u32[]{:S(2)}, u32[]{:S(2)}) async-start(f32[8,1,48]{2,1,0:T(1,128)} %broadcast_in_dim.22), calls=%async_computation.8 | async-start | bytes 8192 | tf_op jit(solution)/shard_map/all_to_all | solution.py:15
  177.5 6.4 %all-to-all-done.8 = f32[8,1,48]{2,1,0:T(1,128)S(1)} async-done(((f32[8,1,48]{2,1,0:T(1,128)}), f32[8,1,48]{2,1,0:T(1,128)S(1)}, u32[]{:S(2)}, u32[]{:S(2)}) %all-to-all-start.8) | async-done | bytes 1568 | tf_op jit(solution)/shard_map/all_to_all | solution.py:15
  184.1 10.3 %all_to_all.53 = bf16[8,48,128]{2,1,0:T(8,128)(2,1)S(1)} all-to-all(bf16[8,48,128]{2,1,0:T(8,128)(2,1)S(1)} %bitcast.217), channel_id=1, replica_groups=mesh['z'=8,'x'=4,'y'=8,'core'=2] {'x','core'}, dimensions={0} | all-to-all | bytes 196608 | tf_op jit(solution)/shard_map/all_to_all | solution.py:15
  194.4 0.6 copy.112
  (77 shorter events, 4.2 us)
Async XLA Ops:
  0.0 2.1 %copy-start.3 = (f32[2,128]{1,0:T(2,128)S(1)}, f32[2,128]{1,0:T(2,128)}, u32[]{:S(2)}) copy-start(f32[2,128]{1,0:T(2,128)} %param.12) | copy-start | bytes 3076
  0.0 2.1 %copy-start.4 = (f32[2,128]{1,0:T(2,128)S(1)}, f32[2,128]{1,0:T(2,128)}, u32[]{:S(2)}) copy-start(f32[2,128]{1,0:T(2,128)} %param.13) | copy-start | bytes 3076
  0.0 2.1 %copy-start = (bf16[384,128]{1,0:T(8,128)(2,1)S(1)}, bf16[384,128]{1,0:T(8,128)(2,1)}, u32[]{:S(2)}) copy-start(bf16[384,128]{1,0:T(8,128)(2,1)} %param.7) | copy-start | bytes 294916
  3.4 5.0 %copy-start.2 = (f32[2,128]{1,0:T(2,128)S(1)}, f32[2,128]{1,0:T(2,128)}, u32[]{:S(2)}) copy-start(f32[2,128]{1,0:T(2,128)} %param.11) | copy-start | bytes 3076
  3.4 5.1 %copy-start.1 = (f32[2,1024,128]{2,1,0:T(8,128)S(1)}, f32[2,1024,128]{2,1,0:T(8,128)}, u32[]{:S(2)}) copy-start(f32[2,1024,128]{2,1,0:T(8,128)} %param.10) | copy-start | bytes 3145732
  3.4 13.4 %all-to-all-start = ((bf16[4,96,1024]{2,1,0:T(8,128)(2,1)}), bf16[4,96,1024]{2,1,0:T(8,128)(2,1)S(1)}, u32[]{:S(2)}, u32[]{:S(2)}) async-start(bf16[4,96,1024]{2,1,0:T(8,128)(2,1)} %bitcast.8), calls=%async_computation | async-start | bytes 1572864 | tf_op jit(solution)/shard_map/all_to_all | solution.py:15
  8.7 35.1 %collective-permute-start.2 = (bf16[1136,128]{1,0:T(8,128)(2,1)S(1)}, bf16[1136,128]{1,0:T(8,128)(2,1)}, u32[]{:S(2)}, u32[]{:S(2)}) collective-permute-start(bf16[1136,128]{1,0:T(8,128)(2,1)S(1)} %concatenate.29), channel_id=1, source_target_pairs={{0,16},{16,32},{32,48},{48,0},{1,17},{17,33},{33,49},{49,1},{2,18}... | collective-permute-start | bytes 872456 | tf_op jit(solution)/shard_map/ppermute | solution.py:77
  17.7 29.6 %all-to-all-start.1 = ((bf16[8,96,128]{2,1,0:T(8,128)(2,1)}), bf16[8,96,128]{2,1,0:T(8,128)(2,1)S(1)}, u32[]{:S(2)}, u32[]{:S(2)}) async-start(bf16[8,96,128]{2,1,0:T(8,128)(2,1)} %copy.25), calls=%async_computation.1 | async-start | bytes 393216 | tf_op jit(solution)/shard_map/all_to_all | solution.py:15
  30.8 82.0 %collective-permute-start.7 = (bf16[2048,128]{1,0:T(8,128)(2,1)S(1)}, bf16[2048,128]{1,0:T(8,128)(2,1)S(1)}, u32[]{:S(2)}, u32[]{:S(2)}) collective-permute-start(bf16[2048,128]{1,0:T(8,128)(2,1)S(1)} %pad_maximum_fusion.1), channel_id=1, source_target_pairs={{0,16},{16,32},{32,48},{48,0},{1,17},{17,33},{33,49},{49,1},{2,18}... | collective-permute-start | bytes 1572872 | tf_op jit(solution)/shard_map/ppermute | solution.py:77
  32.9 79.8 %collective-permute-start.6 = (bf16[2048,128]{1,0:T(8,128)(2,1)S(1)}, bf16[2048,128]{1,0:T(8,128)(2,1)S(1)}, u32[]{:S(2)}, u32[]{:S(2)}) collective-permute-start(bf16[2048,128]{1,0:T(8,128)(2,1)S(1)} %pad_maximum_fusion.1), channel_id=1, source_target_pairs={{0,32},{16,48},{32,0},{48,16},{1,33},{17,49},{33,1},{49,17},{2,34}... | collective-permute-start | bytes 1572872 | tf_op jit(solution)/shard_map/ppermute | solution.py:77
  36.6 76.2 %collective-permute-start.5 = (bf16[2048,128]{1,0:T(8,128)(2,1)S(1)}, bf16[2048,128]{1,0:T(8,128)(2,1)}, u32[]{:S(2)}, u32[]{:S(2)}) collective-permute-start(bf16[2048,128]{1,0:T(8,128)(2,1)S(1)} %pad_maximum_fusion.1), channel_id=1, source_target_pairs={{0,48},{16,0},{32,16},{48,32},{1,49},{17,1},{33,17},{49,33},{2,50}... | collective-permute-start | bytes 1572872 | tf_op jit(solution)/shard_map/ppermute | solution.py:77
  39.4 22.8 %collective-permute-start.1 = (bf16[1136,128]{1,0:T(8,128)(2,1)S(1)}, bf16[1136,128]{1,0:T(8,128)(2,1)}, u32[]{:S(2)}, u32[]{:S(2)}) collective-permute-start(bf16[1136,128]{1,0:T(8,128)(2,1)S(1)} %concatenate.28), channel_id=1, source_target_pairs={{0,32},{16,48},{32,0},{48,16},{1,33},{17,49},{33,1},{49,17},{2,34}... | collective-permute-start | bytes 872456 | tf_op jit(solution)/shard_map/ppermute | solution.py:77
  43.9 29.0 %collective-permute-start = (bf16[1136,128]{1,0:T(8,128)(2,1)S(1)}, bf16[1136,128]{1,0:T(8,128)(2,1)}, u32[]{:S(2)}, u32[]{:S(2)}) collective-permute-start(bf16[1136,128]{1,0:T(8,128)(2,1)S(1)} %concatenate.27), channel_id=1, source_target_pairs={{0,48},{16,0},{32,16},{48,32},{1,49},{17,1},{33,17},{49,33},{2,50}... | collective-permute-start | bytes 872456 | tf_op jit(solution)/shard_map/ppermute | solution.py:77
  48.1 25.5 %all-to-all-start.2 = ((bf16[8,96,128]{2,1,0:T(8,128)(2,1)}), bf16[8,96,128]{2,1,0:T(8,128)(2,1)S(1)}, u32[]{:S(2)}, u32[]{:S(2)}) async-start(bf16[8,96,128]{2,1,0:T(8,128)(2,1)} %broadcast_in_dim.17), calls=%async_computation.2 | async-start | bytes 393216 | tf_op jit(solution)/shard_map/all_to_all | solution.py:15
  77.3 4.5 %collective-permute-start.3 = (bf16[4,48,128]{2,1,0:T(8,128)(2,1)S(1)}, bf16[4,48,128]{2,1,0:T(8,128)(2,1)S(1)}, u32[]{:S(2)}, u32[]{:S(2)}) collective-permute-start(bf16[4,48,128]{2,1,0:T(8,128)(2,1)S(1)} %dynamic-slice_convert_fusion.1), channel_id=1, source_target_pairs={{0,1},{1,0},{2,3},{3,2},{4,5},{5,4},{6,7},{7,6},{8,9},{9,8},{10,11... | collective-permute-start | bytes 147464 | tf_op jit(solution)/shard_map/ppermute | solution.py:29
  82.6 22.0 %all-to-all-start.3 = ((bf16[8,4,48,128]{3,2,1,0:T(8,128)(2,1)}), bf16[8,4,48,128]{3,2,1,0:T(8,128)(2,1)S(1)}, u32[]{:S(2)}, u32[]{:S(2)}) async-start(bf16[8,4,48,128]{3,2,1,0:T(8,128)(2,1)} %broadcast_in_dim.18), calls=%async_computation.3 | async-start | bytes 786432 | tf_op jit(solution)/shard_map/all_to_all | solution.py:15
  105.4 13.1 %all-to-all-start.4 = ((f32[8,1,48]{2,1,0:T(1,128)}), f32[8,1,48]{2,1,0:T(1,128)S(1)}, u32[]{:S(2)}, u32[]{:S(2)}) async-start(f32[8,1,48]{2,1,0:T(1,128)} %broadcast_in_dim.19), calls=%async_computation.4 | async-start | bytes 8192 | tf_op jit(solution)/shard_map/all_to_all | solution.py:15
  118.6 4.7 %collective-permute-start.4 = (bf16[4,48,128]{2,1,0:T(8,128)(2,1)S(1)}, bf16[4,48,128]{2,1,0:T(8,128)(2,1)S(1)}, u32[]{:S(2)}, u32[]{:S(2)}) collective-permute-start(bf16[4,48,128]{2,1,0:T(8,128)(2,1)S(1)} %get-tuple-element.5), channel_id=1, source_target_pairs={{0,1},{1,0},{2,3},{3,2},{4,5},{5,4},{6,7},{7,6},{8,9},{9,8},{10,11... | collective-permute-start | bytes 147464 | tf_op jit(solution)/shard_map/ppermute | solution.py:29
  150.1 5.7 %collective-permute-start.8 = (bf16[4,48,128]{2,1,0:T(8,128)(2,1)S(1)}, bf16[4,48,128]{2,1,0:T(8,128)(2,1)S(1)}, u32[]{:S(2)}, u32[]{:S(2)}) collective-permute-start(bf16[4,48,128]{2,1,0:T(8,128)(2,1)S(1)} %dynamic-slice_convert_fusion), channel_id=1, source_target_pairs={{0,1},{1,0},{2,3},{3,2},{4,5},{5,4},{6,7},{7,6},{8,9},{9,8},{10,11... | collective-permute-start | bytes 147464 | tf_op jit(solution)/shard_map/ppermute | solution.py:29
  174.2 9.7 %all-to-all-start.8 = ((f32[8,1,48]{2,1,0:T(1,128)}), f32[8,1,48]{2,1,0:T(1,128)S(1)}, u32[]{:S(2)}, u32[]{:S(2)}) async-start(f32[8,1,48]{2,1,0:T(1,128)} %broadcast_in_dim.22), calls=%async_computation.8 | async-start | bytes 8192 | tf_op jit(solution)/shard_map/all_to_all | solution.py:15

commit v3 on v2

v3 whole, which is shorter than its diff:
```python
import jax
import jax.numpy as jnp
from jax import lax
from jax.sharding import Mesh, PartitionSpec as P


norm_eps = 1e-06
residual_keep = 0.5
Z, X, Y, C = 8, 4, 8, 2
bf16 = jnp.bfloat16
f32 = jnp.float32


def exchange(pieces, axis):
    return lax.all_to_all(pieces, axis, split_axis=0, concat_axis=0, tiled=True)


def to_all(shard, axis):
    size = lax.axis_size(axis)
    return exchange(jnp.broadcast_to(shard[None], (size, *shard.shape)), axis)


def high_low(v):
    high = lax.reduce_precision(v, 8, 7)
    return high.astype(bf16), (v - high).astype(bf16)


def shared(chunk):
    whole = to_all(chunk, "z")
    return whole.transpose(1, 0, 2).reshape(whole.shape[1], -1)


def activation(up):
    return jnp.square(jnp.maximum(up, 0.0)).astype(bf16)


def down_share(hidden, weight):
    part = jnp.stack(
        [jnp.dot(hidden, weight[i], preferred_element_type=f32) for i in range(X)]
    ).astype(bf16)
    pieces = part.reshape(Y * C, -1, part.shape[2])
    return exchange(pieces, ("y", "core")).astype(f32).sum(axis=0).astype(bf16)


def down_whole(mine):
    return to_all(mine, ("y", "core")).reshape(X, -1, mine.shape[1])


def after(blocks, value):
    return [lax.optimization_barrier((b, value))[0] for b in blocks]


def inner(tokens, up_weight, up_scale, down_weight, down_scale, pre_gain, post_gain):
    n_tok, feats = tokens.shape
    hid = up_weight.shape[2]
    width = feats * X * Z
    t_x = n_tok // X
    x = lax.axis_index("x")

    scaled = (tokens.astype(f32) * pre_gain[0][None, :]).astype(bf16)
    part = jnp.dot(scaled, up_weight[0].astype(bf16), preferred_element_type=f32)
    part = (part * up_scale[0][None, :]).astype(bf16).reshape(X, t_x, hid)
    part = exchange(part, "x").astype(f32).sum(axis=0)

    def from_x(send):
        blocks = []
        for s in (1, 2, 3):
            pairs = [(i, (i - s) % X) for i in range(X)]
            blocks.append(lax.ppermute(send(s), "x", pairs))
        return blocks

    vectors = [down_scale[0], post_gain[0], pre_gain[1], down_scale[1], post_gain[1]]
    highs, lows = high_low(jnp.stack(vectors))
    nothing = jnp.zeros((3, feats), bf16)
    columns = jnp.concatenate([highs, nothing, lows, nothing])
    down_w0 = down_weight[0].astype(bf16)

    def tokens_of(s):
        return lax.dynamic_slice_in_dim(tokens, (x - s) % X * t_x, t_x, 0)

    first = from_x(lambda s: jnp.concatenate([down_w0, columns, tokens_of(s)]))

    up_w1 = up_weight[1].astype(bf16).reshape(feats, Z, hid // Z).transpose(1, 0, 2)
    down_w1 = down_weight[1].astype(bf16)
    both = jnp.concatenate([up_w1.reshape(hid, feats), down_w1])
    second = from_x(lambda s: both)

    pieces = part.astype(bf16).reshape(t_x, Z, hid // Z).transpose(1, 0, 2)
    summed = exchange(pieces, "z").astype(f32).sum(axis=0)
    hidden = shared(activation(summed))
    came = after(first, hidden)
    down_w0 = [down_w0, *(b[:hid] for b in came)]
    columns = jnp.stack([columns, *(b[hid : hid + 16] for b in came)]).astype(f32)
    columns = columns[:, :8] + columns[:, 8:]
    down_0, post_0, pre_1, down_1, post_1 = [columns[:, k : k + 1] for k in range(5)]
    own_tokens = jnp.stack([tokens_of(0), *(b[hid + 16 :] for b in came)])
    own_tokens = own_tokens.astype(f32)
    mine = down_share(hidden, down_w0)
    came = after(second, mine)
    up_w1 = jnp.concatenate([up_w1, *(b[:hid].reshape(up_w1.shape) for b in came)], axis=1)
    down_w1 = [down_w1, *(b[hid:] for b in came)]
    branch_in = down_whole(mine).astype(f32) * down_0

    kept = residual_keep * own_tokens
    squares = jnp.sum(branch_in * branch_in, axis=(0, 2))
    terms = jnp.concatenate([kept * pre_1, branch_in * (post_0 * pre_1)], axis=1).astype(bf16)
    terms = terms.transpose(1, 0, 2).reshape(2 * t_x, X * feats)
    part = jnp.stack(
        [jnp.dot(terms, up_w1[c], preferred_element_type=f32) for c in range(Z)]
    )
    part = (part * up_scale[1].reshape(Z, 1, hid // Z)).astype(bf16)
    rows = jnp.stack(high_low(jnp.pad(squares, (0, feats - t_x))))
    rows = jnp.broadcast_to(jnp.pad(rows, ((0, 6), (0, 0)))[None], (Z, 8, feats))
    came = exchange(jnp.concatenate([part, rows], axis=1), "z").astype(f32)
    summed = came[:, : 2 * t_x].sum(axis=0)
    squares = came[:, 2 * t_x : 2 * t_x + 2].sum(axis=(0, 1))[:t_x]
    inv = lax.rsqrt(squares / width + norm_eps)[:, None]
    hidden = shared(activation(summed[:t_x] + summed[t_x:] * inv))
    stream = (kept + branch_in * inv[None] * post_0).astype(bf16)

    branch_in = down_whole(down_share(hidden, down_w1)).astype(f32) * down_1
    squares = jnp.sum(branch_in * branch_in, axis=(0, 2))
    squares = to_all(squares[None], "z").sum(axis=0)[0]
    inv = lax.rsqrt(squares / width + norm_eps)[None, :, None]
    out = (residual_keep * stream.astype(f32) + branch_in * inv * post_1).astype(bf16)
    out = lax.dynamic_slice_in_dim(jnp.concatenate([out, out]), (X - x) % X, X, 0)
    return exchange(out, "x").reshape(n_tok, feats)


def solution(mesh):
    split = Mesh(mesh.devices.reshape(Z, X, Y, C), ("z", "x", "y", "core"))
    ra, cb = ("z", "x"), ("y", "core")
    return jax.shard_map(
        inner,
        mesh=split,
        in_specs=(
            P(None, ra),
            P(None, ra, cb),
            P(None, cb),
            P(None, cb, ra),
            P(None, ra),
            P(None, ra),
            P(None, ra),
        ),
        out_specs=P(None, ra),
        check_vma=False,
    )
```

time: 196 us -> 196 us (level)
  starting transfers between devices: 72.5 us -> 58.2 us
  blocking collectives: 51.2 us -> 65 us
    all_to_all x4 -> x5, blocking collectives: 51.2 us -> 65 us  [exchange(): return lax.all_to_all(pieces, axis, split_axis=0, concat_axis=0, tiled=True)]
    ppermute x3 -> x0, starting transfers between devices: 12.3 us -> none  [other_core(): return lax.ppermute(v, 'core', [(0, 1), (1, 0)])]
    ppermute x6, waiting for transfers between devices: 17.5 us -> 20.7 us  [from_x(): blocks.append(lax.ppermute(send(s), 'x', pairs))]
    ppermute x3 -> x0, waiting for transfers between devices: 2.48 us -> none  [other_core(): return lax.ppermute(v, 'core', [(0, 1), (1, 0)])]
  transfers between devices with their start and end apart: 15 -> 12, of which waited for: 9 -> 8; matrix products, arithmetic and copies ran while one was open for 7% -> 4% of each run, Pallas kernels for 0% -> 0%
where the time goes in v3:
time: 196 us; the launch traced here: 194 us
  blocking collectives  65 us (33%)
  starting transfers between devices  58.2 us (30%)
  waiting for transfers between devices  50.4 us (26%)
  local copies, waits for them, and re-layouts  9.6 us (5%)
  matrix products  7.26 us (4%)
  other arithmetic  3.27 us (2%)
    all_to_all x5, blocking collectives, exchange(): return lax.all_to_all(pieces, axis, split_axis=0, concat_axis=0, tiled=True)  65 us
    all_to_all x6, starting transfers between devices, exchange(): return lax.all_to_all(pieces, axis, split_axis=0, concat_axis=0, tiled=True)  40.2 us
    all_to_all x6, waiting for transfers between devices, exchange(): return lax.all_to_all(pieces, axis, split_axis=0, concat_axis=0, tiled=True)  29.7 us
    ppermute x6, waiting for transfers between devices, from_x(): blocks.append(lax.ppermute(send(s), 'x', pairs))  20.7 us
    ppermute x6, starting transfers between devices, from_x(): blocks.append(lax.ppermute(send(s), 'x', pairs))  18 us
    dot_general x8, matrix products, down_share(): jnp.dot(hidden, weight[i], preferred_element_type=f32)  4.46 us
  transfers between devices with their start and end apart: 12, of which 8 were waited for; matrix products, arithmetic and copies ran while one was open for 4% of the time, Pallas kernels for 0%

profile of v3, /device:TPU:1, one launch (start us, length us, event | category | flops | bytes accessed | tf_op | source)
XLA Modules:
  0.0 194.4 jit_solution(16573320907706178722)
XLA Ops:
  0.0 0.8 fusion.69
  0.8 1.3 convert.47
  2.1 1.2 multiply_convert_fusion
  3.4 4.8 %all-to-all-start = ((bf16[4,96,1024]{2,1,0:T(8,128)(2,1)}), bf16[4,96,1024]{2,1,0:T(8,128)(2,1)S(1)}, u32[]{:S(2)}, u32[]{:S(2)}) async-start(bf16[4,96,1024]{2,1,0:T(8,128)(2,1)} %bitcast.5), calls=%async_computation | async-start | bytes 1572864 | tf_op jit(solution)/shard_map/all_to_all | solution.py:15
  8.3 1.1 copy-done.1
  9.5 7.0 %all-to-all-done = bf16[4,96,1024]{2,1,0:T(8,128)(2,1)S(1)} async-done(((bf16[4,96,1024]{2,1,0:T(8,128)(2,1)}), bf16[4,96,1024]{2,1,0:T(8,128)(2,1)S(1)}, u32[]{:S(2)}, u32[]{:S(2)}) %all-to-all-start) | async-done | bytes 786464 | tf_op jit(solution)/shard_map/all_to_all | solution.py:15
  16.7 0.7 copy.25
  17.4 13.1 %all-to-all-start.1 = ((bf16[8,96,128]{2,1,0:T(8,128)(2,1)}), bf16[8,96,128]{2,1,0:T(8,128)(2,1)S(1)}, u32[]{:S(2)}, u32[]{:S(2)}) async-start(bf16[8,96,128]{2,1,0:T(8,128)(2,1)} %copy.25), calls=%async_computation.1 | async-start | bytes 393216 | tf_op jit(solution)/shard_map/all_to_all | solution.py:15
  30.6 2.2 %collective-permute-start.5 = (bf16[2048,128]{1,0:T(8,128)(2,1)S(1)}, bf16[2048,128]{1,0:T(8,128)(2,1)S(1)}, u32[]{:S(2)}, u32[]{:S(2)}) collective-permute-start(bf16[2048,128]{1,0:T(8,128)(2,1)S(1)} %pad_maximum_fusion.1), channel_id=1, source_target_pairs={{0,16},{16,32},{32,48},{48,0},{1,17},{17,33},{33,49},{49,1},{2,18}... | collective-permute-start | bytes 1572872 | tf_op jit(solution)/shard_map/ppermute | solution.py:69
  32.8 3.7 %collective-permute-start.4 = (bf16[2048,128]{1,0:T(8,128)(2,1)S(1)}, bf16[2048,128]{1,0:T(8,128)(2,1)}, u32[]{:S(2)}, u32[]{:S(2)}) collective-permute-start(bf16[2048,128]{1,0:T(8,128)(2,1)S(1)} %pad_maximum_fusion.1), channel_id=1, source_target_pairs={{0,32},{16,48},{32,0},{48,16},{1,33},{17,49},{33,1},{49,17},{2,34}... | collective-permute-start | bytes 1572872 | tf_op jit(solution)/shard_map/ppermute | solution.py:69
  36.5 2.5 %collective-permute-start.3 = (bf16[2048,128]{1,0:T(8,128)(2,1)S(1)}, bf16[2048,128]{1,0:T(8,128)(2,1)}, u32[]{:S(2)}, u32[]{:S(2)}) collective-permute-start(bf16[2048,128]{1,0:T(8,128)(2,1)S(1)} %pad_maximum_fusion.1), channel_id=1, source_target_pairs={{0,48},{16,0},{32,16},{48,32},{1,49},{17,1},{33,17},{49,33},{2,50}... | collective-permute-start | bytes 1572872 | tf_op jit(solution)/shard_map/ppermute | solution.py:69
  39.3 0.7 broadcast_in_dim.15
  40.0 6.6 %all-to-all-start.2 = ((bf16[8,96,128]{2,1,0:T(8,128)(2,1)}), bf16[8,96,128]{2,1,0:T(8,128)(2,1)S(1)}, u32[]{:S(2)}, u32[]{:S(2)}) async-start(bf16[8,96,128]{2,1,0:T(8,128)(2,1)} %broadcast_in_dim.15), calls=%async_computation.2 | async-start | bytes 393216 | tf_op jit(solution)/shard_map/all_to_all | solution.py:15
  46.8 2.7 %collective-permute-start = (bf16[1136,128]{1,0:T(8,128)(2,1)S(1)}, bf16[1136,128]{1,0:T(8,128)(2,1)S(1)}, u32[]{:S(2)}, u32[]{:S(2)}) collective-permute-start(bf16[1136,128]{1,0:T(8,128)(2,1)S(1)} %concatenate.31), channel_id=1, source_target_pairs={{0,48},{16,0},{32,16},{48,32},{1,49},{17,1},{33,17},{49,33},{2,50}... | collective-permute-start | bytes 872456 | tf_op jit(solution)/shard_map/ppermute | solution.py:69
  49.8 3.7 %collective-permute-start.1 = (bf16[1136,128]{1,0:T(8,128)(2,1)S(1)}, bf16[1136,128]{1,0:T(8,128)(2,1)}, u32[]{:S(2)}, u32[]{:S(2)}) collective-permute-start(bf16[1136,128]{1,0:T(8,128)(2,1)S(1)} %concatenate.32), channel_id=1, source_target_pairs={{0,32},{16,48},{32,0},{48,16},{1,33},{17,49},{33,1},{49,17},{2,34}... | collective-permute-start | bytes 872456 | tf_op jit(solution)/shard_map/ppermute | solution.py:69
  53.6 1.6 all-to-all-done.2
  55.2 13.5 %collective-permute-done = bf16[1136,128]{1,0:T(8,128)(2,1)S(1)} collective-permute-done((bf16[1136,128]{1,0:T(8,128)(2,1)S(1)}, bf16[1136,128]{1,0:T(8,128)(2,1)S(1)}, u32[]{:S(2)}, u32[]{:S(2)}) %collective-permute-start) | collective-permute-done | bytes 290848 | tf_op jit(solution)/shard_map/ppermute | solution.py:69
  68.7 3.1 %collective-permute-start.2 = (bf16[1136,128]{1,0:T(8,128)(2,1)S(1)}, bf16[1136,128]{1,0:T(8,128)(2,1)S(1)}, u32[]{:S(2)}, u32[]{:S(2)}) collective-permute-start(bf16[1136,128]{1,0:T(8,128)(2,1)S(1)} %concatenate.33), channel_id=1, source_target_pairs={{0,16},{16,32},{32,48},{48,0},{1,17},{17,33},{33,49},{49,1},{2,18}... | collective-permute-start | bytes 872456 | tf_op jit(solution)/shard_map/ppermute | solution.py:69
  71.9 0.7 slice_bitcast_fusion.23
  72.6 0.7 slice_bitcast_fusion.20
  73.3 7.3 %collective-permute-done.2 = bf16[1136,128]{1,0:T(8,128)(2,1)S(1)} collective-permute-done((bf16[1136,128]{1,0:T(8,128)(2,1)S(1)}, bf16[1136,128]{1,0:T(8,128)(2,1)S(1)}, u32[]{:S(2)}, u32[]{:S(2)}) %collective-permute-start.2) | collective-permute-done | bytes 290848 | tf_op jit(solution)/shard_map/ppermute | solution.py:69
  80.6 0.2 fusion.8
  80.8 0.2 fusion.9
  81.0 1.1 fusion.10
  82.1 0.2 fusion.11
  82.3 0.7 pad_maximum_fusion.4
  83.0 8.9 %all-to-all-start.3 = ((bf16[16,24,128]{2,1,0:T(8,128)(2,1)}), bf16[16,24,128]{2,1,0:T(8,128)(2,1)S(1)}, u32[]{:S(2)}, u32[]{:S(2)}) async-start(bf16[16,24,128]{2,1,0:T(8,128)(2,1)} %bitcast.15), calls=%async_computation.3 | async-start | bytes 196608 | tf_op jit(solution)/shard_map/all_to_all | solution.py:15
  92.0 8.4 %all-to-all-done.3 = bf16[16,24,128]{2,1,0:T(8,128)(2,1)S(1)} async-done(((bf16[16,24,128]{2,1,0:T(8,128)(2,1)}), bf16[16,24,128]{2,1,0:T(8,128)(2,1)S(1)}, u32[]{:S(2)}, u32[]{:S(2)}) %all-to-all-start.3) | async-done | bytes 98336 | tf_op jit(solution)/shard_map/all_to_all | solution.py:15
  100.4 0.7 broadcast_in_dim.16
  101.1 3.4 %all-to-all-start.4 = ((bf16[16,24,128]{2,1,0:T(8,128)(2,1)}), bf16[16,24,128]{2,1,0:T(8,128)(2,1)S(1)}, u32[]{:S(2)}, u32[]{:S(2)}) async-start(bf16[16,24,128]{2,1,0:T(8,128)(2,1)} %broadcast_in_dim.16), calls=%async_computation.4 | async-start | bytes 196608 | tf_op jit(solution)/shard_map/all_to_all | solution.py:15
  104.6 1.0 slice.169
  105.5 1.0 slice.168
  106.6 6.2 %all-to-all-done.4 = bf16[16,24,128]{2,1,0:T(8,128)(2,1)S(1)} async-done(((bf16[16,24,128]{2,1,0:T(8,128)(2,1)}), bf16[16,24,128]{2,1,0:T(8,128)(2,1)S(1)}, u32[]{:S(2)}, u32[]{:S(2)}) %all-to-all-start.4) | async-done | bytes 98336 | tf_op jit(solution)/shard_map/all_to_all | solution.py:15
  113.3 0.2 fusion.6
  114.1 0.2 fusion.2
  114.9 22.3 %all_to_all.55 = bf16[8,200,128]{2,1,0:T(8,128)(2,1)S(1)} all-to-all(bf16[8,200,128]{2,1,0:T(8,128)(2,1)S(1)} %pad_maximum_fusion.2), channel_id=1, replica_groups=mesh['z'=8,'x'=4,'y'=8,'core'=2] {'z'}, dimensions={0} | all-to-all | bytes 819200 | tf_op jit(solution)/shard_map/all_to_all | solution.py:15
  137.4 12.1 %all_to_all.56 = bf16[8,96,128]{2,1,0:T(8,128)(2,1)S(1)} all-to-all(bf16[8,96,128]{2,1,0:T(8,128)(2,1)S(1)} %broadcast_in_dim.18), channel_id=1, replica_groups=mesh['z'=8,'x'=4,'y'=8,'core'=2] {'z'}, dimensions={0} | all-to-all | bytes 393216 | tf_op jit(solution)/shard_map/all_to_all | solution.py:15
  149.5 1.1 fusion.13
  150.7 1.1 fusion.14
  151.8 0.2 fusion.15
  152.0 0.2 fusion.12
  152.2 12.6 %all_to_all.57 = bf16[16,24,128]{2,1,0:T(8,128)(2,1)S(1)} all-to-all(bf16[16,24,128]{2,1,0:T(8,128)(2,1)S(1)} %bitcast.247), channel_id=1, replica_groups=mesh['z'=8,'x'=4,'y'=8,'core'=2] {'y','core'}, dimensions={0} | all-to-all | bytes 196608 | tf_op jit(solution)/shard_map/all_to_all | solution.py:15
  164.9 10.9 %all_to_all.58 = bf16[16,24,128]{2,1,0:T(8,128)(2,1)S(1)} all-to-all(bf16[16,24,128]{2,1,0:T(8,128)(2,1)S(1)} %broadcast_in_dim.19), channel_id=1, replica_groups=mesh['z'=8,'x'=4,'y'=8,'core'=2] {'y','core'}, dimensions={0} | all-to-all | bytes 196608 | tf_op jit(solution)/shard_map/all_to_all | solution.py:15
  176.0 0.6 broadcast_in_dim.20
  176.6 3.3 %all-to-all-start.9 = ((f32[8,1,96]{2,1,0:T(1,128)}), f32[8,1,96]{2,1,0:T(1,128)S(1)}, u32[]{:S(2)}, u32[]{:S(2)}) async-start(f32[8,1,96]{2,1,0:T(1,128)} %broadcast_in_dim.20), calls=%async_computation.9 | async-start | bytes 8192 | tf_op jit(solution)/shard_map/all_to_all | solution.py:15
  180.0 6.4 %all-to-all-done.9 = f32[8,1,96]{2,1,0:T(1,128)S(1)} async-done(((f32[8,1,96]{2,1,0:T(1,128)}), f32[8,1,96]{2,1,0:T(1,128)S(1)}, u32[]{:S(2)}, u32[]{:S(2)}) %all-to-all-start.9) | async-done | bytes 3104 | tf_op jit(solution)/shard_map/all_to_all | solution.py:15
  186.6 7.2 %all_to_all.59 = bf16[4,96,128]{2,1,0:T(8,128)(2,1)S(1)} all-to-all(bf16[4,96,128]{2,1,0:T(8,128)(2,1)S(1)} %fusion.47), channel_id=1, replica_groups=mesh['z'=8,'x'=4,'y'=8,'core'=2] {'x'}, dimensions={0} | all-to-all | bytes 196608 | tf_op jit(solution)/shard_map/all_to_all | solution.py:15
  193.7 0.6 copy.100
  (79 shorter events, 3.6 us)
Async XLA Ops:
  0.0 2.1 %copy-start.4 = (f32[2,128]{1,0:T(2,128)S(1)}, f32[2,128]{1,0:T(2,128)}, u32[]{:S(2)}) copy-start(f32[2,128]{1,0:T(2,128)} %param.13) | copy-start | bytes 3076
  0.0 2.1 %copy-start.3 = (f32[2,128]{1,0:T(2,128)S(1)}, f32[2,128]{1,0:T(2,128)}, u32[]{:S(2)}) copy-start(f32[2,128]{1,0:T(2,128)} %param.12) | copy-start | bytes 3076
  0.0 2.1 %copy-start = (bf16[384,128]{1,0:T(8,128)(2,1)S(1)}, bf16[384,128]{1,0:T(8,128)(2,1)}, u32[]{:S(2)}) copy-start(bf16[384,128]{1,0:T(8,128)(2,1)} %param.7) | copy-start | bytes 294916
  3.4 13.2 %all-to-all-start = ((bf16[4,96,1024]{2,1,0:T(8,128)(2,1)}), bf16[4,96,1024]{2,1,0:T(8,128)(2,1)S(1)}, u32[]{:S(2)}, u32[]{:S(2)}) async-start(bf16[4,96,1024]{2,1,0:T(8,128)(2,1)} %bitcast.5), calls=%async_computation | async-start | bytes 1572864 | tf_op jit(solution)/shard_map/all_to_all | solution.py:15
  8.2 1.2 copy-start.1
  16.7 22.4 %copy-start.2 = (f32[2,128]{1,0:T(2,128)S(1)}, f32[2,128]{1,0:T(2,128)}, u32[]{:S(2)}) copy-start(f32[2,128]{1,0:T(2,128)} %param.11) | copy-start | bytes 3076
  17.4 21.8 %all-to-all-start.1 = ((bf16[8,96,128]{2,1,0:T(8,128)(2,1)}), bf16[8,96,128]{2,1,0:T(8,128)(2,1)S(1)}, u32[]{:S(2)}, u32[]{:S(2)}) async-start(bf16[8,96,128]{2,1,0:T(8,128)(2,1)} %copy.25), calls=%async_computation.1 | async-start | bytes 393216 | tf_op jit(solution)/shard_map/all_to_all | solution.py:15
  30.6 73.9 %collective-permute-start.5 = (bf16[2048,128]{1,0:T(8,128)(2,1)S(1)}, bf16[2048,128]{1,0:T(8,128)(2,1)S(1)}, u32[]{:S(2)}, u32[]{:S(2)}) collective-permute-start(bf16[2048,128]{1,0:T(8,128)(2,1)S(1)} %pad_maximum_fusion.1), channel_id=1, source_target_pairs={{0,16},{16,32},{32,48},{48,0},{1,17},{17,33},{33,49},{49,1},{2,18}... | collective-permute-start | bytes 1572872 | tf_op jit(solution)/shard_map/ppermute | solution.py:69
  32.8 71.7 %collective-permute-start.4 = (bf16[2048,128]{1,0:T(8,128)(2,1)S(1)}, bf16[2048,128]{1,0:T(8,128)(2,1)}, u32[]{:S(2)}, u32[]{:S(2)}) collective-permute-start(bf16[2048,128]{1,0:T(8,128)(2,1)S(1)} %pad_maximum_fusion.1), channel_id=1, source_target_pairs={{0,32},{16,48},{32,0},{48,16},{1,33},{17,49},{33,1},{49,17},{2,34}... | collective-permute-start | bytes 1572872 | tf_op jit(solution)/shard_map/ppermute | solution.py:69
  36.5 69.0 %collective-permute-start.3 = (bf16[2048,128]{1,0:T(8,128)(2,1)S(1)}, bf16[2048,128]{1,0:T(8,128)(2,1)}, u32[]{:S(2)}, u32[]{:S(2)}) collective-permute-start(bf16[2048,128]{1,0:T(8,128)(2,1)S(1)} %pad_maximum_fusion.1), channel_id=1, source_target_pairs={{0,48},{16,0},{32,16},{48,32},{1,49},{17,1},{33,17},{49,33},{2,50}... | collective-permute-start | bytes 1572872 | tf_op jit(solution)/shard_map/ppermute | solution.py:69
  40.0 15.2 %all-to-all-start.2 = ((bf16[8,96,128]{2,1,0:T(8,128)(2,1)}), bf16[8,96,128]{2,1,0:T(8,128)(2,1)S(1)}, u32[]{:S(2)}, u32[]{:S(2)}) async-start(bf16[8,96,128]{2,1,0:T(8,128)(2,1)} %broadcast_in_dim.15), calls=%async_computation.2 | async-start | bytes 393216 | tf_op jit(solution)/shard_map/all_to_all | solution.py:15
  46.8 21.9 %collective-permute-start = (bf16[1136,128]{1,0:T(8,128)(2,1)S(1)}, bf16[1136,128]{1,0:T(8,128)(2,1)S(1)}, u32[]{:S(2)}, u32[]{:S(2)}) collective-permute-start(bf16[1136,128]{1,0:T(8,128)(2,1)S(1)} %concatenate.31), channel_id=1, source_target_pairs={{0,48},{16,0},{32,16},{48,32},{1,49},{17,1},{33,17},{49,33},{2,50}... | collective-permute-start | bytes 872456 | tf_op jit(solution)/shard_map/ppermute | solution.py:69
  49.8 22.1 %collective-permute-start.1 = (bf16[1136,128]{1,0:T(8,128)(2,1)S(1)}, bf16[1136,128]{1,0:T(8,128)(2,1)}, u32[]{:S(2)}, u32[]{:S(2)}) collective-permute-start(bf16[1136,128]{1,0:T(8,128)(2,1)S(1)} %concatenate.32), channel_id=1, source_target_pairs={{0,32},{16,48},{32,0},{48,16},{1,33},{17,49},{33,1},{49,17},{2,34}... | collective-permute-start | bytes 872456 | tf_op jit(solution)/shard_map/ppermute | solution.py:69
  68.7 11.9 %collective-permute-start.2 = (bf16[1136,128]{1,0:T(8,128)(2,1)S(1)}, bf16[1136,128]{1,0:T(8,128)(2,1)S(1)}, u32[]{:S(2)}, u32[]{:S(2)}) collective-permute-start(bf16[1136,128]{1,0:T(8,128)(2,1)S(1)} %concatenate.33), channel_id=1, source_target_pairs={{0,16},{16,32},{32,48},{48,0},{1,17},{17,33},{33,49},{49,1},{2,18}... | collective-permute-start | bytes 872456 | tf_op jit(solution)/shard_map/ppermute | solution.py:69
  83.0 17.4 %all-to-all-start.3 = ((bf16[16,24,128]{2,1,0:T(8,128)(2,1)}), bf16[16,24,128]{2,1,0:T(8,128)(2,1)S(1)}, u32[]{:S(2)}, u32[]{:S(2)}) async-start(bf16[16,24,128]{2,1,0:T(8,128)(2,1)} %bitcast.15), calls=%async_computation.3 | async-start | bytes 196608 | tf_op jit(solution)/shard_map/all_to_all | solution.py:15
  101.1 11.8 %all-to-all-start.4 = ((bf16[16,24,128]{2,1,0:T(8,128)(2,1)}), bf16[16,24,128]{2,1,0:T(8,128)(2,1)S(1)}, u32[]{:S(2)}, u32[]{:S(2)}) async-start(bf16[16,24,128]{2,1,0:T(8,128)(2,1)} %broadcast_in_dim.16), calls=%async_computation.4 | async-start | bytes 196608 | tf_op jit(solution)/shard_map/all_to_all | solution.py:15
  176.6 9.7 %all-to-all-start.9 = ((f32[8,1,96]{2,1,0:T(1,128)}), f32[8,1,96]{2,1,0:T(1,128)S(1)}, u32[]{:S(2)}, u32[]{:S(2)}) async-start(f32[8,1,96]{2,1,0:T(1,128)} %broadcast_in_dim.20), calls=%async_computation.9 | async-start | bytes 8192 | tf_op jit(solution)/shard_map/all_to_all | solution.py:15

commit v4 on v3

v4 whole, which is shorter than its diff:
```python
import jax
import jax.numpy as jnp
from jax import lax
from jax.experimental import pallas as pl
from jax.experimental.pallas import tpu as pltpu
from jax.sharding import Mesh, PartitionSpec as P


norm_eps = 1e-06
residual_keep = 0.5
Z, X, Y, C = 8, 4, 8, 2
bf16 = jnp.bfloat16
f32 = jnp.float32


def exchange(pieces, axis):
    return lax.all_to_all(pieces, axis, split_axis=0, concat_axis=0, tiled=True)


def to_all(shard, axis):
    size = lax.axis_size(axis)
    return exchange(jnp.broadcast_to(shard[None], (size, *shard.shape)), axis)


def high_low(v):
    high = lax.reduce_precision(v, 8, 7)
    return high.astype(bf16), (v - high).astype(bf16)


def activation(up):
    return jnp.square(jnp.maximum(up, 0.0)).astype(bf16)


def near(v):
    return pltpu.with_memory_space_constraint(v, pltpu.VMEM)


def down_kernel(row, hidden_ref, *refs):
    weights, out_ref, held, sems = refs[:X], refs[X], refs[X + 1], refs[X + 2]
    copies = []
    for i, w in enumerate(weights):
        rows = w.at[pl.ds(row if w.shape[0] > held.shape[1] else 0, held.shape[1])]
        copies.append(pltpu.make_async_copy(rows, held.at[i], sems.at[i]))
        copies[-1].start()
    hidden = jnp.concatenate([hidden_ref[z] for z in range(Z)], axis=1)
    for i in range(X):
        copies[i].wait()
        out_ref[i] = jnp.dot(hidden, held[i], preferred_element_type=f32).astype(bf16)


def down_product(hidden, blocks, row):
    _, t, share = hidden.shape
    feats = blocks[0].shape[1]
    return pl.pallas_call(
        lambda *refs: down_kernel(row, *refs),
        out_shape=pltpu.VMEM((X, t, feats), bf16),
        in_specs=[
            pl.BlockSpec(memory_space=pltpu.VMEM),
            *[pl.BlockSpec(memory_space=pl.ANY)] * X,
        ],
        out_specs=pl.BlockSpec(memory_space=pltpu.VMEM),
        scratch_shapes=[
            pltpu.VMEM((X, Z * share, feats), bf16),
            pltpu.SemaphoreType.DMA((X,)),
        ],
        compiler_params=pltpu.CompilerParams(vmem_limit_bytes=8 << 20),
        name="down_product",
    )(near(hidden), *blocks)


def down_sum(hidden, blocks, row):
    part = down_product(hidden, blocks, row)
    pieces = part.reshape(Y * C, -1, part.shape[2])
    mine = exchange(pieces, ("y", "core")).astype(f32).sum(axis=0).astype(bf16)
    return to_all(mine, ("y", "core")).reshape(part.shape)


def turn_kernel(at, sum_ref, extra_ref, scale_ref, *refs):
    firsts, seconds = refs[: X - 1], refs[X - 1 : 2 * X - 1]
    out_ref, kept_ref, branch_ref, columns_ref = refs[2 * X - 1 : 2 * X + 3]
    extra, held, sems, held_sems = refs[2 * X + 3 :]
    t, feats = sum_ref.shape[1:]
    copies = []
    for i, block in enumerate(firsts):
        rows = block.at[pl.ds(at, extra.shape[1])]
        copies.append(pltpu.make_async_copy(rows, extra.at[i], sems.at[i]))
        copies[-1].start()
    held_copies = []
    for i, block in enumerate(seconds):
        here = held.at[:, pl.ds(i * feats, feats)]
        held_copies.append(pltpu.make_async_copy(block.at[pl.ds(0, Z)], here, held_sems.at[i]))
        held_copies[-1].start()
    for copy in copies:
        copy.wait()
    kept_terms, branch_terms, squares = [], [], jnp.zeros((8, t), f32)
    for i in range(X):
        block = extra_ref[...] if i == 0 else extra[i - 1]
        columns = block[:8].astype(f32) + block[8:16].astype(f32)
        columns_ref[i] = columns
        down_0, post_0, pre_1 = [columns[k : k + 1] for k in range(3)]
        kept = residual_keep * block[16:].astype(f32)
        branch_in = sum_ref[i].astype(f32) * down_0
        branch = branch_in * post_0
        kept_ref[i] = kept
        branch_ref[i] = branch
        kept_terms.append((kept * pre_1).astype(bf16))
        branch_terms.append((branch * pre_1).astype(bf16))
        squares += lax.dot_general(
            jnp.ones((8, feats), f32),
            branch_in * branch_in,
            (((1,), (1,)), ((), ())),
            precision=lax.Precision.HIGHEST,
            preferred_element_type=f32,
        )
    high = squares.astype(bf16).astype(f32)
    row = lax.broadcasted_iota(jnp.int32, squares.shape, 0)
    squares = jnp.where(row == 0, high, jnp.where(row == 1, squares - high, 0.0)).astype(bf16)
    terms = jnp.concatenate(
        [jnp.concatenate(kept_terms, axis=1), jnp.concatenate(branch_terms, axis=1)], axis=0
    )
    for copy in held_copies:
        copy.wait()
    for c in range(Z):
        part = jnp.dot(terms, held[c], preferred_element_type=f32)
        out_ref[c, : 2 * t] = (part * scale_ref[c]).astype(bf16)
        out_ref[c, 2 * t :] = jnp.zeros((8, feats), bf16)
        out_ref[c, 2 * t :, :t] = squares


def turn(summed, extra, scale, firsts, seconds, at):
    _, t, feats = summed.shape
    return pl.pallas_call(
        lambda *refs: turn_kernel(at, *refs),
        out_shape=(
            pltpu.VMEM((Z, 2 * t + 8, feats), bf16),
            pltpu.VMEM((X, t, feats), f32),
            pltpu.VMEM((X, t, feats), f32),
            pltpu.VMEM((X, 8, feats), f32),
        ),
        in_specs=[
            *[pl.BlockSpec(memory_space=pltpu.VMEM)] * 3,
            *[pl.BlockSpec(memory_space=pl.ANY)] * (2 * X - 1),
        ],
        out_specs=(pl.BlockSpec(memory_space=pltpu.VMEM),) * 4,
        scratch_shapes=[
            pltpu.VMEM((X - 1, 16 + t, feats), bf16),
            pltpu.VMEM((Z, X * feats, feats), bf16),
            pltpu.SemaphoreType.DMA((X - 1,)),
            pltpu.SemaphoreType.DMA((X,)),
        ],
        compiler_params=pltpu.CompilerParams(vmem_limit_bytes=12 << 20),
        name="turn",
    )(near(summed), near(extra), near(scale), *firsts, *seconds)


def inner(tokens, up_weight, up_scale, down_weight, down_scale, pre_gain, post_gain):
    n_tok, feats = tokens.shape
    hid = up_weight.shape[2]
    width = feats * X * Z
    t_x = n_tok // X
    x = lax.axis_index("x")

    scaled = (tokens.astype(f32) * pre_gain[0][None, :]).astype(bf16)
    part = jnp.dot(scaled, up_weight[0].astype(bf16), preferred_element_type=f32)
    part = (part * up_scale[0][None, :]).astype(bf16).reshape(X, t_x, hid)
    part = exchange(part, "x").astype(f32).sum(axis=0)

    def from_x(send):
        blocks = []
        for s in (1, 2, 3):
            pairs = [(i, (i - s) % X) for i in range(X)]
            blocks.append(lax.ppermute(send(s), "x", pairs))
        return blocks

    vectors = [down_scale[0], post_gain[0], pre_gain[1], down_scale[1], post_gain[1]]
    highs, lows = high_low(jnp.stack(vectors))
    nothing = jnp.zeros((3, feats), bf16)
    columns = jnp.concatenate([highs, nothing, lows, nothing])
    down_w0 = down_weight[0].astype(bf16)

    def tokens_of(s):
        return lax.dynamic_slice_in_dim(tokens, (x - s) % X * t_x, t_x, 0)

    first = from_x(lambda s: jnp.concatenate([down_w0, columns, tokens_of(s)]))

    up_w1 = up_weight[1].astype(bf16).reshape(feats, Z, hid // Z).transpose(1, 0, 2)
    down_w1 = down_weight[1].astype(bf16)
    both = jnp.concatenate([up_w1.reshape(hid, feats), down_w1])
    second = [both, *from_x(lambda s: both)]

    pieces = part.astype(bf16).reshape(t_x, Z, hid // Z).transpose(1, 0, 2)
    summed = exchange(pieces, "z").astype(f32).sum(axis=0)
    hidden = to_all(activation(summed), "z")
    summed = down_sum(hidden, [down_w0, *first], 0)

    extra = jnp.concatenate([columns, tokens_of(0)])
    scale = up_scale[1].reshape(Z, 1, hid // Z)
    blocks = [b.reshape(2 * Z, feats, hid // Z) for b in second]
    part, kept, branch, columns = turn(summed, extra, scale, first, blocks, hid)
    came = exchange(part, "z").astype(f32)
    summed = came[:, : 2 * t_x].sum(axis=0)
    squares = came[:, 2 * t_x : 2 * t_x + 2].sum(axis=(0, 1))[:t_x]
    inv = lax.rsqrt(squares / width + norm_eps)[:, None]
    hidden = to_all(activation(summed[:t_x] + summed[t_x:] * inv), "z")
    stream = (kept + branch * inv[None]).astype(bf16)
    down_1, post_1 = columns[:, 3:4], columns[:, 4:5]

    branch_in = down_sum(hidden, second, hid).astype(f32) * down_1
    squares = jnp.sum(branch_in * branch_in, axis=(0, 2))
    squares = to_all(squares[None], "z").sum(axis=0)[0]
    inv = lax.rsqrt(squares / width + norm_eps)[None, :, None]
    out = (residual_keep * stream.astype(f32) + branch_in * inv * post_1).astype(bf16)
    out = lax.dynamic_slice_in_dim(jnp.concatenate([out, out]), (X - x) % X, X, 0)
    return exchange(out, "x").reshape(n_tok, feats)


def solution(mesh):
    split = Mesh(mesh.devices.reshape(Z, X, Y, C), ("z", "x", "y", "core"))
    ra, cb = ("z", "x"), ("y", "core")
    return jax.shard_map(
        inner,
        mesh=split,
        in_specs=(
            P(None, ra),
            P(None, ra, cb),
            P(None, cb),
            P(None, cb, ra),
            P(None, ra),
            P(None, ra),
            P(None, ra),
        ),
        out_specs=P(None, ra),
        check_vma=False,
    )
```

time: 196 us -> 181 us (0.923)
  waiting for transfers between devices: 50.4 us -> 29.8 us
  blocking collectives: 65 us -> 73.8 us
  matrix products: 7.26 us -> 1.24 us
  local copies, waits for them, and re-layouts: 9.6 us -> 15 us
  starting transfers between devices: 58.2 us -> 53.4 us
  Pallas kernels: 0 us -> 3.68 us
    ppermute x6, waiting for transfers between devices: 20.7 us -> 0.02 us  [from_x(): blocks.append(lax.ppermute(send(s), 'x', pairs))]
    all_to_all x5, blocking collectives: 65 us -> 73.8 us  [exchange(): return lax.all_to_all(pieces, axis, split_axis=0, concat_axis=0, tiled=True)]
    concatenate x3, local copies, waits for them, and re-layouts: 0.54 us -> 7.79 us  [inner(): first = from_x(lambda s: jnp.concatenate([down_w0, columns, tokens_of(s)]))]
    dot_general x16 -> x0, matrix products: 6.02 us -> none  [the longest x8 4.46 us: down_share(): jnp.dot(hidden, weight[i], preferred_element_type=f32)]
    all_to_all x6, starting transfers between devices: 40.2 us -> 34.9 us  [exchange(): return lax.all_to_all(pieces, axis, split_axis=0, concat_axis=0, tiled=True)]
    pallas_call x0 -> x3, Pallas kernels: none -> 3.68 us  [the longest x2 1.87 us: down_product(): pl.pallas_call(lambda *refs: down_kernel(row, *refs), out_shape=pltpu.VME...]
    slice x5 -> x3, local copies, waits for them, and re-layouts: 2.74 us -> 0.77 us  [the longest x1 0.76 us: inner(): pre_gain[1]]
  transfers between devices with their start and end apart: 12 -> 12, of which waited for: 8 -> 4; matrix products, arithmetic and copies ran while one was open for 4% -> 6% of each run, Pallas kernels for 0% -> 1%
where the time goes in v4:
time: 181 us; the launch traced here: 180 us
  blocking collectives  73.8 us (41%)
  starting transfers between devices  53.4 us (30%)
  waiting for transfers between devices  29.8 us (16%)
  local copies, waits for them, and re-layouts  15 us (8%)
  Pallas kernels  3.68 us (2%)
  other arithmetic  2.22 us (1%)
    all_to_all x5, blocking collectives, exchange(): return lax.all_to_all(pieces, axis, split_axis=0, concat_axis=0, tiled=True)  73.8 us
    all_to_all x6, starting transfers between devices, exchange(): return lax.all_to_all(pieces, axis, split_axis=0, concat_axis=0, tiled=True)  34.9 us
    all_to_all x6, waiting for transfers between devices, exchange(): return lax.all_to_all(pieces, axis, split_axis=0, concat_axis=0, tiled=True)  29.8 us
    ppermute x6, starting transfers between devices, from_x(): blocks.append(lax.ppermute(send(s), 'x', pairs))  18.5 us
    concatenate x3, local copies, waits for them, and re-layouts, inner(): first = from_x(lambda s: jnp.concatenate([down_w0, columns, tokens_of(s)]))  7.79 us
  transfers between devices with their start and end apart: 12, of which 4 were waited for; matrix products, arithmetic and copies ran while one was open for 6% of the time, Pallas kernels for 1%

profile of v4, /device:TPU:1, one launch (start us, length us, event | category | flops | bytes accessed | tf_op | source)
XLA Modules:
  0.0 179.6 jit_solution(9695780364757916396)
XLA Ops:
  0.0 0.8 fusion.14
  0.8 0.8 slice_bitcast_fusion.5
  1.5 1.3 convert.12
  2.9 1.2 multiply_convert_fusion
  4.1 5.0 %all-to-all-start = ((bf16[4,96,1024]{2,1,0:T(8,128)(2,1)}), bf16[4,96,1024]{2,1,0:T(8,128)(2,1)S(1)}, u32[]{:S(2)}, u32[]{:S(2)}) async-start(bf16[4,96,1024]{2,1,0:T(8,128)(2,1)} %bitcast.3), calls=%async_computation | async-start | bytes 1572864 | tf_op jit(solution)/shard_map/all_to_all | solution.py:17
  9.1 0.1 convert.13
  9.2 0.6 copy-done.9
  9.8 0.7 slice_bitcast_fusion
  10.5 6.8 %all-to-all-done = bf16[4,96,1024]{2,1,0:T(8,128)(2,1)S(1)} async-done(((bf16[4,96,1024]{2,1,0:T(8,128)(2,1)}), bf16[4,96,1024]{2,1,0:T(8,128)(2,1)S(1)}, u32[]{:S(2)}, u32[]{:S(2)}) %all-to-all-start) | async-done | bytes 786464 | tf_op jit(solution)/shard_map/all_to_all | solution.py:17
  17.4 0.1 reduce_sum.88
  17.6 0.7 copy.14
  18.3 13.1 %all-to-all-start.1 = ((bf16[8,96,128]{2,1,0:T(8,128)(2,1)}), bf16[8,96,128]{2,1,0:T(8,128)(2,1)S(1)}, u32[]{:S(2)}, u32[]{:S(2)}) async-start(bf16[8,96,128]{2,1,0:T(8,128)(2,1)} %copy.14), calls=%async_computation.1 | async-start | bytes 393216 | tf_op jit(solution)/shard_map/all_to_all | solution.py:17
  31.4 2.6 %concatenate.23 = bf16[1136,128]{1,0:T(8,128)(2,1)} concatenate(bf16[1024,128]{1,0:T(8,128)(2,1)S(1)} %get-tuple-element.14.refs_1_, bf16[5,128]{1,0:T(8,128)(2,1)S(1)} %get-tuple-element.24, bf16[3,128]{1,0:T(4,128)(2,1)S(1)} %broadcast_in_dim.13, bf16[5,128]{1,0:T(8,128)(2,1)S(1)} %get-tuple-element.23, bf16[3,128]{1,0:T(4,128)(2,1)S(1)} %broadcast_in_dim.13, ...), dimensions={0} | concatenate | bytes 581632 | tf_op jit(solution)/shard_map/concatenate | solution.py:184
  34.0 2.8 %collective-permute-start = (bf16[1136,128]{1,0:T(8,128)(2,1)}, bf16[1136,128]{1,0:T(8,128)(2,1)S(1)}, u32[]{:S(2)}, u32[]{:S(2)}) collective-permute-start(bf16[1136,128]{1,0:T(8,128)(2,1)} %concatenate.23), channel_id=1, source_target_pairs={{0,48},{16,0},{32,16},{48,32},{1,49},{17,1},{33,17},{49,33},{2,50}... | collective-permute-start | bytes 872456 | tf_op jit(solution)/shard_map/ppermute | solution.py:172
  36.8 2.6 %concatenate.24 = bf16[1136,128]{1,0:T(8,128)(2,1)} concatenate(bf16[1024,128]{1,0:T(8,128)(2,1)S(1)} %get-tuple-element.14.refs_1_, bf16[5,128]{1,0:T(8,128)(2,1)S(1)} %get-tuple-element.24, bf16[3,128]{1,0:T(4,128)(2,1)S(1)} %broadcast_in_dim.13, bf16[5,128]{1,0:T(8,128)(2,1)S(1)} %get-tuple-element.23, bf16[3,128]{1,0:T(4,128)(2,1)S(1)} %broadcast_in_dim.13, ...), dimensions={0} | concatenate | bytes 581632 | tf_op jit(solution)/shard_map/concatenate | solution.py:184
  39.4 3.1 %collective-permute-start.1 = (bf16[1136,128]{1,0:T(8,128)(2,1)}, bf16[1136,128]{1,0:T(8,128)(2,1)S(1)}, u32[]{:S(2)}, u32[]{:S(2)}) collective-permute-start(bf16[1136,128]{1,0:T(8,128)(2,1)} %concatenate.24), channel_id=1, source_target_pairs={{0,32},{16,48},{32,0},{48,16},{1,33},{17,49},{33,1},{49,17},{2,34}... | collective-permute-start | bytes 872456 | tf_op jit(solution)/shard_map/ppermute | solution.py:172
  42.5 2.6 %concatenate.25 = bf16[1136,128]{1,0:T(8,128)(2,1)} concatenate(bf16[1024,128]{1,0:T(8,128)(2,1)S(1)} %get-tuple-element.14.refs_1_, bf16[5,128]{1,0:T(8,128)(2,1)S(1)} %get-tuple-element.24, bf16[3,128]{1,0:T(4,128)(2,1)S(1)} %broadcast_in_dim.13, bf16[5,128]{1,0:T(8,128)(2,1)S(1)} %get-tuple-element.23, bf16[3,128]{1,0:T(4,128)(2,1)S(1)} %broadcast_in_dim.13, ...), dimensions={0} | concatenate | bytes 581632 | tf_op jit(solution)/shard_map/concatenate | solution.py:184
  45.1 1.9 %collective-permute-start.2 = (bf16[1136,128]{1,0:T(8,128)(2,1)}, bf16[1136,128]{1,0:T(8,128)(2,1)S(1)}, u32[]{:S(2)}, u32[]{:S(2)}) collective-permute-start(bf16[1136,128]{1,0:T(8,128)(2,1)} %concatenate.25), channel_id=1, source_target_pairs={{0,16},{16,32},{32,48},{48,0},{1,17},{17,33},{33,49},{49,1},{2,18}... | collective-permute-start | bytes 872456 | tf_op jit(solution)/shard_map/ppermute | solution.py:172
  47.2 0.7 broadcast_in_dim.12
  48.0 6.6 %all-to-all-start.2 = ((bf16[8,96,128]{2,1,0:T(8,128)(2,1)}), bf16[8,96,128]{2,1,0:T(8,128)(2,1)S(1)}, u32[]{:S(2)}, u32[]{:S(2)}) async-start(bf16[8,96,128]{2,1,0:T(8,128)(2,1)} %broadcast_in_dim.12), calls=%async_computation.2 | async-start | bytes 393216 | tf_op jit(solution)/shard_map/all_to_all | solution.py:17
  54.7 3.4 %collective-permute-start.5 = (bf16[2048,128]{1,0:T(8,128)(2,1)S(1)}, bf16[2048,128]{1,0:T(8,128)(2,1)S(1)}, u32[]{:S(2)}, u32[]{:S(2)}) collective-permute-start(bf16[2048,128]{1,0:T(8,128)(2,1)S(1)} %pad_maximum_fusion.refs_1_), channel_id=1, source_target_pairs={{0,16},{16,32},{32,48},{48,0},{1,17},{17,33},{33,49},{49,1},{2,18}... | collective-permute-start | bytes 1572872 | tf_op jit(solution)/shard_map/ppermute | solution.py:172
  58.1 4.3 %collective-permute-start.4 = (bf16[2048,128]{1,0:T(8,128)(2,1)S(1)}, bf16[2048,128]{1,0:T(8,128)(2,1)S(1)}, u32[]{:S(2)}, u32[]{:S(2)}) collective-permute-start(bf16[2048,128]{1,0:T(8,128)(2,1)S(1)} %pad_maximum_fusion.refs_1_), channel_id=1, source_target_pairs={{0,32},{16,48},{32,0},{48,16},{1,33},{17,49},{33,1},{49,17},{2,34}... | collective-permute-start | bytes 1572872 | tf_op jit(solution)/shard_map/ppermute | solution.py:172
  62.4 3.1 %collective-permute-start.3 = (bf16[2048,128]{1,0:T(8,128)(2,1)S(1)}, bf16[2048,128]{1,0:T(8,128)(2,1)S(1)}, u32[]{:S(2)}, u32[]{:S(2)}) collective-permute-start(bf16[2048,128]{1,0:T(8,128)(2,1)S(1)} %pad_maximum_fusion.refs_1_), channel_id=1, source_target_pairs={{0,48},{16,0},{32,16},{48,32},{1,49},{17,1},{33,17},{49,33},{2,50}... | collective-permute-start | bytes 1572872 | tf_op jit(solution)/shard_map/ppermute | solution.py:172
  65.5 0.9 down_product.2
  66.4 19.7 %all_to_all.55 = bf16[16,24,128]{2,1,0:T(8,128)(2,1)S(1)} all-to-all(bf16[16,24,128]{2,1,0:T(8,128)(2,1)S(1)} %bitcast.53), channel_id=1, replica_groups=mesh['z'=8,'x'=4,'y'=8,'core'=2] {'y','core'}, dimensions={0} | all-to-all | bytes 196608 | tf_op jit(solution)/shard_map/all_to_all | solution.py:17
  86.2 0.7 broadcast_in_dim.14
  86.8 3.4 %all-to-all-start.4 = ((bf16[16,24,128]{2,1,0:T(8,128)(2,1)}), bf16[16,24,128]{2,1,0:T(8,128)(2,1)S(1)}, u32[]{:S(2)}, u32[]{:S(2)}) async-start(bf16[16,24,128]{2,1,0:T(8,128)(2,1)} %broadcast_in_dim.14), calls=%async_computation.4 | async-start | bytes 196608 | tf_op jit(solution)/shard_map/all_to_all | solution.py:17
  90.3 0.1 concatenate.26.refs_1_
  90.3 8.2 %all-to-all-done.4 = bf16[16,24,128]{2,1,0:T(8,128)(2,1)S(1)} async-done(((bf16[16,24,128]{2,1,0:T(8,128)(2,1)}), bf16[16,24,128]{2,1,0:T(8,128)(2,1)S(1)}, u32[]{:S(2)}, u32[]{:S(2)}) %all-to-all-start.4) | async-done | bytes 98336 | tf_op jit(solution)/shard_map/all_to_all | solution.py:17
  98.6 1.8 %turn.1 = (bf16[8,200,128]{2,1,0:T(8,128)(2,1)S(1)}, f32[4,96,128]{2,1,0:T(8,128)S(1)}, f32[4,96,128]{2,1,0:T(8,128)S(1)}, f32[4,8,128]{2,1,0:T(8,128)S(1)}) custom-call(bf16[4,96,128]{2,1,0:T(8,128)(2,1)S(1)} %bitcast.51, bf16[112,128]{1,0:T(8,128)(2,1)S(1)} %concatenate.26.refs_1_, f32[8,1,128]{2,1,0:T(1,128)S(1)} %get-tuple-element.21.refs_2_, ...), custom_call_target="tpu_custom_call" | custom-call | tf_op jit(solution)/shard_map/turn/pallas_call | solution.py:132
  100.4 22.2 %all_to_all.56 = bf16[8,200,128]{2,1,0:T(8,128)(2,1)S(1)} all-to-all(bf16[8,200,128]{2,1,0:T(8,128)(2,1)S(1)} %get-tuple-element.11), channel_id=1, replica_groups=mesh['z'=8,'x'=4,'y'=8,'core'=2] {'z'}, dimensions={0} | all-to-all | bytes 819200 | tf_op jit(solution)/shard_map/all_to_all | solution.py:17
  122.7 0.1 convert_element_type.82
  122.8 0.1 fusion.9
  122.9 12.1 %all_to_all.57.refs_0_ = bf16[8,96,128]{2,1,0:T(8,128)(2,1)S(1)} all-to-all(bf16[8,96,128]{2,1,0:T(8,128)(2,1)S(1)} %broadcast_in_dim.15), channel_id=1, replica_groups=mesh['z'=8,'x'=4,'y'=8,'core'=2] {'z'}, dimensions={0} | all-to-all | bytes 393216 | tf_op jit(solution)/shard_map/all_to_all | solution.py:17
  135.0 0.9 down_product.3
  136.0 12.8 %all_to_all.58 = bf16[16,24,128]{2,1,0:T(8,128)(2,1)S(1)} all-to-all(bf16[16,24,128]{2,1,0:T(8,128)(2,1)S(1)} %bitcast.52), channel_id=1, replica_groups=mesh['z'=8,'x'=4,'y'=8,'core'=2] {'y','core'}, dimensions={0} | all-to-all | bytes 196608 | tf_op jit(solution)/shard_map/all_to_all | solution.py:17
  148.8 0.7 broadcast_in_dim.16
  149.4 3.4 %all-to-all-start.8 = ((bf16[16,24,128]{2,1,0:T(8,128)(2,1)}), bf16[16,24,128]{2,1,0:T(8,128)(2,1)S(1)}, u32[]{:S(2)}, u32[]{:S(2)}) async-start(bf16[16,24,128]{2,1,0:T(8,128)(2,1)} %broadcast_in_dim.16), calls=%async_computation.8 | async-start | bytes 196608 | tf_op jit(solution)/shard_map/all_to_all | solution.py:17
  152.8 8.3 %all-to-all-done.8 = bf16[16,24,128]{2,1,0:T(8,128)(2,1)S(1)} async-done(((bf16[16,24,128]{2,1,0:T(8,128)(2,1)}), bf16[16,24,128]{2,1,0:T(8,128)(2,1)S(1)}, u32[]{:S(2)}, u32[]{:S(2)}) %all-to-all-start.8) | async-done | bytes 98336 | tf_op jit(solution)/shard_map/all_to_all | solution.py:17
  161.2 0.1 multiply_reduce_fusion
  161.3 0.1 reduce_sum.95
  161.4 0.6 broadcast_in_dim.17
  162.0 3.3 %all-to-all-start.9 = ((f32[8,1,96]{2,1,0:T(1,128)}), f32[8,1,96]{2,1,0:T(1,128)S(1)}, u32[]{:S(2)}, u32[]{:S(2)}) async-start(f32[8,1,96]{2,1,0:T(1,128)} %broadcast_in_dim.17), calls=%async_computation.9 | async-start | bytes 8192 | tf_op jit(solution)/shard_map/all_to_all | solution.py:17
  165.4 6.4 %all-to-all-done.9 = f32[8,1,96]{2,1,0:T(1,128)S(1)} async-done(((f32[8,1,96]{2,1,0:T(1,128)}), f32[8,1,96]{2,1,0:T(1,128)S(1)}, u32[]{:S(2)}, u32[]{:S(2)}) %all-to-all-start.9) | async-done | bytes 3104 | tf_op jit(solution)/shard_map/all_to_all | solution.py:17
  171.8 0.1 fusion.3
  171.9 0.1 fusion.4
  171.9 7.0 %all_to_all.59 = bf16[4,96,128]{2,1,0:T(8,128)(2,1)S(1)} all-to-all(bf16[4,96,128]{2,1,0:T(8,128)(2,1)S(1)} %fusion.4), channel_id=1, replica_groups=mesh['z'=8,'x'=4,'y'=8,'core'=2] {'x'}, dimensions={0} | all-to-all | bytes 196608 | tf_op jit(solution)/shard_map/all_to_all | solution.py:17
  179.0 0.6 copy.20
  (53 shorter events, 0.5 us)
Async XLA Ops:
  0.0 2.8 %copy-start.4 = (bf16[384,128]{1,0:T(8,128)(2,1)S(1)}, bf16[384,128]{1,0:T(8,128)(2,1)}, u32[]{:S(2)}) copy-start(bf16[384,128]{1,0:T(8,128)(2,1)} %param.7) | copy-start | bytes 294916
  4.1 5.0 %copy-start.2 = (f32[2,1024,128]{2,1,0:T(8,128)S(1)}, f32[2,1024,128]{2,1,0:T(8,128)}, u32[]{:S(2)}) copy-start(f32[2,1024,128]{2,1,0:T(8,128)} %param.10) | copy-start | bytes 3145732
  4.1 13.3 %all-to-all-start = ((bf16[4,96,1024]{2,1,0:T(8,128)(2,1)}), bf16[4,96,1024]{2,1,0:T(8,128)(2,1)S(1)}, u32[]{:S(2)}, u32[]{:S(2)}) async-start(bf16[4,96,1024]{2,1,0:T(8,128)(2,1)} %bitcast.3), calls=%async_computation | async-start | bytes 1572864 | tf_op jit(solution)/shard_map/all_to_all | solution.py:17
  9.1 0.7 copy-start.9
  9.1 0.7 copy-start.10
  9.8 32.7 %copy-start.5 = (bf16[5,128]{1,0:T(8,128)(2,1)}, bf16[5,128]{1,0:T(8,128)(2,1)S(1)}, u32[]{:S(2)}) copy-start(bf16[5,128]{1,0:T(8,128)(2,1)S(1)} %get-tuple-element.23) | copy-start | bytes 3844
  9.8 32.7 %copy-start.7 = (bf16[5,128]{1,0:T(8,128)(2,1)}, bf16[5,128]{1,0:T(8,128)(2,1)S(1)}, u32[]{:S(2)}) copy-start(bf16[5,128]{1,0:T(8,128)(2,1)S(1)} %get-tuple-element.24) | copy-start | bytes 3844
  18.3 28.9 %all-to-all-start.1 = ((bf16[8,96,128]{2,1,0:T(8,128)(2,1)}), bf16[8,96,128]{2,1,0:T(8,128)(2,1)S(1)}, u32[]{:S(2)}, u32[]{:S(2)}) async-start(bf16[8,96,128]{2,1,0:T(8,128)(2,1)} %copy.14), calls=%async_computation.1 | async-start | bytes 393216 | tf_op jit(solution)/shard_map/all_to_all | solution.py:17
  34.0 28.3 %collective-permute-start = (bf16[1136,128]{1,0:T(8,128)(2,1)}, bf16[1136,128]{1,0:T(8,128)(2,1)S(1)}, u32[]{:S(2)}, u32[]{:S(2)}) collective-permute-start(bf16[1136,128]{1,0:T(8,128)(2,1)} %concatenate.23), channel_id=1, source_target_pairs={{0,48},{16,0},{32,16},{48,32},{1,49},{17,1},{33,17},{49,33},{2,50}... | collective-permute-start | bytes 872456 | tf_op jit(solution)/shard_map/ppermute | solution.py:172
  39.4 26.0 %collective-permute-start.1 = (bf16[1136,128]{1,0:T(8,128)(2,1)}, bf16[1136,128]{1,0:T(8,128)(2,1)S(1)}, u32[]{:S(2)}, u32[]{:S(2)}) collective-permute-start(bf16[1136,128]{1,0:T(8,128)(2,1)} %concatenate.24), channel_id=1, source_target_pairs={{0,32},{16,48},{32,0},{48,16},{1,33},{17,49},{33,1},{49,17},{2,34}... | collective-permute-start | bytes 872456 | tf_op jit(solution)/shard_map/ppermute | solution.py:172
  45.1 20.3 %collective-permute-start.2 = (bf16[1136,128]{1,0:T(8,128)(2,1)}, bf16[1136,128]{1,0:T(8,128)(2,1)S(1)}, u32[]{:S(2)}, u32[]{:S(2)}) collective-permute-start(bf16[1136,128]{1,0:T(8,128)(2,1)} %concatenate.25), channel_id=1, source_target_pairs={{0,16},{16,32},{32,48},{48,0},{1,17},{17,33},{33,49},{49,1},{2,18}... | collective-permute-start | bytes 872456 | tf_op jit(solution)/shard_map/ppermute | solution.py:172
  47.1 7.5 %copy-start.3 = (bf16[1024,128]{1,0:T(8,128)(2,1)S(1)}, bf16[1024,128]{1,0:T(8,128)(2,1)}, u32[]{:S(2)}) copy-start(bf16[1024,128]{1,0:T(8,128)(2,1)} %get-tuple-element.13) | copy-start | bytes 786436
  48.0 17.5 %all-to-all-start.2 = ((bf16[8,96,128]{2,1,0:T(8,128)(2,1)}), bf16[8,96,128]{2,1,0:T(8,128)(2,1)S(1)}, u32[]{:S(2)}, u32[]{:S(2)}) async-start(bf16[8,96,128]{2,1,0:T(8,128)(2,1)} %broadcast_in_dim.12), calls=%async_computation.2 | async-start | bytes 393216 | tf_op jit(solution)/shard_map/all_to_all | solution.py:17
  54.7 35.6 %copy-start.6 = (bf16[5,128]{1,0:T(8,128)(2,1)S(1)}, bf16[5,128]{1,0:T(8,128)(2,1)}, u32[]{:S(2)}) copy-start(bf16[5,128]{1,0:T(8,128)(2,1)} %copy-done.5) | copy-start | bytes 3844
  54.7 35.6 %copy-start.8 = (bf16[5,128]{1,0:T(8,128)(2,1)S(1)}, bf16[5,128]{1,0:T(8,128)(2,1)}, u32[]{:S(2)}) copy-start(bf16[5,128]{1,0:T(8,128)(2,1)} %copy-done.7) | copy-start | bytes 3844
  54.7 35.6 %collective-permute-start.5 = (bf16[2048,128]{1,0:T(8,128)(2,1)S(1)}, bf16[2048,128]{1,0:T(8,128)(2,1)S(1)}, u32[]{:S(2)}, u32[]{:S(2)}) collective-permute-start(bf16[2048,128]{1,0:T(8,128)(2,1)S(1)} %pad_maximum_fusion.refs_1_), channel_id=1, source_target_pairs={{0,16},{16,32},{32,48},{48,0},{1,17},{17,33},{33,49},{49,1},{2,18}... | collective-permute-start | bytes 1572872 | tf_op jit(solution)/shard_map/ppermute | solution.py:172
  58.1 32.3 %collective-permute-start.4 = (bf16[2048,128]{1,0:T(8,128)(2,1)S(1)}, bf16[2048,128]{1,0:T(8,128)(2,1)S(1)}, u32[]{:S(2)}, u32[]{:S(2)}) collective-permute-start(bf16[2048,128]{1,0:T(8,128)(2,1)S(1)} %pad_maximum_fusion.refs_1_), channel_id=1, source_target_pairs={{0,32},{16,48},{32,0},{48,16},{1,33},{17,49},{33,1},{49,17},{2,34}... | collective-permute-start | bytes 1572872 | tf_op jit(solution)/shard_map/ppermute | solution.py:172
  62.4 28.0 %collective-permute-start.3 = (bf16[2048,128]{1,0:T(8,128)(2,1)S(1)}, bf16[2048,128]{1,0:T(8,128)(2,1)S(1)}, u32[]{:S(2)}, u32[]{:S(2)}) collective-permute-start(bf16[2048,128]{1,0:T(8,128)(2,1)S(1)} %pad_maximum_fusion.refs_1_), channel_id=1, source_target_pairs={{0,48},{16,0},{32,16},{48,32},{1,49},{17,1},{33,17},{49,33},{2,50}... | collective-permute-start | bytes 1572872 | tf_op jit(solution)/shard_map/ppermute | solution.py:172
  86.8 11.8 %all-to-all-start.4 = ((bf16[16,24,128]{2,1,0:T(8,128)(2,1)}), bf16[16,24,128]{2,1,0:T(8,128)(2,1)S(1)}, u32[]{:S(2)}, u32[]{:S(2)}) async-start(bf16[16,24,128]{2,1,0:T(8,128)(2,1)} %broadcast_in_dim.14), calls=%async_computation.4 | async-start | bytes 196608 | tf_op jit(solution)/shard_map/all_to_all | solution.py:17
  100.4 22.4 %copy-start = (f32[4,96,128]{2,1,0:T(8,128)}, f32[4,96,128]{2,1,0:T(8,128)S(1)}, u32[]{:S(2)}) copy-start(f32[4,96,128]{2,1,0:T(8,128)S(1)} %get-tuple-element.10) | copy-start | bytes 589828
  136.0 35.8 %copy-start.1 = (f32[4,96,128]{2,1,0:T(8,128)S(1)}, f32[4,96,128]{2,1,0:T(8,128)}, u32[]{:S(2)}) copy-start(f32[4,96,128]{2,1,0:T(8,128)} %copy-done) | copy-start | bytes 589828
  149.4 11.7 %all-to-all-start.8 = ((bf16[16,24,128]{2,1,0:T(8,128)(2,1)}), bf16[16,24,128]{2,1,0:T(8,128)(2,1)S(1)}, u32[]{:S(2)}, u32[]{:S(2)}) async-start(bf16[16,24,128]{2,1,0:T(8,128)(2,1)} %broadcast_in_dim.16), calls=%async_computation.8 | async-start | bytes 196608 | tf_op jit(solution)/shard_map/all_to_all | solution.py:17
  162.0 9.7 %all-to-all-start.9 = ((f32[8,1,96]{2,1,0:T(1,128)}), f32[8,1,96]{2,1,0:T(1,128)S(1)}, u32[]{:S(2)}, u32[]{:S(2)}) async-start(f32[8,1,96]{2,1,0:T(1,128)} %broadcast_in_dim.17), calls=%async_computation.9 | async-start | bytes 8192 | tf_op jit(solution)/shard_map/all_to_all | solution.py:17

commit v5 on v4

v5 whole, which is shorter than its diff:
```python
import jax
import jax.numpy as jnp
from jax import lax
from jax.experimental import pallas as pl
from jax.experimental.pallas import tpu as pltpu
from jax.sharding import Mesh, PartitionSpec as P


norm_eps = 1e-06
residual_keep = 0.5
Z, X, Y, C = 8, 4, 8, 2
bf16 = jnp.bfloat16
f32 = jnp.float32
VMEM = pl.BlockSpec(memory_space=pltpu.VMEM)
ANY = pl.BlockSpec(memory_space=pl.ANY)


def exchange(pieces, axis):
    return lax.all_to_all(pieces, axis, split_axis=0, concat_axis=0, tiled=True)


def to_all(shard, axis):
    size = lax.axis_size(axis)
    return exchange(jnp.broadcast_to(shard[None], (size, *shard.shape)), axis)


def activation(up):
    return jnp.square(jnp.maximum(up, 0.0)).astype(bf16)


def near(v):
    return pltpu.with_memory_space_constraint(v, pltpu.VMEM)


def far(v):
    return pltpu.with_memory_space_constraint(v, pltpu.HBM)


def after(blocks, value):
    return [lax.optimization_barrier((b, value))[0] for b in blocks]


def limit(mib):
    return pltpu.CompilerParams(vmem_limit_bytes=mib << 20)


def up_kernel(tokens_ref, gain_ref, weight_ref, scale_ref, out_ref):
    scaled = (tokens_ref[...].astype(f32) * gain_ref[0:1]).astype(bf16)
    part = jnp.dot(scaled, weight_ref[0].astype(bf16), preferred_element_type=f32)
    out_ref[...] = (part * scale_ref[0:1]).astype(bf16)


def up_product(tokens, gain, weight, scale):
    n_tok, feats = tokens.shape
    hid = weight.shape[2]
    step = hid // 4
    return pl.pallas_call(
        up_kernel,
        grid=(hid // step,),
        out_shape=jax.ShapeDtypeStruct((n_tok, hid), bf16),
        in_specs=[
            pl.BlockSpec((n_tok, feats), lambda i: (0, 0)),
            pl.BlockSpec(gain.shape, lambda i: (0, 0)),
            pl.BlockSpec((1, feats, step), lambda i: (0, 0, i)),
            pl.BlockSpec((scale.shape[0], step), lambda i: (0, i)),
        ],
        out_specs=pl.BlockSpec((n_tok, step), lambda i: (0, i)),
        compiler_params=limit(12),
        name="up_product",
    )(far(tokens), far(gain), far(weight), far(scale))


def pack_kernel(down_ref, up_ref, tokens_ref, scale_ref, pre_ref, post_ref, *outs):
    one, two, three, late, own = outs
    hid, feats = down_ref.shape[1:]
    t_x = own.shape[0] - 16
    x = lax.axis_index("x")
    scale, pre, post = scale_ref[...], pre_ref[...], post_ref[...]
    columns = [scale[0:1], post[0:1], pre[1:2], scale[1:2], post[1:2], jnp.zeros((3, feats), f32)]
    columns = jnp.concatenate(columns, axis=0)
    high = columns.astype(bf16).astype(f32)
    columns = jnp.concatenate([high, columns - high], axis=0).astype(bf16)
    for s, ref in ((0, own), (1, one), (2, two), (3, three)):
        at = 0 if s == 0 else hid
        if s:
            ref[:hid] = down_ref[0].astype(bf16)
        ref[at : at + 16] = columns
        rows = pl.multiple_of(lax.rem(x + (X - s), X) * t_x, 32)
        ref[at + 16 : at + 16 + t_x] = tokens_ref[pl.ds(rows, t_x)]
    for ref, at in ((one, hid + 16 + t_x), (three, hid + 16 + t_x), (late, 0)):
        for c in range(hid // feats):
            block = up_ref[0, :, c * feats : (c + 1) * feats].astype(bf16)
            ref[at + c * feats : at + (c + 1) * feats] = block
        ref[at + hid : at + 2 * hid] = down_ref[1].astype(bf16)


def packed(down_weight, up_weight, tokens, scale, pre, post):
    _, hid, feats = down_weight.shape
    t_x = tokens.shape[0] // X
    near_rows, far_rows = hid + 16 + t_x, 2 * hid
    whole = lambda v: pl.BlockSpec(v.shape, lambda i: (0,) * v.ndim)
    rows = (near_rows + far_rows, near_rows, near_rows + far_rows, far_rows, 16 + t_x)
    return pl.pallas_call(
        pack_kernel,
        grid=(1,),
        out_shape=tuple(jax.ShapeDtypeStruct((r, feats), bf16) for r in rows),
        in_specs=[
            whole(down_weight),
            pl.BlockSpec((1, feats, hid), lambda i: (1, 0, 0)),
            *[whole(v) for v in (tokens, scale, pre, post)],
        ],
        out_specs=tuple(pl.BlockSpec((r, feats), lambda i: (0, 0)) for r in rows),
        compiler_params=limit(20),
        name="packed",
    )(*[far(v) for v in (down_weight, up_weight, tokens, scale, pre, post)])


def down_kernel(starts, hidden_ref, *refs):
    weights, out_ref, held, sems = refs[:X], refs[X], refs[X + 1], refs[X + 2]
    copies = []
    for i, w in enumerate(weights):
        rows = w.at[pl.ds(starts[i], held.shape[1])]
        copies.append(pltpu.make_async_copy(rows, held.at[i], sems.at[i]))
        copies[-1].start()
    hidden = jnp.concatenate([hidden_ref[z] for z in range(Z)], axis=1)
    for i in range(X):
        copies[i].wait()
        out_ref[i] = jnp.dot(hidden, held[i], preferred_element_type=f32).astype(bf16)


def down_product(hidden, blocks, starts):
    _, t, share = hidden.shape
    feats = blocks[0].shape[1]
    return pl.pallas_call(
        lambda *refs: down_kernel(starts, *refs),
        out_shape=pltpu.VMEM((X, t, feats), bf16),
        in_specs=[VMEM, *[ANY] * X],
        out_specs=VMEM,
        scratch_shapes=[
            pltpu.VMEM((X, Z * share, feats), bf16),
            pltpu.SemaphoreType.DMA((X,)),
        ],
        compiler_params=limit(8),
        name="down_product",
    )(near(hidden), *blocks)


def down_sum(hidden, blocks, starts):
    part = down_product(hidden, blocks, starts)
    pieces = part.reshape(Y * C, -1, part.shape[2])
    mine = exchange(pieces, ("y", "core")).astype(f32).sum(axis=0).astype(bf16)
    return to_all(mine, ("y", "core")).reshape(part.shape)


def squares_in_rows(values):
    total = 0.0
    for v in values:
        total += lax.dot_general(
            jnp.ones((8, v.shape[1]), f32),
            v * v,
            (((1,), (1,)), ((), ())),
            precision=lax.Precision.HIGHEST,
            preferred_element_type=f32,
        )
    return total


def inverse(row, width, t):
    inv = lax.rsqrt(row * (1.0 / width) + norm_eps)
    return jnp.transpose(jnp.broadcast_to(inv, (128, 128)))[:t]


def turn_kernel(firsts_at, seconds_at, sum_ref, own_ref, scale_ref, *refs):
    firsts, seconds = refs[: X - 1], refs[X - 1 : 2 * X - 1]
    out_ref, kept_ref, branch_ref, columns_ref = refs[2 * X - 1 : 2 * X + 3]
    extra, held, sems, held_sems = refs[2 * X + 3 :]
    t, feats = sum_ref.shape[1:]
    copies = []
    for i, block in enumerate(firsts):
        rows = block.at[pl.ds(firsts_at[i], extra.shape[1])]
        copies.append(pltpu.make_async_copy(rows, extra.at[i], sems.at[i]))
        copies[-1].start()
    held_copies = []
    for i, block in enumerate(seconds):
        for c in range(Z):
            rows = block.at[pl.ds(seconds_at[i] + c * feats, feats)]
            here = held.at[c, pl.ds(i * feats, feats)]
            held_copies.append(pltpu.make_async_copy(rows, here, held_sems.at[i, c]))
            held_copies[-1].start()
    for copy in copies:
        copy.wait()
    kept_terms, branch_terms, branches = [], [], []
    for i in range(X):
        block = own_ref[...] if i == 0 else extra[i - 1]
        columns = block[:8].astype(f32) + block[8:16].astype(f32)
        columns_ref[i] = columns
        down_0, post_0, pre_1 = [columns[k : k + 1] for k in range(3)]
        kept = residual_keep * block[16:].astype(f32)
        branch_in = sum_ref[i].astype(f32) * down_0
        branch = branch_in * post_0
        kept_ref[i] = kept
        branch_ref[i] = branch
        kept_terms.append((kept * pre_1).astype(bf16))
        branch_terms.append((branch * pre_1).astype(bf16))
        branches.append(branch_in)
    squares = squares_in_rows(branches)
    high = squares.astype(bf16).astype(f32)
    row = lax.broadcasted_iota(jnp.int32, squares.shape, 0)
    squares = jnp.where(row == 0, high, jnp.where(row == 1, squares - high, 0.0)).astype(bf16)
    terms = jnp.concatenate(
        [jnp.concatenate(kept_terms, axis=1), jnp.concatenate(branch_terms, axis=1)], axis=0
    )
    for copy in held_copies:
        copy.wait()
    for c in range(Z):
        part = jnp.dot(terms, held[c], preferred_element_type=f32)
        scale = scale_ref[1:2, c * feats : (c + 1) * feats]
        out_ref[c, : 2 * t] = (part * scale).astype(bf16)
        out_ref[c, 2 * t :] = jnp.zeros((8, feats), bf16)
        out_ref[c, 2 * t :, :t] = squares


def turn(summed, own, scale, firsts, firsts_at, seconds, seconds_at):
    _, t, feats = summed.shape
    return pl.pallas_call(
        lambda *refs: turn_kernel(firsts_at, seconds_at, *refs),
        out_shape=(
            pltpu.VMEM((Z, 2 * t + 8, feats), bf16),
            pltpu.VMEM((X, t, feats), f32),
            pltpu.VMEM((X, t, feats), f32),
            pltpu.VMEM((X, 8, feats), f32),
        ),
        in_specs=[*[VMEM] * 3, *[ANY] * (2 * X - 1)],
        out_specs=(VMEM,) * 4,
        scratch_shapes=[
            pltpu.VMEM((X - 1, 16 + t, feats), bf16),
            pltpu.VMEM((Z, X * feats, feats), bf16),
            pltpu.SemaphoreType.DMA((X - 1,)),
            pltpu.SemaphoreType.DMA((X, Z)),
        ],
        compiler_params=limit(12),
        name="turn",
    )(near(summed), near(own), near(scale), *firsts, *seconds)


def hidden_kernel(width, came_ref, kept_ref, branch_ref, out_ref, stream_ref):
    t = out_ref.shape[1]
    total = came_ref[0].astype(f32)
    for z in range(1, Z):
        total += came_ref[z].astype(f32)
    inv = inverse(total[2 * t : 2 * t + 1] + total[2 * t + 1 : 2 * t + 2], width, t)
    hidden = activation(total[:t] + total[t : 2 * t] * inv)
    for z in range(Z):
        out_ref[z] = hidden
    for i in range(X):
        stream_ref[i] = (kept_ref[i] + branch_ref[i] * inv).astype(bf16)


def second_hidden(came, kept, branch, width):
    _, t, feats = kept.shape
    return pl.pallas_call(
        lambda *refs: hidden_kernel(width, *refs),
        out_shape=(pltpu.VMEM((Z, t, feats), bf16), pltpu.VMEM(kept.shape, bf16)),
        in_specs=[VMEM] * 3,
        out_specs=(VMEM,) * 2,
        compiler_params=limit(8),
        name="second_hidden",
    )(near(came), near(kept), near(branch))


def squares_kernel(sum_ref, columns_ref, out_ref):
    t = sum_ref.shape[1]
    values = [sum_ref[i].astype(f32) * columns_ref[i, 3:4] for i in range(X)]
    squares = squares_in_rows(values)
    for z in range(Z):
        out_ref[z] = jnp.zeros(out_ref.shape[1:], f32)
        out_ref[z, :, :t] = squares


def squares_of(summed, columns):
    return pl.pallas_call(
        squares_kernel,
        out_shape=pltpu.VMEM((Z, 8, summed.shape[2]), f32),
        in_specs=[VMEM] * 2,
        out_specs=VMEM,
        compiler_params=limit(8),
        name="squares",
    )(near(summed), near(columns))


def last_kernel(width, squares_ref, sum_ref, columns_ref, stream_ref, out_ref):
    t = sum_ref.shape[1]
    total = squares_ref[0]
    for z in range(1, Z):
        total += squares_ref[z]
    inv = inverse(total[0:1], width, t)
    x = lax.axis_index("x")
    for i in range(X):
        branch = sum_ref[i].astype(f32) * columns_ref[i, 3:4] * inv * columns_ref[i, 4:5]
        stream = residual_keep * stream_ref[i].astype(f32) + branch
        out_ref[lax.rem(x + i, X)] = stream.astype(bf16)


def last(squares, summed, columns, stream, width):
    return pl.pallas_call(
        lambda *refs: last_kernel(width, *refs),
        out_shape=pltpu.VMEM(summed.shape, bf16),
        in_specs=[VMEM] * 4,
        out_specs=VMEM,
        compiler_params=limit(8),
        name="last",
    )(near(squares), near(summed), near(columns), near(stream))


def inner(tokens, up_weight, up_scale, down_weight, down_scale, pre_gain, post_gain):
    n_tok, feats = tokens.shape
    hid = up_weight.shape[2]
    width = feats * X * Z
    t_x = n_tok // X

    part = up_product(tokens, pre_gain, up_weight, up_scale).reshape(X, t_x, hid)
    part = exchange(part, "x").astype(f32).sum(axis=0)

    def from_x(payload, s):
        return lax.ppermute(payload, "x", [(i, (i - s) % X) for i in range(X)])

    one, two, three, late, own = packed(
        down_weight, up_weight, tokens, down_scale, pre_gain, post_gain
    )
    firsts = [from_x(one, 1), from_x(two, 2), from_x(three, 3)]
    seconds = [late, firsts[0], from_x(late, 2), firsts[2]]
    near_rows = hid + 16 + t_x
    seconds_at = [0, near_rows, 0, near_rows]

    pieces = part.astype(bf16).reshape(t_x, Z, hid // Z).transpose(1, 0, 2)
    summed = exchange(pieces, "z").astype(f32).sum(axis=0)
    hidden = to_all(activation(summed), "z")
    summed = down_sum(hidden, [one, *after(firsts, hidden)], [0] * X)

    firsts, seconds = after(firsts, summed), after(seconds, summed)
    part, kept, branch, columns = turn(
        summed, own, up_scale, firsts, [hid] * (X - 1), seconds, seconds_at
    )
    came = exchange(part, "z")
    hidden, stream = second_hidden(came, kept, branch, width)
    hidden = exchange(hidden, "z")
    summed = down_sum(hidden, seconds, [at + hid for at in seconds_at])

    squares = squares_of(summed, columns)
    squares = exchange(squares, "z")
    out = last(squares, summed, columns, stream, width)
    return exchange(out, "x").reshape(n_tok, feats)


def solution(mesh):
    split = Mesh(mesh.devices.reshape(Z, X, Y, C), ("z", "x", "y", "core"))
    ra, cb = ("z", "x"), ("y", "core")
    return jax.shard_map(
        inner,
        mesh=split,
        in_specs=(
            P(None, ra),
            P(None, ra, cb),
            P(None, cb),
            P(None, cb, ra),
            P(None, ra),
            P(None, ra),
            P(None, ra),
        ),
        out_specs=P(None, ra),
        check_vma=False,
    )
```

time: 181 us -> 186 us (1.028)
  blocking collectives: 73.8 us -> 131 us
  waiting for transfers between devices: 29.8 us -> 5.9 us
  starting transfers between devices: 53.4 us -> 33 us
  local copies, waits for them, and re-layouts: 15 us -> 2.14 us
  Pallas kernels: 3.68 us -> 12.1 us
  other arithmetic: 2.22 us -> 0.22 us
    all_to_all x5 -> x9, blocking collectives: 73.8 us -> 131 us  [exchange(): return lax.all_to_all(pieces, axis, split_axis=0, concat_axis=0, tiled=True)]
    all_to_all x6 -> x2, waiting for transfers between devices: 29.8 us -> 0.01 us  [exchange(): return lax.all_to_all(pieces, axis, split_axis=0, concat_axis=0, tiled=True)]
    all_to_all x6 -> x2, starting transfers between devices: 34.9 us -> 19.8 us  [exchange(): return lax.all_to_all(pieces, axis, split_axis=0, concat_axis=0, tiled=True)]
    pallas_call x3 -> x8, Pallas kernels: 3.68 us -> 12.1 us  [the longest x1 3.42 us: turn(): pl.pallas_call(lambda *refs: turn_kernel(firsts_at, seconds_at, *refs), o...]
    concatenate x4 -> x0, local copies, waits for them, and re-layouts: 7.86 us -> none  [the longest x3 7.79 us: inner(): first = from_x(lambda s: jnp.concatenate([down_w0, columns, tokens_of(s)]))]
    ppermute x6 -> x4, waiting for transfers between devices: 0.02 us -> 5.9 us  [from_x(): return lax.ppermute(payload, 'x', [(i, (i - s) % X) for i in range(X)])]
    ppermute x6 -> x4, starting transfers between devices: 18.5 us -> 13.3 us  [from_x(): return lax.ppermute(payload, 'x', [(i, (i - s) % X) for i in range(X)])]
    broadcast_in_dim x5 -> x3, local copies, waits for them, and re-layouts: 2.65 us -> 0.74 us  [to_all(): return exchange(jnp.broadcast_to(shard[None], (size, *shard.shape)), axis)]
  transfers between devices with their start and end apart: 12 -> 6, of which waited for: 4 -> 1; matrix products, arithmetic and copies ran while one was open for 6% -> 0% of each run, Pallas kernels for 1% -> 2%
where the time goes in v5:
time: 186 us; the launch traced here: 185 us
  blocking collectives  131 us (70%)
  starting transfers between devices  33 us (18%)
  Pallas kernels  12.1 us (7%)
  waiting for transfers between devices  5.9 us (3%)
  local copies, waits for them, and re-layouts  2.14 us (1%)
    all_to_all x9, blocking collectives, exchange(): return lax.all_to_all(pieces, axis, split_axis=0, concat_axis=0, tiled=True)  131 us
    all_to_all x2, starting transfers between devices, exchange(): return lax.all_to_all(pieces, axis, split_axis=0, concat_axis=0, tiled=True)  19.8 us
    ppermute x4, starting transfers between devices, from_x(): return lax.ppermute(payload, 'x', [(i, (i - s) % X) for i in range(X)])  13.3 us
    ppermute x4, waiting for transfers between devices, from_x(): return lax.ppermute(payload, 'x', [(i, (i - s) % X) for i in range(X)])  5.9 us
  transfers between devices with their start and end apart: 6, of which 1 were waited for; matrix products, arithmetic and copies ran while one was open for 0% of the time, Pallas kernels for 2%

profile of v5, /device:TPU:1, one launch (start us, length us, event | category | flops | bytes accessed | tf_op | source)
XLA Modules:
  0.0 184.6 jit_solution(14145134493088799180)
XLA Ops:
  0.0 2.6 %up_product.1 = bf16[384,1024]{1,0:T(8,128)(2,1)S(1)} custom-call(bf16[384,128]{1,0:T(8,128)(2,1)} %tokens_ref.3, f32[2,128]{1,0:T(2,128)} %pre_ref.1, f32[2,128,1024]{2,1,0:T(8,128)} %up_ref.1, f32[2,1024]{1,0:T(2,128)} %refs_2_.1), custom_call_target="tpu_custom_call" | custom-call | tf_op jit(solution)/shard_map/up_product/pallas_call | solution.py:57
  2.6 13.0 %all_to_all.55 = bf16[4,96,1024]{2,1,0:T(8,128)(2,1)S(1)} all-to-all(bf16[4,96,1024]{2,1,0:T(8,128)(2,1)S(1)} %bitcast.10), channel_id=1, replica_groups=mesh['z'=8,'x'=4,'y'=8,'core'=2] {'x'}, dimensions={0} | all-to-all | bytes 1572864 | tf_op jit(solution)/shard_map/all_to_all | solution.py:19
  15.6 0.1 reduce_sum.45
  15.8 0.7 copy.8
  16.5 13.1 %all-to-all-start.1 = ((bf16[8,96,128]{2,1,0:T(8,128)(2,1)}), bf16[8,96,128]{2,1,0:T(8,128)(2,1)S(1)}, u32[]{:S(2)}, u32[]{:S(2)}) async-start(bf16[8,96,128]{2,1,0:T(8,128)(2,1)} %copy.8), calls=%async_computation.1 | async-start | bytes 393216 | tf_op jit(solution)/shard_map/all_to_all | solution.py:19
  29.6 2.7 %packed.1 = (bf16[3184,128]{1,0:T(8,128)(2,1)}, bf16[1136,128]{1,0:T(8,128)(2,1)S(1)}, bf16[3184,128]{1,0:T(8,128)(2,1)}, bf16[2048,128]{1,0:T(8,128)(2,1)S(1)}, bf16[112,128]{1,0:T(8,128)(2,1)S(1)}) custom-call(f32[2,1024,128]{2,1,0:T(8,128)} %down_ref.1, f32[2,128,1024]{2,1,0:T(8,128)} %up_ref.1, bf16[384,128]{1,0:T(8,128)(2,1)} %tokens_ref.3, ...), custom_call_target="tpu_custom_call" | custom-call | tf_op jit(solution)/shard_map/packed/pallas_call | solution.py:103
  32.3 2.2 %collective-permute-start.2 = (bf16[3184,128]{1,0:T(8,128)(2,1)}, bf16[3184,128]{1,0:T(8,128)(2,1)S(1)}, u32[]{:S(2)}, u32[]{:S(2)}) collective-permute-start(bf16[3184,128]{1,0:T(8,128)(2,1)} %get-tuple-element.28), channel_id=1, source_target_pairs={{0,16},{16,32},{32,48},{48,0},{1,17},{17,33},{33,49},{49,1},{2,18}... | collective-permute-start | bytes 2445320 | tf_op jit(solution)/shard_map/ppermute | solution.py:325
  34.5 4.3 %collective-permute-start = (bf16[3184,128]{1,0:T(8,128)(2,1)}, bf16[3184,128]{1,0:T(8,128)(2,1)S(1)}, u32[]{:S(2)}, u32[]{:S(2)}) collective-permute-start(bf16[3184,128]{1,0:T(8,128)(2,1)} %get-tuple-element.24.refs_1_), channel_id=1, source_target_pairs={{0,48},{16,0},{32,16},{48,32},{1,49},{17,1},{33,17},{49,33},{2,50}... | collective-permute-start | bytes 2445320 | tf_op jit(solution)/shard_map/ppermute | solution.py:325
  38.8 0.0 all-to-all-done.1
  38.9 0.7 broadcast_in_dim.6
  39.6 6.6 %all-to-all-start.2 = ((bf16[8,96,128]{2,1,0:T(8,128)(2,1)}), bf16[8,96,128]{2,1,0:T(8,128)(2,1)S(1)}, u32[]{:S(2)}, u32[]{:S(2)}) async-start(bf16[8,96,128]{2,1,0:T(8,128)(2,1)} %broadcast_in_dim.6), calls=%async_computation.2 | async-start | bytes 393216 | tf_op jit(solution)/shard_map/all_to_all | solution.py:19
  46.2 1.9 %collective-permute-start.1 = (bf16[1136,128]{1,0:T(8,128)(2,1)S(1)}, bf16[1136,128]{1,0:T(8,128)(2,1)S(1)}, u32[]{:S(2)}, u32[]{:S(2)}) collective-permute-start(bf16[1136,128]{1,0:T(8,128)(2,1)S(1)} %get-tuple-element.26), channel_id=1, source_target_pairs={{0,32},{16,48},{32,0},{48,16},{1,33},{17,49},{33,1},{49,17},{2,34}... | collective-permute-start | bytes 872456 | tf_op jit(solution)/shard_map/ppermute | solution.py:325
  48.2 4.9 %collective-permute-start.3 = (bf16[2048,128]{1,0:T(8,128)(2,1)S(1)}, bf16[2048,128]{1,0:T(8,128)(2,1)S(1)}, u32[]{:S(2)}, u32[]{:S(2)}) collective-permute-start(bf16[2048,128]{1,0:T(8,128)(2,1)S(1)} %get-tuple-element.35.refs_6_.refs_1_), channel_id=1, source_target_pairs={{0,32},{16,48},{32,0},{48,16},{1,33},{17,49},{33,1},{49,17},{2,34}... | collective-permute-start | bytes 1572872 | tf_op jit(solution)/shard_map/ppermute | solution.py:325
  53.0 5.9 %collective-permute-done.1.refs_3_.refs_4_ = bf16[1136,128]{1,0:T(8,128)(2,1)S(1)} collective-permute-done((bf16[1136,128]{1,0:T(8,128)(2,1)S(1)}, bf16[1136,128]{1,0:T(8,128)(2,1)S(1)}, u32[]{:S(2)}, u32[]{:S(2)}) %collective-permute-start.1) | collective-permute-done | bytes 290848 | tf_op jit(solution)/shard_map/ppermute | solution.py:325
  58.9 0.0 all-to-all-done.2.refs_0_
  58.9 0.0 collective-permute-done.2.refs_4_.refs_5_.refs_9_
  58.9 0.0 collective-permute-done.refs_2_.refs_3_.refs_7_
  58.9 1.8 down_product.2
  60.7 31.4 %all_to_all.56 = bf16[16,24,128]{2,1,0:T(8,128)(2,1)S(1)} all-to-all(bf16[16,24,128]{2,1,0:T(8,128)(2,1)S(1)} %bitcast.14), channel_id=1, replica_groups=mesh['z'=8,'x'=4,'y'=8,'core'=2] {'y','core'}, dimensions={0} | all-to-all | bytes 196608 | tf_op jit(solution)/shard_map/all_to_all | solution.py:19
  92.2 0.0 copy-start
  92.2 10.9 %all_to_all.57 = bf16[16,24,128]{2,1,0:T(8,128)(2,1)S(1)} all-to-all(bf16[16,24,128]{2,1,0:T(8,128)(2,1)S(1)} %broadcast_in_dim.7), channel_id=1, replica_groups=mesh['z'=8,'x'=4,'y'=8,'core'=2] {'y','core'}, dimensions={0} | all-to-all | bytes 196608 | tf_op jit(solution)/shard_map/all_to_all | solution.py:19
  103.1 0.0 collective-permute-done.3.refs_8_.refs_3_
  103.1 0.0 copy-done
  103.1 3.4 %turn.1 = (bf16[8,200,128]{2,1,0:T(8,128)(2,1)S(1)}, f32[4,96,128]{2,1,0:T(8,128)S(1)}, f32[4,96,128]{2,1,0:T(8,128)S(1)}, f32[4,8,128]{2,1,0:T(8,128)S(1)}) custom-call(bf16[4,96,128]{2,1,0:T(8,128)(2,1)S(1)} %bitcast.15, bf16[112,128]{1,0:T(8,128)(2,1)S(1)} %get-tuple-element.30.refs_1_, f32[2,1024]{1,0:T(2,128)S(1)} %copy-done, ...), custom_call_target="tpu_custom_call" | custom-call | tf_op jit(solution)/shard_map/turn/pallas_call | solution.py:225
  106.5 22.0 %all_to_all.58.refs_0_ = bf16[8,200,128]{2,1,0:T(8,128)(2,1)S(1)} all-to-all(bf16[8,200,128]{2,1,0:T(8,128)(2,1)S(1)} %get-tuple-element.37), channel_id=1, replica_groups=mesh['z'=8,'x'=4,'y'=8,'core'=2] {'z'}, dimensions={0} | all-to-all | bytes 819200 | tf_op jit(solution)/shard_map/all_to_all | solution.py:19
  128.5 0.1 second_hidden.1
  128.6 12.1 %all_to_all.59.refs_0_ = bf16[8,96,128]{2,1,0:T(8,128)(2,1)S(1)} all-to-all(bf16[8,96,128]{2,1,0:T(8,128)(2,1)S(1)} %get-tuple-element.40), channel_id=1, replica_groups=mesh['z'=8,'x'=4,'y'=8,'core'=2] {'z'}, dimensions={0} | all-to-all | bytes 393216 | tf_op jit(solution)/shard_map/all_to_all | solution.py:19
  140.7 0.9 down_product.3
  141.6 12.6 %all_to_all.60 = bf16[16,24,128]{2,1,0:T(8,128)(2,1)S(1)} all-to-all(bf16[16,24,128]{2,1,0:T(8,128)(2,1)S(1)} %bitcast.13), channel_id=1, replica_groups=mesh['z'=8,'x'=4,'y'=8,'core'=2] {'y','core'}, dimensions={0} | all-to-all | bytes 196608 | tf_op jit(solution)/shard_map/all_to_all | solution.py:19
  154.3 10.9 %all_to_all.61 = bf16[16,24,128]{2,1,0:T(8,128)(2,1)S(1)} all-to-all(bf16[16,24,128]{2,1,0:T(8,128)(2,1)S(1)} %broadcast_in_dim.8), channel_id=1, replica_groups=mesh['z'=8,'x'=4,'y'=8,'core'=2] {'y','core'}, dimensions={0} | all-to-all | bytes 196608 | tf_op jit(solution)/shard_map/all_to_all | solution.py:19
  165.2 0.4 squares.1
  165.6 9.3 %all_to_all.62.refs_0_ = f32[8,8,128]{2,1,0:T(8,128)S(1)} all-to-all(f32[8,8,128]{2,1,0:T(8,128)S(1)} %squares.1), channel_id=1, replica_groups=mesh['z'=8,'x'=4,'y'=8,'core'=2] {'z'}, dimensions={0} | all-to-all | bytes 65536 | tf_op jit(solution)/shard_map/all_to_all | solution.py:19
  174.8 0.1 last.1
  174.9 9.0 %all_to_all.63 = bf16[4,96,128]{2,1,0:T(8,128)(2,1)S(1)} all-to-all(bf16[4,96,128]{2,1,0:T(8,128)(2,1)S(1)} %last.1), channel_id=1, replica_groups=mesh['z'=8,'x'=4,'y'=8,'core'=2] {'x'}, dimensions={0} | all-to-all | bytes 196608 | tf_op jit(solution)/shard_map/all_to_all | solution.py:19
  183.9 0.6 copy.11
  (7 shorter events, 0.1 us)
Async XLA Ops:
  16.5 22.3 %all-to-all-start.1 = ((bf16[8,96,128]{2,1,0:T(8,128)(2,1)}), bf16[8,96,128]{2,1,0:T(8,128)(2,1)S(1)}, u32[]{:S(2)}, u32[]{:S(2)}) async-start(bf16[8,96,128]{2,1,0:T(8,128)(2,1)} %copy.8), calls=%async_computation.1 | async-start | bytes 393216 | tf_op jit(solution)/shard_map/all_to_all | solution.py:19
  32.3 26.6 %collective-permute-start.2 = (bf16[3184,128]{1,0:T(8,128)(2,1)}, bf16[3184,128]{1,0:T(8,128)(2,1)S(1)}, u32[]{:S(2)}, u32[]{:S(2)}) collective-permute-start(bf16[3184,128]{1,0:T(8,128)(2,1)} %get-tuple-element.28), channel_id=1, source_target_pairs={{0,16},{16,32},{32,48},{48,0},{1,17},{17,33},{33,49},{49,1},{2,18}... | collective-permute-start | bytes 2445320 | tf_op jit(solution)/shard_map/ppermute | solution.py:325
  34.5 24.4 %collective-permute-start = (bf16[3184,128]{1,0:T(8,128)(2,1)}, bf16[3184,128]{1,0:T(8,128)(2,1)S(1)}, u32[]{:S(2)}, u32[]{:S(2)}) collective-permute-start(bf16[3184,128]{1,0:T(8,128)(2,1)} %get-tuple-element.24.refs_1_), channel_id=1, source_target_pairs={{0,48},{16,0},{32,16},{48,32},{1,49},{17,1},{33,17},{49,33},{2,50}... | collective-permute-start | bytes 2445320 | tf_op jit(solution)/shard_map/ppermute | solution.py:325
  39.6 19.3 %all-to-all-start.2 = ((bf16[8,96,128]{2,1,0:T(8,128)(2,1)}), bf16[8,96,128]{2,1,0:T(8,128)(2,1)S(1)}, u32[]{:S(2)}, u32[]{:S(2)}) async-start(bf16[8,96,128]{2,1,0:T(8,128)(2,1)} %broadcast_in_dim.6), calls=%async_computation.2 | async-start | bytes 393216 | tf_op jit(solution)/shard_map/all_to_all | solution.py:19
  46.2 12.7 %collective-permute-start.1 = (bf16[1136,128]{1,0:T(8,128)(2,1)S(1)}, bf16[1136,128]{1,0:T(8,128)(2,1)S(1)}, u32[]{:S(2)}, u32[]{:S(2)}) collective-permute-start(bf16[1136,128]{1,0:T(8,128)(2,1)S(1)} %get-tuple-element.26), channel_id=1, source_target_pairs={{0,32},{16,48},{32,0},{48,16},{1,33},{17,49},{33,1},{49,17},{2,34}... | collective-permute-start | bytes 872456 | tf_op jit(solution)/shard_map/ppermute | solution.py:325
  48.2 54.9 %collective-permute-start.3 = (bf16[2048,128]{1,0:T(8,128)(2,1)S(1)}, bf16[2048,128]{1,0:T(8,128)(2,1)S(1)}, u32[]{:S(2)}, u32[]{:S(2)}) collective-permute-start(bf16[2048,128]{1,0:T(8,128)(2,1)S(1)} %get-tuple-element.35.refs_6_.refs_1_), channel_id=1, source_target_pairs={{0,32},{16,48},{32,0},{48,16},{1,33},{17,49},{33,1},{49,17},{2,34}... | collective-permute-start | bytes 1572872 | tf_op jit(solution)/shard_map/ppermute | solution.py:325
  92.2 10.9 %copy-start = (f32[2,1024]{1,0:T(2,128)S(1)}, f32[2,1024]{1,0:T(2,128)}, u32[]{:S(2)}) copy-start(f32[2,1024]{1,0:T(2,128)} %refs_2_.1) | copy-start | bytes 24580

commit v6 on v5

--- a/solution.py
+++ b/solution.py
@@ -44,27 +44,55 @@
     return pltpu.CompilerParams(vmem_limit_bytes=mib << 20)
 
 
-def up_kernel(tokens_ref, gain_ref, weight_ref, scale_ref, out_ref):
-    scaled = (tokens_ref[...].astype(f32) * gain_ref[0:1]).astype(bf16)
-    part = jnp.dot(scaled, weight_ref[0].astype(bf16), preferred_element_type=f32)
-    out_ref[...] = (part * scale_ref[0:1]).astype(bf16)
+def up_kernel(tokens_ref, gain_ref, weight_ref, scale_ref, out_ref, *scratch):
+    tokens, gain, weight, scale, out, in_sems, weight_sems, out_sems = scratch
+    parts, _, step = weight.shape
+    small = [
+        pltpu.make_async_copy(tokens_ref, tokens, in_sems.at[0]),
+        pltpu.make_async_copy(gain_ref, gain, in_sems.at[1]),
+        pltpu.make_async_copy(scale_ref, scale, in_sems.at[2]),
+    ]
+    for copy in small:
+        copy.start()
+    copies = []
+    for i in range(parts):
+        here = weight_ref.at[0, :, pl.ds(i * step, step)]
+        copies.append(pltpu.make_async_copy(here, weight.at[i], weight_sems.at[i]))
+        copies[-1].start()
+    for copy in small:
+        copy.wait()
+    scaled = (tokens[...].astype(f32) * gain[0:1]).astype(bf16)
+    sent = []
+    for i in range(parts):
+        copies[i].wait()
+        part = jnp.dot(scaled, weight[i].astype(bf16), preferred_element_type=f32)
+        out[i] = (part * scale[0:1, i * step : (i + 1) * step]).astype(bf16)
+        there = out_ref.at[:, pl.ds(i * step, step)]
+        sent.append(pltpu.make_async_copy(out.at[i], there, out_sems.at[i]))
+        sent[-1].start()
+    for copy in sent:
+        copy.wait()
 
 
 def up_product(tokens, gain, weight, scale):
     n_tok, feats = tokens.shape
     hid = weight.shape[2]
-    step = hid // 4
+    parts = 4
     return pl.pallas_call(
         up_kernel,
-        grid=(hid // step,),
         out_shape=jax.ShapeDtypeStruct((n_tok, hid), bf16),
-        in_specs=[
-            pl.BlockSpec((n_tok, feats), lambda i: (0, 0)),
-            pl.BlockSpec(gain.shape, lambda i: (0, 0)),
-            pl.BlockSpec((1, feats, step), lambda i: (0, 0, i)),
-            pl.BlockSpec((scale.shape[0], step), lambda i: (0, i)),
+        in_specs=[ANY] * 4,
+        out_specs=ANY,
+        scratch_shapes=[
+            pltpu.VMEM(tokens.shape, bf16),
+            pltpu.VMEM(gain.shape, f32),
+            pltpu.VMEM((parts, feats, hid // parts), f32),
+            pltpu.VMEM(scale.shape, f32),
+            pltpu.VMEM((parts, n_tok, hid // parts), bf16),
+            pltpu.SemaphoreType.DMA((3,)),
+            pltpu.SemaphoreType.DMA((parts,)),
+            pltpu.SemaphoreType.DMA((parts,)),
         ],
-        out_specs=pl.BlockSpec((n_tok, step), lambda i: (0, i)),
         compiler_params=limit(12),
         name="up_product",
     )(far(tokens), far(gain), far(weight), far(scale))
@@ -145,11 +173,14 @@
     )(near(hidden), *blocks)
 
 
-def down_sum(hidden, blocks, starts):
+def down_share(hidden, blocks, starts):
     part = down_product(hidden, blocks, starts)
     pieces = part.reshape(Y * C, -1, part.shape[2])
-    mine = exchange(pieces, ("y", "core")).astype(f32).sum(axis=0).astype(bf16)
-    return to_all(mine, ("y", "core")).reshape(part.shape)
+    return exchange(pieces, ("y", "core")).astype(f32).sum(axis=0).astype(bf16)
+
+
+def down_whole(mine):
+    return to_all(mine, ("y", "core")).reshape(X, -1, mine.shape[1])
 
 
 def squares_in_rows(values):
@@ -335,16 +366,19 @@
     pieces = part.astype(bf16).reshape(t_x, Z, hid // Z).transpose(1, 0, 2)
     summed = exchange(pieces, "z").astype(f32).sum(axis=0)
     hidden = to_all(activation(summed), "z")
-    summed = down_sum(hidden, [one, *after(firsts, hidden)], [0] * X)
-
-    firsts, seconds = after(firsts, summed), after(seconds, summed)
+    firsts = after(firsts, hidden)
+    mine = down_share(hidden, [one, *firsts], [0] * X)
+    summed = down_whole(mine)
+
+    seconds = [seconds[0], firsts[0], *after(seconds[2:3], summed), firsts[2]]
     part, kept, branch, columns = turn(
         summed, own, up_scale, firsts, [hid] * (X - 1), seconds, seconds_at
     )
     came = exchange(part, "z")
     hidden, stream = second_hidden(came, kept, branch, width)
     hidden = exchange(hidden, "z")
-    summed = down_sum(hidden, seconds, [at + hid for at in seconds_at])
+    mine = down_share(hidden, seconds, [at + hid for at in seconds_at])
+    summed = down_whole(mine)
 
     squares = squares_of(summed, columns)
     squares = exchange(squares, "z")

time: 186 us -> 187 us (level)
  blocking collectives: 131 us -> 120 us
  waiting for transfers between devices: 5.9 us -> 14.2 us
  starting transfers between devices: 33 us -> 36.6 us
    all_to_all x9 -> x8, blocking collectives: 131 us -> 120 us  [exchange(): return lax.all_to_all(pieces, axis, split_axis=0, concat_axis=0, tiled=True)]
    all_to_all x2 -> x3, waiting for transfers between devices: 0.01 us -> 8.34 us  [exchange(): return lax.all_to_all(pieces, axis, split_axis=0, concat_axis=0, tiled=True)]
    all_to_all x2 -> x3, starting transfers between devices: 19.8 us -> 23.3 us  [exchange(): return lax.all_to_all(pieces, axis, split_axis=0, concat_axis=0, tiled=True)]
  transfers between devices with their start and end apart: 6 -> 7, of which waited for: 1 -> 2; matrix products, arithmetic and copies ran while one was open for 0% -> 1% of each run, Pallas kernels for 2% -> 2%
where the time goes in v6:
time: 187 us; the launch traced here: 186 us
  blocking collectives  120 us (64%)
  starting transfers between devices  36.6 us (20%)
  waiting for transfers between devices  14.2 us (8%)
  Pallas kernels  11.6 us (6%)
  local copies, waits for them, and re-layouts  2.76 us (1%)
    all_to_all x8, blocking collectives, exchange(): return lax.all_to_all(pieces, axis, split_axis=0, concat_axis=0, tiled=True)  120 us
    all_to_all x3, starting transfers between devices, exchange(): return lax.all_to_all(pieces, axis, split_axis=0, concat_axis=0, tiled=True)  23.3 us
    ppermute x4, starting transfers between devices, from_x(): return lax.ppermute(payload, 'x', [(i, (i - s) % X) for i in range(X)])  13.3 us
    all_to_all x3, waiting for transfers between devices, exchange(): return lax.all_to_all(pieces, axis, split_axis=0, concat_axis=0, tiled=True)  8.34 us
    ppermute x4, waiting for transfers between devices, from_x(): return lax.ppermute(payload, 'x', [(i, (i - s) % X) for i in range(X)])  5.9 us
  transfers between devices with their start and end apart: 7, of which 2 were waited for; matrix products, arithmetic and copies ran while one was open for 1% of the time, Pallas kernels for 2%

profile of v6, /device:TPU:1, one launch (start us, length us, event | category | flops | bytes accessed | tf_op | source)
XLA Modules:
  0.0 185.7 jit_solution(10777618427338701690)
XLA Ops:
  0.0 2.1 %up_product.1 = bf16[384,1024]{1,0:T(8,128)(2,1)S(1)} custom-call(bf16[384,128]{1,0:T(8,128)(2,1)} %tokens_ref.3, f32[2,128]{1,0:T(2,128)} %pre_ref.1, f32[2,128,1024]{2,1,0:T(8,128)} %up_ref.1, f32[2,1024]{1,0:T(2,128)} %refs_2_.1), custom_call_target="tpu_custom_call" | custom-call | tf_op jit(solution)/shard_map/up_product/pallas_call | solution.py:81
  2.1 13.0 %all_to_all.55 = bf16[4,96,1024]{2,1,0:T(8,128)(2,1)S(1)} all-to-all(bf16[4,96,1024]{2,1,0:T(8,128)(2,1)S(1)} %bitcast.10), channel_id=1, replica_groups=mesh['z'=8,'x'=4,'y'=8,'core'=2] {'x'}, dimensions={0} | all-to-all | bytes 1572864 | tf_op jit(solution)/shard_map/all_to_all | solution.py:19
  15.1 0.1 reduce_sum.45
  15.3 0.7 copy.8
  16.0 13.1 %all-to-all-start.1 = ((bf16[8,96,128]{2,1,0:T(8,128)(2,1)}), bf16[8,96,128]{2,1,0:T(8,128)(2,1)S(1)}, u32[]{:S(2)}, u32[]{:S(2)}) async-start(bf16[8,96,128]{2,1,0:T(8,128)(2,1)} %copy.8), calls=%async_computation.1 | async-start | bytes 393216 | tf_op jit(solution)/shard_map/all_to_all | solution.py:19
  29.1 2.7 %packed.1 = (bf16[3184,128]{1,0:T(8,128)(2,1)}, bf16[1136,128]{1,0:T(8,128)(2,1)S(1)}, bf16[3184,128]{1,0:T(8,128)(2,1)}, bf16[2048,128]{1,0:T(8,128)(2,1)S(1)}, bf16[112,128]{1,0:T(8,128)(2,1)S(1)}) custom-call(f32[2,1024,128]{2,1,0:T(8,128)} %down_ref.1, f32[2,128,1024]{2,1,0:T(8,128)} %up_ref.1, bf16[384,128]{1,0:T(8,128)(2,1)} %tokens_ref.3, ...), custom_call_target="tpu_custom_call" | custom-call | tf_op jit(solution)/shard_map/packed/pallas_call | solution.py:131
  31.8 2.2 %collective-permute-start.2 = (bf16[3184,128]{1,0:T(8,128)(2,1)}, bf16[3184,128]{1,0:T(8,128)(2,1)S(1)}, u32[]{:S(2)}, u32[]{:S(2)}) collective-permute-start(bf16[3184,128]{1,0:T(8,128)(2,1)} %get-tuple-element.24), channel_id=1, source_target_pairs={{0,16},{16,32},{32,48},{48,0},{1,17},{17,33},{33,49},{49,1},{2,18}... | collective-permute-start | bytes 2445320 | tf_op jit(solution)/shard_map/ppermute | solution.py:356
  34.0 4.3 %collective-permute-start = (bf16[3184,128]{1,0:T(8,128)(2,1)}, bf16[3184,128]{1,0:T(8,128)(2,1)S(1)}, u32[]{:S(2)}, u32[]{:S(2)}) collective-permute-start(bf16[3184,128]{1,0:T(8,128)(2,1)} %get-tuple-element.20.refs_1_), channel_id=1, source_target_pairs={{0,48},{16,0},{32,16},{48,32},{1,49},{17,1},{33,17},{49,33},{2,50}... | collective-permute-start | bytes 2445320 | tf_op jit(solution)/shard_map/ppermute | solution.py:356
  38.3 0.0 all-to-all-done.1
  38.4 0.7 broadcast_in_dim.6
  39.1 6.6 %all-to-all-start.2 = ((bf16[8,96,128]{2,1,0:T(8,128)(2,1)}), bf16[8,96,128]{2,1,0:T(8,128)(2,1)S(1)}, u32[]{:S(2)}, u32[]{:S(2)}) async-start(bf16[8,96,128]{2,1,0:T(8,128)(2,1)} %broadcast_in_dim.6), calls=%async_computation.2 | async-start | bytes 393216 | tf_op jit(solution)/shard_map/all_to_all | solution.py:19
  45.7 1.9 %collective-permute-start.1 = (bf16[1136,128]{1,0:T(8,128)(2,1)S(1)}, bf16[1136,128]{1,0:T(8,128)(2,1)S(1)}, u32[]{:S(2)}, u32[]{:S(2)}) collective-permute-start(bf16[1136,128]{1,0:T(8,128)(2,1)S(1)} %get-tuple-element.22), channel_id=1, source_target_pairs={{0,32},{16,48},{32,0},{48,16},{1,33},{17,49},{33,1},{49,17},{2,34}... | collective-permute-start | bytes 872456 | tf_op jit(solution)/shard_map/ppermute | solution.py:356
  47.6 4.9 %collective-permute-start.3 = (bf16[2048,128]{1,0:T(8,128)(2,1)S(1)}, bf16[2048,128]{1,0:T(8,128)(2,1)S(1)}, u32[]{:S(2)}, u32[]{:S(2)}) collective-permute-start(bf16[2048,128]{1,0:T(8,128)(2,1)S(1)} %get-tuple-element.27.refs_6_.refs_1_), channel_id=1, source_target_pairs={{0,32},{16,48},{32,0},{48,16},{1,33},{17,49},{33,1},{49,17},{2,34}... | collective-permute-start | bytes 1572872 | tf_op jit(solution)/shard_map/ppermute | solution.py:356
  52.5 5.9 %collective-permute-done.1.refs_3_.refs_4_ = bf16[1136,128]{1,0:T(8,128)(2,1)S(1)} collective-permute-done((bf16[1136,128]{1,0:T(8,128)(2,1)S(1)}, bf16[1136,128]{1,0:T(8,128)(2,1)S(1)}, u32[]{:S(2)}, u32[]{:S(2)}) %collective-permute-start.1) | collective-permute-done | bytes 290848 | tf_op jit(solution)/shard_map/ppermute | solution.py:356
  58.4 0.0 all-to-all-done.2.refs_0_
  58.4 0.0 collective-permute-done.2.refs_4_.refs_5_.refs_9_
  58.4 0.0 collective-permute-done.refs_2_.refs_3_.refs_7_
  58.4 1.8 down_product.2
  60.2 31.4 %all_to_all.56 = bf16[16,24,128]{2,1,0:T(8,128)(2,1)S(1)} all-to-all(bf16[16,24,128]{2,1,0:T(8,128)(2,1)S(1)} %bitcast.14), channel_id=1, replica_groups=mesh['z'=8,'x'=4,'y'=8,'core'=2] {'y','core'}, dimensions={0} | all-to-all | bytes 196608 | tf_op jit(solution)/shard_map/all_to_all | solution.py:19
  91.7 0.7 broadcast_in_dim.7
  92.3 0.0 copy-start
  92.3 3.5 %all-to-all-start.4 = ((bf16[16,24,128]{2,1,0:T(8,128)(2,1)}), bf16[16,24,128]{2,1,0:T(8,128)(2,1)S(1)}, u32[]{:S(2)}, u32[]{:S(2)}) async-start(bf16[16,24,128]{2,1,0:T(8,128)(2,1)} %broadcast_in_dim.7), calls=%async_computation.4 | async-start | bytes 196608 | tf_op jit(solution)/shard_map/all_to_all | solution.py:19
  95.9 0.0 collective-permute-done.3.refs_8_.refs_3_
  95.9 8.3 %all-to-all-done.4 = bf16[16,24,128]{2,1,0:T(8,128)(2,1)S(1)} async-done(((bf16[16,24,128]{2,1,0:T(8,128)(2,1)}), bf16[16,24,128]{2,1,0:T(8,128)(2,1)S(1)}, u32[]{:S(2)}, u32[]{:S(2)}) %all-to-all-start.4) | async-done | bytes 98336 | tf_op jit(solution)/shard_map/all_to_all | solution.py:19
  104.2 0.0 copy-done
  104.2 3.4 %turn.1 = (bf16[8,200,128]{2,1,0:T(8,128)(2,1)S(1)}, f32[4,96,128]{2,1,0:T(8,128)S(1)}, f32[4,96,128]{2,1,0:T(8,128)S(1)}, f32[4,8,128]{2,1,0:T(8,128)S(1)}) custom-call(bf16[4,96,128]{2,1,0:T(8,128)(2,1)S(1)} %bitcast.15, bf16[112,128]{1,0:T(8,128)(2,1)S(1)} %get-tuple-element.26.refs_1_, f32[2,1024]{1,0:T(2,128)S(1)} %copy-done, ...), custom_call_target="tpu_custom_call" | custom-call | tf_op jit(solution)/shard_map/turn/pallas_call | solution.py:256
  107.6 22.0 %all_to_all.57.refs_0_ = bf16[8,200,128]{2,1,0:T(8,128)(2,1)S(1)} all-to-all(bf16[8,200,128]{2,1,0:T(8,128)(2,1)S(1)} %get-tuple-element.29), channel_id=1, replica_groups=mesh['z'=8,'x'=4,'y'=8,'core'=2] {'z'}, dimensions={0} | all-to-all | bytes 819200 | tf_op jit(solution)/shard_map/all_to_all | solution.py:19
  129.6 0.1 second_hidden.1
  129.7 12.1 %all_to_all.58.refs_0_ = bf16[8,96,128]{2,1,0:T(8,128)(2,1)S(1)} all-to-all(bf16[8,96,128]{2,1,0:T(8,128)(2,1)S(1)} %get-tuple-element.32), channel_id=1, replica_groups=mesh['z'=8,'x'=4,'y'=8,'core'=2] {'z'}, dimensions={0} | all-to-all | bytes 393216 | tf_op jit(solution)/shard_map/all_to_all | solution.py:19
  141.8 0.9 down_product.3
  142.8 12.6 %all_to_all.59 = bf16[16,24,128]{2,1,0:T(8,128)(2,1)S(1)} all-to-all(bf16[16,24,128]{2,1,0:T(8,128)(2,1)S(1)} %bitcast.13), channel_id=1, replica_groups=mesh['z'=8,'x'=4,'y'=8,'core'=2] {'y','core'}, dimensions={0} | all-to-all | bytes 196608 | tf_op jit(solution)/shard_map/all_to_all | solution.py:19
  155.4 10.9 %all_to_all.60 = bf16[16,24,128]{2,1,0:T(8,128)(2,1)S(1)} all-to-all(bf16[16,24,128]{2,1,0:T(8,128)(2,1)S(1)} %broadcast_in_dim.8), channel_id=1, replica_groups=mesh['z'=8,'x'=4,'y'=8,'core'=2] {'y','core'}, dimensions={0} | all-to-all | bytes 196608 | tf_op jit(solution)/shard_map/all_to_all | solution.py:19
  166.3 0.4 squares.1
  166.7 9.3 %all_to_all.61.refs_0_ = f32[8,8,128]{2,1,0:T(8,128)S(1)} all-to-all(f32[8,8,128]{2,1,0:T(8,128)S(1)} %squares.1), channel_id=1, replica_groups=mesh['z'=8,'x'=4,'y'=8,'core'=2] {'z'}, dimensions={0} | all-to-all | bytes 65536 | tf_op jit(solution)/shard_map/all_to_all | solution.py:19
  175.9 0.1 last.1
  176.1 9.0 %all_to_all.62 = bf16[4,96,128]{2,1,0:T(8,128)(2,1)S(1)} all-to-all(bf16[4,96,128]{2,1,0:T(8,128)(2,1)S(1)} %last.1), channel_id=1, replica_groups=mesh['z'=8,'x'=4,'y'=8,'core'=2] {'x'}, dimensions={0} | all-to-all | bytes 196608 | tf_op jit(solution)/shard_map/all_to_all | solution.py:19
  185.1 0.6 copy.11
  (6 shorter events, 0.1 us)
Async XLA Ops:
  16.0 22.3 %all-to-all-start.1 = ((bf16[8,96,128]{2,1,0:T(8,128)(2,1)}), bf16[8,96,128]{2,1,0:T(8,128)(2,1)S(1)}, u32[]{:S(2)}, u32[]{:S(2)}) async-start(bf16[8,96,128]{2,1,0:T(8,128)(2,1)} %copy.8), calls=%async_computation.1 | async-start | bytes 393216 | tf_op jit(solution)/shard_map/all_to_all | solution.py:19
  31.8 26.6 %collective-permute-start.2 = (bf16[3184,128]{1,0:T(8,128)(2,1)}, bf16[3184,128]{1,0:T(8,128)(2,1)S(1)}, u32[]{:S(2)}, u32[]{:S(2)}) collective-permute-start(bf16[3184,128]{1,0:T(8,128)(2,1)} %get-tuple-element.24), channel_id=1, source_target_pairs={{0,16},{16,32},{32,48},{48,0},{1,17},{17,33},{33,49},{49,1},{2,18}... | collective-permute-start | bytes 2445320 | tf_op jit(solution)/shard_map/ppermute | solution.py:356
  34.0 24.4 %collective-permute-start = (bf16[3184,128]{1,0:T(8,128)(2,1)}, bf16[3184,128]{1,0:T(8,128)(2,1)S(1)}, u32[]{:S(2)}, u32[]{:S(2)}) collective-permute-start(bf16[3184,128]{1,0:T(8,128)(2,1)} %get-tuple-element.20.refs_1_), channel_id=1, source_target_pairs={{0,48},{16,0},{32,16},{48,32},{1,49},{17,1},{33,17},{49,33},{2,50}... | collective-permute-start | bytes 2445320 | tf_op jit(solution)/shard_map/ppermute | solution.py:356
  39.1 19.3 %all-to-all-start.2 = ((bf16[8,96,128]{2,1,0:T(8,128)(2,1)}), bf16[8,96,128]{2,1,0:T(8,128)(2,1)S(1)}, u32[]{:S(2)}, u32[]{:S(2)}) async-start(bf16[8,96,128]{2,1,0:T(8,128)(2,1)} %broadcast_in_dim.6), calls=%async_computation.2 | async-start | bytes 393216 | tf_op jit(solution)/shard_map/all_to_all | solution.py:19
  45.7 12.7 %collective-permute-start.1 = (bf16[1136,128]{1,0:T(8,128)(2,1)S(1)}, bf16[1136,128]{1,0:T(8,128)(2,1)S(1)}, u32[]{:S(2)}, u32[]{:S(2)}) collective-permute-start(bf16[1136,128]{1,0:T(8,128)(2,1)S(1)} %get-tuple-element.22), channel_id=1, source_target_pairs={{0,32},{16,48},{32,0},{48,16},{1,33},{17,49},{33,1},{49,17},{2,34}... | collective-permute-start | bytes 872456 | tf_op jit(solution)/shard_map/ppermute | solution.py:356
  47.6 48.2 %collective-permute-start.3 = (bf16[2048,128]{1,0:T(8,128)(2,1)S(1)}, bf16[2048,128]{1,0:T(8,128)(2,1)S(1)}, u32[]{:S(2)}, u32[]{:S(2)}) collective-permute-start(bf16[2048,128]{1,0:T(8,128)(2,1)S(1)} %get-tuple-element.27.refs_6_.refs_1_), channel_id=1, source_target_pairs={{0,32},{16,48},{32,0},{48,16},{1,33},{17,49},{33,1},{49,17},{2,34}... | collective-permute-start | bytes 1572872 | tf_op jit(solution)/shard_map/ppermute | solution.py:356
  92.3 11.9 %copy-start = (f32[2,1024]{1,0:T(2,128)S(1)}, f32[2,1024]{1,0:T(2,128)}, u32[]{:S(2)}) copy-start(f32[2,1024]{1,0:T(2,128)} %refs_2_.1) | copy-start | bytes 24580
  92.3 11.9 %all-to-all-start.4 = ((bf16[16,24,128]{2,1,0:T(8,128)(2,1)}), bf16[16,24,128]{2,1,0:T(8,128)(2,1)S(1)}, u32[]{:S(2)}, u32[]{:S(2)}) async-start(bf16[16,24,128]{2,1,0:T(8,128)(2,1)} %broadcast_in_dim.7), calls=%async_computation.4 | async-start | bytes 196608 | tf_op jit(solution)/shard_map/all_to_all | solution.py:19

commit v7 on v6

--- a/solution.py
+++ b/solution.py
@@ -131,7 +131,10 @@
     return pl.pallas_call(
         pack_kernel,
         grid=(1,),
-        out_shape=tuple(jax.ShapeDtypeStruct((r, feats), bf16) for r in rows),
+        out_shape=(
+            *(pltpu.HBM((r, feats), bf16) for r in rows[:-1]),
+            pltpu.VMEM((rows[-1], feats), bf16),
+        ),
         in_specs=[
             whole(down_weight),
             pl.BlockSpec((1, feats, hid), lambda i: (1, 0, 0)),
@@ -201,12 +204,13 @@
     return jnp.transpose(jnp.broadcast_to(inv, (128, 128)))[:t]
 
 
-def turn_kernel(firsts_at, seconds_at, sum_ref, own_ref, scale_ref, *refs):
+def turn_kernel(firsts_at, seconds_at, lead_ref, sum_ref, own_ref, scale_ref, *refs):
     firsts, seconds = refs[: X - 1], refs[X - 1 : 2 * X - 1]
     out_ref, kept_ref, branch_ref, columns_ref = refs[2 * X - 1 : 2 * X + 3]
-    extra, held, sems, held_sems = refs[2 * X + 3 :]
+    extra, held, scales, sems, held_sems = refs[2 * X + 3 :]
     t, feats = sum_ref.shape[1:]
-    copies = []
+    copies = [pltpu.make_async_copy(scale_ref, scales, sems.at[X - 1])]
+    copies[0].start()
     for i, block in enumerate(firsts):
         rows = block.at[pl.ds(firsts_at[i], extra.shape[1])]
         copies.append(pltpu.make_async_copy(rows, extra.at[i], sems.at[i]))
@@ -227,7 +231,7 @@
         columns_ref[i] = columns
         down_0, post_0, pre_1 = [columns[k : k + 1] for k in range(3)]
         kept = residual_keep * block[16:].astype(f32)
-        branch_in = sum_ref[i].astype(f32) * down_0
+        branch_in = (lead_ref[...] if i == 0 else sum_ref[i].astype(f32)) * down_0
         branch = branch_in * post_0
         kept_ref[i] = kept
         branch_ref[i] = branch
@@ -245,7 +249,7 @@
         copy.wait()
     for c in range(Z):
         part = jnp.dot(terms, held[c], preferred_element_type=f32)
-        scale = scale_ref[1:2, c * feats : (c + 1) * feats]
+        scale = scales[1:2, c * feats : (c + 1) * feats]
         out_ref[c, : 2 * t] = (part * scale).astype(bf16)
         out_ref[c, 2 * t :] = jnp.zeros((8, feats), bf16)
         out_ref[c, 2 * t :, :t] = squares
@@ -253,6 +257,7 @@
 
 def turn(summed, own, scale, firsts, firsts_at, seconds, seconds_at):
     _, t, feats = summed.shape
+    lead = summed[0].astype(f32)
     return pl.pallas_call(
         lambda *refs: turn_kernel(firsts_at, seconds_at, *refs),
         out_shape=(
@@ -261,17 +266,18 @@
             pltpu.VMEM((X, t, feats), f32),
             pltpu.VMEM((X, 8, feats), f32),
         ),
-        in_specs=[*[VMEM] * 3, *[ANY] * (2 * X - 1)],
+        in_specs=[*[VMEM] * 3, *[ANY] * (2 * X)],
         out_specs=(VMEM,) * 4,
         scratch_shapes=[
             pltpu.VMEM((X - 1, 16 + t, feats), bf16),
             pltpu.VMEM((Z, X * feats, feats), bf16),
-            pltpu.SemaphoreType.DMA((X - 1,)),
+            pltpu.VMEM(scale.shape, f32),
+            pltpu.SemaphoreType.DMA((X,)),
             pltpu.SemaphoreType.DMA((X, Z)),
         ],
         compiler_params=limit(12),
         name="turn",
-    )(near(summed), near(own), near(scale), *firsts, *seconds)
+    )(near(lead), near(summed), near(own), far(scale), *firsts, *seconds)
 
 
 def hidden_kernel(width, came_ref, kept_ref, branch_ref, out_ref, stream_ref):
@@ -367,10 +373,10 @@
     summed = exchange(pieces, "z").astype(f32).sum(axis=0)
     hidden = to_all(activation(summed), "z")
     firsts = after(firsts, hidden)
-    mine = down_share(hidden, [one, *firsts], [0] * X)
+    mine = down_share(hidden, [far(one), *firsts], [0] * X)
     summed = down_whole(mine)
 
-    seconds = [seconds[0], firsts[0], *after(seconds[2:3], summed), firsts[2]]
+    seconds = [far(seconds[0]), firsts[0], *after(seconds[2:3], summed), firsts[2]]
     part, kept, branch, columns = turn(
         summed, own, up_scale, firsts, [hid] * (X - 1), seconds, seconds_at
     )

time: 187 us -> 188 us (level)
  transfers between devices with their start and end apart: 7 -> 7, of which waited for: 2 -> 2; matrix products, arithmetic and copies ran while one was open for 1% -> 1% of each run, Pallas kernels for 2% -> 3%
where the time goes in v7:
time: 188 us; the launch traced here: 187 us
  blocking collectives  120 us (64%)
  starting transfers between devices  36.6 us (19%)
  waiting for transfers between devices  14.2 us (8%)
  Pallas kernels  12.4 us (7%)
  local copies, waits for them, and re-layouts  2.76 us (1%)
    all_to_all x8, blocking collectives, exchange(): return lax.all_to_all(pieces, axis, split_axis=0, concat_axis=0, tiled=True)  120 us
    all_to_all x3, starting transfers between devices, exchange(): return lax.all_to_all(pieces, axis, split_axis=0, concat_axis=0, tiled=True)  23.2 us
    ppermute x4, starting transfers between devices, from_x(): return lax.ppermute(payload, 'x', [(i, (i - s) % X) for i in range(X)])  13.4 us
    all_to_all x3, waiting for transfers between devices, exchange(): return lax.all_to_all(pieces, axis, split_axis=0, concat_axis=0, tiled=True)  8.34 us
    ppermute x4, waiting for transfers between devices, from_x(): return lax.ppermute(payload, 'x', [(i, (i - s) % X) for i in range(X)])  5.86 us
  transfers between devices with their start and end apart: 7, of which 2 were waited for; matrix products, arithmetic and copies ran while one was open for 1% of the time, Pallas kernels for 3%

profile of v7, /device:TPU:1, one launch (start us, length us, event | category | flops | bytes accessed | tf_op | source)
XLA Modules:
  0.0 186.5 jit_solution(9510272785010577897)
XLA Ops:
  0.0 2.1 %up_product.1 = bf16[384,1024]{1,0:T(8,128)(2,1)S(1)} custom-call(bf16[384,128]{1,0:T(8,128)(2,1)} %tokens_ref.3, f32[2,128]{1,0:T(2,128)} %pre_ref.1, f32[2,128,1024]{2,1,0:T(8,128)} %up_ref.1, f32[2,1024]{1,0:T(2,128)} %refs_3_.1), custom_call_target="tpu_custom_call" | custom-call | tf_op jit(solution)/shard_map/up_product/pallas_call | solution.py:81
  2.1 13.0 %all_to_all.55 = bf16[4,96,1024]{2,1,0:T(8,128)(2,1)S(1)} all-to-all(bf16[4,96,1024]{2,1,0:T(8,128)(2,1)S(1)} %bitcast.13), channel_id=1, replica_groups=mesh['z'=8,'x'=4,'y'=8,'core'=2] {'x'}, dimensions={0} | all-to-all | bytes 1572864 | tf_op jit(solution)/shard_map/all_to_all | solution.py:19
  15.1 0.1 reduce_sum.45
  15.3 0.7 copy.8
  16.0 13.1 %all-to-all-start.1 = ((bf16[8,96,128]{2,1,0:T(8,128)(2,1)}), bf16[8,96,128]{2,1,0:T(8,128)(2,1)S(1)}, u32[]{:S(2)}, u32[]{:S(2)}) async-start(bf16[8,96,128]{2,1,0:T(8,128)(2,1)} %copy.8), calls=%async_computation.1 | async-start | bytes 393216 | tf_op jit(solution)/shard_map/all_to_all | solution.py:19
  29.1 2.9 %packed.1 = (bf16[3184,128]{1,0:T(8,128)(2,1)}, bf16[1136,128]{1,0:T(8,128)(2,1)}, bf16[3184,128]{1,0:T(8,128)(2,1)}, bf16[2048,128]{1,0:T(8,128)(2,1)}, bf16[112,128]{1,0:T(8,128)(2,1)S(1)}) custom-call(f32[2,1024,128]{2,1,0:T(8,128)} %down_ref.1, f32[2,128,1024]{2,1,0:T(8,128)} %up_ref.1, bf16[384,128]{1,0:T(8,128)(2,1)} %tokens_ref.3, ...), custom_call_target="tpu_custom_call" | custom-call | tf_op jit(solution)/shard_map/packed/pallas_call | solution.py:131
  32.0 0.0 copy-start
  32.0 2.3 %collective-permute-start.2 = (bf16[3184,128]{1,0:T(8,128)(2,1)}, bf16[3184,128]{1,0:T(8,128)(2,1)S(1)}, u32[]{:S(2)}, u32[]{:S(2)}) collective-permute-start(bf16[3184,128]{1,0:T(8,128)(2,1)} %get-tuple-element.24), channel_id=1, source_target_pairs={{0,16},{16,32},{32,48},{48,0},{1,17},{17,33},{33,49},{49,1},{2,18}... | collective-permute-start | bytes 2445320 | tf_op jit(solution)/shard_map/ppermute | solution.py:362
  34.4 4.3 %collective-permute-start = (bf16[3184,128]{1,0:T(8,128)(2,1)}, bf16[3184,128]{1,0:T(8,128)(2,1)S(1)}, u32[]{:S(2)}, u32[]{:S(2)}) collective-permute-start(bf16[3184,128]{1,0:T(8,128)(2,1)} %get-tuple-element.20.refs_1_), channel_id=1, source_target_pairs={{0,48},{16,0},{32,16},{48,32},{1,49},{17,1},{33,17},{49,33},{2,50}... | collective-permute-start | bytes 2445320 | tf_op jit(solution)/shard_map/ppermute | solution.py:362
  38.7 0.0 all-to-all-done.1
  38.7 0.0 copy-start.1
  38.7 0.7 broadcast_in_dim.6
  39.4 6.6 %all-to-all-start.2 = ((bf16[8,96,128]{2,1,0:T(8,128)(2,1)}), bf16[8,96,128]{2,1,0:T(8,128)(2,1)S(1)}, u32[]{:S(2)}, u32[]{:S(2)}) async-start(bf16[8,96,128]{2,1,0:T(8,128)(2,1)} %broadcast_in_dim.6), calls=%async_computation.2 | async-start | bytes 393216 | tf_op jit(solution)/shard_map/all_to_all | solution.py:19
  46.1 0.0 copy-done.1
  46.1 1.9 %collective-permute-start.1 = (bf16[1136,128]{1,0:T(8,128)(2,1)S(1)}, bf16[1136,128]{1,0:T(8,128)(2,1)S(1)}, u32[]{:S(2)}, u32[]{:S(2)}) collective-permute-start(bf16[1136,128]{1,0:T(8,128)(2,1)S(1)} %copy-done.1), channel_id=1, source_target_pairs={{0,32},{16,48},{32,0},{48,16},{1,33},{17,49},{33,1},{49,17},{2,34}... | collective-permute-start | bytes 872456 | tf_op jit(solution)/shard_map/ppermute | solution.py:362
  48.0 0.0 copy-done
  48.0 4.9 %collective-permute-start.3 = (bf16[2048,128]{1,0:T(8,128)(2,1)S(1)}, bf16[2048,128]{1,0:T(8,128)(2,1)S(1)}, u32[]{:S(2)}, u32[]{:S(2)}) collective-permute-start(bf16[2048,128]{1,0:T(8,128)(2,1)S(1)} %copy-done), channel_id=1, source_target_pairs={{0,32},{16,48},{32,0},{48,16},{1,33},{17,49},{33,1},{49,17},{2,34}... | collective-permute-start | bytes 1572872 | tf_op jit(solution)/shard_map/ppermute | solution.py:362
  52.9 5.9 %collective-permute-done.1.refs_3_.refs_5_ = bf16[1136,128]{1,0:T(8,128)(2,1)S(1)} collective-permute-done((bf16[1136,128]{1,0:T(8,128)(2,1)S(1)}, bf16[1136,128]{1,0:T(8,128)(2,1)S(1)}, u32[]{:S(2)}, u32[]{:S(2)}) %collective-permute-start.1) | collective-permute-done | bytes 290848 | tf_op jit(solution)/shard_map/ppermute | solution.py:362
  58.8 0.0 all-to-all-done.2.refs_0_
  58.8 0.0 collective-permute-done.2.refs_4_.refs_6_.refs_10_
  58.8 0.0 collective-permute-done.refs_2_.refs_4_.refs_8_
  58.8 1.8 down_product.2
  60.6 31.4 %all_to_all.56 = bf16[16,24,128]{2,1,0:T(8,128)(2,1)S(1)} all-to-all(bf16[16,24,128]{2,1,0:T(8,128)(2,1)S(1)} %bitcast.18), channel_id=1, replica_groups=mesh['z'=8,'x'=4,'y'=8,'core'=2] {'y','core'}, dimensions={0} | all-to-all | bytes 196608 | tf_op jit(solution)/shard_map/all_to_all | solution.py:19
  92.0 0.7 broadcast_in_dim.7
  92.7 3.4 %all-to-all-start.4 = ((bf16[16,24,128]{2,1,0:T(8,128)(2,1)}), bf16[16,24,128]{2,1,0:T(8,128)(2,1)S(1)}, u32[]{:S(2)}, u32[]{:S(2)}) async-start(bf16[16,24,128]{2,1,0:T(8,128)(2,1)} %broadcast_in_dim.7), calls=%async_computation.4 | async-start | bytes 196608 | tf_op jit(solution)/shard_map/all_to_all | solution.py:19
  96.1 0.0 collective-permute-done.3.refs_9_.refs_3_
  96.1 8.3 %all-to-all-done.4 = bf16[16,24,128]{2,1,0:T(8,128)(2,1)S(1)} async-done(((bf16[16,24,128]{2,1,0:T(8,128)(2,1)}), bf16[16,24,128]{2,1,0:T(8,128)(2,1)S(1)}, u32[]{:S(2)}, u32[]{:S(2)}) %all-to-all-start.4) | async-done | bytes 98336 | tf_op jit(solution)/shard_map/all_to_all | solution.py:19
  104.5 3.1 %turn.1 = (bf16[8,200,128]{2,1,0:T(8,128)(2,1)S(1)}, f32[4,96,128]{2,1,0:T(8,128)S(1)}, f32[4,96,128]{2,1,0:T(8,128)S(1)}, f32[4,8,128]{2,1,0:T(8,128)S(1)}) custom-call(f32[96,128]{1,0:T(8,128)S(1)} %bitcast_convert_fusion.refs_0_, bf16[4,96,128]{2,1,0:T(8,128)(2,1)S(1)} %bitcast.16, bf16[112,128]{1,0:T(8,128)(2,1)S(1)} %get-tuple-element.26.refs_2_, ...), custom_call_target="tpu_custom_call" | custom-call | tf_op jit(solution)/shard_map/turn/pallas_call | solution.py:261
  107.6 22.0 %all_to_all.57.refs_0_ = bf16[8,200,128]{2,1,0:T(8,128)(2,1)S(1)} all-to-all(bf16[8,200,128]{2,1,0:T(8,128)(2,1)S(1)} %get-tuple-element.29), channel_id=1, replica_groups=mesh['z'=8,'x'=4,'y'=8,'core'=2] {'z'}, dimensions={0} | all-to-all | bytes 819200 | tf_op jit(solution)/shard_map/all_to_all | solution.py:19
  129.6 0.1 second_hidden.1
  129.7 12.1 %all_to_all.58.refs_0_ = bf16[8,96,128]{2,1,0:T(8,128)(2,1)S(1)} all-to-all(bf16[8,96,128]{2,1,0:T(8,128)(2,1)S(1)} %get-tuple-element.32), channel_id=1, replica_groups=mesh['z'=8,'x'=4,'y'=8,'core'=2] {'z'}, dimensions={0} | all-to-all | bytes 393216 | tf_op jit(solution)/shard_map/all_to_all | solution.py:19
  141.8 1.8 down_product.3
  143.6 12.6 %all_to_all.59 = bf16[16,24,128]{2,1,0:T(8,128)(2,1)S(1)} all-to-all(bf16[16,24,128]{2,1,0:T(8,128)(2,1)S(1)} %bitcast.17), channel_id=1, replica_groups=mesh['z'=8,'x'=4,'y'=8,'core'=2] {'y','core'}, dimensions={0} | all-to-all | bytes 196608 | tf_op jit(solution)/shard_map/all_to_all | solution.py:19
  156.2 10.9 %all_to_all.60 = bf16[16,24,128]{2,1,0:T(8,128)(2,1)S(1)} all-to-all(bf16[16,24,128]{2,1,0:T(8,128)(2,1)S(1)} %broadcast_in_dim.8), channel_id=1, replica_groups=mesh['z'=8,'x'=4,'y'=8,'core'=2] {'y','core'}, dimensions={0} | all-to-all | bytes 196608 | tf_op jit(solution)/shard_map/all_to_all | solution.py:19
  167.1 0.4 squares.1
  167.5 9.3 %all_to_all.61.refs_0_ = f32[8,8,128]{2,1,0:T(8,128)S(1)} all-to-all(f32[8,8,128]{2,1,0:T(8,128)S(1)} %squares.1), channel_id=1, replica_groups=mesh['z'=8,'x'=4,'y'=8,'core'=2] {'z'}, dimensions={0} | all-to-all | bytes 65536 | tf_op jit(solution)/shard_map/all_to_all | solution.py:19
  176.8 0.1 last.1
  176.9 9.0 %all_to_all.62 = bf16[4,96,128]{2,1,0:T(8,128)(2,1)S(1)} all-to-all(bf16[4,96,128]{2,1,0:T(8,128)(2,1)S(1)} %last.1), channel_id=1, replica_groups=mesh['z'=8,'x'=4,'y'=8,'core'=2] {'x'}, dimensions={0} | all-to-all | bytes 196608 | tf_op jit(solution)/shard_map/all_to_all | solution.py:19
  185.9 0.6 copy.11
  (8 shorter events, 0.1 us)
Async XLA Ops:
  16.0 22.7 %all-to-all-start.1 = ((bf16[8,96,128]{2,1,0:T(8,128)(2,1)}), bf16[8,96,128]{2,1,0:T(8,128)(2,1)S(1)}, u32[]{:S(2)}, u32[]{:S(2)}) async-start(bf16[8,96,128]{2,1,0:T(8,128)(2,1)} %copy.8), calls=%async_computation.1 | async-start | bytes 393216 | tf_op jit(solution)/shard_map/all_to_all | solution.py:19
  32.0 16.0 %copy-start = (bf16[2048,128]{1,0:T(8,128)(2,1)S(1)}, bf16[2048,128]{1,0:T(8,128)(2,1)}, u32[]{:S(2)}) copy-start(bf16[2048,128]{1,0:T(8,128)(2,1)} %get-tuple-element.27.refs_7_.refs_1_) | copy-start | bytes 1572868
  32.0 26.7 %collective-permute-start.2 = (bf16[3184,128]{1,0:T(8,128)(2,1)}, bf16[3184,128]{1,0:T(8,128)(2,1)S(1)}, u32[]{:S(2)}, u32[]{:S(2)}) collective-permute-start(bf16[3184,128]{1,0:T(8,128)(2,1)} %get-tuple-element.24), channel_id=1, source_target_pairs={{0,16},{16,32},{32,48},{48,0},{1,17},{17,33},{33,49},{49,1},{2,18}... | collective-permute-start | bytes 2445320 | tf_op jit(solution)/shard_map/ppermute | solution.py:362
  34.4 24.4 %collective-permute-start = (bf16[3184,128]{1,0:T(8,128)(2,1)}, bf16[3184,128]{1,0:T(8,128)(2,1)S(1)}, u32[]{:S(2)}, u32[]{:S(2)}) collective-permute-start(bf16[3184,128]{1,0:T(8,128)(2,1)} %get-tuple-element.20.refs_1_), channel_id=1, source_target_pairs={{0,48},{16,0},{32,16},{48,32},{1,49},{17,1},{33,17},{49,33},{2,50}... | collective-permute-start | bytes 2445320 | tf_op jit(solution)/shard_map/ppermute | solution.py:362
  38.7 7.4 %copy-start.1 = (bf16[1136,128]{1,0:T(8,128)(2,1)S(1)}, bf16[1136,128]{1,0:T(8,128)(2,1)}, u32[]{:S(2)}) copy-start(bf16[1136,128]{1,0:T(8,128)(2,1)} %get-tuple-element.22) | copy-start | bytes 872452
  39.4 19.3 %all-to-all-start.2 = ((bf16[8,96,128]{2,1,0:T(8,128)(2,1)}), bf16[8,96,128]{2,1,0:T(8,128)(2,1)S(1)}, u32[]{:S(2)}, u32[]{:S(2)}) async-start(bf16[8,96,128]{2,1,0:T(8,128)(2,1)} %broadcast_in_dim.6), calls=%async_computation.2 | async-start | bytes 393216 | tf_op jit(solution)/shard_map/all_to_all | solution.py:19
  46.1 12.7 %collective-permute-start.1 = (bf16[1136,128]{1,0:T(8,128)(2,1)S(1)}, bf16[1136,128]{1,0:T(8,128)(2,1)S(1)}, u32[]{:S(2)}, u32[]{:S(2)}) collective-permute-start(bf16[1136,128]{1,0:T(8,128)(2,1)S(1)} %copy-done.1), channel_id=1, source_target_pairs={{0,32},{16,48},{32,0},{48,16},{1,33},{17,49},{33,1},{49,17},{2,34}... | collective-permute-start | bytes 872456 | tf_op jit(solution)/shard_map/ppermute | solution.py:362
  48.0 48.1 %collective-permute-start.3 = (bf16[2048,128]{1,0:T(8,128)(2,1)S(1)}, bf16[2048,128]{1,0:T(8,128)(2,1)S(1)}, u32[]{:S(2)}, u32[]{:S(2)}) collective-permute-start(bf16[2048,128]{1,0:T(8,128)(2,1)S(1)} %copy-done), channel_id=1, source_target_pairs={{0,32},{16,48},{32,0},{48,16},{1,33},{17,49},{33,1},{49,17},{2,34}... | collective-permute-start | bytes 1572872 | tf_op jit(solution)/shard_map/ppermute | solution.py:362
  92.7 11.8 %all-to-all-start.4 = ((bf16[16,24,128]{2,1,0:T(8,128)(2,1)}), bf16[16,24,128]{2,1,0:T(8,128)(2,1)S(1)}, u32[]{:S(2)}, u32[]{:S(2)}) async-start(bf16[16,24,128]{2,1,0:T(8,128)(2,1)} %broadcast_in_dim.7), calls=%async_computation.4 | async-start | bytes 196608 | tf_op jit(solution)/shard_map/all_to_all | solution.py:19

commit v8 on v7

--- a/solution.py
+++ b/solution.py
@@ -46,7 +46,7 @@
 
 def up_kernel(tokens_ref, gain_ref, weight_ref, scale_ref, out_ref, *scratch):
     tokens, gain, weight, scale, out, in_sems, weight_sems, out_sems = scratch
-    parts, _, step = weight.shape
+    parts, feats, step = weight.shape
     small = [
         pltpu.make_async_copy(tokens_ref, tokens, in_sems.at[0]),
         pltpu.make_async_copy(gain_ref, gain, in_sems.at[1]),
@@ -66,10 +66,12 @@
     for i in range(parts):
         copies[i].wait()
         part = jnp.dot(scaled, weight[i].astype(bf16), preferred_element_type=f32)
-        out[i] = (part * scale[0:1, i * step : (i + 1) * step]).astype(bf16)
-        there = out_ref.at[:, pl.ds(i * step, step)]
-        sent.append(pltpu.make_async_copy(out.at[i], there, out_sems.at[i]))
-        sent[-1].start()
+        part = (part * scale[0:1, i * step : (i + 1) * step]).astype(bf16)
+        for c in range(step // feats):
+            z = i * (step // feats) + c
+            out[z] = part[:, c * feats : (c + 1) * feats]
+            sent.append(pltpu.make_async_copy(out.at[z], out_ref.at[z], out_sems.at[z]))
+            sent[-1].start()
     for copy in sent:
         copy.wait()
 
@@ -80,7 +82,7 @@
     parts = 4
     return pl.pallas_call(
         up_kernel,
-        out_shape=jax.ShapeDtypeStruct((n_tok, hid), bf16),
+        out_shape=jax.ShapeDtypeStruct((Z, n_tok, hid // Z), bf16),
         in_specs=[ANY] * 4,
         out_specs=ANY,
         scratch_shapes=[
@@ -88,10 +90,10 @@
             pltpu.VMEM(gain.shape, f32),
             pltpu.VMEM((parts, feats, hid // parts), f32),
             pltpu.VMEM(scale.shape, f32),
-            pltpu.VMEM((parts, n_tok, hid // parts), bf16),
+            pltpu.VMEM((Z, n_tok, hid // Z), bf16),
             pltpu.SemaphoreType.DMA((3,)),
             pltpu.SemaphoreType.DMA((parts,)),
-            pltpu.SemaphoreType.DMA((parts,)),
+            pltpu.SemaphoreType.DMA((Z,)),
         ],
         compiler_params=limit(12),
         name="up_product",
@@ -101,6 +103,7 @@
 def pack_kernel(down_ref, up_ref, tokens_ref, scale_ref, pre_ref, post_ref, *outs):
     one, two, three, late, own = outs
     hid, feats = down_ref.shape[1:]
+    n = hid // feats
     t_x = own.shape[0] - 16
     x = lax.axis_index("x")
     scale, pre, post = scale_ref[...], pre_ref[...], post_ref[...]
@@ -108,72 +111,79 @@
     columns = jnp.concatenate(columns, axis=0)
     high = columns.astype(bf16).astype(f32)
     columns = jnp.concatenate([high, columns - high], axis=0).astype(bf16)
+    rest = jnp.zeros((feats - 16 - t_x, feats), bf16)
     for s, ref in ((0, own), (1, one), (2, two), (3, three)):
-        at = 0 if s == 0 else hid
+        rows = pl.multiple_of(lax.rem(x + (X - s), X) * t_x, 32)
+        block = [columns, tokens_ref[pl.ds(rows, t_x)]]
         if s:
-            ref[:hid] = down_ref[0].astype(bf16)
-        ref[at : at + 16] = columns
-        rows = pl.multiple_of(lax.rem(x + (X - s), X) * t_x, 32)
-        ref[at + 16 : at + 16 + t_x] = tokens_ref[pl.ds(rows, t_x)]
-    for ref, at in ((one, hid + 16 + t_x), (three, hid + 16 + t_x), (late, 0)):
-        for c in range(hid // feats):
-            block = up_ref[0, :, c * feats : (c + 1) * feats].astype(bf16)
-            ref[at + c * feats : at + (c + 1) * feats] = block
-        ref[at + hid : at + 2 * hid] = down_ref[1].astype(bf16)
+            ref[:n] = down_ref[0].astype(bf16).reshape(n, feats, feats)
+            ref[n] = jnp.concatenate([*block, rest], axis=0)
+        else:
+            ref[...] = jnp.concatenate(block, axis=0)
+    for ref, at in ((one, n + 1), (three, n + 1), (late, 0)):
+        for c in range(n):
+            ref[at + c] = up_ref[0, :, c * feats : (c + 1) * feats].astype(bf16)
+        ref[at + n : at + 2 * n] = down_ref[1].astype(bf16).reshape(n, feats, feats)
 
 
 def packed(down_weight, up_weight, tokens, scale, pre, post):
     _, hid, feats = down_weight.shape
     t_x = tokens.shape[0] // X
-    near_rows, far_rows = hid + 16 + t_x, 2 * hid
+    n = hid // feats
     whole = lambda v: pl.BlockSpec(v.shape, lambda i: (0,) * v.ndim)
-    rows = (near_rows + far_rows, near_rows, near_rows + far_rows, far_rows, 16 + t_x)
+    blocks = (3 * n + 1, n + 1, 3 * n + 1, 2 * n)
     return pl.pallas_call(
         pack_kernel,
         grid=(1,),
         out_shape=(
-            *(pltpu.HBM((r, feats), bf16) for r in rows[:-1]),
-            pltpu.VMEM((rows[-1], feats), bf16),
+            *(pltpu.HBM((b, feats, feats), bf16) for b in blocks),
+            pltpu.VMEM((16 + t_x, feats), bf16),
         ),
         in_specs=[
             whole(down_weight),
             pl.BlockSpec((1, feats, hid), lambda i: (1, 0, 0)),
             *[whole(v) for v in (tokens, scale, pre, post)],
         ],
-        out_specs=tuple(pl.BlockSpec((r, feats), lambda i: (0, 0)) for r in rows),
+        out_specs=(
+            *(pl.BlockSpec((b, feats, feats), lambda i: (0, 0, 0)) for b in blocks),
+            pl.BlockSpec((16 + t_x, feats), lambda i: (0, 0)),
+        ),
         compiler_params=limit(20),
         name="packed",
     )(*[far(v) for v in (down_weight, up_weight, tokens, scale, pre, post)])
 
 
-def down_kernel(starts, hidden_ref, *refs):
+def down_kernel(starts, lead_ref, hidden_ref, *refs):
     weights, out_ref, held, sems = refs[:X], refs[X], refs[X + 1], refs[X + 2]
     copies = []
     for i, w in enumerate(weights):
-        rows = w.at[pl.ds(starts[i], held.shape[1])]
-        copies.append(pltpu.make_async_copy(rows, held.at[i], sems.at[i]))
+        blocks = w.at[pl.ds(starts[i], held.shape[1])]
+        copies.append(pltpu.make_async_copy(blocks, held.at[i], sems.at[i]))
         copies[-1].start()
-    hidden = jnp.concatenate([hidden_ref[z] for z in range(Z)], axis=1)
-    for i in range(X):
+    hidden = [lead_ref[...].astype(bf16), *(hidden_ref[z] for z in range(1, Z))]
+    hidden = jnp.concatenate(hidden, axis=1)
+    for i in (1, 2, 3, 0):
         copies[i].wait()
-        out_ref[i] = jnp.dot(hidden, held[i], preferred_element_type=f32).astype(bf16)
+        weight = held[i].reshape(hidden.shape[1], -1)
+        out_ref[i] = jnp.dot(hidden, weight, preferred_element_type=f32).astype(bf16)
 
 
 def down_product(hidden, blocks, starts):
     _, t, share = hidden.shape
-    feats = blocks[0].shape[1]
+    feats = blocks[0].shape[2]
+    lead = hidden[0].astype(f32)
     return pl.pallas_call(
         lambda *refs: down_kernel(starts, *refs),
         out_shape=pltpu.VMEM((X, t, feats), bf16),
-        in_specs=[VMEM, *[ANY] * X],
+        in_specs=[*[VMEM] * 2, *[ANY] * X],
         out_specs=VMEM,
         scratch_shapes=[
-            pltpu.VMEM((X, Z * share, feats), bf16),
+            pltpu.VMEM((X, Z * share // feats, feats, feats), bf16),
             pltpu.SemaphoreType.DMA((X,)),
         ],
         compiler_params=limit(8),
         name="down_product",
-    )(near(hidden), *blocks)
+    )(near(lead), near(hidden), *blocks)
 
 
 def down_share(hidden, blocks, starts):
@@ -212,16 +222,15 @@
     copies = [pltpu.make_async_copy(scale_ref, scales, sems.at[X - 1])]
     copies[0].start()
     for i, block in enumerate(firsts):
-        rows = block.at[pl.ds(firsts_at[i], extra.shape[1])]
+        rows = block.at[firsts_at, pl.ds(0, extra.shape[1])]
         copies.append(pltpu.make_async_copy(rows, extra.at[i], sems.at[i]))
         copies[-1].start()
     held_copies = []
     for i, block in enumerate(seconds):
-        for c in range(Z):
-            rows = block.at[pl.ds(seconds_at[i] + c * feats, feats)]
-            here = held.at[c, pl.ds(i * feats, feats)]
-            held_copies.append(pltpu.make_async_copy(rows, here, held_sems.at[i, c]))
-            held_copies[-1].start()
+        here = held.at[:, pl.ds(i * feats, feats)]
+        blocks = block.at[pl.ds(seconds_at[i], Z)]
+        held_copies.append(pltpu.make_async_copy(blocks, here, held_sems.at[i]))
+        held_copies[-1].start()
     for copy in copies:
         copy.wait()
     kept_terms, branch_terms, branches = [], [], []
@@ -273,7 +282,7 @@
             pltpu.VMEM((Z, X * feats, feats), bf16),
             pltpu.VMEM(scale.shape, f32),
             pltpu.SemaphoreType.DMA((X,)),
-            pltpu.SemaphoreType.DMA((X, Z)),
+            pltpu.SemaphoreType.DMA((X,)),
         ],
         compiler_params=limit(12),
         name="turn",
@@ -355,8 +364,8 @@
     width = feats * X * Z
     t_x = n_tok // X
 
-    part = up_product(tokens, pre_gain, up_weight, up_scale).reshape(X, t_x, hid)
-    part = exchange(part, "x").astype(f32).sum(axis=0)
+    part = up_product(tokens, pre_gain, up_weight, up_scale).reshape(Z * X, t_x, feats)
+    summed = exchange(part, ("z", "x")).astype(f32).sum(axis=0)
 
     def from_x(payload, s):
         return lax.ppermute(payload, "x", [(i, (i - s) % X) for i in range(X)])
@@ -366,11 +375,9 @@
     )
     firsts = [from_x(one, 1), from_x(two, 2), from_x(three, 3)]
     seconds = [late, firsts[0], from_x(late, 2), firsts[2]]
-    near_rows = hid + 16 + t_x
-    seconds_at = [0, near_rows, 0, near_rows]
-
-    pieces = part.astype(bf16).reshape(t_x, Z, hid // Z).transpose(1, 0, 2)
-    summed = exchange(pieces, "z").astype(f32).sum(axis=0)
+    n = hid // feats
+    seconds_at = [0, n + 1, 0, n + 1]
+
     hidden = to_all(activation(summed), "z")
     firsts = after(firsts, hidden)
     mine = down_share(hidden, [far(one), *firsts], [0] * X)
@@ -378,12 +385,12 @@
 
     seconds = [far(seconds[0]), firsts[0], *after(seconds[2:3], summed), firsts[2]]
     part, kept, branch, columns = turn(
-        summed, own, up_scale, firsts, [hid] * (X - 1), seconds, seconds_at
+        summed, own, up_scale, firsts, n, seconds, seconds_at
     )
     came = exchange(part, "z")
     hidden, stream = second_hidden(came, kept, branch, width)
     hidden = exchange(hidden, "z")
-    mine = down_share(hidden, seconds, [at + hid for at in seconds_at])
+    mine = down_share(hidden, seconds, [at + n for at in seconds_at])
     summed = down_whole(mine)
 
     squares = squares_of(summed, columns)

time: 188 us -> 168 us (0.89)
  blocking collectives: 120 us -> 94.1 us
  waiting for transfers between devices: 14.2 us -> 24.9 us
  starting transfers between devices: 36.6 us -> 34.7 us
    all_to_all x8 -> x7, blocking collectives: 120 us -> 94.1 us  [exchange(): return lax.all_to_all(pieces, axis, split_axis=0, concat_axis=0, tiled=True)]
    all_to_all x3, waiting for transfers between devices: 8.34 us -> 19.8 us  [exchange(): return lax.all_to_all(pieces, axis, split_axis=0, concat_axis=0, tiled=True)]
    all_to_all x3, starting transfers between devices: 23.2 us -> 21.3 us  [exchange(): return lax.all_to_all(pieces, axis, split_axis=0, concat_axis=0, tiled=True)]
  transfers between devices with their start and end apart: 7 -> 7, of which waited for: 2 -> 3; matrix products, arithmetic and copies ran while one was open for 1% -> 1% of each run, Pallas kernels for 3% -> 2%
where the time goes in v8:
time: 168 us; the launch traced here: 167 us
  blocking collectives  94.1 us (56%)
  starting transfers between devices  34.7 us (21%)
  waiting for transfers between devices  24.9 us (15%)
  Pallas kernels  11 us (7%)
  local copies, waits for them, and re-layouts  2.01 us (1%)
    all_to_all x7, blocking collectives, exchange(): return lax.all_to_all(pieces, axis, split_axis=0, concat_axis=0, tiled=True)  94.1 us
    all_to_all x3, starting transfers between devices, exchange(): return lax.all_to_all(pieces, axis, split_axis=0, concat_axis=0, tiled=True)  21.3 us
    all_to_all x3, waiting for transfers between devices, exchange(): return lax.all_to_all(pieces, axis, split_axis=0, concat_axis=0, tiled=True)  19.8 us
    ppermute x4, starting transfers between devices, from_x(): return lax.ppermute(payload, 'x', [(i, (i - s) % X) for i in range(X)])  13.4 us
    ppermute x4, waiting for transfers between devices, from_x(): return lax.ppermute(payload, 'x', [(i, (i - s) % X) for i in range(X)])  5.05 us
  transfers between devices with their start and end apart: 7, of which 3 were waited for; matrix products, arithmetic and copies ran while one was open for 1% of the time, Pallas kernels for 2%

profile of v8, /device:TPU:1, one launch (start us, length us, event | category | flops | bytes accessed | tf_op | source)
XLA Modules:
  0.0 167.1 jit_solution(12999227415067086038)
XLA Ops:
  0.0 2.8 %up_product.1 = bf16[8,384,128]{2,1,0:T(8,128)(2,1)} custom-call(bf16[384,128]{1,0:T(8,128)(2,1)} %tokens_ref.3, f32[2,128]{1,0:T(2,128)} %pre_ref.1, f32[2,128,1024]{2,1,0:T(8,128)} %up_ref.1, f32[2,1024]{1,0:T(2,128)} %refs_3_.1), custom_call_target="tpu_custom_call" | custom-call | tf_op jit(solution)/shard_map/up_product/pallas_call | solution.py:83
  2.8 13.7 %all-to-all-start = ((bf16[32,96,128]{2,1,0:T(8,128)(2,1)}), bf16[32,96,128]{2,1,0:T(8,128)(2,1)S(1)}, u32[]{:S(2)}, u32[]{:S(2)}) async-start(bf16[32,96,128]{2,1,0:T(8,128)(2,1)} %bitcast), calls=%async_computation | async-start | bytes 1572864 | tf_op jit(solution)/shard_map/all_to_all | solution.py:19
  16.5 2.9 %packed.1 = (bf16[25,128,128]{2,1,0:T(8,128)(2,1)}, bf16[9,128,128]{2,1,0:T(8,128)(2,1)}, bf16[25,128,128]{2,1,0:T(8,128)(2,1)}, bf16[16,128,128]{2,1,0:T(8,128)(2,1)}, bf16[112,128]{1,0:T(8,128)(2,1)S(1)}) custom-call(f32[2,1024,128]{2,1,0:T(8,128)} %down_ref.1, f32[2,128,1024]{2,1,0:T(8,128)} %up_ref.1, bf16[384,128]{1,0:T(8,128)(2,1)} %tokens_ref.3, ...), custom_call_target="tpu_custom_call" | custom-call | tf_op jit(solution)/shard_map/packed/pallas_call | solution.py:135
  19.4 0.0 copy-start.1
  19.4 0.0 copy-start
  19.4 3.3 %collective-permute-start.2 = (bf16[25,128,128]{2,1,0:T(8,128)(2,1)}, bf16[25,128,128]{2,1,0:T(8,128)(2,1)S(1)}, u32[]{:S(2)}, u32[]{:S(2)}) collective-permute-start(bf16[25,128,128]{2,1,0:T(8,128)(2,1)} %get-tuple-element.24), channel_id=1, source_target_pairs={{0,16},{16,32},{32,48},{48,0},{1,17},{17,33},{33,49},{49,1},{2,18}... | collective-permute-start | bytes 2457608 | tf_op jit(solution)/shard_map/ppermute | solution.py:371
  22.7 3.4 %collective-permute-start = (bf16[25,128,128]{2,1,0:T(8,128)(2,1)}, bf16[25,128,128]{2,1,0:T(8,128)(2,1)S(1)}, u32[]{:S(2)}, u32[]{:S(2)}) collective-permute-start(bf16[25,128,128]{2,1,0:T(8,128)(2,1)} %get-tuple-element.20.refs_2_), channel_id=1, source_target_pairs={{0,48},{16,0},{32,16},{48,32},{1,49},{17,1},{33,17},{49,33},{2,50}... | collective-permute-start | bytes 2457608 | tf_op jit(solution)/shard_map/ppermute | solution.py:371
  26.0 11.5 %all-to-all-done = bf16[32,96,128]{2,1,0:T(8,128)(2,1)S(1)} async-done(((bf16[32,96,128]{2,1,0:T(8,128)(2,1)}), bf16[32,96,128]{2,1,0:T(8,128)(2,1)S(1)}, u32[]{:S(2)}, u32[]{:S(2)}) %all-to-all-start) | async-done | bytes 786464 | tf_op jit(solution)/shard_map/all_to_all | solution.py:19
  37.6 0.1 convert_reduce_fusion
  37.7 0.7 broadcast_in_dim.6
  38.4 4.1 %all-to-all-start.1 = ((bf16[8,96,128]{2,1,0:T(8,128)(2,1)}), bf16[8,96,128]{2,1,0:T(8,128)(2,1)S(1)}, u32[]{:S(2)}, u32[]{:S(2)}) async-start(bf16[8,96,128]{2,1,0:T(8,128)(2,1)} %broadcast_in_dim.6), calls=%async_computation.1 | async-start | bytes 393216 | tf_op jit(solution)/shard_map/all_to_all | solution.py:19
  42.5 0.0 copy-done.1
  42.5 4.0 %collective-permute-start.1 = (bf16[9,128,128]{2,1,0:T(8,128)(2,1)S(1)}, bf16[9,128,128]{2,1,0:T(8,128)(2,1)S(1)}, u32[]{:S(2)}, u32[]{:S(2)}) collective-permute-start(bf16[9,128,128]{2,1,0:T(8,128)(2,1)S(1)} %copy-done.1), channel_id=1, source_target_pairs={{0,32},{16,48},{32,0},{48,16},{1,33},{17,49},{33,1},{49,17},{2,34}... | collective-permute-start | bytes 884744 | tf_op jit(solution)/shard_map/ppermute | solution.py:371
  46.5 0.0 copy-done
  46.5 2.8 %collective-permute-start.3 = (bf16[16,128,128]{2,1,0:T(8,128)(2,1)S(1)}, bf16[16,128,128]{2,1,0:T(8,128)(2,1)S(1)}, u32[]{:S(2)}, u32[]{:S(2)}) collective-permute-start(bf16[16,128,128]{2,1,0:T(8,128)(2,1)S(1)} %copy-done), channel_id=1, source_target_pairs={{0,32},{16,48},{32,0},{48,16},{1,33},{17,49},{33,1},{49,17},{2,34}... | collective-permute-start | bytes 1572872 | tf_op jit(solution)/shard_map/ppermute | solution.py:371
  49.3 5.0 %collective-permute-done.1.refs_4_.refs_5_ = bf16[9,128,128]{2,1,0:T(8,128)(2,1)S(1)} collective-permute-done((bf16[9,128,128]{2,1,0:T(8,128)(2,1)S(1)}, bf16[9,128,128]{2,1,0:T(8,128)(2,1)S(1)}, u32[]{:S(2)}, u32[]{:S(2)}) %collective-permute-start.1) | collective-permute-done | bytes 294944 | tf_op jit(solution)/shard_map/ppermute | solution.py:371
  54.4 0.0 all-to-all-done.1.refs_1_
  54.4 0.0 collective-permute-done.2.refs_5_.refs_6_.refs_10_
  54.4 0.0 collective-permute-done.refs_3_.refs_4_.refs_8_
  54.4 1.2 down_product.2
  55.6 19.0 %all_to_all.50 = bf16[16,24,128]{2,1,0:T(8,128)(2,1)S(1)} all-to-all(bf16[16,24,128]{2,1,0:T(8,128)(2,1)S(1)} %bitcast.23), channel_id=1, replica_groups=mesh['z'=8,'x'=4,'y'=8,'core'=2] {'y','core'}, dimensions={0} | all-to-all | bytes 196608 | tf_op jit(solution)/shard_map/all_to_all | solution.py:19
  74.7 0.7 broadcast_in_dim.7
  75.3 3.4 %all-to-all-start.3 = ((bf16[16,24,128]{2,1,0:T(8,128)(2,1)}), bf16[16,24,128]{2,1,0:T(8,128)(2,1)S(1)}, u32[]{:S(2)}, u32[]{:S(2)}) async-start(bf16[16,24,128]{2,1,0:T(8,128)(2,1)} %broadcast_in_dim.7), calls=%async_computation.3 | async-start | bytes 196608 | tf_op jit(solution)/shard_map/all_to_all | solution.py:19
  78.7 0.0 collective-permute-done.3.refs_9_.refs_4_
  78.8 8.3 %all-to-all-done.3 = bf16[16,24,128]{2,1,0:T(8,128)(2,1)S(1)} async-done(((bf16[16,24,128]{2,1,0:T(8,128)(2,1)}), bf16[16,24,128]{2,1,0:T(8,128)(2,1)S(1)}, u32[]{:S(2)}, u32[]{:S(2)}) %all-to-all-start.3) | async-done | bytes 98336 | tf_op jit(solution)/shard_map/all_to_all | solution.py:19
  87.1 2.4 %turn.1 = (bf16[8,200,128]{2,1,0:T(8,128)(2,1)S(1)}, f32[4,96,128]{2,1,0:T(8,128)S(1)}, f32[4,96,128]{2,1,0:T(8,128)S(1)}, f32[4,8,128]{2,1,0:T(8,128)S(1)}) custom-call(f32[96,128]{1,0:T(8,128)S(1)} %bitcast_convert_fusion.refs_0_, bf16[4,96,128]{2,1,0:T(8,128)(2,1)S(1)} %bitcast.21, bf16[112,128]{1,0:T(8,128)(2,1)S(1)} %get-tuple-element.26.refs_2_, ...), custom_call_target="tpu_custom_call" | custom-call | tf_op jit(solution)/shard_map/turn/pallas_call | solution.py:270
  89.5 21.6 %all_to_all.51.refs_0_ = bf16[8,200,128]{2,1,0:T(8,128)(2,1)S(1)} all-to-all(bf16[8,200,128]{2,1,0:T(8,128)(2,1)S(1)} %get-tuple-element.29), channel_id=1, replica_groups=mesh['z'=8,'x'=4,'y'=8,'core'=2] {'z'}, dimensions={0} | all-to-all | bytes 819200 | tf_op jit(solution)/shard_map/all_to_all | solution.py:19
  111.1 0.1 second_hidden.1
  111.3 12.1 %all_to_all.52.refs_1_ = bf16[8,96,128]{2,1,0:T(8,128)(2,1)S(1)} all-to-all(bf16[8,96,128]{2,1,0:T(8,128)(2,1)S(1)} %get-tuple-element.32), channel_id=1, replica_groups=mesh['z'=8,'x'=4,'y'=8,'core'=2] {'z'}, dimensions={0} | all-to-all | bytes 393216 | tf_op jit(solution)/shard_map/all_to_all | solution.py:19
  123.4 1.2 down_product.3
  124.5 12.6 %all_to_all.53 = bf16[16,24,128]{2,1,0:T(8,128)(2,1)S(1)} all-to-all(bf16[16,24,128]{2,1,0:T(8,128)(2,1)S(1)} %bitcast.22), channel_id=1, replica_groups=mesh['z'=8,'x'=4,'y'=8,'core'=2] {'y','core'}, dimensions={0} | all-to-all | bytes 196608 | tf_op jit(solution)/shard_map/all_to_all | solution.py:19
  137.2 10.9 %all_to_all.54 = bf16[16,24,128]{2,1,0:T(8,128)(2,1)S(1)} all-to-all(bf16[16,24,128]{2,1,0:T(8,128)(2,1)S(1)} %broadcast_in_dim.8), channel_id=1, replica_groups=mesh['z'=8,'x'=4,'y'=8,'core'=2] {'y','core'}, dimensions={0} | all-to-all | bytes 196608 | tf_op jit(solution)/shard_map/all_to_all | solution.py:19
  148.1 0.4 squares.1
  148.5 9.3 %all_to_all.55.refs_0_ = f32[8,8,128]{2,1,0:T(8,128)S(1)} all-to-all(f32[8,8,128]{2,1,0:T(8,128)S(1)} %squares.1), channel_id=1, replica_groups=mesh['z'=8,'x'=4,'y'=8,'core'=2] {'z'}, dimensions={0} | all-to-all | bytes 65536 | tf_op jit(solution)/shard_map/all_to_all | solution.py:19
  157.7 0.1 last.1
  157.8 8.6 %all_to_all.56 = bf16[4,96,128]{2,1,0:T(8,128)(2,1)S(1)} all-to-all(bf16[4,96,128]{2,1,0:T(8,128)(2,1)S(1)} %last.1), channel_id=1, replica_groups=mesh['z'=8,'x'=4,'y'=8,'core'=2] {'x'}, dimensions={0} | all-to-all | bytes 196608 | tf_op jit(solution)/shard_map/all_to_all | solution.py:19
  166.4 0.6 copy.9
  (8 shorter events, 0.1 us)
Async XLA Ops:
  2.8 34.8 %all-to-all-start = ((bf16[32,96,128]{2,1,0:T(8,128)(2,1)}), bf16[32,96,128]{2,1,0:T(8,128)(2,1)S(1)}, u32[]{:S(2)}, u32[]{:S(2)}) async-start(bf16[32,96,128]{2,1,0:T(8,128)(2,1)} %bitcast), calls=%async_computation | async-start | bytes 1572864 | tf_op jit(solution)/shard_map/all_to_all | solution.py:19
  19.4 23.1 %copy-start.1 = (bf16[9,128,128]{2,1,0:T(8,128)(2,1)S(1)}, bf16[9,128,128]{2,1,0:T(8,128)(2,1)}, u32[]{:S(2)}) copy-start(bf16[9,128,128]{2,1,0:T(8,128)(2,1)} %get-tuple-element.22) | copy-start | bytes 884740
  19.4 27.1 %copy-start = (bf16[16,128,128]{2,1,0:T(8,128)(2,1)S(1)}, bf16[16,128,128]{2,1,0:T(8,128)(2,1)}, u32[]{:S(2)}) copy-start(bf16[16,128,128]{2,1,0:T(8,128)(2,1)} %get-tuple-element.27.refs_7_.refs_2_) | copy-start | bytes 1572868
  19.4 35.0 %collective-permute-start.2 = (bf16[25,128,128]{2,1,0:T(8,128)(2,1)}, bf16[25,128,128]{2,1,0:T(8,128)(2,1)S(1)}, u32[]{:S(2)}, u32[]{:S(2)}) collective-permute-start(bf16[25,128,128]{2,1,0:T(8,128)(2,1)} %get-tuple-element.24), channel_id=1, source_target_pairs={{0,16},{16,32},{32,48},{48,0},{1,17},{17,33},{33,49},{49,1},{2,18}... | collective-permute-start | bytes 2457608 | tf_op jit(solution)/shard_map/ppermute | solution.py:371
  22.7 31.7 %collective-permute-start = (bf16[25,128,128]{2,1,0:T(8,128)(2,1)}, bf16[25,128,128]{2,1,0:T(8,128)(2,1)S(1)}, u32[]{:S(2)}, u32[]{:S(2)}) collective-permute-start(bf16[25,128,128]{2,1,0:T(8,128)(2,1)} %get-tuple-element.20.refs_2_), channel_id=1, source_target_pairs={{0,48},{16,0},{32,16},{48,32},{1,49},{17,1},{33,17},{49,33},{2,50}... | collective-permute-start | bytes 2457608 | tf_op jit(solution)/shard_map/ppermute | solution.py:371
  38.4 16.0 %all-to-all-start.1 = ((bf16[8,96,128]{2,1,0:T(8,128)(2,1)}), bf16[8,96,128]{2,1,0:T(8,128)(2,1)S(1)}, u32[]{:S(2)}, u32[]{:S(2)}) async-start(bf16[8,96,128]{2,1,0:T(8,128)(2,1)} %broadcast_in_dim.6), calls=%async_computation.1 | async-start | bytes 393216 | tf_op jit(solution)/shard_map/all_to_all | solution.py:19
  42.5 11.9 %collective-permute-start.1 = (bf16[9,128,128]{2,1,0:T(8,128)(2,1)S(1)}, bf16[9,128,128]{2,1,0:T(8,128)(2,1)S(1)}, u32[]{:S(2)}, u32[]{:S(2)}) collective-permute-start(bf16[9,128,128]{2,1,0:T(8,128)(2,1)S(1)} %copy-done.1), channel_id=1, source_target_pairs={{0,32},{16,48},{32,0},{48,16},{1,33},{17,49},{33,1},{49,17},{2,34}... | collective-permute-start | bytes 884744 | tf_op jit(solution)/shard_map/ppermute | solution.py:371
  46.5 32.2 %collective-permute-start.3 = (bf16[16,128,128]{2,1,0:T(8,128)(2,1)S(1)}, bf16[16,128,128]{2,1,0:T(8,128)(2,1)S(1)}, u32[]{:S(2)}, u32[]{:S(2)}) collective-permute-start(bf16[16,128,128]{2,1,0:T(8,128)(2,1)S(1)} %copy-done), channel_id=1, source_target_pairs={{0,32},{16,48},{32,0},{48,16},{1,33},{17,49},{33,1},{49,17},{2,34}... | collective-permute-start | bytes 1572872 | tf_op jit(solution)/shard_map/ppermute | solution.py:371
  75.3 11.8 %all-to-all-start.3 = ((bf16[16,24,128]{2,1,0:T(8,128)(2,1)}), bf16[16,24,128]{2,1,0:T(8,128)(2,1)S(1)}, u32[]{:S(2)}, u32[]{:S(2)}) async-start(bf16[16,24,128]{2,1,0:T(8,128)(2,1)} %broadcast_in_dim.7), calls=%async_computation.3 | async-start | bytes 196608 | tf_op jit(solution)/shard_map/all_to_all | solution.py:19

commit v9 on v8

--- a/solution.py
+++ b/solution.py
@@ -120,10 +120,9 @@
             ref[n] = jnp.concatenate([*block, rest], axis=0)
         else:
             ref[...] = jnp.concatenate(block, axis=0)
-    for ref, at in ((one, n + 1), (three, n + 1), (late, 0)):
-        for c in range(n):
-            ref[at + c] = up_ref[0, :, c * feats : (c + 1) * feats].astype(bf16)
-        ref[at + n : at + 2 * n] = down_ref[1].astype(bf16).reshape(n, feats, feats)
+    for c in range(n):
+        late[c] = up_ref[0, :, c * feats : (c + 1) * feats].astype(bf16)
+    late[n:] = down_ref[1].astype(bf16).reshape(n, feats, feats)
 
 
 def packed(down_weight, up_weight, tokens, scale, pre, post):
@@ -131,7 +130,7 @@
     t_x = tokens.shape[0] // X
     n = hid // feats
     whole = lambda v: pl.BlockSpec(v.shape, lambda i: (0,) * v.ndim)
-    blocks = (3 * n + 1, n + 1, 3 * n + 1, 2 * n)
+    blocks = (n + 1, n + 1, n + 1, 2 * n)
     return pl.pallas_call(
         pack_kernel,
         grid=(1,),
@@ -374,23 +373,22 @@
         down_weight, up_weight, tokens, down_scale, pre_gain, post_gain
     )
     firsts = [from_x(one, 1), from_x(two, 2), from_x(three, 3)]
-    seconds = [late, firsts[0], from_x(late, 2), firsts[2]]
+    seconds = [from_x(late, s) for s in (1, 2, 3)]
     n = hid // feats
-    seconds_at = [0, n + 1, 0, n + 1]
 
     hidden = to_all(activation(summed), "z")
     firsts = after(firsts, hidden)
     mine = down_share(hidden, [far(one), *firsts], [0] * X)
     summed = down_whole(mine)
 
-    seconds = [far(seconds[0]), firsts[0], *after(seconds[2:3], summed), firsts[2]]
+    seconds = [far(late), *after(seconds, summed)]
     part, kept, branch, columns = turn(
-        summed, own, up_scale, firsts, n, seconds, seconds_at
+        summed, own, up_scale, firsts, n, seconds, [0] * X
     )
     came = exchange(part, "z")
     hidden, stream = second_hidden(came, kept, branch, width)
     hidden = exchange(hidden, "z")
-    mine = down_share(hidden, seconds, [at + n for at in seconds_at])
+    mine = down_share(hidden, seconds, [n] * X)
     summed = down_whole(mine)
 
     squares = squares_of(summed, columns)

time: 168 us -> 187 us (1.11)
  starting transfers between devices: 34.7 us -> 52.2 us
  blocking collectives: 94.1 us -> 109 us
  waiting for transfers between devices: 24.9 us -> 10.1 us
    ppermute x4 -> x6, starting transfers between devices: 13.4 us -> 29.8 us  [from_x(): return lax.ppermute(payload, 'x', [(i, (i - s) % X) for i in range(X)])]
    all_to_all x7, blocking collectives: 94.1 us -> 109 us  [exchange(): return lax.all_to_all(pieces, axis, split_axis=0, concat_axis=0, tiled=True)]
    all_to_all x3, waiting for transfers between devices: 19.8 us -> 8.45 us  [exchange(): return lax.all_to_all(pieces, axis, split_axis=0, concat_axis=0, tiled=True)]
    ppermute x4 -> x6, waiting for transfers between devices: 5.05 us -> 1.68 us  [from_x(): return lax.ppermute(payload, 'x', [(i, (i - s) % X) for i in range(X)])]
  transfers between devices with their start and end apart: 7 -> 9, of which waited for: 3 -> 2; matrix products, arithmetic and copies ran while one was open for 1% -> 0% of each run, Pallas kernels for 2% -> 2%
where the time goes in v9:
time: 187 us; the launch traced here: 186 us
  blocking collectives  109 us (58%)
  starting transfers between devices  52.2 us (28%)
  Pallas kernels  11.6 us (6%)
  waiting for transfers between devices  10.1 us (5%)
  local copies, waits for them, and re-layouts  2.01 us (1%)
    all_to_all x7, blocking collectives, exchange(): return lax.all_to_all(pieces, axis, split_axis=0, concat_axis=0, tiled=True)  109 us
    ppermute x6, starting transfers between devices, from_x(): return lax.ppermute(payload, 'x', [(i, (i - s) % X) for i in range(X)])  29.8 us
    all_to_all x3, starting transfers between devices, exchange(): return lax.all_to_all(pieces, axis, split_axis=0, concat_axis=0, tiled=True)  22.4 us
    all_to_all x3, waiting for transfers between devices, exchange(): return lax.all_to_all(pieces, axis, split_axis=0, concat_axis=0, tiled=True)  8.45 us
  transfers between devices with their start and end apart: 9, of which 2 were waited for; matrix products, arithmetic and copies ran while one was open for 0% of the time, Pallas kernels for 2%

profile of v9, /device:TPU:1, one launch (start us, length us, event | category | flops | bytes accessed | tf_op | source)
XLA Modules:
  0.0 185.8 jit_solution(2697596850705070796)
XLA Ops:
  0.0 3.1 %up_product.1 = bf16[8,384,128]{2,1,0:T(8,128)(2,1)S(1)} custom-call(bf16[384,128]{1,0:T(8,128)(2,1)} %tokens_ref.3, f32[2,128]{1,0:T(2,128)} %pre_ref.1, f32[2,128,1024]{2,1,0:T(8,128)} %up_ref.1, f32[2,1024]{1,0:T(2,128)} %refs_3_.1), custom_call_target="tpu_custom_call" | custom-call | tf_op jit(solution)/shard_map/up_product/pallas_call | solution.py:83
  3.1 34.6 %all_to_all.50 = bf16[32,96,128]{2,1,0:T(8,128)(2,1)S(1)} all-to-all(bf16[32,96,128]{2,1,0:T(8,128)(2,1)S(1)} %bitcast.19), channel_id=1, replica_groups=mesh['z'=8,'x'=4,'y'=8,'core'=2] {'z','x'}, dimensions={0} | all-to-all | bytes 1572864 | tf_op jit(solution)/shard_map/all_to_all | solution.py:19
  37.7 0.1 convert_reduce_fusion
  37.8 0.7 broadcast_in_dim.6
  38.5 4.1 %all-to-all-start.1 = ((bf16[8,96,128]{2,1,0:T(8,128)(2,1)}), bf16[8,96,128]{2,1,0:T(8,128)(2,1)S(1)}, u32[]{:S(2)}, u32[]{:S(2)}) async-start(bf16[8,96,128]{2,1,0:T(8,128)(2,1)} %broadcast_in_dim.6), calls=%async_computation.1 | async-start | bytes 393216 | tf_op jit(solution)/shard_map/all_to_all | solution.py:19
  42.6 2.6 %packed.1 = (bf16[9,128,128]{2,1,0:T(8,128)(2,1)}, bf16[9,128,128]{2,1,0:T(8,128)(2,1)}, bf16[9,128,128]{2,1,0:T(8,128)(2,1)}, bf16[16,128,128]{2,1,0:T(8,128)(2,1)}, bf16[112,128]{1,0:T(8,128)(2,1)S(1)}) custom-call(f32[2,1024,128]{2,1,0:T(8,128)} %down_ref.1, f32[2,128,1024]{2,1,0:T(8,128)} %up_ref.1, bf16[384,128]{1,0:T(8,128)(2,1)} %tokens_ref.3, ...), custom_call_target="tpu_custom_call" | custom-call | tf_op jit(solution)/shard_map/packed/pallas_call | solution.py:134
  45.2 0.0 copy-start
  45.2 4.1 %collective-permute-start.1 = (bf16[9,128,128]{2,1,0:T(8,128)(2,1)}, bf16[9,128,128]{2,1,0:T(8,128)(2,1)S(1)}, u32[]{:S(2)}, u32[]{:S(2)}) collective-permute-start(bf16[9,128,128]{2,1,0:T(8,128)(2,1)} %get-tuple-element.24), channel_id=1, source_target_pairs={{0,32},{16,48},{32,0},{48,16},{1,33},{17,49},{33,1},{49,17},{2,34}... | collective-permute-start | bytes 884744 | tf_op jit(solution)/shard_map/ppermute | solution.py:370
  49.3 2.5 %collective-permute-start.2 = (bf16[9,128,128]{2,1,0:T(8,128)(2,1)}, bf16[9,128,128]{2,1,0:T(8,128)(2,1)S(1)}, u32[]{:S(2)}, u32[]{:S(2)}) collective-permute-start(bf16[9,128,128]{2,1,0:T(8,128)(2,1)} %get-tuple-element.26), channel_id=1, source_target_pairs={{0,16},{16,32},{32,48},{48,0},{1,17},{17,33},{33,49},{49,1},{2,18}... | collective-permute-start | bytes 884744 | tf_op jit(solution)/shard_map/ppermute | solution.py:370
  51.9 4.0 %collective-permute-start = (bf16[9,128,128]{2,1,0:T(8,128)(2,1)}, bf16[9,128,128]{2,1,0:T(8,128)(2,1)S(1)}, u32[]{:S(2)}, u32[]{:S(2)}) collective-permute-start(bf16[9,128,128]{2,1,0:T(8,128)(2,1)} %get-tuple-element.22.refs_2_), channel_id=1, source_target_pairs={{0,48},{16,0},{32,16},{48,32},{1,49},{17,1},{33,17},{49,33},{2,50}... | collective-permute-start | bytes 884744 | tf_op jit(solution)/shard_map/ppermute | solution.py:370
  55.8 1.9 %collective-permute-start.5 = (bf16[16,128,128]{2,1,0:T(8,128)(2,1)}, bf16[16,128,128]{2,1,0:T(8,128)(2,1)S(1)}, u32[]{:S(2)}, u32[]{:S(2)}) collective-permute-start(bf16[16,128,128]{2,1,0:T(8,128)(2,1)} %get-tuple-element.29.refs_7_.refs_2_), channel_id=1, source_target_pairs={{0,16},{16,32},{32,48},{48,0},{1,17},{17,33},{33,49},{49,1},{2,18}... | collective-permute-start | bytes 1572872 | tf_op jit(solution)/shard_map/ppermute | solution.py:370
  57.8 3.3 %collective-permute-start.4 = (bf16[16,128,128]{2,1,0:T(8,128)(2,1)}, bf16[16,128,128]{2,1,0:T(8,128)(2,1)S(1)}, u32[]{:S(2)}, u32[]{:S(2)}) collective-permute-start(bf16[16,128,128]{2,1,0:T(8,128)(2,1)} %get-tuple-element.29.refs_7_.refs_2_), channel_id=1, source_target_pairs={{0,32},{16,48},{32,0},{48,16},{1,33},{17,49},{33,1},{49,17},{2,34}... | collective-permute-start | bytes 1572872 | tf_op jit(solution)/shard_map/ppermute | solution.py:370
  61.0 0.0 collective-permute-done.1.refs_4_.refs_5_
  61.0 0.0 all-to-all-done.1.refs_1_
  61.0 1.7 collective-permute-done.2.refs_5_.refs_6_
  62.7 0.0 collective-permute-done.refs_3_.refs_4_
  62.7 1.8 down_product.2
  64.6 10.8 %all-to-all-start.2 = ((bf16[16,24,128]{2,1,0:T(8,128)(2,1)}), bf16[16,24,128]{2,1,0:T(8,128)(2,1)S(1)}, u32[]{:S(2)}, u32[]{:S(2)}) async-start(bf16[16,24,128]{2,1,0:T(8,128)(2,1)} %bitcast.2), calls=%async_computation.2 | async-start | bytes 196608 | tf_op jit(solution)/shard_map/all_to_all | solution.py:19
  75.3 0.0 copy-done
  75.3 14.0 %collective-permute-start.3 = (bf16[16,128,128]{2,1,0:T(8,128)(2,1)S(1)}, bf16[16,128,128]{2,1,0:T(8,128)(2,1)S(1)}, u32[]{:S(2)}, u32[]{:S(2)}) collective-permute-start(bf16[16,128,128]{2,1,0:T(8,128)(2,1)S(1)} %copy-done), channel_id=1, source_target_pairs={{0,48},{16,0},{32,16},{48,32},{1,49},{17,1},{33,17},{49,33},{2,50}... | collective-permute-start | bytes 1572872 | tf_op jit(solution)/shard_map/ppermute | solution.py:370
  89.4 0.0 all-to-all-done.2
  89.4 0.7 broadcast_in_dim.7
  90.1 7.5 %all-to-all-start.3 = ((bf16[16,24,128]{2,1,0:T(8,128)(2,1)}), bf16[16,24,128]{2,1,0:T(8,128)(2,1)S(1)}, u32[]{:S(2)}, u32[]{:S(2)}) async-start(bf16[16,24,128]{2,1,0:T(8,128)(2,1)} %broadcast_in_dim.7), calls=%async_computation.3 | async-start | bytes 196608 | tf_op jit(solution)/shard_map/all_to_all | solution.py:19
  97.6 0.0 collective-permute-done.5.refs_10_.refs_5_
  97.6 8.4 %all-to-all-done.3 = bf16[16,24,128]{2,1,0:T(8,128)(2,1)S(1)} async-done(((bf16[16,24,128]{2,1,0:T(8,128)(2,1)}), bf16[16,24,128]{2,1,0:T(8,128)(2,1)S(1)}, u32[]{:S(2)}, u32[]{:S(2)}) %all-to-all-start.3) | async-done | bytes 98336 | tf_op jit(solution)/shard_map/all_to_all | solution.py:19
  106.0 0.0 collective-permute-done.4.refs_9_.refs_4_
  106.0 0.0 collective-permute-done.3.refs_8_.refs_3_
  106.0 2.4 %turn.1 = (bf16[8,200,128]{2,1,0:T(8,128)(2,1)S(1)}, f32[4,96,128]{2,1,0:T(8,128)S(1)}, f32[4,96,128]{2,1,0:T(8,128)S(1)}, f32[4,8,128]{2,1,0:T(8,128)S(1)}) custom-call(f32[96,128]{1,0:T(8,128)S(1)} %bitcast_convert_fusion.refs_0_, bf16[4,96,128]{2,1,0:T(8,128)(2,1)S(1)} %bitcast.22, bf16[112,128]{1,0:T(8,128)(2,1)S(1)} %get-tuple-element.28.refs_2_, ...), custom_call_target="tpu_custom_call" | custom-call | tf_op jit(solution)/shard_map/turn/pallas_call | solution.py:269
  108.4 22.0 %all_to_all.51.refs_0_ = bf16[8,200,128]{2,1,0:T(8,128)(2,1)S(1)} all-to-all(bf16[8,200,128]{2,1,0:T(8,128)(2,1)S(1)} %get-tuple-element.33), channel_id=1, replica_groups=mesh['z'=8,'x'=4,'y'=8,'core'=2] {'z'}, dimensions={0} | all-to-all | bytes 819200 | tf_op jit(solution)/shard_map/all_to_all | solution.py:19
  130.4 0.1 second_hidden.1
  130.5 12.1 %all_to_all.52.refs_1_ = bf16[8,96,128]{2,1,0:T(8,128)(2,1)S(1)} all-to-all(bf16[8,96,128]{2,1,0:T(8,128)(2,1)S(1)} %get-tuple-element.36), channel_id=1, replica_groups=mesh['z'=8,'x'=4,'y'=8,'core'=2] {'z'}, dimensions={0} | all-to-all | bytes 393216 | tf_op jit(solution)/shard_map/all_to_all | solution.py:19
  142.6 1.2 down_product.3
  143.8 12.6 %all_to_all.53 = bf16[16,24,128]{2,1,0:T(8,128)(2,1)S(1)} all-to-all(bf16[16,24,128]{2,1,0:T(8,128)(2,1)S(1)} %bitcast.23), channel_id=1, replica_groups=mesh['z'=8,'x'=4,'y'=8,'core'=2] {'y','core'}, dimensions={0} | all-to-all | bytes 196608 | tf_op jit(solution)/shard_map/all_to_all | solution.py:19
  156.5 10.9 %all_to_all.54 = bf16[16,24,128]{2,1,0:T(8,128)(2,1)S(1)} all-to-all(bf16[16,24,128]{2,1,0:T(8,128)(2,1)S(1)} %broadcast_in_dim.8), channel_id=1, replica_groups=mesh['z'=8,'x'=4,'y'=8,'core'=2] {'y','core'}, dimensions={0} | all-to-all | bytes 196608 | tf_op jit(solution)/shard_map/all_to_all | solution.py:19
  167.3 0.4 squares.1
  167.7 9.3 %all_to_all.55.refs_0_ = f32[8,8,128]{2,1,0:T(8,128)S(1)} all-to-all(f32[8,8,128]{2,1,0:T(8,128)S(1)} %squares.1), channel_id=1, replica_groups=mesh['z'=8,'x'=4,'y'=8,'core'=2] {'z'}, dimensions={0} | all-to-all | bytes 65536 | tf_op jit(solution)/shard_map/all_to_all | solution.py:19
  177.0 0.1 last.1
  177.1 8.0 %all_to_all.56 = bf16[4,96,128]{2,1,0:T(8,128)(2,1)S(1)} all-to-all(bf16[4,96,128]{2,1,0:T(8,128)(2,1)S(1)} %last.1), channel_id=1, replica_groups=mesh['z'=8,'x'=4,'y'=8,'core'=2] {'x'}, dimensions={0} | all-to-all | bytes 196608 | tf_op jit(solution)/shard_map/all_to_all | solution.py:19
  185.1 0.6 copy.9
  (8 shorter events, 0.1 us)
Async XLA Ops:
  38.5 22.5 %all-to-all-start.1 = ((bf16[8,96,128]{2,1,0:T(8,128)(2,1)}), bf16[8,96,128]{2,1,0:T(8,128)(2,1)S(1)}, u32[]{:S(2)}, u32[]{:S(2)}) async-start(bf16[8,96,128]{2,1,0:T(8,128)(2,1)} %broadcast_in_dim.6), calls=%async_computation.1 | async-start | bytes 393216 | tf_op jit(solution)/shard_map/all_to_all | solution.py:19
  45.2 30.1 %copy-start = (bf16[16,128,128]{2,1,0:T(8,128)(2,1)S(1)}, bf16[16,128,128]{2,1,0:T(8,128)(2,1)}, u32[]{:S(2)}) copy-start(bf16[16,128,128]{2,1,0:T(8,128)(2,1)} %get-tuple-element.29.refs_7_.refs_2_) | copy-start | bytes 1572868
  45.2 15.8 %collective-permute-start.1 = (bf16[9,128,128]{2,1,0:T(8,128)(2,1)}, bf16[9,128,128]{2,1,0:T(8,128)(2,1)S(1)}, u32[]{:S(2)}, u32[]{:S(2)}) collective-permute-start(bf16[9,128,128]{2,1,0:T(8,128)(2,1)} %get-tuple-element.24), channel_id=1, source_target_pairs={{0,32},{16,48},{32,0},{48,16},{1,33},{17,49},{33,1},{49,17},{2,34}... | collective-permute-start | bytes 884744 | tf_op jit(solution)/shard_map/ppermute | solution.py:370
  49.3 13.4 %collective-permute-start.2 = (bf16[9,128,128]{2,1,0:T(8,128)(2,1)}, bf16[9,128,128]{2,1,0:T(8,128)(2,1)S(1)}, u32[]{:S(2)}, u32[]{:S(2)}) collective-permute-start(bf16[9,128,128]{2,1,0:T(8,128)(2,1)} %get-tuple-element.26), channel_id=1, source_target_pairs={{0,16},{16,32},{32,48},{48,0},{1,17},{17,33},{33,49},{49,1},{2,18}... | collective-permute-start | bytes 884744 | tf_op jit(solution)/shard_map/ppermute | solution.py:370
  51.9 10.8 %collective-permute-start = (bf16[9,128,128]{2,1,0:T(8,128)(2,1)}, bf16[9,128,128]{2,1,0:T(8,128)(2,1)S(1)}, u32[]{:S(2)}, u32[]{:S(2)}) collective-permute-start(bf16[9,128,128]{2,1,0:T(8,128)(2,1)} %get-tuple-element.22.refs_2_), channel_id=1, source_target_pairs={{0,48},{16,0},{32,16},{48,32},{1,49},{17,1},{33,17},{49,33},{2,50}... | collective-permute-start | bytes 884744 | tf_op jit(solution)/shard_map/ppermute | solution.py:370
  55.8 41.7 %collective-permute-start.5 = (bf16[16,128,128]{2,1,0:T(8,128)(2,1)}, bf16[16,128,128]{2,1,0:T(8,128)(2,1)S(1)}, u32[]{:S(2)}, u32[]{:S(2)}) collective-permute-start(bf16[16,128,128]{2,1,0:T(8,128)(2,1)} %get-tuple-element.29.refs_7_.refs_2_), channel_id=1, source_target_pairs={{0,16},{16,32},{32,48},{48,0},{1,17},{17,33},{33,49},{49,1},{2,18}... | collective-permute-start | bytes 1572872 | tf_op jit(solution)/shard_map/ppermute | solution.py:370
  57.8 48.3 %collective-permute-start.4 = (bf16[16,128,128]{2,1,0:T(8,128)(2,1)}, bf16[16,128,128]{2,1,0:T(8,128)(2,1)S(1)}, u32[]{:S(2)}, u32[]{:S(2)}) collective-permute-start(bf16[16,128,128]{2,1,0:T(8,128)(2,1)} %get-tuple-element.29.refs_7_.refs_2_), channel_id=1, source_target_pairs={{0,32},{16,48},{32,0},{48,16},{1,33},{17,49},{33,1},{49,17},{2,34}... | collective-permute-start | bytes 1572872 | tf_op jit(solution)/shard_map/ppermute | solution.py:370
  64.6 24.8 %all-to-all-start.2 = ((bf16[16,24,128]{2,1,0:T(8,128)(2,1)}), bf16[16,24,128]{2,1,0:T(8,128)(2,1)S(1)}, u32[]{:S(2)}, u32[]{:S(2)}) async-start(bf16[16,24,128]{2,1,0:T(8,128)(2,1)} %bitcast.2), calls=%async_computation.2 | async-start | bytes 196608 | tf_op jit(solution)/shard_map/all_to_all | solution.py:19
  75.3 30.7 %collective-permute-start.3 = (bf16[16,128,128]{2,1,0:T(8,128)(2,1)S(1)}, bf16[16,128,128]{2,1,0:T(8,128)(2,1)S(1)}, u32[]{:S(2)}, u32[]{:S(2)}) collective-permute-start(bf16[16,128,128]{2,1,0:T(8,128)(2,1)S(1)} %copy-done), channel_id=1, source_target_pairs={{0,48},{16,0},{32,16},{48,32},{1,49},{17,1},{33,17},{49,33},{2,50}... | collective-permute-start | bytes 1572872 | tf_op jit(solution)/shard_map/ppermute | solution.py:370
  90.1 16.0 %all-to-all-start.3 = ((bf16[16,24,128]{2,1,0:T(8,128)(2,1)}), bf16[16,24,128]{2,1,0:T(8,128)(2,1)S(1)}, u32[]{:S(2)}, u32[]{:S(2)}) async-start(bf16[16,24,128]{2,1,0:T(8,128)(2,1)} %broadcast_in_dim.7), calls=%async_computation.3 | async-start | bytes 196608 | tf_op jit(solution)/shard_map/all_to_all | solution.py:19

commit v10 on v9

--- a/solution.py
+++ b/solution.py
@@ -44,8 +44,8 @@
     return pltpu.CompilerParams(vmem_limit_bytes=mib << 20)
 
 
-def up_kernel(tokens_ref, gain_ref, weight_ref, scale_ref, out_ref, *scratch):
-    tokens, gain, weight, scale, out, in_sems, weight_sems, out_sems = scratch
+def up_kernel(tokens_ref, gain_ref, weight_ref, scale_ref, down_ref, out_ref, first_ref, *scratch):
+    tokens, gain, weight, scale, down, out, first, in_sems, weight_sems, out_sems = scratch
     parts, feats, step = weight.shape
     small = [
         pltpu.make_async_copy(tokens_ref, tokens, in_sems.at[0]),
@@ -59,6 +59,8 @@
         here = weight_ref.at[0, :, pl.ds(i * step, step)]
         copies.append(pltpu.make_async_copy(here, weight.at[i], weight_sems.at[i]))
         copies[-1].start()
+    down_copy = pltpu.make_async_copy(down_ref.at[0], down, in_sems.at[3])
+    down_copy.start()
     for copy in small:
         copy.wait()
     scaled = (tokens[...].astype(f32) * gain[0:1]).astype(bf16)
@@ -72,36 +74,43 @@
             out[z] = part[:, c * feats : (c + 1) * feats]
             sent.append(pltpu.make_async_copy(out.at[z], out_ref.at[z], out_sems.at[z]))
             sent[-1].start()
+    down_copy.wait()
+    first[...] = down[...].astype(bf16).reshape(first.shape)
+    sent.append(pltpu.make_async_copy(first, first_ref, in_sems.at[4]))
+    sent[-1].start()
     for copy in sent:
         copy.wait()
 
 
-def up_product(tokens, gain, weight, scale):
+def up_product(tokens, gain, weight, scale, down_weight):
     n_tok, feats = tokens.shape
     hid = weight.shape[2]
     parts = 4
+    blocks = (hid // feats, feats, feats)
     return pl.pallas_call(
         up_kernel,
-        out_shape=jax.ShapeDtypeStruct((Z, n_tok, hid // Z), bf16),
-        in_specs=[ANY] * 4,
-        out_specs=ANY,
+        out_shape=(pltpu.HBM((Z, n_tok, hid // Z), bf16), pltpu.HBM(blocks, bf16)),
+        in_specs=[ANY] * 5,
+        out_specs=(ANY,) * 2,
         scratch_shapes=[
             pltpu.VMEM(tokens.shape, bf16),
             pltpu.VMEM(gain.shape, f32),
             pltpu.VMEM((parts, feats, hid // parts), f32),
             pltpu.VMEM(scale.shape, f32),
+            pltpu.VMEM(down_weight.shape[1:], f32),
             pltpu.VMEM((Z, n_tok, hid // Z), bf16),
-            pltpu.SemaphoreType.DMA((3,)),
+            pltpu.VMEM(blocks, bf16),
+            pltpu.SemaphoreType.DMA((5,)),
             pltpu.SemaphoreType.DMA((parts,)),
             pltpu.SemaphoreType.DMA((Z,)),
         ],
         compiler_params=limit(12),
         name="up_product",
-    )(far(tokens), far(gain), far(weight), far(scale))
+    )(*[far(v) for v in (tokens, gain, weight, scale, down_weight)])
 
 
 def pack_kernel(down_ref, up_ref, tokens_ref, scale_ref, pre_ref, post_ref, *outs):
-    one, two, three, late, own = outs
+    own = outs[-1]
     hid, feats = down_ref.shape[1:]
     n = hid // feats
     t_x = own.shape[0] - 16
@@ -112,39 +121,39 @@
     high = columns.astype(bf16).astype(f32)
     columns = jnp.concatenate([high, columns - high], axis=0).astype(bf16)
     rest = jnp.zeros((feats - 16 - t_x, feats), bf16)
-    for s, ref in ((0, own), (1, one), (2, two), (3, three)):
+    down = down_ref[0].astype(bf16).reshape(n, feats, feats)
+    for s, ref in enumerate((own, *outs[:-1])):
         rows = pl.multiple_of(lax.rem(x + (X - s), X) * t_x, 32)
         block = [columns, tokens_ref[pl.ds(rows, t_x)]]
-        if s:
-            ref[:n] = down_ref[0].astype(bf16).reshape(n, feats, feats)
-            ref[n] = jnp.concatenate([*block, rest], axis=0)
-        else:
+        if s == 0:
             ref[...] = jnp.concatenate(block, axis=0)
-    for c in range(n):
-        late[c] = up_ref[0, :, c * feats : (c + 1) * feats].astype(bf16)
-    late[n:] = down_ref[1].astype(bf16).reshape(n, feats, feats)
+            continue
+        for c in range(n):
+            ref[c] = up_ref[0, :, c * feats : (c + 1) * feats].astype(bf16)
+        ref[n : 2 * n] = down
+        ref[2 * n] = jnp.concatenate([*block, rest], axis=0)
 
 
 def packed(down_weight, up_weight, tokens, scale, pre, post):
     _, hid, feats = down_weight.shape
     t_x = tokens.shape[0] // X
-    n = hid // feats
+    blocks = (2 * (hid // feats) + 1, feats, feats)
     whole = lambda v: pl.BlockSpec(v.shape, lambda i: (0,) * v.ndim)
-    blocks = (n + 1, n + 1, n + 1, 2 * n)
+    last_layer = lambda v: pl.BlockSpec((1, *v.shape[1:]), lambda i: (1, 0, 0))
     return pl.pallas_call(
         pack_kernel,
         grid=(1,),
         out_shape=(
-            *(pltpu.HBM((b, feats, feats), bf16) for b in blocks),
+            *(pltpu.HBM(blocks, bf16) for _ in range(X - 1)),
             pltpu.VMEM((16 + t_x, feats), bf16),
         ),
         in_specs=[
-            whole(down_weight),
-            pl.BlockSpec((1, feats, hid), lambda i: (1, 0, 0)),
+            last_layer(down_weight),
+            last_layer(up_weight),
             *[whole(v) for v in (tokens, scale, pre, post)],
         ],
         out_specs=(
-            *(pl.BlockSpec((b, feats, feats), lambda i: (0, 0, 0)) for b in blocks),
+            *(pl.BlockSpec(blocks, lambda i: (0, 0, 0)) for _ in range(X - 1)),
             pl.BlockSpec((16 + t_x, feats), lambda i: (0, 0)),
         ),
         compiler_params=limit(20),
@@ -152,11 +161,11 @@
     )(*[far(v) for v in (down_weight, up_weight, tokens, scale, pre, post)])
 
 
-def down_kernel(starts, lead_ref, hidden_ref, *refs):
+def down_kernel(start, lead_ref, hidden_ref, *refs):
     weights, out_ref, held, sems = refs[:X], refs[X], refs[X + 1], refs[X + 2]
     copies = []
     for i, w in enumerate(weights):
-        blocks = w.at[pl.ds(starts[i], held.shape[1])]
+        blocks = w.at[pl.ds(start, held.shape[1])]
         copies.append(pltpu.make_async_copy(blocks, held.at[i], sems.at[i]))
         copies[-1].start()
     hidden = [lead_ref[...].astype(bf16), *(hidden_ref[z] for z in range(1, Z))]
@@ -167,12 +176,12 @@
         out_ref[i] = jnp.dot(hidden, weight, preferred_element_type=f32).astype(bf16)
 
 
-def down_product(hidden, blocks, starts):
+def down_product(hidden, blocks, start):
     _, t, share = hidden.shape
     feats = blocks[0].shape[2]
     lead = hidden[0].astype(f32)
     return pl.pallas_call(
-        lambda *refs: down_kernel(starts, *refs),
+        lambda *refs: down_kernel(start, *refs),
         out_shape=pltpu.VMEM((X, t, feats), bf16),
         in_specs=[*[VMEM] * 2, *[ANY] * X],
         out_specs=VMEM,
@@ -185,8 +194,8 @@
     )(near(lead), near(hidden), *blocks)
 
 
-def down_share(hidden, blocks, starts):
-    part = down_product(hidden, blocks, starts)
+def down_share(hidden, blocks, start):
+    part = down_product(hidden, blocks, start)
     pieces = part.reshape(Y * C, -1, part.shape[2])
     return exchange(pieces, ("y", "core")).astype(f32).sum(axis=0).astype(bf16)
 
@@ -213,22 +222,21 @@
     return jnp.transpose(jnp.broadcast_to(inv, (128, 128)))[:t]
 
 
-def turn_kernel(firsts_at, seconds_at, lead_ref, sum_ref, own_ref, scale_ref, *refs):
-    firsts, seconds = refs[: X - 1], refs[X - 1 : 2 * X - 1]
-    out_ref, kept_ref, branch_ref, columns_ref = refs[2 * X - 1 : 2 * X + 3]
-    extra, held, scales, sems, held_sems = refs[2 * X + 3 :]
+def turn_kernel(lead_ref, sum_ref, own_ref, scale_ref, *refs):
+    blocks = refs[:X]
+    out_ref, kept_ref, branch_ref, columns_ref = refs[X : X + 4]
+    extra, held, scales, sems, held_sems = refs[X + 4 :]
     t, feats = sum_ref.shape[1:]
     copies = [pltpu.make_async_copy(scale_ref, scales, sems.at[X - 1])]
     copies[0].start()
-    for i, block in enumerate(firsts):
-        rows = block.at[firsts_at, pl.ds(0, extra.shape[1])]
-        copies.append(pltpu.make_async_copy(rows, extra.at[i], sems.at[i]))
+    for i in range(1, X):
+        rows = blocks[i].at[2 * Z, pl.ds(0, extra.shape[1])]
+        copies.append(pltpu.make_async_copy(rows, extra.at[i - 1], sems.at[i - 1]))
         copies[-1].start()
     held_copies = []
-    for i, block in enumerate(seconds):
+    for i in range(X):
         here = held.at[:, pl.ds(i * feats, feats)]
-        blocks = block.at[pl.ds(seconds_at[i], Z)]
-        held_copies.append(pltpu.make_async_copy(blocks, here, held_sems.at[i]))
+        held_copies.append(pltpu.make_async_copy(blocks[i].at[pl.ds(0, Z)], here, held_sems.at[i]))
         held_copies[-1].start()
     for copy in copies:
         copy.wait()
@@ -263,18 +271,18 @@
         out_ref[c, 2 * t :, :t] = squares
 
 
-def turn(summed, own, scale, firsts, firsts_at, seconds, seconds_at):
+def turn(summed, own, scale, blocks):
     _, t, feats = summed.shape
     lead = summed[0].astype(f32)
     return pl.pallas_call(
-        lambda *refs: turn_kernel(firsts_at, seconds_at, *refs),
+        turn_kernel,
         out_shape=(
             pltpu.VMEM((Z, 2 * t + 8, feats), bf16),
             pltpu.VMEM((X, t, feats), f32),
             pltpu.VMEM((X, t, feats), f32),
             pltpu.VMEM((X, 8, feats), f32),
         ),
-        in_specs=[*[VMEM] * 3, *[ANY] * (2 * X)],
+        in_specs=[*[VMEM] * 3, *[ANY] * (X + 1)],
         out_specs=(VMEM,) * 4,
         scratch_shapes=[
             pltpu.VMEM((X - 1, 16 + t, feats), bf16),
@@ -285,7 +293,7 @@
         ],
         compiler_params=limit(12),
         name="turn",
-    )(near(lead), near(summed), near(own), far(scale), *firsts, *seconds)
+    )(near(lead), near(summed), near(own), far(scale), *blocks)
 
 
 def hidden_kernel(width, came_ref, kept_ref, branch_ref, out_ref, stream_ref):
@@ -363,32 +371,27 @@
     width = feats * X * Z
     t_x = n_tok // X
 
-    part = up_product(tokens, pre_gain, up_weight, up_scale).reshape(Z * X, t_x, feats)
+    part, first = up_product(tokens, pre_gain, up_weight, up_scale, down_weight)
+    part = part.reshape(Z * X, t_x, feats)
     summed = exchange(part, ("z", "x")).astype(f32).sum(axis=0)
 
     def from_x(payload, s):
         return lax.ppermute(payload, "x", [(i, (i - s) % X) for i in range(X)])
 
-    one, two, three, late, own = packed(
-        down_weight, up_weight, tokens, down_scale, pre_gain, post_gain
-    )
-    firsts = [from_x(one, 1), from_x(two, 2), from_x(three, 3)]
-    seconds = [from_x(late, s) for s in (1, 2, 3)]
-    n = hid // feats
+    *payloads, own = packed(down_weight, up_weight, tokens, down_scale, pre_gain, post_gain)
+    firsts = [from_x(first, s) for s in (1, 2, 3)]
+    seconds = [from_x(payloads[s - 1], s) for s in (1, 2, 3)]
 
     hidden = to_all(activation(summed), "z")
-    firsts = after(firsts, hidden)
-    mine = down_share(hidden, [far(one), *firsts], [0] * X)
+    mine = down_share(hidden, [far(first), *after(firsts, hidden)], 0)
     summed = down_whole(mine)
 
-    seconds = [far(late), *after(seconds, summed)]
-    part, kept, branch, columns = turn(
-        summed, own, up_scale, firsts, n, seconds, [0] * X
-    )
+    seconds = [far(payloads[0]), *after(seconds, summed)]
+    part, kept, branch, columns = turn(summed, own, up_scale, seconds)
     came = exchange(part, "z")
     hidden, stream = second_hidden(came, kept, branch, width)
     hidden = exchange(hidden, "z")
-    mine = down_share(hidden, seconds, [n] * X)
+    mine = down_share(hidden, seconds, hid // feats)
     summed = down_whole(mine)
 
     squares = squares_of(summed, columns)

time: 187 us -> 176 us (0.941)
  starting transfers between devices: 52.2 us -> 38.8 us
  waiting for transfers between devices: 10.1 us -> 12.7 us
    ppermute x6, starting transfers between devices: 29.8 us -> 19 us  [from_x(): return lax.ppermute(payload, 'x', [(i, (i - s) % X) for i in range(X)])]
    all_to_all x3, waiting for transfers between devices: 8.45 us -> 12.6 us  [exchange(): return lax.all_to_all(pieces, axis, split_axis=0, concat_axis=0, tiled=True)]
    all_to_all x3, starting transfers between devices: 22.4 us -> 19.8 us  [exchange(): return lax.all_to_all(pieces, axis, split_axis=0, concat_axis=0, tiled=True)]
  transfers between devices with their start and end apart: 9 -> 9, of which waited for: 2 -> 3; matrix products, arithmetic and copies ran while one was open for 0% -> 0% of each run, Pallas kernels for 2% -> 2%
where the time goes in v10:
time: 176 us; the launch traced here: 175 us
  blocking collectives  110 us (62%)
  starting transfers between devices  38.8 us (22%)
  waiting for transfers between devices  12.7 us (7%)
  Pallas kernels  11.4 us (6%)
  local copies, waits for them, and re-layouts  2.04 us (1%)
    all_to_all x7, blocking collectives, exchange(): return lax.all_to_all(pieces, axis, split_axis=0, concat_axis=0, tiled=True)  110 us
    all_to_all x3, starting transfers between devices, exchange(): return lax.all_to_all(pieces, axis, split_axis=0, concat_axis=0, tiled=True)  19.8 us
    ppermute x6, starting transfers between devices, from_x(): return lax.ppermute(payload, 'x', [(i, (i - s) % X) for i in range(X)])  19 us
    all_to_all x3, waiting for transfers between devices, exchange(): return lax.all_to_all(pieces, axis, split_axis=0, concat_axis=0, tiled=True)  12.6 us
  transfers between devices with their start and end apart: 9, of which 3 were waited for; matrix products, arithmetic and copies ran while one was open for 0% of the time, Pallas kernels for 2%

profile of v10, /device:TPU:1, one launch (start us, length us, event | category | flops | bytes accessed | tf_op | source)
XLA Modules:
  0.0 174.9 jit_solution(13769178395432825922)
XLA Ops:
  0.0 2.8 %up_product.1 = (bf16[8,384,128]{2,1,0:T(8,128)(2,1)}, bf16[8,128,128]{2,1,0:T(8,128)(2,1)}) custom-call(bf16[384,128]{1,0:T(8,128)(2,1)} %tokens_ref.3, f32[2,128]{1,0:T(2,128)} %pre_ref.1, f32[2,128,1024]{2,1,0:T(8,128)} %up_ref.1, f32[2,1024]{1,0:T(2,128)} %scale_ref.5, f32[2,1024,128]{2,1,0:T(8,128)} %down_ref.3), custom_call_target="tpu_custom_call" | custom-call | tf_op jit(solution)/shard_map/up_product/pallas_call | solution.py:90
  2.9 34.8 %all_to_all.50 = bf16[32,96,128]{2,1,0:T(8,128)(2,1)S(1)} all-to-all(bf16[32,96,128]{2,1,0:T(8,128)(2,1)} %bitcast.23), channel_id=1, replica_groups=mesh['z'=8,'x'=4,'y'=8,'core'=2] {'z','x'}, dimensions={0} | all-to-all | bytes 1572864 | tf_op jit(solution)/shard_map/all_to_all | solution.py:19
  37.6 0.0 copy-start.1
  37.6 0.1 convert_reduce_fusion
  37.8 0.7 broadcast_in_dim.6
  38.5 4.1 %all-to-all-start.1 = ((bf16[8,96,128]{2,1,0:T(8,128)(2,1)}), bf16[8,96,128]{2,1,0:T(8,128)(2,1)S(1)}, u32[]{:S(2)}, u32[]{:S(2)}) async-start(bf16[8,96,128]{2,1,0:T(8,128)(2,1)} %broadcast_in_dim.6), calls=%async_computation.1 | async-start | bytes 393216 | tf_op jit(solution)/shard_map/all_to_all | solution.py:19
  42.6 0.0 copy-done.1
  42.6 3.0 %collective-permute-start.2 = (bf16[8,128,128]{2,1,0:T(8,128)(2,1)S(1)}, bf16[8,128,128]{2,1,0:T(8,128)(2,1)S(1)}, u32[]{:S(2)}, u32[]{:S(2)}) collective-permute-start(bf16[8,128,128]{2,1,0:T(8,128)(2,1)S(1)} %copy-done.1), channel_id=1, source_target_pairs={{0,16},{16,32},{32,48},{48,0},{1,17},{17,33},{33,49},{49,1},{2,18}... | collective-permute-start | bytes 786440 | tf_op jit(solution)/shard_map/ppermute | solution.py:379
  45.6 4.1 %collective-permute-start.1 = (bf16[8,128,128]{2,1,0:T(8,128)(2,1)S(1)}, bf16[8,128,128]{2,1,0:T(8,128)(2,1)S(1)}, u32[]{:S(2)}, u32[]{:S(2)}) collective-permute-start(bf16[8,128,128]{2,1,0:T(8,128)(2,1)S(1)} %copy-done.1), channel_id=1, source_target_pairs={{0,32},{16,48},{32,0},{48,16},{1,33},{17,49},{33,1},{49,17},{2,34}... | collective-permute-start | bytes 786440 | tf_op jit(solution)/shard_map/ppermute | solution.py:379
  49.8 2.7 %collective-permute-start = (bf16[8,128,128]{2,1,0:T(8,128)(2,1)S(1)}, bf16[8,128,128]{2,1,0:T(8,128)(2,1)S(1)}, u32[]{:S(2)}, u32[]{:S(2)}) collective-permute-start(bf16[8,128,128]{2,1,0:T(8,128)(2,1)S(1)} %copy-done.1), channel_id=1, source_target_pairs={{0,48},{16,0},{32,16},{48,32},{1,49},{17,1},{33,17},{49,33},{2,50}... | collective-permute-start | bytes 786440 | tf_op jit(solution)/shard_map/ppermute | solution.py:379
  52.6 2.5 %packed.1 = (bf16[17,128,128]{2,1,0:T(8,128)(2,1)}, bf16[17,128,128]{2,1,0:T(8,128)(2,1)}, bf16[17,128,128]{2,1,0:T(8,128)(2,1)}, bf16[112,128]{1,0:T(8,128)(2,1)S(1)}) custom-call(f32[2,1024,128]{2,1,0:T(8,128)} %down_ref.3, f32[2,128,1024]{2,1,0:T(8,128)} %up_ref.1, bf16[384,128]{1,0:T(8,128)(2,1)} %tokens_ref.3, f32[2,128]{1,0:T(2,128)} %scale_ref.4, ...), custom_call_target="tpu_custom_call" | custom-call | tf_op jit(solution)/shard_map/packed/pallas_call | solution.py:143
  55.1 0.0 copy-start
  55.1 2.9 %collective-permute-start.4 = (bf16[17,128,128]{2,1,0:T(8,128)(2,1)}, bf16[17,128,128]{2,1,0:T(8,128)(2,1)S(1)}, u32[]{:S(2)}, u32[]{:S(2)}) collective-permute-start(bf16[17,128,128]{2,1,0:T(8,128)(2,1)} %get-tuple-element.31), channel_id=1, source_target_pairs={{0,32},{16,48},{32,0},{48,16},{1,33},{17,49},{33,1},{49,17},{2,34}... | collective-permute-start | bytes 1671176 | tf_op jit(solution)/shard_map/ppermute | solution.py:379
  58.0 1.9 %collective-permute-start.5 = (bf16[17,128,128]{2,1,0:T(8,128)(2,1)}, bf16[17,128,128]{2,1,0:T(8,128)(2,1)S(1)}, u32[]{:S(2)}, u32[]{:S(2)}) collective-permute-start(bf16[17,128,128]{2,1,0:T(8,128)(2,1)} %get-tuple-element.33), channel_id=1, source_target_pairs={{0,16},{16,32},{32,48},{48,0},{1,17},{17,33},{33,49},{49,1},{2,18}... | collective-permute-start | bytes 1671176 | tf_op jit(solution)/shard_map/ppermute | solution.py:379
  59.9 0.0 collective-permute-done.2.refs_5_
  59.9 0.0 all-to-all-done.1.refs_1_
  59.9 0.0 collective-permute-done.1.refs_4_
  59.9 0.1 collective-permute-done.refs_3_
  60.0 1.8 %down_product.2 = bf16[4,96,128]{2,1,0:T(8,128)(2,1)} custom-call(f32[96,128]{1,0:T(8,128)S(1)} %fusion.1.refs_0_, bf16[8,96,128]{2,1,0:T(8,128)(2,1)S(1)} %all-to-all-done.1.refs_1_, bf16[8,128,128]{2,1,0:T(8,128)(2,1)} %get-tuple-element.24.refs_2_, bf16[8,128,128]{2,1,0:T(8,128)(2,1)S(1)} %collective-permute-done.refs_3_, ...), custom_call_target="tpu_custom_call" | custom-call | tf_op jit(solution)/shard_map/down_product/pallas_call | solution.py:183
  61.9 12.2 %all-to-all-start.2 = ((bf16[16,24,128]{2,1,0:T(8,128)(2,1)}), bf16[16,24,128]{2,1,0:T(8,128)(2,1)S(1)}, u32[]{:S(2)}, u32[]{:S(2)}) async-start(bf16[16,24,128]{2,1,0:T(8,128)(2,1)} %bitcast.2), calls=%async_computation.2 | async-start | bytes 196608 | tf_op jit(solution)/shard_map/all_to_all | solution.py:19
  74.1 0.0 copy-done
  74.1 4.3 %collective-permute-start.3 = (bf16[17,128,128]{2,1,0:T(8,128)(2,1)S(1)}, bf16[17,128,128]{2,1,0:T(8,128)(2,1)S(1)}, u32[]{:S(2)}, u32[]{:S(2)}) collective-permute-start(bf16[17,128,128]{2,1,0:T(8,128)(2,1)S(1)} %copy-done), channel_id=1, source_target_pairs={{0,48},{16,0},{32,16},{48,32},{1,49},{17,1},{33,17},{49,33},{2,50}... | collective-permute-start | bytes 1671176 | tf_op jit(solution)/shard_map/ppermute | solution.py:379
  78.4 4.1 %all-to-all-done.2 = bf16[16,24,128]{2,1,0:T(8,128)(2,1)S(1)} async-done(((bf16[16,24,128]{2,1,0:T(8,128)(2,1)}), bf16[16,24,128]{2,1,0:T(8,128)(2,1)S(1)}, u32[]{:S(2)}, u32[]{:S(2)}) %all-to-all-start.2) | async-done | bytes 98336 | tf_op jit(solution)/shard_map/all_to_all | solution.py:19
  82.6 0.7 broadcast_in_dim.7
  83.2 3.4 %all-to-all-start.3 = ((bf16[16,24,128]{2,1,0:T(8,128)(2,1)}), bf16[16,24,128]{2,1,0:T(8,128)(2,1)S(1)}, u32[]{:S(2)}, u32[]{:S(2)}) async-start(bf16[16,24,128]{2,1,0:T(8,128)(2,1)} %broadcast_in_dim.7), calls=%async_computation.3 | async-start | bytes 196608 | tf_op jit(solution)/shard_map/all_to_all | solution.py:19
  86.6 0.0 collective-permute-done.4.refs_2_.refs_4_
  86.7 8.4 %all-to-all-done.3 = bf16[16,24,128]{2,1,0:T(8,128)(2,1)S(1)} async-done(((bf16[16,24,128]{2,1,0:T(8,128)(2,1)}), bf16[16,24,128]{2,1,0:T(8,128)(2,1)S(1)}, u32[]{:S(2)}, u32[]{:S(2)}) %all-to-all-start.3) | async-done | bytes 98336 | tf_op jit(solution)/shard_map/all_to_all | solution.py:19
  95.1 0.0 collective-permute-done.5.refs_3_.refs_5_
  95.1 0.0 collective-permute-done.3.refs_1_.refs_3_
  95.1 2.4 %turn.1 = (bf16[8,200,128]{2,1,0:T(8,128)(2,1)S(1)}, f32[4,96,128]{2,1,0:T(8,128)S(1)}, f32[4,96,128]{2,1,0:T(8,128)S(1)}, f32[4,8,128]{2,1,0:T(8,128)S(1)}) custom-call(f32[96,128]{1,0:T(8,128)S(1)} %bitcast_convert_fusion.lead_ref, bf16[4,96,128]{2,1,0:T(8,128)(2,1)S(1)} %bitcast.21, bf16[112,128]{1,0:T(8,128)(2,1)S(1)} %get-tuple-element.28.own_ref, ...), custom_call_target="tpu_custom_call" | custom-call | tf_op jit(solution)/shard_map/turn/pallas_call | solution.py:277
  97.5 22.5 %all_to_all.51.refs_0_ = bf16[8,200,128]{2,1,0:T(8,128)(2,1)S(1)} all-to-all(bf16[8,200,128]{2,1,0:T(8,128)(2,1)S(1)} %get-tuple-element.35), channel_id=1, replica_groups=mesh['z'=8,'x'=4,'y'=8,'core'=2] {'z'}, dimensions={0} | all-to-all | bytes 819200 | tf_op jit(solution)/shard_map/all_to_all | solution.py:19
  120.0 0.1 second_hidden.1
  120.1 12.1 %all_to_all.52.refs_1_ = bf16[8,96,128]{2,1,0:T(8,128)(2,1)S(1)} all-to-all(bf16[8,96,128]{2,1,0:T(8,128)(2,1)S(1)} %get-tuple-element.38), channel_id=1, replica_groups=mesh['z'=8,'x'=4,'y'=8,'core'=2] {'z'}, dimensions={0} | all-to-all | bytes 393216 | tf_op jit(solution)/shard_map/all_to_all | solution.py:19
  132.2 1.2 down_product.3
  133.4 12.6 %all_to_all.53 = bf16[16,24,128]{2,1,0:T(8,128)(2,1)S(1)} all-to-all(bf16[16,24,128]{2,1,0:T(8,128)(2,1)S(1)} %bitcast.22), channel_id=1, replica_groups=mesh['z'=8,'x'=4,'y'=8,'core'=2] {'y','core'}, dimensions={0} | all-to-all | bytes 196608 | tf_op jit(solution)/shard_map/all_to_all | solution.py:19
  146.1 10.9 %all_to_all.54 = bf16[16,24,128]{2,1,0:T(8,128)(2,1)S(1)} all-to-all(bf16[16,24,128]{2,1,0:T(8,128)(2,1)S(1)} %broadcast_in_dim.8), channel_id=1, replica_groups=mesh['z'=8,'x'=4,'y'=8,'core'=2] {'y','core'}, dimensions={0} | all-to-all | bytes 196608 | tf_op jit(solution)/shard_map/all_to_all | solution.py:19
  156.9 0.4 squares.1
  157.3 9.3 %all_to_all.55.refs_0_ = f32[8,8,128]{2,1,0:T(8,128)S(1)} all-to-all(f32[8,8,128]{2,1,0:T(8,128)S(1)} %squares.1), channel_id=1, replica_groups=mesh['z'=8,'x'=4,'y'=8,'core'=2] {'z'}, dimensions={0} | all-to-all | bytes 65536 | tf_op jit(solution)/shard_map/all_to_all | solution.py:19
  166.6 0.1 last.1
  166.7 7.6 %all_to_all.56 = bf16[4,96,128]{2,1,0:T(8,128)(2,1)S(1)} all-to-all(bf16[4,96,128]{2,1,0:T(8,128)(2,1)S(1)} %last.1), channel_id=1, replica_groups=mesh['z'=8,'x'=4,'y'=8,'core'=2] {'x'}, dimensions={0} | all-to-all | bytes 196608 | tf_op jit(solution)/shard_map/all_to_all | solution.py:19
  174.3 0.6 copy.9
  (8 shorter events, 0.1 us)
Async XLA Ops:
  37.6 5.0 %copy-start.1 = (bf16[8,128,128]{2,1,0:T(8,128)(2,1)S(1)}, bf16[8,128,128]{2,1,0:T(8,128)(2,1)}, u32[]{:S(2)}) copy-start(bf16[8,128,128]{2,1,0:T(8,128)(2,1)} %get-tuple-element.24.refs_2_) | copy-start | bytes 786436
  38.5 21.4 %all-to-all-start.1 = ((bf16[8,96,128]{2,1,0:T(8,128)(2,1)}), bf16[8,96,128]{2,1,0:T(8,128)(2,1)S(1)}, u32[]{:S(2)}, u32[]{:S(2)}) async-start(bf16[8,96,128]{2,1,0:T(8,128)(2,1)} %broadcast_in_dim.6), calls=%async_computation.1 | async-start | bytes 393216 | tf_op jit(solution)/shard_map/all_to_all | solution.py:19
  42.6 17.3 %collective-permute-start.2 = (bf16[8,128,128]{2,1,0:T(8,128)(2,1)S(1)}, bf16[8,128,128]{2,1,0:T(8,128)(2,1)S(1)}, u32[]{:S(2)}, u32[]{:S(2)}) collective-permute-start(bf16[8,128,128]{2,1,0:T(8,128)(2,1)S(1)} %copy-done.1), channel_id=1, source_target_pairs={{0,16},{16,32},{32,48},{48,0},{1,17},{17,33},{33,49},{49,1},{2,18}... | collective-permute-start | bytes 786440 | tf_op jit(solution)/shard_map/ppermute | solution.py:379
  45.6 14.3 %collective-permute-start.1 = (bf16[8,128,128]{2,1,0:T(8,128)(2,1)S(1)}, bf16[8,128,128]{2,1,0:T(8,128)(2,1)S(1)}, u32[]{:S(2)}, u32[]{:S(2)}) collective-permute-start(bf16[8,128,128]{2,1,0:T(8,128)(2,1)S(1)} %copy-done.1), channel_id=1, source_target_pairs={{0,32},{16,48},{32,0},{48,16},{1,33},{17,49},{33,1},{49,17},{2,34}... | collective-permute-start | bytes 786440 | tf_op jit(solution)/shard_map/ppermute | solution.py:379
  49.8 10.2 %collective-permute-start = (bf16[8,128,128]{2,1,0:T(8,128)(2,1)S(1)}, bf16[8,128,128]{2,1,0:T(8,128)(2,1)S(1)}, u32[]{:S(2)}, u32[]{:S(2)}) collective-permute-start(bf16[8,128,128]{2,1,0:T(8,128)(2,1)S(1)} %copy-done.1), channel_id=1, source_target_pairs={{0,48},{16,0},{32,16},{48,32},{1,49},{17,1},{33,17},{49,33},{2,50}... | collective-permute-start | bytes 786440 | tf_op jit(solution)/shard_map/ppermute | solution.py:379
  55.1 19.0 %copy-start = (bf16[17,128,128]{2,1,0:T(8,128)(2,1)S(1)}, bf16[17,128,128]{2,1,0:T(8,128)(2,1)}, u32[]{:S(2)}) copy-start(bf16[17,128,128]{2,1,0:T(8,128)(2,1)} %get-tuple-element.29.refs_0_.refs_2_) | copy-start | bytes 1671172
  55.1 31.6 %collective-permute-start.4 = (bf16[17,128,128]{2,1,0:T(8,128)(2,1)}, bf16[17,128,128]{2,1,0:T(8,128)(2,1)S(1)}, u32[]{:S(2)}, u32[]{:S(2)}) collective-permute-start(bf16[17,128,128]{2,1,0:T(8,128)(2,1)} %get-tuple-element.31), channel_id=1, source_target_pairs={{0,32},{16,48},{32,0},{48,16},{1,33},{17,49},{33,1},{49,17},{2,34}... | collective-permute-start | bytes 1671176 | tf_op jit(solution)/shard_map/ppermute | solution.py:379
  58.0 37.1 %collective-permute-start.5 = (bf16[17,128,128]{2,1,0:T(8,128)(2,1)}, bf16[17,128,128]{2,1,0:T(8,128)(2,1)S(1)}, u32[]{:S(2)}, u32[]{:S(2)}) collective-permute-start(bf16[17,128,128]{2,1,0:T(8,128)(2,1)} %get-tuple-element.33), channel_id=1, source_target_pairs={{0,16},{16,32},{32,48},{48,0},{1,17},{17,33},{33,49},{49,1},{2,18}... | collective-permute-start | bytes 1671176 | tf_op jit(solution)/shard_map/ppermute | solution.py:379
  61.9 20.7 %all-to-all-start.2 = ((bf16[16,24,128]{2,1,0:T(8,128)(2,1)}), bf16[16,24,128]{2,1,0:T(8,128)(2,1)S(1)}, u32[]{:S(2)}, u32[]{:S(2)}) async-start(bf16[16,24,128]{2,1,0:T(8,128)(2,1)} %bitcast.2), calls=%async_computation.2 | async-start | bytes 196608 | tf_op jit(solution)/shard_map/all_to_all | solution.py:19
  74.1 21.0 %collective-permute-start.3 = (bf16[17,128,128]{2,1,0:T(8,128)(2,1)S(1)}, bf16[17,128,128]{2,1,0:T(8,128)(2,1)S(1)}, u32[]{:S(2)}, u32[]{:S(2)}) collective-permute-start(bf16[17,128,128]{2,1,0:T(8,128)(2,1)S(1)} %copy-done), channel_id=1, source_target_pairs={{0,48},{16,0},{32,16},{48,32},{1,49},{17,1},{33,17},{49,33},{2,50}... | collective-permute-start | bytes 1671176 | tf_op jit(solution)/shard_map/ppermute | solution.py:379
  83.2 11.8 %all-to-all-start.3 = ((bf16[16,24,128]{2,1,0:T(8,128)(2,1)}), bf16[16,24,128]{2,1,0:T(8,128)(2,1)S(1)}, u32[]{:S(2)}, u32[]{:S(2)}) async-start(bf16[16,24,128]{2,1,0:T(8,128)(2,1)} %broadcast_in_dim.7), calls=%async_computation.3 | async-start | bytes 196608 | tf_op jit(solution)/shard_map/all_to_all | solution.py:19

commit v11 on v10

--- a/solution.py
+++ b/solution.py
@@ -161,7 +161,7 @@
     )(*[far(v) for v in (down_weight, up_weight, tokens, scale, pre, post)])
 
 
-def down_kernel(start, lead_ref, hidden_ref, *refs):
+def down_kernel(start, rows, lead_ref, hidden_ref, *refs):
     weights, out_ref, held, sems = refs[:X], refs[X], refs[X + 1], refs[X + 2]
     copies = []
     for i, w in enumerate(weights):
@@ -173,16 +173,23 @@
     for i in (1, 2, 3, 0):
         copies[i].wait()
         weight = held[i].reshape(hidden.shape[1], -1)
-        out_ref[i] = jnp.dot(hidden, weight, preferred_element_type=f32).astype(bf16)
-
-
-def down_product(hidden, blocks, start):
+        part = jnp.dot(hidden, weight, preferred_element_type=f32)
+        if not rows:
+            out_ref[i] = part.astype(bf16)
+            continue
+        for k in range(Y * C):
+            at = k * rows
+            piece = part[at : at + rows] if at < part.shape[0] else jnp.zeros((rows, part.shape[1]))
+            out_ref[k, i] = piece.astype(bf16)
+
+
+def down_product(hidden, blocks, start, rows=0):
     _, t, share = hidden.shape
     feats = blocks[0].shape[2]
     lead = hidden[0].astype(f32)
     return pl.pallas_call(
-        lambda *refs: down_kernel(start, *refs),
-        out_shape=pltpu.VMEM((X, t, feats), bf16),
+        lambda *refs: down_kernel(start, rows, *refs),
+        out_shape=pltpu.VMEM((Y * C, X, rows, feats) if rows else (X, t, feats), bf16),
         in_specs=[*[VMEM] * 2, *[ANY] * X],
         out_specs=VMEM,
         scratch_shapes=[
@@ -306,14 +313,14 @@
     for z in range(Z):
         out_ref[z] = hidden
     for i in range(X):
-        stream_ref[i] = (kept_ref[i] + branch_ref[i] * inv).astype(bf16)
+        stream_ref[i] = (kept_ref[i] + branch_ref[i] * inv).astype(bf16).astype(f32)
 
 
 def second_hidden(came, kept, branch, width):
     _, t, feats = kept.shape
     return pl.pallas_call(
         lambda *refs: hidden_kernel(width, *refs),
-        out_shape=(pltpu.VMEM((Z, t, feats), bf16), pltpu.VMEM(kept.shape, bf16)),
+        out_shape=(pltpu.VMEM((Z, t, feats), bf16), pltpu.VMEM(kept.shape, f32)),
         in_specs=[VMEM] * 3,
         out_specs=(VMEM,) * 2,
         compiler_params=limit(8),
@@ -321,48 +328,68 @@
     )(near(came), near(kept), near(branch))
 
 
-def squares_kernel(sum_ref, columns_ref, out_ref):
-    t = sum_ref.shape[1]
-    values = [sum_ref[i].astype(f32) * columns_ref[i, 3:4] for i in range(X)]
-    squares = squares_in_rows(values)
-    for z in range(Z):
-        out_ref[z] = jnp.zeros(out_ref.shape[1:], f32)
-        out_ref[z, :, :t] = squares
-
-
-def squares_of(summed, columns):
-    return pl.pallas_call(
-        squares_kernel,
-        out_shape=pltpu.VMEM((Z, 8, summed.shape[2]), f32),
-        in_specs=[VMEM] * 2,
+def share_kernel(sum_ref, columns_ref, stream_ref, out_ref):
+    rows = sum_ref.shape[2]
+    most = stream_ref.shape[1] // rows - 1
+    mine = jnp.minimum(lax.axis_index("y") * C + lax.axis_index("core"), most)
+    tokens = pl.ds(pl.multiple_of(mine * rows, rows), rows)
+    branches = []
+    for i in range(X):
+        total = sum_ref[0, i].astype(f32)
+        for k in range(1, Y * C):
+            total += sum_ref[k, i].astype(f32)
+        branches.append(total * columns_ref[i, 3:4])
+    squares = squares_in_rows(branches)
+    high = squares.astype(bf16).astype(f32)
+    row = lax.broadcasted_iota(jnp.int32, squares.shape, 0)
+    squares = jnp.where(row == 0, high, jnp.where(row == 1, squares - high, 0.0)).astype(bf16)
+    x = lax.axis_index("x")
+    for i in range(X):
+        branch = (branches[i] * columns_ref[i, 4:5]).astype(bf16)
+        stream = stream_ref[i, tokens].astype(bf16)
+        owner = lax.rem(x + i, X)
+        for z in range(Z):
+            out_ref[z * X + owner, :rows] = branch
+            out_ref[z * X + owner, rows : 2 * rows] = stream
+            out_ref[z * X + owner, 2 * rows :] = jnp.zeros((8, branch.shape[1]), bf16)
+            out_ref[z * X + owner, 2 * rows :, :rows] = squares
+
+
+def shares(came, columns, stream):
+    rows, feats = came.shape[2:]
+    return pl.pallas_call(
+        share_kernel,
+        out_shape=pltpu.VMEM((Z * X, 2 * rows + 8, feats), bf16),
+        in_specs=[VMEM] * 3,
         out_specs=VMEM,
         compiler_params=limit(8),
-        name="squares",
-    )(near(summed), near(columns))
-
-
-def last_kernel(width, squares_ref, sum_ref, columns_ref, stream_ref, out_ref):
-    t = sum_ref.shape[1]
-    total = squares_ref[0]
-    for z in range(1, Z):
-        total += squares_ref[z]
-    inv = inverse(total[0:1], width, t)
-    x = lax.axis_index("x")
-    for i in range(X):
-        branch = sum_ref[i].astype(f32) * columns_ref[i, 3:4] * inv * columns_ref[i, 4:5]
-        stream = residual_keep * stream_ref[i].astype(f32) + branch
-        out_ref[lax.rem(x + i, X)] = stream.astype(bf16)
-
-
-def last(squares, summed, columns, stream, width):
+        name="shares",
+    )(near(came), near(columns), near(stream))
+
+
+def last_kernel(width, came_ref, out_ref):
+    rows = out_ref.shape[2]
+    z = lax.axis_index("z")
+    for i in range(X):
+        total = came_ref[i, 2 * rows :].astype(f32)
+        for k in range(1, Z):
+            total += came_ref[k * X + i, 2 * rows :].astype(f32)
+        inv = inverse(total[0:1] + total[1:2], width, rows)
+        block = came_ref[z * X + i].astype(f32)
+        stream = residual_keep * block[rows : 2 * rows] + block[:rows] * inv
+        for k in range(Y * C):
+            out_ref[k, i] = stream.astype(bf16)
+
+
+def last(came, rows, width):
     return pl.pallas_call(
         lambda *refs: last_kernel(width, *refs),
-        out_shape=pltpu.VMEM(summed.shape, bf16),
-        in_specs=[VMEM] * 4,
+        out_shape=pltpu.VMEM((Y * C, X, rows, came.shape[2]), bf16),
+        in_specs=[VMEM],
         out_specs=VMEM,
         compiler_params=limit(8),
         name="last",
-    )(near(squares), near(summed), near(columns), near(stream))
+    )(near(came))
 
 
 def inner(tokens, up_weight, up_scale, down_weight, down_scale, pre_gain, post_gain):
@@ -391,13 +418,15 @@
     came = exchange(part, "z")
     hidden, stream = second_hidden(came, kept, branch, width)
     hidden = exchange(hidden, "z")
-    mine = down_share(hidden, seconds, hid // feats)
-    summed = down_whole(mine)
-
-    squares = squares_of(summed, columns)
-    squares = exchange(squares, "z")
-    out = last(squares, summed, columns, stream, width)
-    return exchange(out, "x").reshape(n_tok, feats)
+
+    rows = 8
+    part = down_product(hidden, seconds, hid // feats, rows)
+    came = exchange(part, ("y", "core"))
+    pieces = shares(came, columns, stream)
+    came = exchange(pieces, ("z", "x"))
+    out = last(came, rows, width)
+    out = exchange(out, ("y", "core"))
+    return out[: t_x // rows].transpose(1, 0, 2, 3).reshape(n_tok, feats)
 
 
 def solution(mesh):

time: 176 us -> 176 us (level)
    all_to_all x7 -> x6, blocking collectives: 110 us -> 110 us  [exchange(): return lax.all_to_all(pieces, axis, split_axis=0, concat_axis=0, tiled=True)]
where the time goes in v11:
time: 176 us; the launch traced here: 175 us
  blocking collectives  110 us (62%)
  starting transfers between devices  38.8 us (22%)
  waiting for transfers between devices  12.6 us (7%)
  Pallas kernels  11.2 us (6%)
  local copies, waits for them, and re-layouts  2.04 us (1%)
    all_to_all x6, blocking collectives, exchange(): return lax.all_to_all(pieces, axis, split_axis=0, concat_axis=0, tiled=True)  110 us
    all_to_all x3, starting transfers between devices, exchange(): return lax.all_to_all(pieces, axis, split_axis=0, concat_axis=0, tiled=True)  19.8 us
    ppermute x6, starting transfers between devices, from_x(): return lax.ppermute(payload, 'x', [(i, (i - s) % X) for i in range(X)])  19 us
    all_to_all x3, waiting for transfers between devices, exchange(): return lax.all_to_all(pieces, axis, split_axis=0, concat_axis=0, tiled=True)  12.6 us
  transfers between devices with their start and end apart: 9, of which 3 were waited for; matrix products, arithmetic and copies ran while one was open for 0% of the time, Pallas kernels for 2%

profile of v11, /device:TPU:1, one launch (start us, length us, event | category | flops | bytes accessed | tf_op | source)
XLA Modules:
  0.0 175.4 jit_solution(9171307607723638883)
XLA Ops:
  0.0 2.8 %up_product.1 = (bf16[8,384,128]{2,1,0:T(8,128)(2,1)}, bf16[8,128,128]{2,1,0:T(8,128)(2,1)}) custom-call(bf16[384,128]{1,0:T(8,128)(2,1)} %tokens_ref.3, f32[2,128]{1,0:T(2,128)} %pre_ref.1, f32[2,128,1024]{2,1,0:T(8,128)} %up_ref.1, f32[2,1024]{1,0:T(2,128)} %scale_ref.5, f32[2,1024,128]{2,1,0:T(8,128)} %down_ref.3), custom_call_target="tpu_custom_call" | custom-call | tf_op jit(solution)/shard_map/up_product/pallas_call | solution.py:90
  2.8 34.8 %all_to_all.45 = bf16[32,96,128]{2,1,0:T(8,128)(2,1)S(1)} all-to-all(bf16[32,96,128]{2,1,0:T(8,128)(2,1)} %bitcast.20), channel_id=1, replica_groups=mesh['z'=8,'x'=4,'y'=8,'core'=2] {'z','x'}, dimensions={0} | all-to-all | bytes 1572864 | tf_op jit(solution)/shard_map/all_to_all | solution.py:19
  37.6 0.0 copy-start.1
  37.6 0.1 convert_reduce_fusion
  37.8 0.7 broadcast_in_dim.4
  38.5 4.1 %all-to-all-start.1 = ((bf16[8,96,128]{2,1,0:T(8,128)(2,1)}), bf16[8,96,128]{2,1,0:T(8,128)(2,1)S(1)}, u32[]{:S(2)}, u32[]{:S(2)}) async-start(bf16[8,96,128]{2,1,0:T(8,128)(2,1)} %broadcast_in_dim.4), calls=%async_computation.1 | async-start | bytes 393216 | tf_op jit(solution)/shard_map/all_to_all | solution.py:19
  42.6 0.0 copy-done.1
  42.6 3.0 %collective-permute-start.2 = (bf16[8,128,128]{2,1,0:T(8,128)(2,1)S(1)}, bf16[8,128,128]{2,1,0:T(8,128)(2,1)S(1)}, u32[]{:S(2)}, u32[]{:S(2)}) collective-permute-start(bf16[8,128,128]{2,1,0:T(8,128)(2,1)S(1)} %copy-done.1), channel_id=1, source_target_pairs={{0,16},{16,32},{32,48},{48,0},{1,17},{17,33},{33,49},{49,1},{2,18}... | collective-permute-start | bytes 786440 | tf_op jit(solution)/shard_map/ppermute | solution.py:406
  45.6 4.1 %collective-permute-start.1 = (bf16[8,128,128]{2,1,0:T(8,128)(2,1)S(1)}, bf16[8,128,128]{2,1,0:T(8,128)(2,1)S(1)}, u32[]{:S(2)}, u32[]{:S(2)}) collective-permute-start(bf16[8,128,128]{2,1,0:T(8,128)(2,1)S(1)} %copy-done.1), channel_id=1, source_target_pairs={{0,32},{16,48},{32,0},{48,16},{1,33},{17,49},{33,1},{49,17},{2,34}... | collective-permute-start | bytes 786440 | tf_op jit(solution)/shard_map/ppermute | solution.py:406
  49.8 2.7 %collective-permute-start = (bf16[8,128,128]{2,1,0:T(8,128)(2,1)S(1)}, bf16[8,128,128]{2,1,0:T(8,128)(2,1)S(1)}, u32[]{:S(2)}, u32[]{:S(2)}) collective-permute-start(bf16[8,128,128]{2,1,0:T(8,128)(2,1)S(1)} %copy-done.1), channel_id=1, source_target_pairs={{0,48},{16,0},{32,16},{48,32},{1,49},{17,1},{33,17},{49,33},{2,50}... | collective-permute-start | bytes 786440 | tf_op jit(solution)/shard_map/ppermute | solution.py:406
  52.5 2.5 %packed.1 = (bf16[17,128,128]{2,1,0:T(8,128)(2,1)}, bf16[17,128,128]{2,1,0:T(8,128)(2,1)}, bf16[17,128,128]{2,1,0:T(8,128)(2,1)}, bf16[112,128]{1,0:T(8,128)(2,1)S(1)}) custom-call(f32[2,1024,128]{2,1,0:T(8,128)} %down_ref.3, f32[2,128,1024]{2,1,0:T(8,128)} %up_ref.1, bf16[384,128]{1,0:T(8,128)(2,1)} %tokens_ref.3, f32[2,128]{1,0:T(2,128)} %scale_ref.4, ...), custom_call_target="tpu_custom_call" | custom-call | tf_op jit(solution)/shard_map/packed/pallas_call | solution.py:143
  55.0 0.0 copy-start
  55.0 2.9 %collective-permute-start.4 = (bf16[17,128,128]{2,1,0:T(8,128)(2,1)}, bf16[17,128,128]{2,1,0:T(8,128)(2,1)S(1)}, u32[]{:S(2)}, u32[]{:S(2)}) collective-permute-start(bf16[17,128,128]{2,1,0:T(8,128)(2,1)} %get-tuple-element.31), channel_id=1, source_target_pairs={{0,32},{16,48},{32,0},{48,16},{1,33},{17,49},{33,1},{49,17},{2,34}... | collective-permute-start | bytes 1671176 | tf_op jit(solution)/shard_map/ppermute | solution.py:406
  58.0 1.9 %collective-permute-start.5 = (bf16[17,128,128]{2,1,0:T(8,128)(2,1)}, bf16[17,128,128]{2,1,0:T(8,128)(2,1)S(1)}, u32[]{:S(2)}, u32[]{:S(2)}) collective-permute-start(bf16[17,128,128]{2,1,0:T(8,128)(2,1)} %get-tuple-element.33), channel_id=1, source_target_pairs={{0,16},{16,32},{32,48},{48,0},{1,17},{17,33},{33,49},{49,1},{2,18}... | collective-permute-start | bytes 1671176 | tf_op jit(solution)/shard_map/ppermute | solution.py:406
  59.9 0.0 collective-permute-done.2.refs_5_
  59.9 0.0 all-to-all-done.1.refs_1_
  59.9 0.0 collective-permute-done.1.refs_4_
  59.9 0.1 collective-permute-done.refs_3_
  60.0 1.8 %down_product.2 = bf16[4,96,128]{2,1,0:T(8,128)(2,1)} custom-call(f32[96,128]{1,0:T(8,128)S(1)} %fusion.1.refs_0_, bf16[8,96,128]{2,1,0:T(8,128)(2,1)S(1)} %all-to-all-done.1.refs_1_, bf16[8,128,128]{2,1,0:T(8,128)(2,1)} %get-tuple-element.24.refs_2_, bf16[8,128,128]{2,1,0:T(8,128)(2,1)S(1)} %collective-permute-done.refs_3_, ...), custom_call_target="tpu_custom_call" | custom-call | tf_op jit(solution)/shard_map/down_product/pallas_call | solution.py:190
  61.8 12.2 %all-to-all-start.2 = ((bf16[16,24,128]{2,1,0:T(8,128)(2,1)}), bf16[16,24,128]{2,1,0:T(8,128)(2,1)S(1)}, u32[]{:S(2)}, u32[]{:S(2)}) async-start(bf16[16,24,128]{2,1,0:T(8,128)(2,1)} %bitcast.2), calls=%async_computation.2 | async-start | bytes 196608 | tf_op jit(solution)/shard_map/all_to_all | solution.py:19
  74.1 0.0 copy-done
  74.1 4.3 %collective-permute-start.3 = (bf16[17,128,128]{2,1,0:T(8,128)(2,1)S(1)}, bf16[17,128,128]{2,1,0:T(8,128)(2,1)S(1)}, u32[]{:S(2)}, u32[]{:S(2)}) collective-permute-start(bf16[17,128,128]{2,1,0:T(8,128)(2,1)S(1)} %copy-done), channel_id=1, source_target_pairs={{0,48},{16,0},{32,16},{48,32},{1,49},{17,1},{33,17},{49,33},{2,50}... | collective-permute-start | bytes 1671176 | tf_op jit(solution)/shard_map/ppermute | solution.py:406
  78.4 4.1 %all-to-all-done.2 = bf16[16,24,128]{2,1,0:T(8,128)(2,1)S(1)} async-done(((bf16[16,24,128]{2,1,0:T(8,128)(2,1)}), bf16[16,24,128]{2,1,0:T(8,128)(2,1)S(1)}, u32[]{:S(2)}, u32[]{:S(2)}) %all-to-all-start.2) | async-done | bytes 98336 | tf_op jit(solution)/shard_map/all_to_all | solution.py:19
  82.5 0.7 broadcast_in_dim.5
  83.2 3.4 %all-to-all-start.3 = ((bf16[16,24,128]{2,1,0:T(8,128)(2,1)}), bf16[16,24,128]{2,1,0:T(8,128)(2,1)S(1)}, u32[]{:S(2)}, u32[]{:S(2)}) async-start(bf16[16,24,128]{2,1,0:T(8,128)(2,1)} %broadcast_in_dim.5), calls=%async_computation.3 | async-start | bytes 196608 | tf_op jit(solution)/shard_map/all_to_all | solution.py:19
  86.6 0.0 collective-permute-done.4.refs_2_.refs_4_
  86.6 8.4 %all-to-all-done.3 = bf16[16,24,128]{2,1,0:T(8,128)(2,1)S(1)} async-done(((bf16[16,24,128]{2,1,0:T(8,128)(2,1)}), bf16[16,24,128]{2,1,0:T(8,128)(2,1)S(1)}, u32[]{:S(2)}, u32[]{:S(2)}) %all-to-all-start.3) | async-done | bytes 98336 | tf_op jit(solution)/shard_map/all_to_all | solution.py:19
  95.0 0.0 collective-permute-done.5.refs_3_.refs_5_
  95.1 0.0 collective-permute-done.3.refs_1_.refs_3_
  95.1 2.4 %turn.1 = (bf16[8,200,128]{2,1,0:T(8,128)(2,1)S(1)}, f32[4,96,128]{2,1,0:T(8,128)S(1)}, f32[4,96,128]{2,1,0:T(8,128)S(1)}, f32[4,8,128]{2,1,0:T(8,128)S(1)}) custom-call(f32[96,128]{1,0:T(8,128)S(1)} %bitcast_convert_fusion.lead_ref, bf16[4,96,128]{2,1,0:T(8,128)(2,1)S(1)} %bitcast.19, bf16[112,128]{1,0:T(8,128)(2,1)S(1)} %get-tuple-element.28.own_ref, ...), custom_call_target="tpu_custom_call" | custom-call | tf_op jit(solution)/shard_map/turn/pallas_call | solution.py:284
  97.4 22.5 %all_to_all.46.refs_0_ = bf16[8,200,128]{2,1,0:T(8,128)(2,1)S(1)} all-to-all(bf16[8,200,128]{2,1,0:T(8,128)(2,1)S(1)} %get-tuple-element.35), channel_id=1, replica_groups=mesh['z'=8,'x'=4,'y'=8,'core'=2] {'z'}, dimensions={0} | all-to-all | bytes 819200 | tf_op jit(solution)/shard_map/all_to_all | solution.py:19
  120.0 0.1 second_hidden.1
  120.1 12.1 %all_to_all.47.refs_1_ = bf16[8,96,128]{2,1,0:T(8,128)(2,1)S(1)} all-to-all(bf16[8,96,128]{2,1,0:T(8,128)(2,1)S(1)} %get-tuple-element.38), channel_id=1, replica_groups=mesh['z'=8,'x'=4,'y'=8,'core'=2] {'z'}, dimensions={0} | all-to-all | bytes 393216 | tf_op jit(solution)/shard_map/all_to_all | solution.py:19
  132.2 1.2 down_product.3
  133.4 13.3 %all_to_all.48.sum_ref = bf16[16,4,8,128]{3,2,1,0:T(8,128)(2,1)S(1)} all-to-all(bf16[16,4,8,128]{3,2,1,0:T(8,128)(2,1)S(1)} %down_product.3), channel_id=1, replica_groups=mesh['z'=8,'x'=4,'y'=8,'core'=2] {'y','core'}, dimensions={0} | all-to-all | bytes 262144 | tf_op jit(solution)/shard_map/all_to_all | solution.py:19
  146.7 0.2 shares.1
  146.9 14.4 %all_to_all.49.refs_0_ = bf16[32,24,128]{2,1,0:T(8,128)(2,1)S(1)} all-to-all(bf16[32,24,128]{2,1,0:T(8,128)(2,1)S(1)} %shares.1), channel_id=1, replica_groups=mesh['z'=8,'x'=4,'y'=8,'core'=2] {'z','x'}, dimensions={0} | all-to-all | bytes 393216 | tf_op jit(solution)/shard_map/all_to_all | solution.py:19
  161.4 0.1 last.1
  161.5 13.2 %all_to_all.50 = bf16[16,4,8,128]{3,2,1,0:T(8,128)(2,1)S(1)} all-to-all(bf16[16,4,8,128]{3,2,1,0:T(8,128)(2,1)S(1)} %last.1), channel_id=1, replica_groups=mesh['z'=8,'x'=4,'y'=8,'core'=2] {'y','core'}, dimensions={0} | all-to-all | bytes 262144 | tf_op jit(solution)/shard_map/all_to_all | solution.py:19
  174.8 0.7 copy.8
  (7 shorter events, 0.1 us)
Async XLA Ops:
  37.6 5.0 %copy-start.1 = (bf16[8,128,128]{2,1,0:T(8,128)(2,1)S(1)}, bf16[8,128,128]{2,1,0:T(8,128)(2,1)}, u32[]{:S(2)}) copy-start(bf16[8,128,128]{2,1,0:T(8,128)(2,1)} %get-tuple-element.24.refs_2_) | copy-start | bytes 786436
  38.5 21.4 %all-to-all-start.1 = ((bf16[8,96,128]{2,1,0:T(8,128)(2,1)}), bf16[8,96,128]{2,1,0:T(8,128)(2,1)S(1)}, u32[]{:S(2)}, u32[]{:S(2)}) async-start(bf16[8,96,128]{2,1,0:T(8,128)(2,1)} %broadcast_in_dim.4), calls=%async_computation.1 | async-start | bytes 393216 | tf_op jit(solution)/shard_map/all_to_all | solution.py:19
  42.6 17.3 %collective-permute-start.2 = (bf16[8,128,128]{2,1,0:T(8,128)(2,1)S(1)}, bf16[8,128,128]{2,1,0:T(8,128)(2,1)S(1)}, u32[]{:S(2)}, u32[]{:S(2)}) collective-permute-start(bf16[8,128,128]{2,1,0:T(8,128)(2,1)S(1)} %copy-done.1), channel_id=1, source_target_pairs={{0,16},{16,32},{32,48},{48,0},{1,17},{17,33},{33,49},{49,1},{2,18}... | collective-permute-start | bytes 786440 | tf_op jit(solution)/shard_map/ppermute | solution.py:406
  45.6 14.3 %collective-permute-start.1 = (bf16[8,128,128]{2,1,0:T(8,128)(2,1)S(1)}, bf16[8,128,128]{2,1,0:T(8,128)(2,1)S(1)}, u32[]{:S(2)}, u32[]{:S(2)}) collective-permute-start(bf16[8,128,128]{2,1,0:T(8,128)(2,1)S(1)} %copy-done.1), channel_id=1, source_target_pairs={{0,32},{16,48},{32,0},{48,16},{1,33},{17,49},{33,1},{49,17},{2,34}... | collective-permute-start | bytes 786440 | tf_op jit(solution)/shard_map/ppermute | solution.py:406
  49.8 10.2 %collective-permute-start = (bf16[8,128,128]{2,1,0:T(8,128)(2,1)S(1)}, bf16[8,128,128]{2,1,0:T(8,128)(2,1)S(1)}, u32[]{:S(2)}, u32[]{:S(2)}) collective-permute-start(bf16[8,128,128]{2,1,0:T(8,128)(2,1)S(1)} %copy-done.1), channel_id=1, source_target_pairs={{0,48},{16,0},{32,16},{48,32},{1,49},{17,1},{33,17},{49,33},{2,50}... | collective-permute-start | bytes 786440 | tf_op jit(solution)/shard_map/ppermute | solution.py:406
  55.0 19.0 %copy-start = (bf16[17,128,128]{2,1,0:T(8,128)(2,1)S(1)}, bf16[17,128,128]{2,1,0:T(8,128)(2,1)}, u32[]{:S(2)}) copy-start(bf16[17,128,128]{2,1,0:T(8,128)(2,1)} %get-tuple-element.29.refs_0_.refs_2_) | copy-start | bytes 1671172
  55.0 31.6 %collective-permute-start.4 = (bf16[17,128,128]{2,1,0:T(8,128)(2,1)}, bf16[17,128,128]{2,1,0:T(8,128)(2,1)S(1)}, u32[]{:S(2)}, u32[]{:S(2)}) collective-permute-start(bf16[17,128,128]{2,1,0:T(8,128)(2,1)} %get-tuple-element.31), channel_id=1, source_target_pairs={{0,32},{16,48},{32,0},{48,16},{1,33},{17,49},{33,1},{49,17},{2,34}... | collective-permute-start | bytes 1671176 | tf_op jit(solution)/shard_map/ppermute | solution.py:406
  58.0 37.1 %collective-permute-start.5 = (bf16[17,128,128]{2,1,0:T(8,128)(2,1)}, bf16[17,128,128]{2,1,0:T(8,128)(2,1)S(1)}, u32[]{:S(2)}, u32[]{:S(2)}) collective-permute-start(bf16[17,128,128]{2,1,0:T(8,128)(2,1)} %get-tuple-element.33), channel_id=1, source_target_pairs={{0,16},{16,32},{32,48},{48,0},{1,17},{17,33},{33,49},{49,1},{2,18}... | collective-permute-start | bytes 1671176 | tf_op jit(solution)/shard_map/ppermute | solution.py:406
  61.8 20.7 %all-to-all-start.2 = ((bf16[16,24,128]{2,1,0:T(8,128)(2,1)}), bf16[16,24,128]{2,1,0:T(8,128)(2,1)S(1)}, u32[]{:S(2)}, u32[]{:S(2)}) async-start(bf16[16,24,128]{2,1,0:T(8,128)(2,1)} %bitcast.2), calls=%async_computation.2 | async-start | bytes 196608 | tf_op jit(solution)/shard_map/all_to_all | solution.py:19
  74.1 21.0 %collective-permute-start.3 = (bf16[17,128,128]{2,1,0:T(8,128)(2,1)S(1)}, bf16[17,128,128]{2,1,0:T(8,128)(2,1)S(1)}, u32[]{:S(2)}, u32[]{:S(2)}) collective-permute-start(bf16[17,128,128]{2,1,0:T(8,128)(2,1)S(1)} %copy-done), channel_id=1, source_target_pairs={{0,48},{16,0},{32,16},{48,32},{1,49},{17,1},{33,17},{49,33},{2,50}... | collective-permute-start | bytes 1671176 | tf_op jit(solution)/shard_map/ppermute | solution.py:406
  83.2 11.8 %all-to-all-start.3 = ((bf16[16,24,128]{2,1,0:T(8,128)(2,1)}), bf16[16,24,128]{2,1,0:T(8,128)(2,1)S(1)}, u32[]{:S(2)}, u32[]{:S(2)}) async-start(bf16[16,24,128]{2,1,0:T(8,128)(2,1)} %broadcast_in_dim.5), calls=%async_computation.3 | async-start | bytes 196608 | tf_op jit(solution)/shard_map/all_to_all | solution.py:19

commit v12 on v10

--- a/solution.py
+++ b/solution.py
@@ -129,7 +129,8 @@
             ref[...] = jnp.concatenate(block, axis=0)
             continue
         for c in range(n):
-            ref[c] = up_ref[0, :, c * feats : (c + 1) * feats].astype(bf16)
+            block_at = c % 2 * (n // 2) + c // 2
+            ref[block_at] = up_ref[0, :, c * feats : (c + 1) * feats].astype(bf16)
         ref[n : 2 * n] = down
         ref[2 * n] = jnp.concatenate([*block, rest], axis=0)
 
@@ -163,17 +164,21 @@
 
 def down_kernel(start, lead_ref, hidden_ref, *refs):
     weights, out_ref, held, sems = refs[:X], refs[X], refs[X + 1], refs[X + 2]
+    feats = out_ref.shape[2]
     copies = []
     for i, w in enumerate(weights):
-        blocks = w.at[pl.ds(start, held.shape[1])]
-        copies.append(pltpu.make_async_copy(blocks, held.at[i], sems.at[i]))
+        here = held.at[i // 2, :, :, pl.ds(i % 2 * feats, feats)]
+        copies.append(pltpu.make_async_copy(w.at[pl.ds(start, held.shape[1])], here, sems.at[i]))
         copies[-1].start()
     hidden = [lead_ref[...].astype(bf16), *(hidden_ref[z] for z in range(1, Z))]
     hidden = jnp.concatenate(hidden, axis=1)
-    for i in (1, 2, 3, 0):
-        copies[i].wait()
-        weight = held[i].reshape(hidden.shape[1], -1)
-        out_ref[i] = jnp.dot(hidden, weight, preferred_element_type=f32).astype(bf16)
+    for pair in (1, 0):
+        for i in (2 * pair, 2 * pair + 1):
+            copies[i].wait()
+        weight = held[pair].reshape(hidden.shape[1], 2 * feats)
+        part = jnp.dot(hidden, weight, preferred_element_type=f32).astype(bf16)
+        out_ref[2 * pair] = part[:, :feats]
+        out_ref[2 * pair + 1] = part[:, feats:]
 
 
 def down_product(hidden, blocks, start):
@@ -186,7 +191,7 @@
         in_specs=[*[VMEM] * 2, *[ANY] * X],
         out_specs=VMEM,
         scratch_shapes=[
-            pltpu.VMEM((X, Z * share // feats, feats, feats), bf16),
+            pltpu.VMEM((X // 2, Z * share // feats, feats, 2 * feats), bf16),
             pltpu.SemaphoreType.DMA((X,)),
         ],
         compiler_params=limit(8),
@@ -235,9 +240,11 @@
         copies[-1].start()
     held_copies = []
     for i in range(X):
-        here = held.at[:, pl.ds(i * feats, feats)]
-        held_copies.append(pltpu.make_async_copy(blocks[i].at[pl.ds(0, Z)], here, held_sems.at[i]))
-        held_copies[-1].start()
+        for odd in range(2):
+            here = held.at[:, pl.ds(i * feats, feats), pl.ds(odd * feats, feats)]
+            half = blocks[i].at[pl.ds(odd * Z // 2, Z // 2)]
+            held_copies.append(pltpu.make_async_copy(half, here, held_sems.at[i, odd]))
+            held_copies[-1].start()
     for copy in copies:
         copy.wait()
     kept_terms, branch_terms, branches = [], [], []
@@ -263,12 +270,15 @@
     )
     for copy in held_copies:
         copy.wait()
-    for c in range(Z):
-        part = jnp.dot(terms, held[c], preferred_element_type=f32)
-        scale = scales[1:2, c * feats : (c + 1) * feats]
-        out_ref[c, : 2 * t] = (part * scale).astype(bf16)
-        out_ref[c, 2 * t :] = jnp.zeros((8, feats), bf16)
-        out_ref[c, 2 * t :, :t] = squares
+    for pair in range(Z // 2):
+        part = jnp.dot(terms, held[pair], preferred_element_type=f32)
+        scale = scales[1:2, pair * 2 * feats : (pair + 1) * 2 * feats]
+        part = (part * scale).astype(bf16)
+        for c in (2 * pair, 2 * pair + 1):
+            at = c % 2 * feats
+            out_ref[c, : 2 * t] = part[:, at : at + feats]
+            out_ref[c, 2 * t :] = jnp.zeros((8, feats), bf16)
+            out_ref[c, 2 * t :, :t] = squares
 
 
 def turn(summed, own, scale, blocks):
@@ -286,10 +296,10 @@
         out_specs=(VMEM,) * 4,
         scratch_shapes=[
             pltpu.VMEM((X - 1, 16 + t, feats), bf16),
-            pltpu.VMEM((Z, X * feats, feats), bf16),
+            pltpu.VMEM((Z // 2, X * feats, 2 * feats), bf16),
             pltpu.VMEM(scale.shape, f32),
             pltpu.SemaphoreType.DMA((X,)),
-            pltpu.SemaphoreType.DMA((X,)),
+            pltpu.SemaphoreType.DMA((X, 2)),
         ],
         compiler_params=limit(12),
         name="turn",

time: 176 us -> 176 us (level)
  transfers between devices with their start and end apart: 9 -> 9, of which waited for: 3 -> 3; matrix products, arithmetic and copies ran while one was open for 0% -> 0% of each run, Pallas kernels for 2% -> 3%
where the time goes in v12:
time: 176 us; the launch traced here: 175 us
  blocking collectives  110 us (62%)
  starting transfers between devices  38.8 us (22%)
  waiting for transfers between devices  12.7 us (7%)
  Pallas kernels  11.2 us (6%)
  local copies, waits for them, and re-layouts  2.04 us (1%)
    all_to_all x7, blocking collectives, exchange(): return lax.all_to_all(pieces, axis, split_axis=0, concat_axis=0, tiled=True)  110 us
    all_to_all x3, starting transfers between devices, exchange(): return lax.all_to_all(pieces, axis, split_axis=0, concat_axis=0, tiled=True)  19.8 us
    ppermute x6, starting transfers between devices, from_x(): return lax.ppermute(payload, 'x', [(i, (i - s) % X) for i in range(X)])  19 us
    all_to_all x3, waiting for transfers between devices, exchange(): return lax.all_to_all(pieces, axis, split_axis=0, concat_axis=0, tiled=True)  12.6 us
  transfers between devices with their start and end apart: 9, of which 3 were waited for; matrix products, arithmetic and copies ran while one was open for 0% of the time, Pallas kernels for 3%

profile of v12, /device:TPU:1, one launch (start us, length us, event | category | flops | bytes accessed | tf_op | source)
XLA Modules:
  0.0 174.8 jit_solution(3862621984247457452)
XLA Ops:
  0.0 2.8 %up_product.1 = (bf16[8,384,128]{2,1,0:T(8,128)(2,1)}, bf16[8,128,128]{2,1,0:T(8,128)(2,1)}) custom-call(bf16[384,128]{1,0:T(8,128)(2,1)} %tokens_ref.3, f32[2,128]{1,0:T(2,128)} %pre_ref.1, f32[2,128,1024]{2,1,0:T(8,128)} %up_ref.1, f32[2,1024]{1,0:T(2,128)} %scale_ref.5, f32[2,1024,128]{2,1,0:T(8,128)} %down_ref.3), custom_call_target="tpu_custom_call" | custom-call | tf_op jit(solution)/shard_map/up_product/pallas_call | solution.py:90
  2.9 34.8 %all_to_all.50 = bf16[32,96,128]{2,1,0:T(8,128)(2,1)S(1)} all-to-all(bf16[32,96,128]{2,1,0:T(8,128)(2,1)} %bitcast.23), channel_id=1, replica_groups=mesh['z'=8,'x'=4,'y'=8,'core'=2] {'z','x'}, dimensions={0} | all-to-all | bytes 1572864 | tf_op jit(solution)/shard_map/all_to_all | solution.py:19
  37.6 0.0 copy-start.1
  37.6 0.1 convert_reduce_fusion
  37.8 0.7 broadcast_in_dim.6
  38.5 4.1 %all-to-all-start.1 = ((bf16[8,96,128]{2,1,0:T(8,128)(2,1)}), bf16[8,96,128]{2,1,0:T(8,128)(2,1)S(1)}, u32[]{:S(2)}, u32[]{:S(2)}) async-start(bf16[8,96,128]{2,1,0:T(8,128)(2,1)} %broadcast_in_dim.6), calls=%async_computation.1 | async-start | bytes 393216 | tf_op jit(solution)/shard_map/all_to_all | solution.py:19
  42.6 0.0 copy-done.1
  42.6 3.0 %collective-permute-start.2 = (bf16[8,128,128]{2,1,0:T(8,128)(2,1)S(1)}, bf16[8,128,128]{2,1,0:T(8,128)(2,1)S(1)}, u32[]{:S(2)}, u32[]{:S(2)}) collective-permute-start(bf16[8,128,128]{2,1,0:T(8,128)(2,1)S(1)} %copy-done.1), channel_id=1, source_target_pairs={{0,16},{16,32},{32,48},{48,0},{1,17},{17,33},{33,49},{49,1},{2,18}... | collective-permute-start | bytes 786440 | tf_op jit(solution)/shard_map/ppermute | solution.py:389
  45.6 4.1 %collective-permute-start.1 = (bf16[8,128,128]{2,1,0:T(8,128)(2,1)S(1)}, bf16[8,128,128]{2,1,0:T(8,128)(2,1)S(1)}, u32[]{:S(2)}, u32[]{:S(2)}) collective-permute-start(bf16[8,128,128]{2,1,0:T(8,128)(2,1)S(1)} %copy-done.1), channel_id=1, source_target_pairs={{0,32},{16,48},{32,0},{48,16},{1,33},{17,49},{33,1},{49,17},{2,34}... | collective-permute-start | bytes 786440 | tf_op jit(solution)/shard_map/ppermute | solution.py:389
  49.8 2.7 %collective-permute-start = (bf16[8,128,128]{2,1,0:T(8,128)(2,1)S(1)}, bf16[8,128,128]{2,1,0:T(8,128)(2,1)S(1)}, u32[]{:S(2)}, u32[]{:S(2)}) collective-permute-start(bf16[8,128,128]{2,1,0:T(8,128)(2,1)S(1)} %copy-done.1), channel_id=1, source_target_pairs={{0,48},{16,0},{32,16},{48,32},{1,49},{17,1},{33,17},{49,33},{2,50}... | collective-permute-start | bytes 786440 | tf_op jit(solution)/shard_map/ppermute | solution.py:389
  52.6 2.5 %packed.1 = (bf16[17,128,128]{2,1,0:T(8,128)(2,1)}, bf16[17,128,128]{2,1,0:T(8,128)(2,1)}, bf16[17,128,128]{2,1,0:T(8,128)(2,1)}, bf16[112,128]{1,0:T(8,128)(2,1)S(1)}) custom-call(f32[2,1024,128]{2,1,0:T(8,128)} %down_ref.3, f32[2,128,1024]{2,1,0:T(8,128)} %up_ref.1, bf16[384,128]{1,0:T(8,128)(2,1)} %tokens_ref.3, f32[2,128]{1,0:T(2,128)} %scale_ref.4, ...), custom_call_target="tpu_custom_call" | custom-call | tf_op jit(solution)/shard_map/packed/pallas_call | solution.py:144
  55.1 0.0 copy-start
  55.1 2.9 %collective-permute-start.4 = (bf16[17,128,128]{2,1,0:T(8,128)(2,1)}, bf16[17,128,128]{2,1,0:T(8,128)(2,1)S(1)}, u32[]{:S(2)}, u32[]{:S(2)}) collective-permute-start(bf16[17,128,128]{2,1,0:T(8,128)(2,1)} %get-tuple-element.31), channel_id=1, source_target_pairs={{0,32},{16,48},{32,0},{48,16},{1,33},{17,49},{33,1},{49,17},{2,34}... | collective-permute-start | bytes 1671176 | tf_op jit(solution)/shard_map/ppermute | solution.py:389
  58.0 1.9 %collective-permute-start.5 = (bf16[17,128,128]{2,1,0:T(8,128)(2,1)}, bf16[17,128,128]{2,1,0:T(8,128)(2,1)S(1)}, u32[]{:S(2)}, u32[]{:S(2)}) collective-permute-start(bf16[17,128,128]{2,1,0:T(8,128)(2,1)} %get-tuple-element.33), channel_id=1, source_target_pairs={{0,16},{16,32},{32,48},{48,0},{1,17},{17,33},{33,49},{49,1},{2,18}... | collective-permute-start | bytes 1671176 | tf_op jit(solution)/shard_map/ppermute | solution.py:389
  59.9 0.0 collective-permute-done.2.refs_5_
  59.9 0.0 all-to-all-done.1.refs_1_
  59.9 0.0 collective-permute-done.1.refs_4_
  59.9 0.1 collective-permute-done.refs_3_
  60.0 1.9 %down_product.2 = bf16[4,96,128]{2,1,0:T(8,128)(2,1)} custom-call(f32[96,128]{1,0:T(8,128)S(1)} %fusion.1.refs_0_, bf16[8,96,128]{2,1,0:T(8,128)(2,1)S(1)} %all-to-all-done.1.refs_1_, bf16[8,128,128]{2,1,0:T(8,128)(2,1)} %get-tuple-element.24.refs_2_, bf16[8,128,128]{2,1,0:T(8,128)(2,1)S(1)} %collective-permute-done.refs_3_, ...), custom_call_target="tpu_custom_call" | custom-call | tf_op jit(solution)/shard_map/down_product/pallas_call | solution.py:188
  61.9 12.2 %all-to-all-start.2 = ((bf16[16,24,128]{2,1,0:T(8,128)(2,1)}), bf16[16,24,128]{2,1,0:T(8,128)(2,1)S(1)}, u32[]{:S(2)}, u32[]{:S(2)}) async-start(bf16[16,24,128]{2,1,0:T(8,128)(2,1)} %bitcast.2), calls=%async_computation.2 | async-start | bytes 196608 | tf_op jit(solution)/shard_map/all_to_all | solution.py:19
  74.2 0.0 copy-done
  74.2 4.3 %collective-permute-start.3 = (bf16[17,128,128]{2,1,0:T(8,128)(2,1)S(1)}, bf16[17,128,128]{2,1,0:T(8,128)(2,1)S(1)}, u32[]{:S(2)}, u32[]{:S(2)}) collective-permute-start(bf16[17,128,128]{2,1,0:T(8,128)(2,1)S(1)} %copy-done), channel_id=1, source_target_pairs={{0,48},{16,0},{32,16},{48,32},{1,49},{17,1},{33,17},{49,33},{2,50}... | collective-permute-start | bytes 1671176 | tf_op jit(solution)/shard_map/ppermute | solution.py:389
  78.5 4.1 %all-to-all-done.2 = bf16[16,24,128]{2,1,0:T(8,128)(2,1)S(1)} async-done(((bf16[16,24,128]{2,1,0:T(8,128)(2,1)}), bf16[16,24,128]{2,1,0:T(8,128)(2,1)S(1)}, u32[]{:S(2)}, u32[]{:S(2)}) %all-to-all-start.2) | async-done | bytes 98336 | tf_op jit(solution)/shard_map/all_to_all | solution.py:19
  82.7 0.7 broadcast_in_dim.7
  83.3 3.4 %all-to-all-start.3 = ((bf16[16,24,128]{2,1,0:T(8,128)(2,1)}), bf16[16,24,128]{2,1,0:T(8,128)(2,1)S(1)}, u32[]{:S(2)}, u32[]{:S(2)}) async-start(bf16[16,24,128]{2,1,0:T(8,128)(2,1)} %broadcast_in_dim.7), calls=%async_computation.3 | async-start | bytes 196608 | tf_op jit(solution)/shard_map/all_to_all | solution.py:19
  86.7 0.0 collective-permute-done.4.refs_2_.refs_4_
  86.7 8.4 %all-to-all-done.3 = bf16[16,24,128]{2,1,0:T(8,128)(2,1)S(1)} async-done(((bf16[16,24,128]{2,1,0:T(8,128)(2,1)}), bf16[16,24,128]{2,1,0:T(8,128)(2,1)S(1)}, u32[]{:S(2)}, u32[]{:S(2)}) %all-to-all-start.3) | async-done | bytes 98336 | tf_op jit(solution)/shard_map/all_to_all | solution.py:19
  95.1 0.0 collective-permute-done.5.refs_3_.refs_5_
  95.2 0.0 collective-permute-done.3.refs_1_.refs_3_
  95.2 2.0 %turn.1 = (bf16[8,200,128]{2,1,0:T(8,128)(2,1)S(1)}, f32[4,96,128]{2,1,0:T(8,128)S(1)}, f32[4,96,128]{2,1,0:T(8,128)S(1)}, f32[4,8,128]{2,1,0:T(8,128)S(1)}) custom-call(f32[96,128]{1,0:T(8,128)S(1)} %bitcast_convert_fusion.lead_ref, bf16[4,96,128]{2,1,0:T(8,128)(2,1)S(1)} %bitcast.21, bf16[112,128]{1,0:T(8,128)(2,1)S(1)} %get-tuple-element.28.own_ref, ...), custom_call_target="tpu_custom_call" | custom-call | tf_op jit(solution)/shard_map/turn/pallas_call | solution.py:287
  97.2 22.5 %all_to_all.51.refs_0_ = bf16[8,200,128]{2,1,0:T(8,128)(2,1)S(1)} all-to-all(bf16[8,200,128]{2,1,0:T(8,128)(2,1)S(1)} %get-tuple-element.35), channel_id=1, replica_groups=mesh['z'=8,'x'=4,'y'=8,'core'=2] {'z'}, dimensions={0} | all-to-all | bytes 819200 | tf_op jit(solution)/shard_map/all_to_all | solution.py:19
  119.8 0.1 second_hidden.1
  119.9 12.1 %all_to_all.52.refs_1_ = bf16[8,96,128]{2,1,0:T(8,128)(2,1)S(1)} all-to-all(bf16[8,96,128]{2,1,0:T(8,128)(2,1)S(1)} %get-tuple-element.38), channel_id=1, replica_groups=mesh['z'=8,'x'=4,'y'=8,'core'=2] {'z'}, dimensions={0} | all-to-all | bytes 393216 | tf_op jit(solution)/shard_map/all_to_all | solution.py:19
  132.0 1.3 down_product.3
  133.3 12.6 %all_to_all.53 = bf16[16,24,128]{2,1,0:T(8,128)(2,1)S(1)} all-to-all(bf16[16,24,128]{2,1,0:T(8,128)(2,1)S(1)} %bitcast.22), channel_id=1, replica_groups=mesh['z'=8,'x'=4,'y'=8,'core'=2] {'y','core'}, dimensions={0} | all-to-all | bytes 196608 | tf_op jit(solution)/shard_map/all_to_all | solution.py:19
  145.9 10.9 %all_to_all.54 = bf16[16,24,128]{2,1,0:T(8,128)(2,1)S(1)} all-to-all(bf16[16,24,128]{2,1,0:T(8,128)(2,1)S(1)} %broadcast_in_dim.8), channel_id=1, replica_groups=mesh['z'=8,'x'=4,'y'=8,'core'=2] {'y','core'}, dimensions={0} | all-to-all | bytes 196608 | tf_op jit(solution)/shard_map/all_to_all | solution.py:19
  156.8 0.4 squares.1
  157.2 9.3 %all_to_all.55.refs_0_ = f32[8,8,128]{2,1,0:T(8,128)S(1)} all-to-all(f32[8,8,128]{2,1,0:T(8,128)S(1)} %squares.1), channel_id=1, replica_groups=mesh['z'=8,'x'=4,'y'=8,'core'=2] {'z'}, dimensions={0} | all-to-all | bytes 65536 | tf_op jit(solution)/shard_map/all_to_all | solution.py:19
  166.4 0.1 last.1
  166.5 7.6 %all_to_all.56 = bf16[4,96,128]{2,1,0:T(8,128)(2,1)S(1)} all-to-all(bf16[4,96,128]{2,1,0:T(8,128)(2,1)S(1)} %last.1), channel_id=1, replica_groups=mesh['z'=8,'x'=4,'y'=8,'core'=2] {'x'}, dimensions={0} | all-to-all | bytes 196608 | tf_op jit(solution)/shard_map/all_to_all | solution.py:19
  174.1 0.6 copy.9
  (8 shorter events, 0.1 us)
Async XLA Ops:
  37.6 5.0 %copy-start.1 = (bf16[8,128,128]{2,1,0:T(8,128)(2,1)S(1)}, bf16[8,128,128]{2,1,0:T(8,128)(2,1)}, u32[]{:S(2)}) copy-start(bf16[8,128,128]{2,1,0:T(8,128)(2,1)} %get-tuple-element.24.refs_2_) | copy-start | bytes 786436
  38.5 21.4 %all-to-all-start.1 = ((bf16[8,96,128]{2,1,0:T(8,128)(2,1)}), bf16[8,96,128]{2,1,0:T(8,128)(2,1)S(1)}, u32[]{:S(2)}, u32[]{:S(2)}) async-start(bf16[8,96,128]{2,1,0:T(8,128)(2,1)} %broadcast_in_dim.6), calls=%async_computation.1 | async-start | bytes 393216 | tf_op jit(solution)/shard_map/all_to_all | solution.py:19
  42.6 17.3 %collective-permute-start.2 = (bf16[8,128,128]{2,1,0:T(8,128)(2,1)S(1)}, bf16[8,128,128]{2,1,0:T(8,128)(2,1)S(1)}, u32[]{:S(2)}, u32[]{:S(2)}) collective-permute-start(bf16[8,128,128]{2,1,0:T(8,128)(2,1)S(1)} %copy-done.1), channel_id=1, source_target_pairs={{0,16},{16,32},{32,48},{48,0},{1,17},{17,33},{33,49},{49,1},{2,18}... | collective-permute-start | bytes 786440 | tf_op jit(solution)/shard_map/ppermute | solution.py:389
  45.6 14.3 %collective-permute-start.1 = (bf16[8,128,128]{2,1,0:T(8,128)(2,1)S(1)}, bf16[8,128,128]{2,1,0:T(8,128)(2,1)S(1)}, u32[]{:S(2)}, u32[]{:S(2)}) collective-permute-start(bf16[8,128,128]{2,1,0:T(8,128)(2,1)S(1)} %copy-done.1), channel_id=1, source_target_pairs={{0,32},{16,48},{32,0},{48,16},{1,33},{17,49},{33,1},{49,17},{2,34}... | collective-permute-start | bytes 786440 | tf_op jit(solution)/shard_map/ppermute | solution.py:389
  49.8 10.2 %collective-permute-start = (bf16[8,128,128]{2,1,0:T(8,128)(2,1)S(1)}, bf16[8,128,128]{2,1,0:T(8,128)(2,1)S(1)}, u32[]{:S(2)}, u32[]{:S(2)}) collective-permute-start(bf16[8,128,128]{2,1,0:T(8,128)(2,1)S(1)} %copy-done.1), channel_id=1, source_target_pairs={{0,48},{16,0},{32,16},{48,32},{1,49},{17,1},{33,17},{49,33},{2,50}... | collective-permute-start | bytes 786440 | tf_op jit(solution)/shard_map/ppermute | solution.py:389
  55.1 19.1 %copy-start = (bf16[17,128,128]{2,1,0:T(8,128)(2,1)S(1)}, bf16[17,128,128]{2,1,0:T(8,128)(2,1)}, u32[]{:S(2)}) copy-start(bf16[17,128,128]{2,1,0:T(8,128)(2,1)} %get-tuple-element.29.refs_0_.refs_2_) | copy-start | bytes 1671172
  55.1 31.7 %collective-permute-start.4 = (bf16[17,128,128]{2,1,0:T(8,128)(2,1)}, bf16[17,128,128]{2,1,0:T(8,128)(2,1)S(1)}, u32[]{:S(2)}, u32[]{:S(2)}) collective-permute-start(bf16[17,128,128]{2,1,0:T(8,128)(2,1)} %get-tuple-element.31), channel_id=1, source_target_pairs={{0,32},{16,48},{32,0},{48,16},{1,33},{17,49},{33,1},{49,17},{2,34}... | collective-permute-start | bytes 1671176 | tf_op jit(solution)/shard_map/ppermute | solution.py:389
  58.0 37.2 %collective-permute-start.5 = (bf16[17,128,128]{2,1,0:T(8,128)(2,1)}, bf16[17,128,128]{2,1,0:T(8,128)(2,1)S(1)}, u32[]{:S(2)}, u32[]{:S(2)}) collective-permute-start(bf16[17,128,128]{2,1,0:T(8,128)(2,1)} %get-tuple-element.33), channel_id=1, source_target_pairs={{0,16},{16,32},{32,48},{48,0},{1,17},{17,33},{33,49},{49,1},{2,18}... | collective-permute-start | bytes 1671176 | tf_op jit(solution)/shard_map/ppermute | solution.py:389
  61.9 20.7 %all-to-all-start.2 = ((bf16[16,24,128]{2,1,0:T(8,128)(2,1)}), bf16[16,24,128]{2,1,0:T(8,128)(2,1)S(1)}, u32[]{:S(2)}, u32[]{:S(2)}) async-start(bf16[16,24,128]{2,1,0:T(8,128)(2,1)} %bitcast.2), calls=%async_computation.2 | async-start | bytes 196608 | tf_op jit(solution)/shard_map/all_to_all | solution.py:19
  74.2 21.0 %collective-permute-start.3 = (bf16[17,128,128]{2,1,0:T(8,128)(2,1)S(1)}, bf16[17,128,128]{2,1,0:T(8,128)(2,1)S(1)}, u32[]{:S(2)}, u32[]{:S(2)}) collective-permute-start(bf16[17,128,128]{2,1,0:T(8,128)(2,1)S(1)} %copy-done), channel_id=1, source_target_pairs={{0,48},{16,0},{32,16},{48,32},{1,49},{17,1},{33,17},{49,33},{2,50}... | collective-permute-start | bytes 1671176 | tf_op jit(solution)/shard_map/ppermute | solution.py:389
  83.3 11.8 %all-to-all-start.3 = ((bf16[16,24,128]{2,1,0:T(8,128)(2,1)}), bf16[16,24,128]{2,1,0:T(8,128)(2,1)S(1)}, u32[]{:S(2)}, u32[]{:S(2)}) async-start(bf16[16,24,128]{2,1,0:T(8,128)(2,1)} %broadcast_in_dim.7), calls=%async_computation.3 | async-start | bytes 196608 | tf_op jit(solution)/shard_map/all_to_all | solution.py:19

commit v13 on v11

--- a/solution.py
+++ b/solution.py
@@ -129,7 +129,8 @@
             ref[...] = jnp.concatenate(block, axis=0)
             continue
         for c in range(n):
-            ref[c] = up_ref[0, :, c * feats : (c + 1) * feats].astype(bf16)
+            block_at = c % 2 * (n // 2) + c // 2
+            ref[block_at] = up_ref[0, :, c * feats : (c + 1) * feats].astype(bf16)
         ref[n : 2 * n] = down
         ref[2 * n] = jnp.concatenate([*block, rest], axis=0)
 
@@ -242,9 +243,11 @@
         copies[-1].start()
     held_copies = []
     for i in range(X):
-        here = held.at[:, pl.ds(i * feats, feats)]
-        held_copies.append(pltpu.make_async_copy(blocks[i].at[pl.ds(0, Z)], here, held_sems.at[i]))
-        held_copies[-1].start()
+        for odd in range(2):
+            here = held.at[:, pl.ds(i * feats, feats), pl.ds(odd * feats, feats)]
+            half = blocks[i].at[pl.ds(odd * Z // 2, Z // 2)]
+            held_copies.append(pltpu.make_async_copy(half, here, held_sems.at[i, odd]))
+            held_copies[-1].start()
     for copy in copies:
         copy.wait()
     kept_terms, branch_terms, branches = [], [], []
@@ -270,12 +273,15 @@
     )
     for copy in held_copies:
         copy.wait()
-    for c in range(Z):
-        part = jnp.dot(terms, held[c], preferred_element_type=f32)
-        scale = scales[1:2, c * feats : (c + 1) * feats]
-        out_ref[c, : 2 * t] = (part * scale).astype(bf16)
-        out_ref[c, 2 * t :] = jnp.zeros((8, feats), bf16)
-        out_ref[c, 2 * t :, :t] = squares
+    for pair in range(Z // 2):
+        part = jnp.dot(terms, held[pair], preferred_element_type=f32)
+        scale = scales[1:2, pair * 2 * feats : (pair + 1) * 2 * feats]
+        part = (part * scale).astype(bf16)
+        for c in (2 * pair, 2 * pair + 1):
+            at = c % 2 * feats
+            out_ref[c, : 2 * t] = part[:, at : at + feats]
+            out_ref[c, 2 * t :] = jnp.zeros((8, feats), bf16)
+            out_ref[c, 2 * t :, :t] = squares
 
 
 def turn(summed, own, scale, blocks):
@@ -293,10 +299,10 @@
         out_specs=(VMEM,) * 4,
         scratch_shapes=[
             pltpu.VMEM((X - 1, 16 + t, feats), bf16),
-            pltpu.VMEM((Z, X * feats, feats), bf16),
+            pltpu.VMEM((Z // 2, X * feats, 2 * feats), bf16),
             pltpu.VMEM(scale.shape, f32),
             pltpu.SemaphoreType.DMA((X,)),
-            pltpu.SemaphoreType.DMA((X,)),
+            pltpu.SemaphoreType.DMA((X, 2)),
         ],
         compiler_params=limit(12),
         name="turn",

time: 176 us -> 176 us (level)
  no operation moved by 1% of the time
where the time goes in v13:
time: 176 us; the launch traced here: 175 us
  blocking collectives  110 us (62%)
  starting transfers between devices  38.8 us (22%)
  waiting for transfers between devices  12.6 us (7%)
  Pallas kernels  10.9 us (6%)
  local copies, waits for them, and re-layouts  2.04 us (1%)
    all_to_all x6, blocking collectives, exchange(): return lax.all_to_all(pieces, axis, split_axis=0, concat_axis=0, tiled=True)  110 us
    all_to_all x3, starting transfers between devices, exchange(): return lax.all_to_all(pieces, axis, split_axis=0, concat_axis=0, tiled=True)  19.8 us
    ppermute x6, starting transfers between devices, from_x(): return lax.ppermute(payload, 'x', [(i, (i - s) % X) for i in range(X)])  19 us
    all_to_all x3, waiting for transfers between devices, exchange(): return lax.all_to_all(pieces, axis, split_axis=0, concat_axis=0, tiled=True)  12.6 us
  transfers between devices with their start and end apart: 9, of which 3 were waited for; matrix products, arithmetic and copies ran while one was open for 0% of the time, Pallas kernels for 2%

profile of v13, /device:TPU:1, one launch (start us, length us, event | category | flops | bytes accessed | tf_op | source)
XLA Modules:
  0.0 175.1 jit_solution(3601122313149918632)
XLA Ops:
  0.0 2.8 %up_product.1 = (bf16[8,384,128]{2,1,0:T(8,128)(2,1)}, bf16[8,128,128]{2,1,0:T(8,128)(2,1)}) custom-call(bf16[384,128]{1,0:T(8,128)(2,1)} %tokens_ref.3, f32[2,128]{1,0:T(2,128)} %pre_ref.1, f32[2,128,1024]{2,1,0:T(8,128)} %up_ref.1, f32[2,1024]{1,0:T(2,128)} %scale_ref.5, f32[2,1024,128]{2,1,0:T(8,128)} %down_ref.3), custom_call_target="tpu_custom_call" | custom-call | tf_op jit(solution)/shard_map/up_product/pallas_call | solution.py:90
  2.8 34.8 %all_to_all.45 = bf16[32,96,128]{2,1,0:T(8,128)(2,1)S(1)} all-to-all(bf16[32,96,128]{2,1,0:T(8,128)(2,1)} %bitcast.20), channel_id=1, replica_groups=mesh['z'=8,'x'=4,'y'=8,'core'=2] {'z','x'}, dimensions={0} | all-to-all | bytes 1572864 | tf_op jit(solution)/shard_map/all_to_all | solution.py:19
  37.6 0.0 copy-start.1
  37.6 0.1 convert_reduce_fusion
  37.8 0.7 broadcast_in_dim.4
  38.5 4.1 %all-to-all-start.1 = ((bf16[8,96,128]{2,1,0:T(8,128)(2,1)}), bf16[8,96,128]{2,1,0:T(8,128)(2,1)S(1)}, u32[]{:S(2)}, u32[]{:S(2)}) async-start(bf16[8,96,128]{2,1,0:T(8,128)(2,1)} %broadcast_in_dim.4), calls=%async_computation.1 | async-start | bytes 393216 | tf_op jit(solution)/shard_map/all_to_all | solution.py:19
  42.6 0.0 copy-done.1
  42.6 3.0 %collective-permute-start.2 = (bf16[8,128,128]{2,1,0:T(8,128)(2,1)S(1)}, bf16[8,128,128]{2,1,0:T(8,128)(2,1)S(1)}, u32[]{:S(2)}, u32[]{:S(2)}) collective-permute-start(bf16[8,128,128]{2,1,0:T(8,128)(2,1)S(1)} %copy-done.1), channel_id=1, source_target_pairs={{0,16},{16,32},{32,48},{48,0},{1,17},{17,33},{33,49},{49,1},{2,18}... | collective-permute-start | bytes 786440 | tf_op jit(solution)/shard_map/ppermute | solution.py:412
  45.6 4.1 %collective-permute-start.1 = (bf16[8,128,128]{2,1,0:T(8,128)(2,1)S(1)}, bf16[8,128,128]{2,1,0:T(8,128)(2,1)S(1)}, u32[]{:S(2)}, u32[]{:S(2)}) collective-permute-start(bf16[8,128,128]{2,1,0:T(8,128)(2,1)S(1)} %copy-done.1), channel_id=1, source_target_pairs={{0,32},{16,48},{32,0},{48,16},{1,33},{17,49},{33,1},{49,17},{2,34}... | collective-permute-start | bytes 786440 | tf_op jit(solution)/shard_map/ppermute | solution.py:412
  49.8 2.7 %collective-permute-start = (bf16[8,128,128]{2,1,0:T(8,128)(2,1)S(1)}, bf16[8,128,128]{2,1,0:T(8,128)(2,1)S(1)}, u32[]{:S(2)}, u32[]{:S(2)}) collective-permute-start(bf16[8,128,128]{2,1,0:T(8,128)(2,1)S(1)} %copy-done.1), channel_id=1, source_target_pairs={{0,48},{16,0},{32,16},{48,32},{1,49},{17,1},{33,17},{49,33},{2,50}... | collective-permute-start | bytes 786440 | tf_op jit(solution)/shard_map/ppermute | solution.py:412
  52.5 2.5 %packed.1 = (bf16[17,128,128]{2,1,0:T(8,128)(2,1)}, bf16[17,128,128]{2,1,0:T(8,128)(2,1)}, bf16[17,128,128]{2,1,0:T(8,128)(2,1)}, bf16[112,128]{1,0:T(8,128)(2,1)S(1)}) custom-call(f32[2,1024,128]{2,1,0:T(8,128)} %down_ref.3, f32[2,128,1024]{2,1,0:T(8,128)} %up_ref.1, bf16[384,128]{1,0:T(8,128)(2,1)} %tokens_ref.3, f32[2,128]{1,0:T(2,128)} %scale_ref.4, ...), custom_call_target="tpu_custom_call" | custom-call | tf_op jit(solution)/shard_map/packed/pallas_call | solution.py:144
  55.0 0.0 copy-start
  55.0 2.9 %collective-permute-start.4 = (bf16[17,128,128]{2,1,0:T(8,128)(2,1)}, bf16[17,128,128]{2,1,0:T(8,128)(2,1)S(1)}, u32[]{:S(2)}, u32[]{:S(2)}) collective-permute-start(bf16[17,128,128]{2,1,0:T(8,128)(2,1)} %get-tuple-element.31), channel_id=1, source_target_pairs={{0,32},{16,48},{32,0},{48,16},{1,33},{17,49},{33,1},{49,17},{2,34}... | collective-permute-start | bytes 1671176 | tf_op jit(solution)/shard_map/ppermute | solution.py:412
  58.0 1.9 %collective-permute-start.5 = (bf16[17,128,128]{2,1,0:T(8,128)(2,1)}, bf16[17,128,128]{2,1,0:T(8,128)(2,1)S(1)}, u32[]{:S(2)}, u32[]{:S(2)}) collective-permute-start(bf16[17,128,128]{2,1,0:T(8,128)(2,1)} %get-tuple-element.33), channel_id=1, source_target_pairs={{0,16},{16,32},{32,48},{48,0},{1,17},{17,33},{33,49},{49,1},{2,18}... | collective-permute-start | bytes 1671176 | tf_op jit(solution)/shard_map/ppermute | solution.py:412
  59.9 0.0 collective-permute-done.2.refs_5_
  59.9 0.0 all-to-all-done.1.refs_1_
  59.9 0.0 collective-permute-done.1.refs_4_
  59.9 0.1 collective-permute-done.refs_3_
  60.0 1.8 %down_product.2 = bf16[4,96,128]{2,1,0:T(8,128)(2,1)} custom-call(f32[96,128]{1,0:T(8,128)S(1)} %fusion.1.refs_0_, bf16[8,96,128]{2,1,0:T(8,128)(2,1)S(1)} %all-to-all-done.1.refs_1_, bf16[8,128,128]{2,1,0:T(8,128)(2,1)} %get-tuple-element.24.refs_2_, bf16[8,128,128]{2,1,0:T(8,128)(2,1)S(1)} %collective-permute-done.refs_3_, ...), custom_call_target="tpu_custom_call" | custom-call | tf_op jit(solution)/shard_map/down_product/pallas_call | solution.py:191
  61.8 12.2 %all-to-all-start.2 = ((bf16[16,24,128]{2,1,0:T(8,128)(2,1)}), bf16[16,24,128]{2,1,0:T(8,128)(2,1)S(1)}, u32[]{:S(2)}, u32[]{:S(2)}) async-start(bf16[16,24,128]{2,1,0:T(8,128)(2,1)} %bitcast.2), calls=%async_computation.2 | async-start | bytes 196608 | tf_op jit(solution)/shard_map/all_to_all | solution.py:19
  74.1 0.0 copy-done
  74.1 4.3 %collective-permute-start.3 = (bf16[17,128,128]{2,1,0:T(8,128)(2,1)S(1)}, bf16[17,128,128]{2,1,0:T(8,128)(2,1)S(1)}, u32[]{:S(2)}, u32[]{:S(2)}) collective-permute-start(bf16[17,128,128]{2,1,0:T(8,128)(2,1)S(1)} %copy-done), channel_id=1, source_target_pairs={{0,48},{16,0},{32,16},{48,32},{1,49},{17,1},{33,17},{49,33},{2,50}... | collective-permute-start | bytes 1671176 | tf_op jit(solution)/shard_map/ppermute | solution.py:412
  78.4 4.1 %all-to-all-done.2 = bf16[16,24,128]{2,1,0:T(8,128)(2,1)S(1)} async-done(((bf16[16,24,128]{2,1,0:T(8,128)(2,1)}), bf16[16,24,128]{2,1,0:T(8,128)(2,1)S(1)}, u32[]{:S(2)}, u32[]{:S(2)}) %all-to-all-start.2) | async-done | bytes 98336 | tf_op jit(solution)/shard_map/all_to_all | solution.py:19
  82.5 0.7 broadcast_in_dim.5
  83.2 3.4 %all-to-all-start.3 = ((bf16[16,24,128]{2,1,0:T(8,128)(2,1)}), bf16[16,24,128]{2,1,0:T(8,128)(2,1)S(1)}, u32[]{:S(2)}, u32[]{:S(2)}) async-start(bf16[16,24,128]{2,1,0:T(8,128)(2,1)} %broadcast_in_dim.5), calls=%async_computation.3 | async-start | bytes 196608 | tf_op jit(solution)/shard_map/all_to_all | solution.py:19
  86.6 0.0 collective-permute-done.4.refs_2_.refs_4_
  86.6 8.4 %all-to-all-done.3 = bf16[16,24,128]{2,1,0:T(8,128)(2,1)S(1)} async-done(((bf16[16,24,128]{2,1,0:T(8,128)(2,1)}), bf16[16,24,128]{2,1,0:T(8,128)(2,1)S(1)}, u32[]{:S(2)}, u32[]{:S(2)}) %all-to-all-start.3) | async-done | bytes 98336 | tf_op jit(solution)/shard_map/all_to_all | solution.py:19
  95.0 0.0 collective-permute-done.5.refs_3_.refs_5_
  95.1 0.0 collective-permute-done.3.refs_1_.refs_3_
  95.1 2.0 %turn.1 = (bf16[8,200,128]{2,1,0:T(8,128)(2,1)S(1)}, f32[4,96,128]{2,1,0:T(8,128)S(1)}, f32[4,96,128]{2,1,0:T(8,128)S(1)}, f32[4,8,128]{2,1,0:T(8,128)S(1)}) custom-call(f32[96,128]{1,0:T(8,128)S(1)} %bitcast_convert_fusion.lead_ref, bf16[4,96,128]{2,1,0:T(8,128)(2,1)S(1)} %bitcast.19, bf16[112,128]{1,0:T(8,128)(2,1)S(1)} %get-tuple-element.28.own_ref, ...), custom_call_target="tpu_custom_call" | custom-call | tf_op jit(solution)/shard_map/turn/pallas_call | solution.py:290
  97.1 22.5 %all_to_all.46.refs_0_ = bf16[8,200,128]{2,1,0:T(8,128)(2,1)S(1)} all-to-all(bf16[8,200,128]{2,1,0:T(8,128)(2,1)S(1)} %get-tuple-element.35), channel_id=1, replica_groups=mesh['z'=8,'x'=4,'y'=8,'core'=2] {'z'}, dimensions={0} | all-to-all | bytes 819200 | tf_op jit(solution)/shard_map/all_to_all | solution.py:19
  119.7 0.1 second_hidden.1
  119.8 12.1 %all_to_all.47.refs_1_ = bf16[8,96,128]{2,1,0:T(8,128)(2,1)S(1)} all-to-all(bf16[8,96,128]{2,1,0:T(8,128)(2,1)S(1)} %get-tuple-element.38), channel_id=1, replica_groups=mesh['z'=8,'x'=4,'y'=8,'core'=2] {'z'}, dimensions={0} | all-to-all | bytes 393216 | tf_op jit(solution)/shard_map/all_to_all | solution.py:19
  131.9 1.2 down_product.3
  133.1 13.3 %all_to_all.48.sum_ref = bf16[16,4,8,128]{3,2,1,0:T(8,128)(2,1)S(1)} all-to-all(bf16[16,4,8,128]{3,2,1,0:T(8,128)(2,1)S(1)} %down_product.3), channel_id=1, replica_groups=mesh['z'=8,'x'=4,'y'=8,'core'=2] {'y','core'}, dimensions={0} | all-to-all | bytes 262144 | tf_op jit(solution)/shard_map/all_to_all | solution.py:19
  146.4 0.2 shares.1
  146.6 14.4 %all_to_all.49.refs_0_ = bf16[32,24,128]{2,1,0:T(8,128)(2,1)S(1)} all-to-all(bf16[32,24,128]{2,1,0:T(8,128)(2,1)S(1)} %shares.1), channel_id=1, replica_groups=mesh['z'=8,'x'=4,'y'=8,'core'=2] {'z','x'}, dimensions={0} | all-to-all | bytes 393216 | tf_op jit(solution)/shard_map/all_to_all | solution.py:19
  161.0 0.1 last.1
  161.2 13.2 %all_to_all.50 = bf16[16,4,8,128]{3,2,1,0:T(8,128)(2,1)S(1)} all-to-all(bf16[16,4,8,128]{3,2,1,0:T(8,128)(2,1)S(1)} %last.1), channel_id=1, replica_groups=mesh['z'=8,'x'=4,'y'=8,'core'=2] {'y','core'}, dimensions={0} | all-to-all | bytes 262144 | tf_op jit(solution)/shard_map/all_to_all | solution.py:19
  174.4 0.7 copy.8
  (7 shorter events, 0.1 us)
Async XLA Ops:
  37.6 5.0 %copy-start.1 = (bf16[8,128,128]{2,1,0:T(8,128)(2,1)S(1)}, bf16[8,128,128]{2,1,0:T(8,128)(2,1)}, u32[]{:S(2)}) copy-start(bf16[8,128,128]{2,1,0:T(8,128)(2,1)} %get-tuple-element.24.refs_2_) | copy-start | bytes 786436
  38.5 21.4 %all-to-all-start.1 = ((bf16[8,96,128]{2,1,0:T(8,128)(2,1)}), bf16[8,96,128]{2,1,0:T(8,128)(2,1)S(1)}, u32[]{:S(2)}, u32[]{:S(2)}) async-start(bf16[8,96,128]{2,1,0:T(8,128)(2,1)} %broadcast_in_dim.4), calls=%async_computation.1 | async-start | bytes 393216 | tf_op jit(solution)/shard_map/all_to_all | solution.py:19
  42.6 17.3 %collective-permute-start.2 = (bf16[8,128,128]{2,1,0:T(8,128)(2,1)S(1)}, bf16[8,128,128]{2,1,0:T(8,128)(2,1)S(1)}, u32[]{:S(2)}, u32[]{:S(2)}) collective-permute-start(bf16[8,128,128]{2,1,0:T(8,128)(2,1)S(1)} %copy-done.1), channel_id=1, source_target_pairs={{0,16},{16,32},{32,48},{48,0},{1,17},{17,33},{33,49},{49,1},{2,18}... | collective-permute-start | bytes 786440 | tf_op jit(solution)/shard_map/ppermute | solution.py:412
  45.6 14.3 %collective-permute-start.1 = (bf16[8,128,128]{2,1,0:T(8,128)(2,1)S(1)}, bf16[8,128,128]{2,1,0:T(8,128)(2,1)S(1)}, u32[]{:S(2)}, u32[]{:S(2)}) collective-permute-start(bf16[8,128,128]{2,1,0:T(8,128)(2,1)S(1)} %copy-done.1), channel_id=1, source_target_pairs={{0,32},{16,48},{32,0},{48,16},{1,33},{17,49},{33,1},{49,17},{2,34}... | collective-permute-start | bytes 786440 | tf_op jit(solution)/shard_map/ppermute | solution.py:412
  49.8 10.2 %collective-permute-start = (bf16[8,128,128]{2,1,0:T(8,128)(2,1)S(1)}, bf16[8,128,128]{2,1,0:T(8,128)(2,1)S(1)}, u32[]{:S(2)}, u32[]{:S(2)}) collective-permute-start(bf16[8,128,128]{2,1,0:T(8,128)(2,1)S(1)} %copy-done.1), channel_id=1, source_target_pairs={{0,48},{16,0},{32,16},{48,32},{1,49},{17,1},{33,17},{49,33},{2,50}... | collective-permute-start | bytes 786440 | tf_op jit(solution)/shard_map/ppermute | solution.py:412
  55.0 19.0 %copy-start = (bf16[17,128,128]{2,1,0:T(8,128)(2,1)S(1)}, bf16[17,128,128]{2,1,0:T(8,128)(2,1)}, u32[]{:S(2)}) copy-start(bf16[17,128,128]{2,1,0:T(8,128)(2,1)} %get-tuple-element.29.refs_0_.refs_2_) | copy-start | bytes 1671172
  55.0 31.6 %collective-permute-start.4 = (bf16[17,128,128]{2,1,0:T(8,128)(2,1)}, bf16[17,128,128]{2,1,0:T(8,128)(2,1)S(1)}, u32[]{:S(2)}, u32[]{:S(2)}) collective-permute-start(bf16[17,128,128]{2,1,0:T(8,128)(2,1)} %get-tuple-element.31), channel_id=1, source_target_pairs={{0,32},{16,48},{32,0},{48,16},{1,33},{17,49},{33,1},{49,17},{2,34}... | collective-permute-start | bytes 1671176 | tf_op jit(solution)/shard_map/ppermute | solution.py:412
  58.0 37.1 %collective-permute-start.5 = (bf16[17,128,128]{2,1,0:T(8,128)(2,1)}, bf16[17,128,128]{2,1,0:T(8,128)(2,1)S(1)}, u32[]{:S(2)}, u32[]{:S(2)}) collective-permute-start(bf16[17,128,128]{2,1,0:T(8,128)(2,1)} %get-tuple-element.33), channel_id=1, source_target_pairs={{0,16},{16,32},{32,48},{48,0},{1,17},{17,33},{33,49},{49,1},{2,18}... | collective-permute-start | bytes 1671176 | tf_op jit(solution)/shard_map/ppermute | solution.py:412
  61.8 20.7 %all-to-all-start.2 = ((bf16[16,24,128]{2,1,0:T(8,128)(2,1)}), bf16[16,24,128]{2,1,0:T(8,128)(2,1)S(1)}, u32[]{:S(2)}, u32[]{:S(2)}) async-start(bf16[16,24,128]{2,1,0:T(8,128)(2,1)} %bitcast.2), calls=%async_computation.2 | async-start | bytes 196608 | tf_op jit(solution)/shard_map/all_to_all | solution.py:19
  74.1 21.0 %collective-permute-start.3 = (bf16[17,128,128]{2,1,0:T(8,128)(2,1)S(1)}, bf16[17,128,128]{2,1,0:T(8,128)(2,1)S(1)}, u32[]{:S(2)}, u32[]{:S(2)}) collective-permute-start(bf16[17,128,128]{2,1,0:T(8,128)(2,1)S(1)} %copy-done), channel_id=1, source_target_pairs={{0,48},{16,0},{32,16},{48,32},{1,49},{17,1},{33,17},{49,33},{2,50}... | collective-permute-start | bytes 1671176 | tf_op jit(solution)/shard_map/ppermute | solution.py:412
  83.2 11.8 %all-to-all-start.3 = ((bf16[16,24,128]{2,1,0:T(8,128)(2,1)}), bf16[16,24,128]{2,1,0:T(8,128)(2,1)S(1)}, u32[]{:S(2)}, u32[]{:S(2)}) async-start(bf16[16,24,128]{2,1,0:T(8,128)(2,1)} %broadcast_in_dim.5), calls=%async_computation.3 | async-start | bytes 196608 | tf_op jit(solution)/shard_map/all_to_all | solution.py:19

commit v14 on v12

--- a/solution.py
+++ b/solution.py
@@ -66,6 +66,11 @@
     scaled = (tokens[...].astype(f32) * gain[0:1]).astype(bf16)
     sent = []
     for i in range(parts):
+        if i == parts // 2:
+            down_copy.wait()
+            first[...] = down[...].astype(bf16).reshape(first.shape)
+            sent.append(pltpu.make_async_copy(first, first_ref, in_sems.at[4]))
+            sent[-1].start()
         copies[i].wait()
         part = jnp.dot(scaled, weight[i].astype(bf16), preferred_element_type=f32)
         part = (part * scale[0:1, i * step : (i + 1) * step]).astype(bf16)
@@ -74,10 +79,6 @@
             out[z] = part[:, c * feats : (c + 1) * feats]
             sent.append(pltpu.make_async_copy(out.at[z], out_ref.at[z], out_sems.at[z]))
             sent[-1].start()
-    down_copy.wait()
-    first[...] = down[...].astype(bf16).reshape(first.shape)
-    sent.append(pltpu.make_async_copy(first, first_ref, in_sems.at[4]))
-    sent[-1].start()
     for copy in sent:
         copy.wait()
 
@@ -162,23 +163,19 @@
     )(*[far(v) for v in (down_weight, up_weight, tokens, scale, pre, post)])
 
 
-def down_kernel(start, lead_ref, hidden_ref, *refs):
-    weights, out_ref, held, sems = refs[:X], refs[X], refs[X + 1], refs[X + 2]
-    feats = out_ref.shape[2]
-    copies = []
-    for i, w in enumerate(weights):
-        here = held.at[i // 2, :, :, pl.ds(i % 2 * feats, feats)]
-        copies.append(pltpu.make_async_copy(w.at[pl.ds(start, held.shape[1])], here, sems.at[i]))
-        copies[-1].start()
+def down_kernel(start, lead_ref, hidden_ref, own_ref, *refs):
+    others, (out_ref, held, sem) = refs[: X - 1], refs[X - 1 :]
+    n = held.shape[0]
+    copy = pltpu.make_async_copy(own_ref.at[pl.ds(start, n)], held, sem)
+    copy.start()
     hidden = [lead_ref[...].astype(bf16), *(hidden_ref[z] for z in range(1, Z))]
     hidden = jnp.concatenate(hidden, axis=1)
-    for pair in (1, 0):
-        for i in (2 * pair, 2 * pair + 1):
-            copies[i].wait()
-        weight = held[pair].reshape(hidden.shape[1], 2 * feats)
-        part = jnp.dot(hidden, weight, preferred_element_type=f32).astype(bf16)
-        out_ref[2 * pair] = part[:, :feats]
-        out_ref[2 * pair + 1] = part[:, feats:]
+    for i in (1, 2, 3, 0):
+        if i == 0:
+            copy.wait()
+        weight = others[i - 1][start : start + n] if i else held[...]
+        weight = weight.reshape(hidden.shape[1], -1)
+        out_ref[i] = jnp.dot(hidden, weight, preferred_element_type=f32).astype(bf16)
 
 
 def down_product(hidden, blocks, start):
@@ -188,15 +185,15 @@
     return pl.pallas_call(
         lambda *refs: down_kernel(start, *refs),
         out_shape=pltpu.VMEM((X, t, feats), bf16),
-        in_specs=[*[VMEM] * 2, *[ANY] * X],
+        in_specs=[*[VMEM] * 2, ANY, *[VMEM] * (X - 1)],
         out_specs=VMEM,
         scratch_shapes=[
-            pltpu.VMEM((X // 2, Z * share // feats, feats, 2 * feats), bf16),
-            pltpu.SemaphoreType.DMA((X,)),
+            pltpu.VMEM((Z * share // feats, feats, feats), bf16),
+            pltpu.SemaphoreType.DMA,
         ],
         compiler_params=limit(8),
         name="down_product",
-    )(near(lead), near(hidden), *blocks)
+    )(near(lead), near(hidden), blocks[0], *[near(b) for b in blocks[1:]])
 
 
 def down_share(hidden, blocks, start):
@@ -337,13 +334,13 @@
     squares = squares_in_rows(values)
     for z in range(Z):
         out_ref[z] = jnp.zeros(out_ref.shape[1:], f32)
-        out_ref[z, :, :t] = squares
+        out_ref[z, :, :t] = squares[0:1]
 
 
 def squares_of(summed, columns):
     return pl.pallas_call(
         squares_kernel,
-        out_shape=pltpu.VMEM((Z, 8, summed.shape[2]), f32),
+        out_shape=pltpu.VMEM((Z, 1, summed.shape[2]), f32),
         in_specs=[VMEM] * 2,
         out_specs=VMEM,
         compiler_params=limit(8),

time: 176 us -> 175 us (level)
  no operation moved by 1% of the time
where the time goes in v14:
time: 175 us; the launch traced here: 174 us
  blocking collectives  109 us (62%)
  starting transfers between devices  38.8 us (22%)
  waiting for transfers between devices  12.7 us (7%)
  Pallas kernels  11.1 us (6%)
  local copies, waits for them, and re-layouts  2.04 us (1%)
    all_to_all x7, blocking collectives, exchange(): return lax.all_to_all(pieces, axis, split_axis=0, concat_axis=0, tiled=True)  109 us
    all_to_all x3, starting transfers between devices, exchange(): return lax.all_to_all(pieces, axis, split_axis=0, concat_axis=0, tiled=True)  19.8 us
    ppermute x6, starting transfers between devices, from_x(): return lax.ppermute(payload, 'x', [(i, (i - s) % X) for i in range(X)])  19 us
    all_to_all x3, waiting for transfers between devices, exchange(): return lax.all_to_all(pieces, axis, split_axis=0, concat_axis=0, tiled=True)  12.6 us
  transfers between devices with their start and end apart: 9, of which 3 were waited for; matrix products, arithmetic and copies ran while one was open for 0% of the time, Pallas kernels for 3%

profile of v14, /device:TPU:1, one launch (start us, length us, event | category | flops | bytes accessed | tf_op | source)
XLA Modules:
  0.0 174.4 jit_solution(2835148571436476063)
XLA Ops:
  0.0 2.8 %up_product.1 = (bf16[8,384,128]{2,1,0:T(8,128)(2,1)}, bf16[8,128,128]{2,1,0:T(8,128)(2,1)}) custom-call(bf16[384,128]{1,0:T(8,128)(2,1)} %tokens_ref.3, f32[2,128]{1,0:T(2,128)} %pre_ref.1, f32[2,128,1024]{2,1,0:T(8,128)} %up_ref.1, f32[2,1024]{1,0:T(2,128)} %scale_ref.5, f32[2,1024,128]{2,1,0:T(8,128)} %down_ref.3), custom_call_target="tpu_custom_call" | custom-call | tf_op jit(solution)/shard_map/up_product/pallas_call | solution.py:91
  2.8 34.8 %all_to_all.50 = bf16[32,96,128]{2,1,0:T(8,128)(2,1)S(1)} all-to-all(bf16[32,96,128]{2,1,0:T(8,128)(2,1)} %bitcast.23), channel_id=1, replica_groups=mesh['z'=8,'x'=4,'y'=8,'core'=2] {'z','x'}, dimensions={0} | all-to-all | bytes 1572864 | tf_op jit(solution)/shard_map/all_to_all | solution.py:19
  37.6 0.0 copy-start.1
  37.6 0.1 convert_reduce_fusion
  37.7 0.7 broadcast_in_dim.6
  38.4 4.1 %all-to-all-start.1 = ((bf16[8,96,128]{2,1,0:T(8,128)(2,1)}), bf16[8,96,128]{2,1,0:T(8,128)(2,1)S(1)}, u32[]{:S(2)}, u32[]{:S(2)}) async-start(bf16[8,96,128]{2,1,0:T(8,128)(2,1)} %broadcast_in_dim.6), calls=%async_computation.1 | async-start | bytes 393216 | tf_op jit(solution)/shard_map/all_to_all | solution.py:19
  42.6 0.0 copy-done.1
  42.6 3.0 %collective-permute-start.2 = (bf16[8,128,128]{2,1,0:T(8,128)(2,1)S(1)}, bf16[8,128,128]{2,1,0:T(8,128)(2,1)S(1)}, u32[]{:S(2)}, u32[]{:S(2)}) collective-permute-start(bf16[8,128,128]{2,1,0:T(8,128)(2,1)S(1)} %copy-done.1), channel_id=1, source_target_pairs={{0,16},{16,32},{32,48},{48,0},{1,17},{17,33},{33,49},{49,1},{2,18}... | collective-permute-start | bytes 786440 | tf_op jit(solution)/shard_map/ppermute | solution.py:386
  45.6 4.1 %collective-permute-start.1 = (bf16[8,128,128]{2,1,0:T(8,128)(2,1)S(1)}, bf16[8,128,128]{2,1,0:T(8,128)(2,1)S(1)}, u32[]{:S(2)}, u32[]{:S(2)}) collective-permute-start(bf16[8,128,128]{2,1,0:T(8,128)(2,1)S(1)} %copy-done.1), channel_id=1, source_target_pairs={{0,32},{16,48},{32,0},{48,16},{1,33},{17,49},{33,1},{49,17},{2,34}... | collective-permute-start | bytes 786440 | tf_op jit(solution)/shard_map/ppermute | solution.py:386
  49.7 2.7 %collective-permute-start = (bf16[8,128,128]{2,1,0:T(8,128)(2,1)S(1)}, bf16[8,128,128]{2,1,0:T(8,128)(2,1)S(1)}, u32[]{:S(2)}, u32[]{:S(2)}) collective-permute-start(bf16[8,128,128]{2,1,0:T(8,128)(2,1)S(1)} %copy-done.1), channel_id=1, source_target_pairs={{0,48},{16,0},{32,16},{48,32},{1,49},{17,1},{33,17},{49,33},{2,50}... | collective-permute-start | bytes 786440 | tf_op jit(solution)/shard_map/ppermute | solution.py:386
  52.5 2.5 %packed.1 = (bf16[17,128,128]{2,1,0:T(8,128)(2,1)}, bf16[17,128,128]{2,1,0:T(8,128)(2,1)}, bf16[17,128,128]{2,1,0:T(8,128)(2,1)}, bf16[112,128]{1,0:T(8,128)(2,1)S(1)}) custom-call(f32[2,1024,128]{2,1,0:T(8,128)} %down_ref.3, f32[2,128,1024]{2,1,0:T(8,128)} %up_ref.1, bf16[384,128]{1,0:T(8,128)(2,1)} %tokens_ref.3, f32[2,128]{1,0:T(2,128)} %scale_ref.4, ...), custom_call_target="tpu_custom_call" | custom-call | tf_op jit(solution)/shard_map/packed/pallas_call | solution.py:145
  55.0 0.0 copy-start
  55.0 2.9 %collective-permute-start.4 = (bf16[17,128,128]{2,1,0:T(8,128)(2,1)}, bf16[17,128,128]{2,1,0:T(8,128)(2,1)S(1)}, u32[]{:S(2)}, u32[]{:S(2)}) collective-permute-start(bf16[17,128,128]{2,1,0:T(8,128)(2,1)} %get-tuple-element.31), channel_id=1, source_target_pairs={{0,32},{16,48},{32,0},{48,16},{1,33},{17,49},{33,1},{49,17},{2,34}... | collective-permute-start | bytes 1671176 | tf_op jit(solution)/shard_map/ppermute | solution.py:386
  57.9 1.9 %collective-permute-start.5 = (bf16[17,128,128]{2,1,0:T(8,128)(2,1)}, bf16[17,128,128]{2,1,0:T(8,128)(2,1)S(1)}, u32[]{:S(2)}, u32[]{:S(2)}) collective-permute-start(bf16[17,128,128]{2,1,0:T(8,128)(2,1)} %get-tuple-element.33), channel_id=1, source_target_pairs={{0,16},{16,32},{32,48},{48,0},{1,17},{17,33},{33,49},{49,1},{2,18}... | collective-permute-start | bytes 1671176 | tf_op jit(solution)/shard_map/ppermute | solution.py:386
  59.8 0.0 collective-permute-done.2.refs_5_
  59.8 0.0 all-to-all-done.1.refs_1_
  59.9 0.0 collective-permute-done.1.refs_4_
  59.9 0.1 collective-permute-done.refs_3_
  60.0 2.0 %down_product.2 = bf16[4,96,128]{2,1,0:T(8,128)(2,1)} custom-call(f32[96,128]{1,0:T(8,128)S(1)} %fusion.1.refs_0_, bf16[8,96,128]{2,1,0:T(8,128)(2,1)S(1)} %all-to-all-done.1.refs_1_, bf16[8,128,128]{2,1,0:T(8,128)(2,1)} %get-tuple-element.24.refs_2_, bf16[8,128,128]{2,1,0:T(8,128)(2,1)S(1)} %collective-permute-done.refs_3_, ...), custom_call_target="tpu_custom_call" | custom-call | tf_op jit(solution)/shard_map/down_product/pallas_call | solution.py:185
  62.0 12.2 %all-to-all-start.2 = ((bf16[16,24,128]{2,1,0:T(8,128)(2,1)}), bf16[16,24,128]{2,1,0:T(8,128)(2,1)S(1)}, u32[]{:S(2)}, u32[]{:S(2)}) async-start(bf16[16,24,128]{2,1,0:T(8,128)(2,1)} %bitcast.2), calls=%async_computation.2 | async-start | bytes 196608 | tf_op jit(solution)/shard_map/all_to_all | solution.py:19
  74.2 0.0 copy-done
  74.2 4.3 %collective-permute-start.3 = (bf16[17,128,128]{2,1,0:T(8,128)(2,1)S(1)}, bf16[17,128,128]{2,1,0:T(8,128)(2,1)S(1)}, u32[]{:S(2)}, u32[]{:S(2)}) collective-permute-start(bf16[17,128,128]{2,1,0:T(8,128)(2,1)S(1)} %copy-done), channel_id=1, source_target_pairs={{0,48},{16,0},{32,16},{48,32},{1,49},{17,1},{33,17},{49,33},{2,50}... | collective-permute-start | bytes 1671176 | tf_op jit(solution)/shard_map/ppermute | solution.py:386
  78.5 4.1 %all-to-all-done.2 = bf16[16,24,128]{2,1,0:T(8,128)(2,1)S(1)} async-done(((bf16[16,24,128]{2,1,0:T(8,128)(2,1)}), bf16[16,24,128]{2,1,0:T(8,128)(2,1)S(1)}, u32[]{:S(2)}, u32[]{:S(2)}) %all-to-all-start.2) | async-done | bytes 98336 | tf_op jit(solution)/shard_map/all_to_all | solution.py:19
  82.7 0.7 broadcast_in_dim.7
  83.3 3.4 %all-to-all-start.3 = ((bf16[16,24,128]{2,1,0:T(8,128)(2,1)}), bf16[16,24,128]{2,1,0:T(8,128)(2,1)S(1)}, u32[]{:S(2)}, u32[]{:S(2)}) async-start(bf16[16,24,128]{2,1,0:T(8,128)(2,1)} %broadcast_in_dim.7), calls=%async_computation.3 | async-start | bytes 196608 | tf_op jit(solution)/shard_map/all_to_all | solution.py:19
  86.7 0.0 collective-permute-done.4.refs_2_.refs_4_
  86.8 8.4 %all-to-all-done.3 = bf16[16,24,128]{2,1,0:T(8,128)(2,1)S(1)} async-done(((bf16[16,24,128]{2,1,0:T(8,128)(2,1)}), bf16[16,24,128]{2,1,0:T(8,128)(2,1)S(1)}, u32[]{:S(2)}, u32[]{:S(2)}) %all-to-all-start.3) | async-done | bytes 98336 | tf_op jit(solution)/shard_map/all_to_all | solution.py:19
  95.2 0.0 collective-permute-done.5.refs_3_.refs_5_
  95.2 0.0 collective-permute-done.3.refs_1_.refs_3_
  95.2 2.0 %turn.1 = (bf16[8,200,128]{2,1,0:T(8,128)(2,1)S(1)}, f32[4,96,128]{2,1,0:T(8,128)S(1)}, f32[4,96,128]{2,1,0:T(8,128)S(1)}, f32[4,8,128]{2,1,0:T(8,128)S(1)}) custom-call(f32[96,128]{1,0:T(8,128)S(1)} %bitcast_convert_fusion.lead_ref, bf16[4,96,128]{2,1,0:T(8,128)(2,1)S(1)} %bitcast.21, bf16[112,128]{1,0:T(8,128)(2,1)S(1)} %get-tuple-element.28.own_ref, ...), custom_call_target="tpu_custom_call" | custom-call | tf_op jit(solution)/shard_map/turn/pallas_call | solution.py:284
  97.2 22.5 %all_to_all.51.refs_0_ = bf16[8,200,128]{2,1,0:T(8,128)(2,1)S(1)} all-to-all(bf16[8,200,128]{2,1,0:T(8,128)(2,1)S(1)} %get-tuple-element.35), channel_id=1, replica_groups=mesh['z'=8,'x'=4,'y'=8,'core'=2] {'z'}, dimensions={0} | all-to-all | bytes 819200 | tf_op jit(solution)/shard_map/all_to_all | solution.py:19
  119.8 0.1 second_hidden.1
  119.9 12.1 %all_to_all.52.refs_1_ = bf16[8,96,128]{2,1,0:T(8,128)(2,1)S(1)} all-to-all(bf16[8,96,128]{2,1,0:T(8,128)(2,1)S(1)} %get-tuple-element.38), channel_id=1, replica_groups=mesh['z'=8,'x'=4,'y'=8,'core'=2] {'z'}, dimensions={0} | all-to-all | bytes 393216 | tf_op jit(solution)/shard_map/all_to_all | solution.py:19
  132.0 1.2 down_product.3
  133.2 12.6 %all_to_all.53 = bf16[16,24,128]{2,1,0:T(8,128)(2,1)S(1)} all-to-all(bf16[16,24,128]{2,1,0:T(8,128)(2,1)S(1)} %bitcast.22), channel_id=1, replica_groups=mesh['z'=8,'x'=4,'y'=8,'core'=2] {'y','core'}, dimensions={0} | all-to-all | bytes 196608 | tf_op jit(solution)/shard_map/all_to_all | solution.py:19
  145.8 10.9 %all_to_all.54 = bf16[16,24,128]{2,1,0:T(8,128)(2,1)S(1)} all-to-all(bf16[16,24,128]{2,1,0:T(8,128)(2,1)S(1)} %broadcast_in_dim.8), channel_id=1, replica_groups=mesh['z'=8,'x'=4,'y'=8,'core'=2] {'y','core'}, dimensions={0} | all-to-all | bytes 196608 | tf_op jit(solution)/shard_map/all_to_all | solution.py:19
  156.7 0.4 squares.1
  157.1 8.9 %all_to_all.55.refs_0_ = f32[8,1,128]{2,1,0:T(1,128)S(1)} all-to-all(f32[8,1,128]{2,1,0:T(1,128)S(1)} %squares.1), channel_id=1, replica_groups=mesh['z'=8,'x'=4,'y'=8,'core'=2] {'z'}, dimensions={0} | all-to-all | bytes 8192 | tf_op jit(solution)/shard_map/all_to_all | solution.py:19
  166.0 0.1 last.1
  166.2 7.6 %all_to_all.56 = bf16[4,96,128]{2,1,0:T(8,128)(2,1)S(1)} all-to-all(bf16[4,96,128]{2,1,0:T(8,128)(2,1)S(1)} %last.1), channel_id=1, replica_groups=mesh['z'=8,'x'=4,'y'=8,'core'=2] {'x'}, dimensions={0} | all-to-all | bytes 196608 | tf_op jit(solution)/shard_map/all_to_all | solution.py:19
  173.7 0.6 copy.9
  (8 shorter events, 0.1 us)
Async XLA Ops:
  37.6 5.0 %copy-start.1 = (bf16[8,128,128]{2,1,0:T(8,128)(2,1)S(1)}, bf16[8,128,128]{2,1,0:T(8,128)(2,1)}, u32[]{:S(2)}) copy-start(bf16[8,128,128]{2,1,0:T(8,128)(2,1)} %get-tuple-element.24.refs_2_) | copy-start | bytes 786436
  38.4 21.4 %all-to-all-start.1 = ((bf16[8,96,128]{2,1,0:T(8,128)(2,1)}), bf16[8,96,128]{2,1,0:T(8,128)(2,1)S(1)}, u32[]{:S(2)}, u32[]{:S(2)}) async-start(bf16[8,96,128]{2,1,0:T(8,128)(2,1)} %broadcast_in_dim.6), calls=%async_computation.1 | async-start | bytes 393216 | tf_op jit(solution)/shard_map/all_to_all | solution.py:19
  42.6 17.3 %collective-permute-start.2 = (bf16[8,128,128]{2,1,0:T(8,128)(2,1)S(1)}, bf16[8,128,128]{2,1,0:T(8,128)(2,1)S(1)}, u32[]{:S(2)}, u32[]{:S(2)}) collective-permute-start(bf16[8,128,128]{2,1,0:T(8,128)(2,1)S(1)} %copy-done.1), channel_id=1, source_target_pairs={{0,16},{16,32},{32,48},{48,0},{1,17},{17,33},{33,49},{49,1},{2,18}... | collective-permute-start | bytes 786440 | tf_op jit(solution)/shard_map/ppermute | solution.py:386
  45.6 14.3 %collective-permute-start.1 = (bf16[8,128,128]{2,1,0:T(8,128)(2,1)S(1)}, bf16[8,128,128]{2,1,0:T(8,128)(2,1)S(1)}, u32[]{:S(2)}, u32[]{:S(2)}) collective-permute-start(bf16[8,128,128]{2,1,0:T(8,128)(2,1)S(1)} %copy-done.1), channel_id=1, source_target_pairs={{0,32},{16,48},{32,0},{48,16},{1,33},{17,49},{33,1},{49,17},{2,34}... | collective-permute-start | bytes 786440 | tf_op jit(solution)/shard_map/ppermute | solution.py:386
  49.7 10.2 %collective-permute-start = (bf16[8,128,128]{2,1,0:T(8,128)(2,1)S(1)}, bf16[8,128,128]{2,1,0:T(8,128)(2,1)S(1)}, u32[]{:S(2)}, u32[]{:S(2)}) collective-permute-start(bf16[8,128,128]{2,1,0:T(8,128)(2,1)S(1)} %copy-done.1), channel_id=1, source_target_pairs={{0,48},{16,0},{32,16},{48,32},{1,49},{17,1},{33,17},{49,33},{2,50}... | collective-permute-start | bytes 786440 | tf_op jit(solution)/shard_map/ppermute | solution.py:386
  55.0 19.2 %copy-start = (bf16[17,128,128]{2,1,0:T(8,128)(2,1)S(1)}, bf16[17,128,128]{2,1,0:T(8,128)(2,1)}, u32[]{:S(2)}) copy-start(bf16[17,128,128]{2,1,0:T(8,128)(2,1)} %get-tuple-element.29.refs_0_.refs_2_) | copy-start | bytes 1671172
  55.0 31.8 %collective-permute-start.4 = (bf16[17,128,128]{2,1,0:T(8,128)(2,1)}, bf16[17,128,128]{2,1,0:T(8,128)(2,1)S(1)}, u32[]{:S(2)}, u32[]{:S(2)}) collective-permute-start(bf16[17,128,128]{2,1,0:T(8,128)(2,1)} %get-tuple-element.31), channel_id=1, source_target_pairs={{0,32},{16,48},{32,0},{48,16},{1,33},{17,49},{33,1},{49,17},{2,34}... | collective-permute-start | bytes 1671176 | tf_op jit(solution)/shard_map/ppermute | solution.py:386
  57.9 37.3 %collective-permute-start.5 = (bf16[17,128,128]{2,1,0:T(8,128)(2,1)}, bf16[17,128,128]{2,1,0:T(8,128)(2,1)S(1)}, u32[]{:S(2)}, u32[]{:S(2)}) collective-permute-start(bf16[17,128,128]{2,1,0:T(8,128)(2,1)} %get-tuple-element.33), channel_id=1, source_target_pairs={{0,16},{16,32},{32,48},{48,0},{1,17},{17,33},{33,49},{49,1},{2,18}... | collective-permute-start | bytes 1671176 | tf_op jit(solution)/shard_map/ppermute | solution.py:386
  62.0 20.7 %all-to-all-start.2 = ((bf16[16,24,128]{2,1,0:T(8,128)(2,1)}), bf16[16,24,128]{2,1,0:T(8,128)(2,1)S(1)}, u32[]{:S(2)}, u32[]{:S(2)}) async-start(bf16[16,24,128]{2,1,0:T(8,128)(2,1)} %bitcast.2), calls=%async_computation.2 | async-start | bytes 196608 | tf_op jit(solution)/shard_map/all_to_all | solution.py:19
  74.2 21.0 %collective-permute-start.3 = (bf16[17,128,128]{2,1,0:T(8,128)(2,1)S(1)}, bf16[17,128,128]{2,1,0:T(8,128)(2,1)S(1)}, u32[]{:S(2)}, u32[]{:S(2)}) collective-permute-start(bf16[17,128,128]{2,1,0:T(8,128)(2,1)S(1)} %copy-done), channel_id=1, source_target_pairs={{0,48},{16,0},{32,16},{48,32},{1,49},{17,1},{33,17},{49,33},{2,50}... | collective-permute-start | bytes 1671176 | tf_op jit(solution)/shard_map/ppermute | solution.py:386
  83.3 11.8 %all-to-all-start.3 = ((bf16[16,24,128]{2,1,0:T(8,128)(2,1)}), bf16[16,24,128]{2,1,0:T(8,128)(2,1)S(1)}, u32[]{:S(2)}, u32[]{:S(2)}) async-start(bf16[16,24,128]{2,1,0:T(8,128)(2,1)} %broadcast_in_dim.7), calls=%async_computation.3 | async-start | bytes 196608 | tf_op jit(solution)/shard_map/all_to_all | solution.py:19

commit v15 on v14

--- a/solution.py
+++ b/solution.py
@@ -163,18 +163,18 @@
     )(*[far(v) for v in (down_weight, up_weight, tokens, scale, pre, post)])
 
 
-def down_kernel(start, lead_ref, hidden_ref, own_ref, *refs):
-    others, (out_ref, held, sem) = refs[: X - 1], refs[X - 1 :]
-    n = held.shape[0]
-    copy = pltpu.make_async_copy(own_ref.at[pl.ds(start, n)], held, sem)
-    copy.start()
+def down_kernel(start, lead_ref, hidden_ref, *refs):
+    weights, out_ref, held, sems = refs[:X], refs[X], refs[X + 1], refs[X + 2]
+    copies = []
+    for i, w in enumerate(weights):
+        blocks = w.at[pl.ds(start, held.shape[1])]
+        copies.append(pltpu.make_async_copy(blocks, held.at[i], sems.at[i]))
+        copies[-1].start()
     hidden = [lead_ref[...].astype(bf16), *(hidden_ref[z] for z in range(1, Z))]
     hidden = jnp.concatenate(hidden, axis=1)
     for i in (1, 2, 3, 0):
-        if i == 0:
-            copy.wait()
-        weight = others[i - 1][start : start + n] if i else held[...]
-        weight = weight.reshape(hidden.shape[1], -1)
+        copies[i].wait()
+        weight = held[i].reshape(hidden.shape[1], -1)
         out_ref[i] = jnp.dot(hidden, weight, preferred_element_type=f32).astype(bf16)
 
 
@@ -185,15 +185,15 @@
     return pl.pallas_call(
         lambda *refs: down_kernel(start, *refs),
         out_shape=pltpu.VMEM((X, t, feats), bf16),
-        in_specs=[*[VMEM] * 2, ANY, *[VMEM] * (X - 1)],
+        in_specs=[*[VMEM] * 2, *[ANY] * X],
         out_specs=VMEM,
         scratch_shapes=[
-            pltpu.VMEM((Z * share // feats, feats, feats), bf16),
-            pltpu.SemaphoreType.DMA,
+            pltpu.VMEM((X, Z * share // feats, feats, feats), bf16),
+            pltpu.SemaphoreType.DMA((X,)),
         ],
         compiler_params=limit(8),
         name="down_product",
-    )(near(lead), near(hidden), blocks[0], *[near(b) for b in blocks[1:]])
+    )(near(lead), near(hidden), *blocks)
 
 
 def down_share(hidden, blocks, start):

time: 175 us -> 175 us (level)
  transfers between devices with their start and end apart: 9 -> 9, of which waited for: 3 -> 3; matrix products, arithmetic and copies ran while one was open for 0% -> 0% of each run, Pallas kernels for 3% -> 2%
where the time goes in v15:
time: 175 us; the launch traced here: 174 us
  blocking collectives  109 us (62%)
  starting transfers between devices  38.8 us (22%)
  waiting for transfers between devices  12.7 us (7%)
  Pallas kernels  11 us (6%)
  local copies, waits for them, and re-layouts  2.04 us (1%)
    all_to_all x7, blocking collectives, exchange(): return lax.all_to_all(pieces, axis, split_axis=0, concat_axis=0, tiled=True)  109 us
    all_to_all x3, starting transfers between devices, exchange(): return lax.all_to_all(pieces, axis, split_axis=0, concat_axis=0, tiled=True)  19.8 us
    ppermute x6, starting transfers between devices, from_x(): return lax.ppermute(payload, 'x', [(i, (i - s) % X) for i in range(X)])  19 us
    all_to_all x3, waiting for transfers between devices, exchange(): return lax.all_to_all(pieces, axis, split_axis=0, concat_axis=0, tiled=True)  12.6 us
  transfers between devices with their start and end apart: 9, of which 3 were waited for; matrix products, arithmetic and copies ran while one was open for 0% of the time, Pallas kernels for 2%

profile of v15, /device:TPU:1, one launch (start us, length us, event | category | flops | bytes accessed | tf_op | source)
XLA Modules:
  0.0 174.2 jit_solution(3929374684160393973)
XLA Ops:
  0.0 2.8 %up_product.1 = (bf16[8,384,128]{2,1,0:T(8,128)(2,1)}, bf16[8,128,128]{2,1,0:T(8,128)(2,1)}) custom-call(bf16[384,128]{1,0:T(8,128)(2,1)} %tokens_ref.3, f32[2,128]{1,0:T(2,128)} %pre_ref.1, f32[2,128,1024]{2,1,0:T(8,128)} %up_ref.1, f32[2,1024]{1,0:T(2,128)} %scale_ref.5, f32[2,1024,128]{2,1,0:T(8,128)} %down_ref.3), custom_call_target="tpu_custom_call" | custom-call | tf_op jit(solution)/shard_map/up_product/pallas_call | solution.py:91
  2.8 34.8 %all_to_all.50 = bf16[32,96,128]{2,1,0:T(8,128)(2,1)S(1)} all-to-all(bf16[32,96,128]{2,1,0:T(8,128)(2,1)} %bitcast.23), channel_id=1, replica_groups=mesh['z'=8,'x'=4,'y'=8,'core'=2] {'z','x'}, dimensions={0} | all-to-all | bytes 1572864 | tf_op jit(solution)/shard_map/all_to_all | solution.py:19
  37.6 0.0 copy-start.1
  37.6 0.1 convert_reduce_fusion
  37.7 0.7 broadcast_in_dim.6
  38.4 4.1 %all-to-all-start.1 = ((bf16[8,96,128]{2,1,0:T(8,128)(2,1)}), bf16[8,96,128]{2,1,0:T(8,128)(2,1)S(1)}, u32[]{:S(2)}, u32[]{:S(2)}) async-start(bf16[8,96,128]{2,1,0:T(8,128)(2,1)} %broadcast_in_dim.6), calls=%async_computation.1 | async-start | bytes 393216 | tf_op jit(solution)/shard_map/all_to_all | solution.py:19
  42.6 0.0 copy-done.1
  42.6 3.0 %collective-permute-start.2 = (bf16[8,128,128]{2,1,0:T(8,128)(2,1)S(1)}, bf16[8,128,128]{2,1,0:T(8,128)(2,1)S(1)}, u32[]{:S(2)}, u32[]{:S(2)}) collective-permute-start(bf16[8,128,128]{2,1,0:T(8,128)(2,1)S(1)} %copy-done.1), channel_id=1, source_target_pairs={{0,16},{16,32},{32,48},{48,0},{1,17},{17,33},{33,49},{49,1},{2,18}... | collective-permute-start | bytes 786440 | tf_op jit(solution)/shard_map/ppermute | solution.py:386
  45.6 4.1 %collective-permute-start.1 = (bf16[8,128,128]{2,1,0:T(8,128)(2,1)S(1)}, bf16[8,128,128]{2,1,0:T(8,128)(2,1)S(1)}, u32[]{:S(2)}, u32[]{:S(2)}) collective-permute-start(bf16[8,128,128]{2,1,0:T(8,128)(2,1)S(1)} %copy-done.1), channel_id=1, source_target_pairs={{0,32},{16,48},{32,0},{48,16},{1,33},{17,49},{33,1},{49,17},{2,34}... | collective-permute-start | bytes 786440 | tf_op jit(solution)/shard_map/ppermute | solution.py:386
  49.7 2.7 %collective-permute-start = (bf16[8,128,128]{2,1,0:T(8,128)(2,1)S(1)}, bf16[8,128,128]{2,1,0:T(8,128)(2,1)S(1)}, u32[]{:S(2)}, u32[]{:S(2)}) collective-permute-start(bf16[8,128,128]{2,1,0:T(8,128)(2,1)S(1)} %copy-done.1), channel_id=1, source_target_pairs={{0,48},{16,0},{32,16},{48,32},{1,49},{17,1},{33,17},{49,33},{2,50}... | collective-permute-start | bytes 786440 | tf_op jit(solution)/shard_map/ppermute | solution.py:386
  52.5 2.5 %packed.1 = (bf16[17,128,128]{2,1,0:T(8,128)(2,1)}, bf16[17,128,128]{2,1,0:T(8,128)(2,1)}, bf16[17,128,128]{2,1,0:T(8,128)(2,1)}, bf16[112,128]{1,0:T(8,128)(2,1)S(1)}) custom-call(f32[2,1024,128]{2,1,0:T(8,128)} %down_ref.3, f32[2,128,1024]{2,1,0:T(8,128)} %up_ref.1, bf16[384,128]{1,0:T(8,128)(2,1)} %tokens_ref.3, f32[2,128]{1,0:T(2,128)} %scale_ref.4, ...), custom_call_target="tpu_custom_call" | custom-call | tf_op jit(solution)/shard_map/packed/pallas_call | solution.py:145
  55.0 0.0 copy-start
  55.0 2.9 %collective-permute-start.4 = (bf16[17,128,128]{2,1,0:T(8,128)(2,1)}, bf16[17,128,128]{2,1,0:T(8,128)(2,1)S(1)}, u32[]{:S(2)}, u32[]{:S(2)}) collective-permute-start(bf16[17,128,128]{2,1,0:T(8,128)(2,1)} %get-tuple-element.31), channel_id=1, source_target_pairs={{0,32},{16,48},{32,0},{48,16},{1,33},{17,49},{33,1},{49,17},{2,34}... | collective-permute-start | bytes 1671176 | tf_op jit(solution)/shard_map/ppermute | solution.py:386
  57.9 1.9 %collective-permute-start.5 = (bf16[17,128,128]{2,1,0:T(8,128)(2,1)}, bf16[17,128,128]{2,1,0:T(8,128)(2,1)S(1)}, u32[]{:S(2)}, u32[]{:S(2)}) collective-permute-start(bf16[17,128,128]{2,1,0:T(8,128)(2,1)} %get-tuple-element.33), channel_id=1, source_target_pairs={{0,16},{16,32},{32,48},{48,0},{1,17},{17,33},{33,49},{49,1},{2,18}... | collective-permute-start | bytes 1671176 | tf_op jit(solution)/shard_map/ppermute | solution.py:386
  59.8 0.0 collective-permute-done.2.refs_5_
  59.8 0.0 all-to-all-done.1.refs_1_
  59.9 0.0 collective-permute-done.1.refs_4_
  59.9 0.1 collective-permute-done.refs_3_
  60.0 1.8 %down_product.2 = bf16[4,96,128]{2,1,0:T(8,128)(2,1)} custom-call(f32[96,128]{1,0:T(8,128)S(1)} %fusion.1.refs_0_, bf16[8,96,128]{2,1,0:T(8,128)(2,1)S(1)} %all-to-all-done.1.refs_1_, bf16[8,128,128]{2,1,0:T(8,128)(2,1)} %get-tuple-element.24.refs_2_, bf16[8,128,128]{2,1,0:T(8,128)(2,1)S(1)} %collective-permute-done.refs_3_, ...), custom_call_target="tpu_custom_call" | custom-call | tf_op jit(solution)/shard_map/down_product/pallas_call | solution.py:185
  61.8 12.2 %all-to-all-start.2 = ((bf16[16,24,128]{2,1,0:T(8,128)(2,1)}), bf16[16,24,128]{2,1,0:T(8,128)(2,1)S(1)}, u32[]{:S(2)}, u32[]{:S(2)}) async-start(bf16[16,24,128]{2,1,0:T(8,128)(2,1)} %bitcast.2), calls=%async_computation.2 | async-start | bytes 196608 | tf_op jit(solution)/shard_map/all_to_all | solution.py:19
  74.0 0.0 copy-done
  74.0 4.3 %collective-permute-start.3 = (bf16[17,128,128]{2,1,0:T(8,128)(2,1)S(1)}, bf16[17,128,128]{2,1,0:T(8,128)(2,1)S(1)}, u32[]{:S(2)}, u32[]{:S(2)}) collective-permute-start(bf16[17,128,128]{2,1,0:T(8,128)(2,1)S(1)} %copy-done), channel_id=1, source_target_pairs={{0,48},{16,0},{32,16},{48,32},{1,49},{17,1},{33,17},{49,33},{2,50}... | collective-permute-start | bytes 1671176 | tf_op jit(solution)/shard_map/ppermute | solution.py:386
  78.3 4.1 %all-to-all-done.2 = bf16[16,24,128]{2,1,0:T(8,128)(2,1)S(1)} async-done(((bf16[16,24,128]{2,1,0:T(8,128)(2,1)}), bf16[16,24,128]{2,1,0:T(8,128)(2,1)S(1)}, u32[]{:S(2)}, u32[]{:S(2)}) %all-to-all-start.2) | async-done | bytes 98336 | tf_op jit(solution)/shard_map/all_to_all | solution.py:19
  82.5 0.7 broadcast_in_dim.7
  83.2 3.4 %all-to-all-start.3 = ((bf16[16,24,128]{2,1,0:T(8,128)(2,1)}), bf16[16,24,128]{2,1,0:T(8,128)(2,1)S(1)}, u32[]{:S(2)}, u32[]{:S(2)}) async-start(bf16[16,24,128]{2,1,0:T(8,128)(2,1)} %broadcast_in_dim.7), calls=%async_computation.3 | async-start | bytes 196608 | tf_op jit(solution)/shard_map/all_to_all | solution.py:19
  86.6 0.0 collective-permute-done.4.refs_2_.refs_4_
  86.6 8.4 %all-to-all-done.3 = bf16[16,24,128]{2,1,0:T(8,128)(2,1)S(1)} async-done(((bf16[16,24,128]{2,1,0:T(8,128)(2,1)}), bf16[16,24,128]{2,1,0:T(8,128)(2,1)S(1)}, u32[]{:S(2)}, u32[]{:S(2)}) %all-to-all-start.3) | async-done | bytes 98336 | tf_op jit(solution)/shard_map/all_to_all | solution.py:19
  95.0 0.0 collective-permute-done.5.refs_3_.refs_5_
  95.0 0.0 collective-permute-done.3.refs_1_.refs_3_
  95.0 2.0 %turn.1 = (bf16[8,200,128]{2,1,0:T(8,128)(2,1)S(1)}, f32[4,96,128]{2,1,0:T(8,128)S(1)}, f32[4,96,128]{2,1,0:T(8,128)S(1)}, f32[4,8,128]{2,1,0:T(8,128)S(1)}) custom-call(f32[96,128]{1,0:T(8,128)S(1)} %bitcast_convert_fusion.lead_ref, bf16[4,96,128]{2,1,0:T(8,128)(2,1)S(1)} %bitcast.21, bf16[112,128]{1,0:T(8,128)(2,1)S(1)} %get-tuple-element.28.own_ref, ...), custom_call_target="tpu_custom_call" | custom-call | tf_op jit(solution)/shard_map/turn/pallas_call | solution.py:284
  97.1 22.5 %all_to_all.51.refs_0_ = bf16[8,200,128]{2,1,0:T(8,128)(2,1)S(1)} all-to-all(bf16[8,200,128]{2,1,0:T(8,128)(2,1)S(1)} %get-tuple-element.35), channel_id=1, replica_groups=mesh['z'=8,'x'=4,'y'=8,'core'=2] {'z'}, dimensions={0} | all-to-all | bytes 819200 | tf_op jit(solution)/shard_map/all_to_all | solution.py:19
  119.6 0.1 second_hidden.1
  119.7 12.1 %all_to_all.52.refs_1_ = bf16[8,96,128]{2,1,0:T(8,128)(2,1)S(1)} all-to-all(bf16[8,96,128]{2,1,0:T(8,128)(2,1)S(1)} %get-tuple-element.38), channel_id=1, replica_groups=mesh['z'=8,'x'=4,'y'=8,'core'=2] {'z'}, dimensions={0} | all-to-all | bytes 393216 | tf_op jit(solution)/shard_map/all_to_all | solution.py:19
  131.8 1.2 down_product.3
  133.0 12.6 %all_to_all.53 = bf16[16,24,128]{2,1,0:T(8,128)(2,1)S(1)} all-to-all(bf16[16,24,128]{2,1,0:T(8,128)(2,1)S(1)} %bitcast.22), channel_id=1, replica_groups=mesh['z'=8,'x'=4,'y'=8,'core'=2] {'y','core'}, dimensions={0} | all-to-all | bytes 196608 | tf_op jit(solution)/shard_map/all_to_all | solution.py:19
  145.7 10.9 %all_to_all.54 = bf16[16,24,128]{2,1,0:T(8,128)(2,1)S(1)} all-to-all(bf16[16,24,128]{2,1,0:T(8,128)(2,1)S(1)} %broadcast_in_dim.8), channel_id=1, replica_groups=mesh['z'=8,'x'=4,'y'=8,'core'=2] {'y','core'}, dimensions={0} | all-to-all | bytes 196608 | tf_op jit(solution)/shard_map/all_to_all | solution.py:19
  156.5 0.4 squares.1
  156.9 8.9 %all_to_all.55.refs_0_ = f32[8,1,128]{2,1,0:T(1,128)S(1)} all-to-all(f32[8,1,128]{2,1,0:T(1,128)S(1)} %squares.1), channel_id=1, replica_groups=mesh['z'=8,'x'=4,'y'=8,'core'=2] {'z'}, dimensions={0} | all-to-all | bytes 8192 | tf_op jit(solution)/shard_map/all_to_all | solution.py:19
  165.9 0.1 last.1
  166.0 7.6 %all_to_all.56 = bf16[4,96,128]{2,1,0:T(8,128)(2,1)S(1)} all-to-all(bf16[4,96,128]{2,1,0:T(8,128)(2,1)S(1)} %last.1), channel_id=1, replica_groups=mesh['z'=8,'x'=4,'y'=8,'core'=2] {'x'}, dimensions={0} | all-to-all | bytes 196608 | tf_op jit(solution)/shard_map/all_to_all | solution.py:19
  173.6 0.6 copy.9
  (8 shorter events, 0.1 us)
Async XLA Ops:
  37.6 5.0 %copy-start.1 = (bf16[8,128,128]{2,1,0:T(8,128)(2,1)S(1)}, bf16[8,128,128]{2,1,0:T(8,128)(2,1)}, u32[]{:S(2)}) copy-start(bf16[8,128,128]{2,1,0:T(8,128)(2,1)} %get-tuple-element.24.refs_2_) | copy-start | bytes 786436
  38.4 21.4 %all-to-all-start.1 = ((bf16[8,96,128]{2,1,0:T(8,128)(2,1)}), bf16[8,96,128]{2,1,0:T(8,128)(2,1)S(1)}, u32[]{:S(2)}, u32[]{:S(2)}) async-start(bf16[8,96,128]{2,1,0:T(8,128)(2,1)} %broadcast_in_dim.6), calls=%async_computation.1 | async-start | bytes 393216 | tf_op jit(solution)/shard_map/all_to_all | solution.py:19
  42.6 17.3 %collective-permute-start.2 = (bf16[8,128,128]{2,1,0:T(8,128)(2,1)S(1)}, bf16[8,128,128]{2,1,0:T(8,128)(2,1)S(1)}, u32[]{:S(2)}, u32[]{:S(2)}) collective-permute-start(bf16[8,128,128]{2,1,0:T(8,128)(2,1)S(1)} %copy-done.1), channel_id=1, source_target_pairs={{0,16},{16,32},{32,48},{48,0},{1,17},{17,33},{33,49},{49,1},{2,18}... | collective-permute-start | bytes 786440 | tf_op jit(solution)/shard_map/ppermute | solution.py:386
  45.6 14.3 %collective-permute-start.1 = (bf16[8,128,128]{2,1,0:T(8,128)(2,1)S(1)}, bf16[8,128,128]{2,1,0:T(8,128)(2,1)S(1)}, u32[]{:S(2)}, u32[]{:S(2)}) collective-permute-start(bf16[8,128,128]{2,1,0:T(8,128)(2,1)S(1)} %copy-done.1), channel_id=1, source_target_pairs={{0,32},{16,48},{32,0},{48,16},{1,33},{17,49},{33,1},{49,17},{2,34}... | collective-permute-start | bytes 786440 | tf_op jit(solution)/shard_map/ppermute | solution.py:386
  49.7 10.2 %collective-permute-start = (bf16[8,128,128]{2,1,0:T(8,128)(2,1)S(1)}, bf16[8,128,128]{2,1,0:T(8,128)(2,1)S(1)}, u32[]{:S(2)}, u32[]{:S(2)}) collective-permute-start(bf16[8,128,128]{2,1,0:T(8,128)(2,1)S(1)} %copy-done.1), channel_id=1, source_target_pairs={{0,48},{16,0},{32,16},{48,32},{1,49},{17,1},{33,17},{49,33},{2,50}... | collective-permute-start | bytes 786440 | tf_op jit(solution)/shard_map/ppermute | solution.py:386
  55.0 19.0 %copy-start = (bf16[17,128,128]{2,1,0:T(8,128)(2,1)S(1)}, bf16[17,128,128]{2,1,0:T(8,128)(2,1)}, u32[]{:S(2)}) copy-start(bf16[17,128,128]{2,1,0:T(8,128)(2,1)} %get-tuple-element.29.refs_0_.refs_2_) | copy-start | bytes 1671172
  55.0 31.6 %collective-permute-start.4 = (bf16[17,128,128]{2,1,0:T(8,128)(2,1)}, bf16[17,128,128]{2,1,0:T(8,128)(2,1)S(1)}, u32[]{:S(2)}, u32[]{:S(2)}) collective-permute-start(bf16[17,128,128]{2,1,0:T(8,128)(2,1)} %get-tuple-element.31), channel_id=1, source_target_pairs={{0,32},{16,48},{32,0},{48,16},{1,33},{17,49},{33,1},{49,17},{2,34}... | collective-permute-start | bytes 1671176 | tf_op jit(solution)/shard_map/ppermute | solution.py:386
  57.9 37.1 %collective-permute-start.5 = (bf16[17,128,128]{2,1,0:T(8,128)(2,1)}, bf16[17,128,128]{2,1,0:T(8,128)(2,1)S(1)}, u32[]{:S(2)}, u32[]{:S(2)}) collective-permute-start(bf16[17,128,128]{2,1,0:T(8,128)(2,1)} %get-tuple-element.33), channel_id=1, source_target_pairs={{0,16},{16,32},{32,48},{48,0},{1,17},{17,33},{33,49},{49,1},{2,18}... | collective-permute-start | bytes 1671176 | tf_op jit(solution)/shard_map/ppermute | solution.py:386
  61.8 20.7 %all-to-all-start.2 = ((bf16[16,24,128]{2,1,0:T(8,128)(2,1)}), bf16[16,24,128]{2,1,0:T(8,128)(2,1)S(1)}, u32[]{:S(2)}, u32[]{:S(2)}) async-start(bf16[16,24,128]{2,1,0:T(8,128)(2,1)} %bitcast.2), calls=%async_computation.2 | async-start | bytes 196608 | tf_op jit(solution)/shard_map/all_to_all | solution.py:19
  74.0 21.0 %collective-permute-start.3 = (bf16[17,128,128]{2,1,0:T(8,128)(2,1)S(1)}, bf16[17,128,128]{2,1,0:T(8,128)(2,1)S(1)}, u32[]{:S(2)}, u32[]{:S(2)}) collective-permute-start(bf16[17,128,128]{2,1,0:T(8,128)(2,1)S(1)} %copy-done), channel_id=1, source_target_pairs={{0,48},{16,0},{32,16},{48,32},{1,49},{17,1},{33,17},{49,33},{2,50}... | collective-permute-start | bytes 1671176 | tf_op jit(solution)/shard_map/ppermute | solution.py:386
  83.2 11.8 %all-to-all-start.3 = ((bf16[16,24,128]{2,1,0:T(8,128)(2,1)}), bf16[16,24,128]{2,1,0:T(8,128)(2,1)S(1)}, u32[]{:S(2)}, u32[]{:S(2)}) async-start(bf16[16,24,128]{2,1,0:T(8,128)(2,1)} %broadcast_in_dim.7), calls=%async_computation.3 | async-start | bytes 196608 | tf_op jit(solution)/shard_map/all_to_all | solution.py:19
